TPU v7x, 512 devices: a whole 4x4x16 slice. The times are simulated.
512 devices in a mesh: sp: 64 (over z, y), tp: 8 (over x, core).
Axes of the slice: x: 4, y: 4, z: 16, core: 2. Of those that a mesh axis runs over, the one named last changes fastest.
Arguments:
- latent: bfloat16 [16384, 2048], P(('sp', 'tp')), may hold values from -36 to 36
- condition: float32 [2048], replicated, may hold values from -16 to 16
- context: bfloat16 [256, 2048], P('sp'), may hold values from -6 to 6
- context_condition_vector: float32 [2048], replicated, may hold values from -6 to 6
- modulation_matrix: bfloat16 [3, 2048, 2048], P(None, 'sp', 'tp'), may hold values from -0.125 to 0.125
- query_matrix: bfloat16 [2048, 2048], P(None, 'tp'), may hold values from -0.125 to 0.125
- key_matrix: bfloat16 [2048, 2048], P(None, 'tp'), may hold values from -0.125 to 0.125
- value_matrix: bfloat16 [2048, 2048], P(None, 'tp'), may hold values from -0.125 to 0.125
- decay_input_weight: bfloat16 [2048, 32], replicated, may hold values from -0.125 to 0.125
- write_strength_weight: bfloat16 [2048, 32], replicated, may hold values from -0.125 to 0.125
- head_decay_rate: float32 [32], replicated, may hold values from 0 to 1, as said below
- write_strength_bias: float32 [32], replicated, may hold values from -20 to 0
- context_write_offset_bias: float32 [32], replicated, may hold values from 1.5 to 4.5
- log_spike_added: float32 [16384, 32], P('sp'), may hold values from -2 to 0, as said below
- head_norm_gain: float32 [128], replicated, may hold values from 0.1 to 1.9
- output_matrix: bfloat16 [2048, 2048], P('tp'), may hold values from -0.125 to 0.125
Outputs:
- mixed: bfloat16 [16384, 2048], P(('sp', 'tp'))
Inputs may be any that keep to these rules, and one draw needn't show every extreme that they name: `head_decay_rate`: positive. `log_spike_added`: no entry is positive.
All inputs are finite; a program needn't handle non-finite values.
Results may differ from a plain program's by a relative error of at most 0.018.
Values may be sent and summed in bfloat16 or wider, within the bound.
No kernel may reach another device: no remote copies, remote signals or barrier semaphores. Data moves between devices by JAX's collectives and lax.ppermute only.
A program may use at most 128 MiB of HBM per device.

v0:
```python
import jax
import jax.numpy as jnp
from jax import lax
from jax.experimental import pallas as pl
from jax.experimental.pallas import tpu as pltpu
from jax.sharding import Mesh
from jax.sharding import PartitionSpec as P

D = 2048
DK = 128
EPS = 1e-06
HI = lax.Precision.HIGHEST
F32 = jnp.float32
BF = jnp.bfloat16
Z = ("zh", "zl")
TP = ("x", "c")
SP = ("zh", "zl", "y")
ALL = ("zh", "zl", "y", "x", "c")
VM = pl.BlockSpec(memory_space=pltpu.VMEM)
SM = pl.BlockSpec(memory_space=pltpu.SMEM)


def mm(a, b, dims=((1,), (0,))):
    return lax.dot_general(
        a.astype(BF), b.astype(BF), (dims, ((), ())), preferred_element_type=F32
    )


def norm_rows(rows, scale, shift):
    wide = rows.astype(F32)
    centred = wide - jnp.mean(wide, axis=-1, keepdims=True)
    spread = jnp.mean(centred * centred, axis=-1, keepdims=True)
    return (centred * lax.rsqrt(spread + EPS) * (1.0 + scale) + shift).astype(BF)


def column(matrix, lane):
    lanes = lax.broadcasted_iota(jnp.int32, matrix.shape, 1)
    return jnp.sum(jnp.where(lanes == lane, matrix, 0.0), axis=1, keepdims=True)


def softplus(t):
    return jnp.maximum(t, 0.0) + jnp.log1p(jnp.exp(-jnp.abs(t)))


def sigmoid(t):
    return 1.0 / (1.0 + jnp.exp(-t))


def inverse_of(lower, row, col):
    eye = (row == col).astype(F32)
    own = (row // 16) == (col // 16)
    base = [jnp.where(own, m, 0.0) for m in lower]
    inv = [eye - m for m in base]
    power = [mm(m, m) for m in base]
    for step in range(3):
        inv = [p + mm(p, x) for p, x in zip(inv, power)]
        if step < 2:
            power = [mm(x, x) for x in power]
    size = 16
    while size < 256:
        here = ((row // (2 * size)) == (col // (2 * size))) & ((row // size) != (col // size))
        side = [mm(jnp.where(here, m, 0.0), p) for m, p in zip(lower, inv)]
        inv = [p - mm(p, s) for p, s in zip(inv, side)]
        size *= 2
    out = []
    for m, p in zip(lower, inv):
        first = p.astype(BF)
        high = m.astype(BF)
        low = (m - high.astype(F32)).astype(BF)
        wide = first.astype(F32)
        left = (eye - wide) - (mm(high, first) + mm(low, first))
        out.append(wide + mm(first, left))
    return out


def project_kernel(pos, lat, ctx, fac, wq, wk, wv, wd, ww, q_o, k_o, v_o, r_o, w_o, c_o, hid):
    factors = [[], [], [], []]
    for t in range(8):
        f = (fac[t] + fac[8 + t]) + (fac[16 + t] + fac[24 + t])
        for slot, r in enumerate((0, 1, 3, 4)):
            factors[slot].append(f[r : r + 1])
    shift, scale, c_shift, c_scale = (jnp.concatenate(f, axis=1) for f in factors)
    for t in range(8):
        hid[32 * t : 32 * t + 32] = norm_rows(lat[t], scale, shift)
    hid[256:272] = norm_rows(ctx[...], c_scale, c_shift)
    rows = hid[...]
    q_o[...] = mm(hid[0:256], wq[...]).astype(BF)
    keys = mm(rows, wk[...]).astype(BF)
    values = mm(rows, wv[...]).astype(BF)
    rate = mm(rows, wd[...]).astype(BF).astype(F32)
    write = mm(rows, ww[...]).astype(BF).astype(F32)
    k_o[...] = keys[:256]
    v_o[...] = values[:256]
    r_o[...] = rate[:256]
    w_o[...] = write[:256]
    combo = pos[0]
    first = combo < 2
    ck, cv = (keys[256:272].astype(F32), values[256:272].astype(F32))
    c_o[:, 0:128] = jnp.where(first, ck[:, :128], ck[:, 128:]).astype(BF)
    c_o[:, 128:256] = jnp.where(first, cv[:, :128], cv[:, 128:]).astype(BF)
    lane = pos[1] * 4 + combo
    lanes = lax.broadcasted_iota(jnp.int32, (16, 128), 1)
    gates = jnp.where(lanes == 0, column(rate[256:272], lane), 0.0)
    gates = jnp.where(lanes == 1, column(write[256:272], lane), gates)
    c_o[:, 256:384] = gates.astype(BF)


def chunk_kernel(pos, q, k, v, rate, write, spike, decay, bias, m_o, r_o, o_o):
    row = lax.broadcasted_iota(jnp.int32, (256, 256), 0)
    col = lax.broadcasted_iota(jnp.int32, (256, 256), 1)
    eye = row == col
    logs = -decay[...] * softplus(rate[...]) + spike[...]
    strength = sigmoid(write[...] + bias[...])
    below = (row >= col).astype(F32)
    above = (row <= col).astype(F32)
    sums = (
        jnp.dot(below, logs, precision=HI, preferred_element_type=F32),
        jnp.dot(above, logs, precision=HI, preferred_element_type=F32),
    )
    lowers, parts = ([], [])
    for h in range(2):
        kh = k[:, 128 * h : 128 * h + 128]
        qh = q[:, 128 * h : 128 * h + 128]
        kf = kh.astype(F32)
        unit = lax.rsqrt(jnp.sum(kf * kf, axis=1, keepdims=True) + EPS)
        unit_row = jnp.sum(jnp.where(eye, unit, 0.0), axis=0, keepdims=True)
        gram = mm(kh, kh, ((1,), (1,))) * unit_row
        cross = mm(qh, kh, ((1,), (1,))) * unit_row
        for e in range(2):
            lane = pos[1] * 4 + 2 * h + e
            total = column(sums[e], lane)
            b = column(strength, lane)
            total_row = jnp.sum(jnp.where(eye, total, 0.0), axis=0, keepdims=True)
            last = total[255:256] if e == 0 else total[0:1]
            inside = row >= col if e == 0 else row <= col
            fade = jnp.where(inside, jnp.exp(jnp.where(inside, total - total_row, 0.0)), 0.0)
            lowers.append(jnp.where(eye, 0.0, (b * unit) * gram * fade))
            grown = jnp.exp(total)
            right = jnp.concatenate(
                [
                    b * v[:, 128 * h : 128 * h + 128].astype(F32),
                    (b * unit * grown) * kf,
                ],
                axis=1,
            ).astype(BF)
            faded = (kf * (unit * jnp.exp(last - total))).astype(BF)
            scores = (cross * fade).astype(BF)
            parts.append((right, faded, scores, grown * qh.astype(F32), jnp.exp(last) - 1.0))
    solved = inverse_of(lowers, row, col)
    small = lax.broadcasted_iota(jnp.int32, (128, 128), 0) == lax.broadcasted_iota(
        jnp.int32, (128, 128), 1
    )
    outs = [None, None]
    for j in range(4):
        right, faded, scores, grown_q, short = parts[j]
        both = mm(solved[j], right).astype(BF)
        maps = mm(faded, both, ((0,), (0,)))
        read = mm(scores, both)
        m_o[j, :, 0:128] = (jnp.where(small, short, 0.0) - maps[:, 128:]).astype(BF)
        m_o[j, :, 128:256] = maps[:, :128].astype(BF)
        h, e = divmod(j, 2)
        r_o[h, :, 128 * e : 128 * e + 128] = (grown_q - read[:, 128:]).astype(BF)
        outs[h] = read[:, :128] if e == 0 else outs[h] + read[:, :128]
    o_o[:, 0:128] = outs[0]
    o_o[:, 128:256] = outs[1]


def context_kernel(pos, rows, decay, bias, extra, s_o):
    row = lax.broadcasted_iota(jnp.int32, (256, 256), 0)
    col = lax.broadcasted_iota(jnp.int32, (256, 256), 1)
    eye = row == col
    lane = pos[1] * 4 + pos[0]
    ahead = (row - col) * (1 - 2 * (pos[0] % 2))
    inside = ahead >= 0
    kh = rows[:, 0:128]
    kf = kh.astype(F32)
    gates = rows[:, 256:384].astype(F32)
    logs = -column(decay[...], lane) * softplus(gates)
    b = column(sigmoid(gates + column(bias[...], lane) + column(extra[...], lane)), 1)
    sums = jnp.dot(inside.astype(F32), logs, precision=HI, preferred_element_type=F32)
    total = column(sums, 0)
    total_row = jnp.sum(jnp.where(eye, total, 0.0), axis=0, keepdims=True)
    last = jnp.min(total, axis=0, keepdims=True)
    unit = lax.rsqrt(jnp.sum(kf * kf, axis=1, keepdims=True) + EPS)
    unit_row = jnp.sum(jnp.where(eye, unit, 0.0), axis=0, keepdims=True)
    fade = jnp.where(inside, jnp.exp(jnp.where(inside, total - total_row, 0.0)), 0.0)
    lower = jnp.where(
        eye, 0.0, (b * unit) * (mm(kh, kh, ((1,), (1,))) * unit_row) * fade
    )
    solved = inverse_of([lower], row, col)[0]
    fresh = mm(solved, b * rows[:, 128:256].astype(F32))
    faded = kf * (unit * jnp.exp(last - total))
    s_o[...] = mm(faded, fresh, ((0,), (0,)))


def apply_to(linear, state):
    high = state.astype(BF)
    low = (state - high.astype(F32)).astype(BF)
    both = mm(linear, jnp.concatenate([high, low], axis=1))
    n = state.shape[1]
    return both[:, :n] + both[:, n:]


def compose_kernel(pos, maps, o):
    back = pos[0] % 2
    at = back * 3
    step = 1 - 2 * back
    total = maps[at].astype(F32)
    for _ in range(3):
        at = at + step
        total = total + maps[at].astype(F32) + apply_to(maps[at][:, 0:128], total)
    out = total.astype(BF)
    for i in range(4):
        o[i] = out


def scan_kernel(pos, start, high, low, own, o):
    back = pos[0] % 2
    step = 1 - 2 * back
    state = start[...]
    for maps, mine in ((high, pos[2]), (low, pos[3])):
        at = back * 3
        for _ in range(3):
            moved = state + maps[at][:, 128:256].astype(F32) + apply_to(maps[at][:, 0:128], state)
            state = jnp.where((mine - at) * step > 0, moved, state)
            at = at + step
    at = back * 3
    for i in range(4):
        o[at] = state.astype(BF)
        if i < 3:
            state = state + own[at][:, 128:256].astype(F32) + apply_to(own[at][:, 0:128], state)
        at = at + step


def read_kernel(states, reads, base, gain, o):
    for h in range(2):
        total = base[:, 128 * h : 128 * h + 128] + mm(reads[h], states[h])
        mean = jnp.mean(total * total, axis=1, keepdims=True)
        o[:, 128 * h : 128 * h + 128] = (total * lax.rsqrt(mean + EPS) * gain[...]).astype(BF)


def output_kernel(at, rows, fac, lat, *rest):
    weights, o = (rest[:8], rest[8])
    branch = mm(rows[at[0]], weights[0][...])
    for i in range(1, 8):
        branch = branch + mm(rows[at[i]], weights[i][...])
    gates = []
    for t in range(8):
        f = (fac[t] + fac[8 + t]) + (fac[16 + t] + fac[24 + t])
        gates.append(f[2:3])
    gate = jnp.concatenate(gates, axis=1)
    o[...] = (lat[...].astype(F32) + gate * branch).astype(BF)


def call(kernel, outs, specs, scratch=(), flops=1):
    def shape(s):
        return jax.ShapeDtypeStruct(*s)

    many = isinstance(outs, list)
    return pl.pallas_call(
        kernel,
        out_shape=[shape(s) for s in outs] if many else shape(outs),
        in_specs=specs,
        out_specs=[VM] * len(outs) if many else VM,
        scratch_shapes=scratch,
        cost_estimate=pl.CostEstimate(flops=flops, bytes_accessed=1, transcendentals=0),
    )


def to_all(value, axes, count):
    return lax.all_to_all(
        jnp.broadcast_to(value[None], (count, *value.shape)), axes, 0, 0, tiled=True
    )


def per_device(
    latent,
    condition,
    context,
    context_condition_vector,
    modulation_matrix,
    query_matrix,
    key_matrix,
    value_matrix,
    decay_input_weight,
    write_strength_weight,
    head_decay_rate,
    write_strength_bias,
    context_write_offset_bias,
    log_spike_added,
    head_norm_gain,
    output_matrix,
):
    zh, zl, y = (lax.axis_index("zh"), lax.axis_index("zl"), lax.axis_index("y"))
    x, c = (lax.axis_index("x"), lax.axis_index("c"))
    pos = jnp.stack([y, x * 2 + c, zh, zl]).astype(jnp.int32)
    sp_index = lax.axis_index(SP)
    signals = jnp.stack([condition, context_condition_vector])
    signals = lax.dynamic_slice_in_dim(jax.nn.silu(signals), sp_index * 32, 32, 1)
    mod = modulation_matrix.astype(F32)
    part = jnp.concatenate(
        [
            jnp.sum(mod * signals[0][None, :, None], axis=1),
            jnp.sum(mod[:2] * signals[1][None, :, None], axis=1),
        ]
    )
    part = jnp.sum(to_all(part, Z, 16), axis=0)
    fac = to_all(part, ("y", "x", "c"), 32)
    lat = to_all(latent, TP, 8)
    ctx = to_all(context, "y", 4).reshape(16, D)

    weights = [output_matrix]
    own = lax.optimization_barrier((output_matrix, lat))[0]
    for d in range(1, 4):
        weights.append(lax.ppermute(own, "x", [(i, (i + d) % 4) for i in range(4)]))
    for d in range(4):
        weights.append(lax.ppermute(weights[d], "c", [(0, 1), (1, 0)]))
    shifted = (x - jnp.arange(4, dtype=jnp.int32)) % 4
    where = jnp.concatenate([shifted * 2 + c, shifted * 2 + 1 - c]).astype(jnp.int32)

    queries, keys, values, rate, write, rows = call(
        project_kernel,
        [
            ((256, 256), BF),
            ((256, 256), BF),
            ((256, 256), BF),
            ((256, 32), F32),
            ((256, 32), F32),
            ((16, 384), BF),
        ],
        [SM] + [VM] * 8,
        [pltpu.VMEM((272, D), BF)],
        flops=10**9,
    )(
        pos,
        lat,
        ctx,
        fac,
        query_matrix,
        key_matrix,
        value_matrix,
        decay_input_weight,
        write_strength_weight,
    )
    all_rows = to_all(rows, Z, 16).reshape(256, 384)
    decay = head_decay_rate.reshape(1, 32)
    bias = write_strength_bias.reshape(1, 32)
    extra = context_write_offset_bias.reshape(1, 32)
    maps, reads, base = call(
        chunk_kernel,
        [((4, 128, 256), BF), ((2, 256, 256), BF), ((256, 256), F32)],
        [SM] + [VM] * 8,
        flops=4 * 10**9,
    )(pos, queries, keys, values, rate, write, log_spike_added, decay, bias)
    of_y = lax.all_to_all(maps, "y", 0, 0, tiled=True)
    start = call(context_kernel, ((128, 128), F32), [SM] + [VM] * 4, flops=10**9)(
        pos, all_rows, decay, bias, extra
    )
    group = call(compose_kernel, ((4, 128, 256), BF), [SM, VM], flops=10**8)
    of_low = lax.all_to_all(group(pos, of_y), "zl", 0, 0, tiled=True)
    of_high = lax.all_to_all(group(pos, of_low), "zh", 0, 0, tiled=True)
    states = call(scan_kernel, ((4, 128, 128), BF), [SM] + [VM] * 4, flops=10**8)(
        pos, start, of_high, of_low, of_y
    )
    states = lax.all_to_all(states, "y", 0, 0, tiled=True).reshape(2, 256, 128)
    normed = call(read_kernel, ((256, 256), BF), [VM] * 4, flops=10**8)(
        states, reads, base, head_norm_gain.reshape(1, 128)
    )
    heads = lax.all_to_all(normed.reshape(8, 32, 256), TP, 0, 0, tiled=True)
    return call(output_kernel, ((32, D), BF), [SM] + [VM] * 11, flops=10**9)(
        where, heads, fac, latent, *weights
    )


def solution(mesh):
    split = Mesh(mesh.devices.reshape(4, 4, 4, 4, 2), ALL)
    return jax.shard_map(
        per_device,
        mesh=split,
        in_specs=(
            P(ALL, None),
            P(),
            P(SP, None),
            P(),
            P(None, SP, TP),
            P(None, TP),
            P(None, TP),
            P(None, TP),
            P(),
            P(),
            P(),
            P(),
            P(),
            P(SP, None),
            P(),
            P(TP, None),
        ),
        out_specs=P(ALL, None),
        check_vma=False,
    )
```

profile of v0, /device:TPU:1, one launch (start us, length us, event | category | flops | bytes accessed | tf_op | source)
XLA Modules:
  0.0 200.2 jit_solution(8450863652408544448)
XLA Ops:
  0.0 0.8 divide_multiply_fusion
  0.8 0.1 copy-done.8
  0.8 0.1 multiply_reduce_fusion
  0.9 0.1 fusion
  1.1 0.0 copy-start.12
  1.1 27.5 %all_to_all.50 = f32[16,5,256]{2,1,0:T(8,128)S(1)} all-to-all(f32[16,5,256]{2,1,0:T(8,128)S(1)} %broadcast_in_dim.12), channel_id=1, replica_groups=mesh['zh'=4,'zl'=4,'y'=4,'x'=4,'c'=2] {'zh','zl'}, dimensions={0} | all-to-all | bytes 163840 | tf_op jit(solution)/shard_map/all_to_all | solution.py:271
  28.6 0.6 broadcast_in_dim.11
  29.2 4.2 %all-to-all-start.1 = ((bf16[4,4,2048]{2,1,0:T(4,128)(2,1)}), bf16[4,4,2048]{2,1,0:T(4,128)(2,1)S(1)}, u32[]{:S(2)}, u32[]{:S(2)}) async-start(bf16[4,4,2048]{2,1,0:T(4,128)(2,1)} %broadcast_in_dim.11), calls=%async_computation.1 | async-start | bytes 131072 | tf_op jit(solution)/shard_map/all_to_all | solution.py:271
  33.4 4.5 %all-to-all-done.1 = bf16[4,4,2048]{2,1,0:T(4,128)(2,1)S(1)} async-done(((bf16[4,4,2048]{2,1,0:T(4,128)(2,1)}), bf16[4,4,2048]{2,1,0:T(4,128)(2,1)S(1)}, u32[]{:S(2)}, u32[]{:S(2)}) %all-to-all-start.1) | async-done | bytes 65568 | tf_op jit(solution)/shard_map/all_to_all | solution.py:271
  37.9 19.2 %all_to_all.51.fac = f32[32,5,256]{2,1,0:T(8,128)} all-to-all(f32[32,5,256]{2,1,0:T(8,128)S(1)} %broadcast_in_dim.13), channel_id=1, replica_groups=mesh['zh'=4,'zl'=4,'y'=4,'x'=4,'c'=2] {'y','x','c'}, dimensions={0} | all-to-all | bytes 327680 | tf_op jit(solution)/shard_map/all_to_all | solution.py:271
  57.1 1.1 broadcast_in_dim.10
  58.2 3.7 %all-to-all-start = ((bf16[8,32,2048]{2,1,0:T(8,128)(2,1)}), bf16[8,32,2048]{2,1,0:T(8,128)(2,1)S(1)}, u32[]{:S(2)}, u32[]{:S(2)}) async-start(bf16[8,32,2048]{2,1,0:T(8,128)(2,1)} %broadcast_in_dim.10), calls=%async_computation | async-start | bytes 2097152 | tf_op jit(solution)/shard_map/all_to_all | solution.py:271
  62.0 0.7 copy.26.spike
  62.7 0.2 copy-done.9
  62.9 1.0 copy.24.wd
  63.9 1.0 copy.25.ww
  64.9 0.6 pad_add_fusion.1.pos
  65.5 0.6 reshape.31.ctx
  66.1 10.8 %all-to-all-done.lat = bf16[8,32,2048]{2,1,0:T(8,128)(2,1)S(1)} async-done(((bf16[8,32,2048]{2,1,0:T(8,128)(2,1)}), bf16[8,32,2048]{2,1,0:T(8,128)(2,1)S(1)}, u32[]{:S(2)}, u32[]{:S(2)}) %all-to-all-start) | async-done | bytes 1048608 | tf_op jit(solution)/shard_map/all_to_all | solution.py:271
  77.0 1.0 copy-done
  78.0 5.4 %shard_map.154 = (bf16[256,256]{1,0:T(8,128)(2,1)}, bf16[256,256]{1,0:T(8,128)(2,1)}, bf16[256,256]{1,0:T(8,128)(2,1)}, f32[256,32]{1,0:T(8,128)}, f32[256,32]{1,0:T(8,128)}, /*index=5*/bf16[16,384]{1,0:T(8,128)(2,1)}) custom-call(s32[4]{0:T(128)} %pad_add_fusion.1.pos, bf16[8,32,2048]{2,1,0:T(8,128)(2,1)} %copy-done, bf16[16,2048]{1,0:T(8,128)(2,1)} %reshape.31.ctx, ...), custom_call_target="tpu_custom_call" | custom-call | flops 1000000000 | bytes 1 | tf_op jit(solution)/shard_map/pallas_call | solution.py:321
  83.4 8.1 %shard_map.156 = (bf16[4,128,256]{2,1,0:T(8,128)(2,1)}, bf16[2,256,256]{2,1,0:T(8,128)(2,1)}, f32[256,256]{1,0:T(8,128)}) custom-call(s32[4]{0:T(128)} %pad_add_fusion.1.pos, bf16[256,256]{1,0:T(8,128)(2,1)} %get-tuple-element.16.q, bf16[256,256]{1,0:T(8,128)(2,1)} %get-tuple-element.17.k, bf16[256,256]{1,0:T(8,128)(2,1)} %get-tuple-element.18.v, ...), custom_call_target="tpu_custom_call" | custom-call | flops 4000000000 | bytes 1 | tf_op jit(solution)/shard_map/pallas_call | solution.py:349
  91.4 9.8 %all_to_all.52.maps.own = bf16[4,128,256]{2,1,0:T(8,128)(2,1)} all-to-all(bf16[4,128,256]{2,1,0:T(8,128)(2,1)} %get-tuple-element.21), channel_id=1, replica_groups=mesh['zh'=4,'zl'=4,'y'=4,'x'=4,'c'=2] {'y'}, dimensions={0} | all-to-all | bytes 524288 | tf_op jit(solution)/shard_map/all_to_all | solution.py:355
  101.2 2.2 %shard_map.157 = bf16[4,128,256]{2,1,0:T(8,128)(2,1)} custom-call(s32[4]{0:T(128)} %pad_add_fusion.1.pos, bf16[4,128,256]{2,1,0:T(8,128)(2,1)} %all_to_all.52.maps.own), custom_call_target="tpu_custom_call" | custom-call | flops 100000000 | bytes 1 | tf_op jit(solution)/shard_map/pallas_call | solution.py:360
  103.5 3.5 %all-to-all-start.6 = ((bf16[4,128,256]{2,1,0:T(8,128)(2,1)}), bf16[4,128,256]{2,1,0:T(8,128)(2,1)S(1)}, u32[]{:S(2)}, u32[]{:S(2)}) async-start(bf16[4,128,256]{2,1,0:T(8,128)(2,1)} %shard_map.157), calls=%async_computation.6 | async-start | bytes 524288 | tf_op jit(solution)/shard_map/all_to_all | solution.py:360
  107.0 2.8 %collective-permute-start.2 = (bf16[256,2048]{1,0:T(8,128)(2,1)S(1)}, bf16[256,2048]{1,0:T(8,128)(2,1)S(1)}, u32[]{:S(2)}, u32[]{:S(2)}) collective-permute-start(bf16[256,2048]{1,0:T(8,128)(2,1)S(1)} %copy-done.2), channel_id=1, source_target_pairs={{0,6},{2,0},{4,2},{6,4},{1,7},{3,1},{5,3},{7,5},{8,14},{10,8},{12,... | collective-permute-start | bytes 3145736 | tf_op jit(solution)/shard_map/ppermute | solution.py:315
  109.8 3.1 %collective-permute-start.1 = (bf16[256,2048]{1,0:T(8,128)(2,1)S(1)}, bf16[256,2048]{1,0:T(8,128)(2,1)S(1)}, u32[]{:S(2)}, u32[]{:S(2)}) collective-permute-start(bf16[256,2048]{1,0:T(8,128)(2,1)S(1)} %copy-done.2), channel_id=1, source_target_pairs={{0,4},{2,6},{4,0},{6,2},{1,5},{3,7},{5,1},{7,3},{8,12},{10,14},{12... | collective-permute-start | bytes 3145736 | tf_op jit(solution)/shard_map/ppermute | solution.py:315
  112.9 1.9 collective-permute-start
  114.9 0.8 broadcast_in_dim.14
  115.7 6.0 %all-to-all-start.4 = ((bf16[16,16,384]{2,1,0:T(8,128)(2,1)}), bf16[16,16,384]{2,1,0:T(8,128)(2,1)}, u32[]{:S(2)}, u32[]{:S(2)}) async-start(bf16[16,16,384]{2,1,0:T(8,128)(2,1)} %broadcast_in_dim.14), calls=%async_computation.4 | async-start | bytes 393216 | tf_op jit(solution)/shard_map/all_to_all | solution.py:271
  121.7 2.2 %shard_map.158 = bf16[4,128,256]{2,1,0:T(8,128)(2,1)} custom-call(s32[4]{0:T(128)} %pad_add_fusion.1.pos, bf16[4,128,256]{2,1,0:T(8,128)(2,1)} %copy-done.1), custom_call_target="tpu_custom_call" | custom-call | flops 100000000 | bytes 1 | tf_op jit(solution)/shard_map/pallas_call | solution.py:361
  123.9 10.1 %all-to-all-done.4 = bf16[16,16,384]{2,1,0:T(8,128)(2,1)} async-done(((bf16[16,16,384]{2,1,0:T(8,128)(2,1)}), bf16[16,16,384]{2,1,0:T(8,128)(2,1)}, u32[]{:S(2)}, u32[]{:S(2)}) %all-to-all-start.4) | async-done | bytes 196640 | tf_op jit(solution)/shard_map/all_to_all | solution.py:271
  134.0 6.8 %all-to-all-start.7 = ((bf16[4,128,256]{2,1,0:T(8,128)(2,1)}), bf16[4,128,256]{2,1,0:T(8,128)(2,1)S(1)}, u32[]{:S(2)}, u32[]{:S(2)}) async-start(bf16[4,128,256]{2,1,0:T(8,128)(2,1)} %shard_map.158), calls=%async_computation.7 | async-start | bytes 524288 | tf_op jit(solution)/shard_map/all_to_all | solution.py:361
  140.8 5.0 %collective-permute-start.3 = (bf16[256,2048]{1,0:T(8,128)(2,1)S(1)}, bf16[256,2048]{1,0:T(8,128)(2,1)}, u32[]{:S(2)}, u32[]{:S(2)}) collective-permute-start(bf16[256,2048]{1,0:T(8,128)(2,1)S(1)} %copy-done.2), channel_id=1, source_target_pairs={{0,1},{1,0},{2,3},{3,2},{4,5},{5,4},{6,7},{7,6},{8,9},{9,8},{10,11... | collective-permute-start | bytes 3145736 | tf_op jit(solution)/shard_map/ppermute | solution.py:317
  145.9 1.9 collective-permute-start.6
  147.8 2.4 %collective-permute-start.5 = (bf16[256,2048]{1,0:T(8,128)(2,1)S(1)}, bf16[256,2048]{1,0:T(8,128)(2,1)}, u32[]{:S(2)}, u32[]{:S(2)}) collective-permute-start(bf16[256,2048]{1,0:T(8,128)(2,1)S(1)} %collective-permute-done.1.rest_2_), channel_id=1, source_target_pairs={{0,1},{1,0},{2,3},{3,2},{4,5},{5,4},{6,7},{7,6},{8,9},{9,8},{10,11... | collective-permute-start | bytes 3145736 | tf_op jit(solution)/shard_map/ppermute | solution.py:317
  150.2 10.6 %collective-permute-done.rest_1_ = bf16[256,2048]{1,0:T(8,128)(2,1)} collective-permute-done((bf16[256,2048]{1,0:T(8,128)(2,1)S(1)}, bf16[256,2048]{1,0:T(8,128)(2,1)}, u32[]{:S(2)}, u32[]{:S(2)}) %collective-permute-start) | collective-permute-done | bytes 1048608 | tf_op jit(solution)/shard_map/ppermute | solution.py:315
  160.9 2.6 %collective-permute-start.4 = (bf16[256,2048]{1,0:T(8,128)(2,1)}, bf16[256,2048]{1,0:T(8,128)(2,1)}, u32[]{:S(2)}, u32[]{:S(2)}) collective-permute-start(bf16[256,2048]{1,0:T(8,128)(2,1)} %collective-permute-done.rest_1_), channel_id=1, source_target_pairs={{0,1},{1,0},{2,3},{3,2},{4,5},{5,4},{6,7},{7,6},{8,9},{9,8},{10,11... | collective-permute-start | bytes 3145736 | tf_op jit(solution)/shard_map/ppermute | solution.py:317
  163.4 5.5 %shard_map.155.start = f32[128,128]{1,0:T(8,128)} custom-call(s32[4]{0:T(128)} %pad_add_fusion.1.pos, bf16[256,384]{1,0:T(8,128)(2,1)} %bitcast.8.rows, f32[1,32]{1,0:T(1,128)} %bitcast.23, f32[1,32]{1,0:T(1,128)} %bitcast.25, f32[1,32]{1,0:T(1,128)} %bitcast.26), custom_call_target="tpu_custom_call" | custom-call | flops 1000000000 | bytes 1 | tf_op jit(solution)/shard_map/pallas_call | solution.py:356
  169.0 0.7 copy-done.5
  169.7 3.2 %shard_map.159 = bf16[4,128,128]{2,1,0:T(8,128)(2,1)} custom-call(s32[4]{0:T(128)} %pad_add_fusion.1.pos, f32[128,128]{1,0:T(8,128)} %shard_map.155.start, bf16[4,128,256]{2,1,0:T(8,128)(2,1)} %copy-done.5, bf16[4,128,256]{2,1,0:T(8,128)(2,1)} %copy-done.1, bf16[4,128,256]{2,1,0:T(8,128)(2,1)} %all_to_all.52.maps.own), custom_call_target="tpu_custom_call" | custom-call | flops 100000000 | bytes 1 | tf_op jit(solution)/shard_map/pallas_call | solution.py:362
  172.9 9.1 %all_to_all.53 = bf16[4,128,128]{2,1,0:T(8,128)(2,1)} all-to-all(bf16[4,128,128]{2,1,0:T(8,128)(2,1)} %shard_map.159), channel_id=1, replica_groups=mesh['zh'=4,'zl'=4,'y'=4,'x'=4,'c'=2] {'y'}, dimensions={0} | all-to-all | bytes 262144 | tf_op jit(solution)/shard_map/all_to_all | solution.py:365
  182.0 2.1 %shard_map.160 = bf16[256,256]{1,0:T(8,128)(2,1)} custom-call(bf16[2,256,128]{2,1,0:T(8,128)(2,1)} %bitcast.18, bf16[2,256,256]{2,1,0:T(8,128)(2,1)} %get-tuple-element.22.reads, f32[256,256]{1,0:T(8,128)} %get-tuple-element.23.base, f32[1,128]{1,0:T(1,128)} %bitcast.21), custom_call_target="tpu_custom_call" | custom-call | flops 100000000 | bytes 1 | tf_op jit(solution)/shard_map/pallas_call | solution.py:366
  184.0 4.4 %all-to-all-start.9 = ((bf16[8,32,256]{2,1,0:T(8,128)(2,1)}), bf16[8,32,256]{2,1,0:T(8,128)(2,1)S(1)}, u32[]{:S(2)}, u32[]{:S(2)}) async-start(bf16[8,32,256]{2,1,0:T(8,128)(2,1)} %bitcast.17), calls=%async_computation.9 | async-start | bytes 262144 | tf_op jit(solution)/shard_map/all_to_all | solution.py:369
  188.5 0.6 pad_add_fusion.at
  189.0 4.7 %all-to-all-done.9.rows = bf16[8,32,256]{2,1,0:T(8,128)(2,1)S(1)} async-done(((bf16[8,32,256]{2,1,0:T(8,128)(2,1)}), bf16[8,32,256]{2,1,0:T(8,128)(2,1)S(1)}, u32[]{:S(2)}, u32[]{:S(2)}) %all-to-all-start.9) | async-done | bytes 131104 | tf_op jit(solution)/shard_map/all_to_all | solution.py:369
  193.7 0.6 copy-done.7
  194.4 5.8 %shard_map.161 = bf16[32,2048]{1,0:T(8,128)(2,1)} custom-call(s32[8]{0:T(128)} %pad_add_fusion.at, bf16[8,32,256]{2,1,0:T(8,128)(2,1)} %copy-done.7, f32[32,5,256]{2,1,0:T(8,128)} %all_to_all.51.fac, bf16[32,2048]{1,0:T(8,128)(2,1)} %lat.1, bf16[256,2048]{1,0:T(8,128)(2,1)} %rest_0_.1, bf16[256,2048]{1,0:T(8,128)(2,1)} %collective-permute-done.rest_1_, ...), custom_call_target="tpu_custom_call" | custom-call | flops 1000000000 | bytes 1 | tf_op jit(solution)/shard_map/pallas_call | solution.py:370
  (37 shorter events, 0.2 us)
Async XLA Ops:
  0.0 0.8 copy-start.8
  1.1 27.5 %copy-start.12 = (bf16[4,2048]{1,0:T(4,128)(2,1)S(1)}, bf16[4,2048]{1,0:T(4,128)(2,1)}, u32[]{:S(2)}) copy-start(bf16[4,2048]{1,0:T(4,128)(2,1)} %param.18) | copy-start | bytes 49156
  29.2 8.7 %all-to-all-start.1 = ((bf16[4,4,2048]{2,1,0:T(4,128)(2,1)}), bf16[4,4,2048]{2,1,0:T(4,128)(2,1)S(1)}, u32[]{:S(2)}, u32[]{:S(2)}) async-start(bf16[4,4,2048]{2,1,0:T(4,128)(2,1)} %broadcast_in_dim.11), calls=%async_computation.1 | async-start | bytes 131072 | tf_op jit(solution)/shard_map/all_to_all | solution.py:271
  37.9 19.2 %copy-start.6 = (bf16[32,2048]{1,0:T(8,128)(2,1)S(1)}, bf16[32,2048]{1,0:T(8,128)(2,1)}, u32[]{:S(2)}) copy-start(bf16[32,2048]{1,0:T(8,128)(2,1)} %lat.1) | copy-start | bytes 393220
  58.2 3.7 %copy-start.11 = (f32[256,32]{0,1:T(8,128)S(1)}, f32[256,32]{0,1:T(8,128)}, u32[]{:S(2)}) copy-start(f32[256,32]{0,1:T(8,128)} %param.29) | copy-start | bytes 98308
  58.2 18.7 %all-to-all-start = ((bf16[8,32,2048]{2,1,0:T(8,128)(2,1)}), bf16[8,32,2048]{2,1,0:T(8,128)(2,1)S(1)}, u32[]{:S(2)}, u32[]{:S(2)}) async-start(bf16[8,32,2048]{2,1,0:T(8,128)(2,1)} %broadcast_in_dim.10), calls=%async_computation | async-start | bytes 2097152 | tf_op jit(solution)/shard_map/all_to_all | solution.py:271
  62.0 0.9 copy-start.9
  62.9 1.0 copy-start.10
  77.0 1.0 copy-start
  91.4 15.6 %copy-start.2 = (bf16[256,2048]{1,0:T(8,128)(2,1)S(1)}, bf16[256,2048]{1,0:T(8,128)(2,1)}, u32[]{:S(2)}) copy-start(bf16[256,2048]{1,0:T(8,128)(2,1)} %rest_0_.1) | copy-start | bytes 3145732
  103.5 11.4 %copy-start.13 = (bf16[16,384]{1,0:T(8,128)(2,1)S(1)}, bf16[16,384]{1,0:T(8,128)(2,1)}, u32[]{:S(2)}) copy-start(bf16[16,384]{1,0:T(8,128)(2,1)} %get-tuple-element.15) | copy-start | bytes 36868
  103.5 11.4 %all-to-all-start.6 = ((bf16[4,128,256]{2,1,0:T(8,128)(2,1)}), bf16[4,128,256]{2,1,0:T(8,128)(2,1)S(1)}, u32[]{:S(2)}, u32[]{:S(2)}) async-start(bf16[4,128,256]{2,1,0:T(8,128)(2,1)} %shard_map.157), calls=%async_computation.6 | async-start | bytes 524288 | tf_op jit(solution)/shard_map/all_to_all | solution.py:360
  107.0 38.8 %collective-permute-start.2 = (bf16[256,2048]{1,0:T(8,128)(2,1)S(1)}, bf16[256,2048]{1,0:T(8,128)(2,1)S(1)}, u32[]{:S(2)}, u32[]{:S(2)}) collective-permute-start(bf16[256,2048]{1,0:T(8,128)(2,1)S(1)} %copy-done.2), channel_id=1, source_target_pairs={{0,6},{2,0},{4,2},{6,4},{1,7},{3,1},{5,3},{7,5},{8,14},{10,8},{12,... | collective-permute-start | bytes 3145736 | tf_op jit(solution)/shard_map/ppermute | solution.py:315
  109.8 38.0 %collective-permute-start.1 = (bf16[256,2048]{1,0:T(8,128)(2,1)S(1)}, bf16[256,2048]{1,0:T(8,128)(2,1)S(1)}, u32[]{:S(2)}, u32[]{:S(2)}) collective-permute-start(bf16[256,2048]{1,0:T(8,128)(2,1)S(1)} %copy-done.2), channel_id=1, source_target_pairs={{0,4},{2,6},{4,0},{6,2},{1,5},{3,7},{5,1},{7,3},{8,12},{10,14},{12... | collective-permute-start | bytes 3145736 | tf_op jit(solution)/shard_map/ppermute | solution.py:315
  112.9 47.9 %collective-permute-start = (bf16[256,2048]{1,0:T(8,128)(2,1)S(1)}, bf16[256,2048]{1,0:T(8,128)(2,1)}, u32[]{:S(2)}, u32[]{:S(2)}) collective-permute-start(bf16[256,2048]{1,0:T(8,128)(2,1)S(1)} %copy-done.2), channel_id=1, source_target_pairs={{0,2},{2,4},{4,6},{6,0},{1,3},{3,5},{5,7},{7,1},{8,10},{10,12},{12... | collective-permute-start | bytes 3145736 | tf_op jit(solution)/shard_map/ppermute | solution.py:315
  114.9 0.8 copy-start.1
  115.7 18.3 %all-to-all-start.4 = ((bf16[16,16,384]{2,1,0:T(8,128)(2,1)}), bf16[16,16,384]{2,1,0:T(8,128)(2,1)}, u32[]{:S(2)}, u32[]{:S(2)}) async-start(bf16[16,16,384]{2,1,0:T(8,128)(2,1)} %broadcast_in_dim.14), calls=%async_computation.4 | async-start | bytes 393216 | tf_op jit(solution)/shard_map/all_to_all | solution.py:271
  134.0 34.9 %all-to-all-start.7 = ((bf16[4,128,256]{2,1,0:T(8,128)(2,1)}), bf16[4,128,256]{2,1,0:T(8,128)(2,1)S(1)}, u32[]{:S(2)}, u32[]{:S(2)}) async-start(bf16[4,128,256]{2,1,0:T(8,128)(2,1)} %shard_map.158), calls=%async_computation.7 | async-start | bytes 524288 | tf_op jit(solution)/shard_map/all_to_all | solution.py:361
  140.8 48.2 %collective-permute-start.3 = (bf16[256,2048]{1,0:T(8,128)(2,1)S(1)}, bf16[256,2048]{1,0:T(8,128)(2,1)}, u32[]{:S(2)}, u32[]{:S(2)}) collective-permute-start(bf16[256,2048]{1,0:T(8,128)(2,1)S(1)} %copy-done.2), channel_id=1, source_target_pairs={{0,1},{1,0},{2,3},{3,2},{4,5},{5,4},{6,7},{7,6},{8,9},{9,8},{10,11... | collective-permute-start | bytes 3145736 | tf_op jit(solution)/shard_map/ppermute | solution.py:317
  145.8 23.1 %copy-start.3 = (bf16[256,2048]{1,0:T(8,128)(2,1)}, bf16[256,2048]{1,0:T(8,128)(2,1)S(1)}, u32[]{:S(2)}) copy-start(bf16[256,2048]{1,0:T(8,128)(2,1)S(1)} %collective-permute-done.2.rest_3_) | copy-start | bytes 3145732
  145.9 47.9 %collective-permute-start.6 = (bf16[256,2048]{1,0:T(8,128)(2,1)S(1)}, bf16[256,2048]{1,0:T(8,128)(2,1)}, u32[]{:S(2)}, u32[]{:S(2)}) collective-permute-start(bf16[256,2048]{1,0:T(8,128)(2,1)S(1)} %collective-permute-done.2.rest_3_), channel_id=1, source_target_pairs={{0,1},{1,0},{2,3},{3,2},{4,5},{5,4},{6,7},{7,6},{8,9},{9,8},{10,11... | collective-permute-start | bytes 3145736 | tf_op jit(solution)/shard_map/ppermute | solution.py:317
  147.8 21.2 %copy-start.4 = (bf16[256,2048]{1,0:T(8,128)(2,1)}, bf16[256,2048]{1,0:T(8,128)(2,1)S(1)}, u32[]{:S(2)}) copy-start(bf16[256,2048]{1,0:T(8,128)(2,1)S(1)} %collective-permute-done.1.rest_2_) | copy-start | bytes 3145732
  147.8 45.9 %collective-permute-start.5 = (bf16[256,2048]{1,0:T(8,128)(2,1)S(1)}, bf16[256,2048]{1,0:T(8,128)(2,1)}, u32[]{:S(2)}, u32[]{:S(2)}) collective-permute-start(bf16[256,2048]{1,0:T(8,128)(2,1)S(1)} %collective-permute-done.1.rest_2_), channel_id=1, source_target_pairs={{0,1},{1,0},{2,3},{3,2},{4,5},{5,4},{6,7},{7,6},{8,9},{9,8},{10,11... | collective-permute-start | bytes 3145736 | tf_op jit(solution)/shard_map/ppermute | solution.py:317
  160.9 32.9 %collective-permute-start.4 = (bf16[256,2048]{1,0:T(8,128)(2,1)}, bf16[256,2048]{1,0:T(8,128)(2,1)}, u32[]{:S(2)}, u32[]{:S(2)}) collective-permute-start(bf16[256,2048]{1,0:T(8,128)(2,1)} %collective-permute-done.rest_1_), channel_id=1, source_target_pairs={{0,1},{1,0},{2,3},{3,2},{4,5},{5,4},{6,7},{7,6},{8,9},{9,8},{10,11... | collective-permute-start | bytes 3145736 | tf_op jit(solution)/shard_map/ppermute | solution.py:317
  169.0 0.7 copy-start.5
  184.0 9.7 %all-to-all-start.9 = ((bf16[8,32,256]{2,1,0:T(8,128)(2,1)}), bf16[8,32,256]{2,1,0:T(8,128)(2,1)S(1)}, u32[]{:S(2)}, u32[]{:S(2)}) async-start(bf16[8,32,256]{2,1,0:T(8,128)(2,1)} %bitcast.17), calls=%async_computation.9 | async-start | bytes 262144 | tf_op jit(solution)/shard_map/all_to_all | solution.py:369
  193.7 0.7 copy-start.7
where the time goes:
time: 202 us; the launch traced here: 200 us
  blocking collectives  65.5 us (32%)
  starting transfers between devices  48.4 us (24%)
  waiting for transfers between devices  40.8 us (20%)
  Pallas kernels  34.5 us (17%)
  local copies, waits for them, and re-layouts  8.63 us (4%)
  other arithmetic  2.15 us (1%)
    all_to_all x2, blocking collectives, to_all(): lax.all_to_all(jnp.broadcast_to(value[None], (count, *value.shape)), axes...  46.7 us
    all_to_all x3, waiting for transfers between devices, to_all(): lax.all_to_all(jnp.broadcast_to(value[None], (count, *value.shape)), axes...  25.4 us
    all_to_all x3, starting transfers between devices, to_all(): lax.all_to_all(jnp.broadcast_to(value[None], (count, *value.shape)), axes...  13.9 us
    ppermute x4, starting transfers between devices, per_device(): weights.append(lax.ppermute(weights[d], 'c', [(0, 1), (1, 0)]))  11.9 us
    ppermute x3, waiting for transfers between devices, per_device(): weights.append(lax.ppermute(own, 'x', [(i, (i + d) % 4) for i in range(4)]))  10.6 us
    all_to_all x1, blocking collectives, per_device(): of_y = lax.all_to_all(maps, 'y', 0, 0, tiled=True)  9.8 us
    all_to_all x1, blocking collectives, per_device(): states = lax.all_to_all(states, 'y', 0, 0, tiled=True).reshape(2, 256, 128)  9.06 us
    pallas_call x1, Pallas kernels, per_device(): call(chunk_kernel, [((4, 128, 256), BF), ((2, 256, 256), BF), ((256, 256)...  8.07 us
  transfers between devices with their start and end apart: 13, of which 5 were waited for; matrix products, arithmetic and copies ran while one was open for 3% of the time, Pallas kernels for 7%

commit v1 on v0

v1 whole, which is shorter than its diff:
```python
from functools import partial

import jax
import jax.numpy as jnp
from jax import lax
from jax.experimental import pallas as pl
from jax.experimental.pallas import tpu as pltpu
from jax.sharding import Mesh
from jax.sharding import PartitionSpec as P


D = 2048
EPS = 1e-06
HI = lax.Precision.HIGHEST
F32 = jnp.float32
BF = jnp.bfloat16
Z = ("zh", "zl")
TP = ("x", "c")
SP = ("zh", "zl", "y")
ALL = ("zh", "zl", "y", "x", "c")
VM = pl.BlockSpec(memory_space=pltpu.VMEM)
SM = pl.BlockSpec(memory_space=pltpu.SMEM)


def mm(a, b, dims=((1,), (0,))):
    return lax.dot_general(
        a.astype(BF), b.astype(BF), (dims, ((), ())), preferred_element_type=F32
    )


def norm_rows(rows, scale, shift):
    wide = rows.astype(F32)
    centred = wide - jnp.mean(wide, axis=-1, keepdims=True)
    spread = jnp.mean(centred * centred, axis=-1, keepdims=True)
    return (centred * lax.rsqrt(spread + EPS) * (1.0 + scale) + shift).astype(BF)


def column(matrix, lane):
    lanes = lax.broadcasted_iota(jnp.int32, matrix.shape, 1)
    return jnp.sum(jnp.where(lanes == lane, matrix, 0.0), axis=1, keepdims=True)


def softplus(t):
    return jnp.maximum(t, 0.0) + jnp.log1p(jnp.exp(-jnp.abs(t)))


def sigmoid(t):
    return 1.0 / (1.0 + jnp.exp(-t))


def inverse_of(lower, row, col):
    eye = (row == col).astype(F32)
    own = (row // 16) == (col // 16)
    base = [jnp.where(own, m, 0.0) for m in lower]
    inv = [eye - m for m in base]
    power = [mm(m, m) for m in base]
    for step in range(3):
        inv = [p + mm(p, x) for p, x in zip(inv, power)]
        if step < 2:
            power = [mm(x, x) for x in power]
    size = 16
    while size < 256:
        here = ((row // (2 * size)) == (col // (2 * size))) & ((row // size) != (col // size))
        side = [mm(jnp.where(here, m, 0.0), p) for m, p in zip(lower, inv)]
        inv = [p - mm(p, s) for p, s in zip(inv, side)]
        size *= 2
    out = []
    for m, p in zip(lower, inv):
        first = p.astype(BF)
        high = m.astype(BF)
        low = (m - high.astype(F32)).astype(BF)
        wide = first.astype(F32)
        left = (eye - wide) - (mm(high, first) + mm(low, first))
        out.append(wide + mm(first, left))
    return out


def project_kernel(pos, one, two, ctx, fac, wq, wk, wv, wd, ww, q_o, k_o, v_o, r_o, w_o, c_o, hid):
    factors = [[], [], [], []]
    for t in range(8):
        f = (fac[t] + fac[8 + t]) + (fac[16 + t] + fac[24 + t])
        for slot, r in enumerate((0, 1, 3, 4)):
            factors[slot].append(f[r : r + 1])
    shift, scale, c_shift, c_scale = (jnp.concatenate(f, axis=1) for f in factors)
    for d in range(4):
        for lat, core in ((one, pos[6]), (two, 1 - pos[6])):
            spot = (2 * ((pos[7] + 4 - d) % 4) + core) * 32
            hid[pl.ds(pl.multiple_of(spot, 32), 32)] = norm_rows(lat[d], scale, shift)
    hid[256:260] = norm_rows(ctx[...], c_scale, c_shift)
    hid[260:272] = jnp.zeros((12, D), BF)
    rows = hid[...]
    q_o[...] = mm(hid[0:256], wq[...]).astype(BF)
    keys = mm(rows, wk[...]).astype(BF)
    values = mm(rows, wv[...]).astype(BF)
    k_o[...] = keys[:256]
    v_o[...] = values[:256]
    last_two = ((1,), (1,))
    r_o[...] = mm(wd[...], hid[0:256], last_two).astype(BF).astype(F32)
    w_o[...] = mm(ww[...], hid[0:256], last_two).astype(BF).astype(F32)
    rate = mm(hid[256:264], wd[...], last_two).astype(BF).astype(F32)
    write = mm(hid[256:264], ww[...], last_two).astype(BF).astype(F32)
    lanes = lax.broadcasted_iota(jnp.int32, (8, 256), 1)
    spots = lanes == lax.broadcasted_iota(jnp.int32, (8, 256), 0) + pos[5]
    wide = [rows_of[256:264].astype(F32) for rows_of in (keys, values)]
    for j in range(4):
        h = j // 2
        to = (j + pos[4]) % 4
        lane = pos[1] * 4 + j
        pieces = [
            jnp.concatenate([w[0:4, 128 * h : 128 * h + 128] for w in wide], axis=1),
            jnp.sum(jnp.where(spots, column(rate, lane), 0.0), axis=0, keepdims=True),
            jnp.sum(jnp.where(spots, column(write, lane), 0.0), axis=0, keepdims=True),
            jnp.zeros((10, 256), F32),
        ]
        c_o[to] = jnp.concatenate(pieces, axis=0).astype(BF)


def chunk_kernel(pos, q, k, v, rate, write, rows, spike, decay, bias, m_o, r_o, o_o):
    row = lax.broadcasted_iota(jnp.int32, (256, 256), 0)
    col = lax.broadcasted_iota(jnp.int32, (256, 256), 1)
    eye = row == col
    logs = -decay[...] * softplus(rate[...]) + spike[...]
    strength = sigmoid(write[...] + bias[...])
    entry = lax.broadcasted_iota(jnp.int32, (32, 256), 0) - pos[1] * 4
    below = (row >= col).astype(F32)
    above = (row <= col).astype(F32)
    sums = (
        jnp.dot(logs, above, precision=HI, preferred_element_type=F32),
        jnp.dot(logs, below, precision=HI, preferred_element_type=F32),
    )

    def upright(line):
        return jnp.sum(jnp.where(eye, line, 0.0), axis=1, keepdims=True)

    lowers, parts = ([], [])
    for h in range(2):
        kh = k[:, 128 * h : 128 * h + 128]
        qh = q[:, 128 * h : 128 * h + 128]
        kf = kh.astype(F32)
        unit = lax.rsqrt(jnp.sum(kf * kf, axis=1, keepdims=True) + EPS)
        unit_row = jnp.sum(jnp.where(eye, unit, 0.0), axis=0, keepdims=True)
        gram = mm(kh, kh, ((1,), (1,))) * unit_row
        cross = mm(qh, kh, ((1,), (1,))) * unit_row
        for e in range(2):
            j = 2 * h + e
            total_row = jnp.sum(jnp.where(entry == j, sums[e], 0.0), axis=0, keepdims=True)
            total = upright(total_row)
            b = upright(jnp.sum(jnp.where(entry == j, strength, 0.0), axis=0, keepdims=True))
            last = total[255:256] if e == 0 else total[0:1]
            inside = row >= col if e == 0 else row <= col
            fade = jnp.where(inside, jnp.exp(jnp.where(inside, total - total_row, 0.0)), 0.0)
            lowers.append(jnp.where(eye, 0.0, (b * unit) * gram * fade))
            grown = jnp.exp(total)
            right = jnp.concatenate(
                [
                    b * v[:, 128 * h : 128 * h + 128].astype(F32),
                    (b * unit * grown) * kf,
                ],
                axis=1,
            ).astype(BF)
            faded = (kf * (unit * jnp.exp(last - total))).astype(BF)
            scores = (cross * fade).astype(BF)
            parts.append((right, faded, scores, grown * qh.astype(F32), jnp.exp(last) - 1.0))
    solved = inverse_of(lowers, row, col)
    small = lax.broadcasted_iota(jnp.int32, (128, 128), 0) == lax.broadcasted_iota(
        jnp.int32, (128, 128), 1
    )
    outs = [None, None]
    for j in range(4):
        right, faded, scores, grown_q, short = parts[j]
        both = mm(solved[j], right).astype(BF)
        maps = mm(faded, both, ((0,), (0,)))
        read = mm(scores, both)
        to = (j + pos[4]) % 4
        m_o[to, 0:128, 0:128] = (jnp.where(small, short, 0.0) - maps[:, 128:]).astype(BF)
        m_o[to, 0:128, 128:256] = maps[:, :128].astype(BF)
        h, e = divmod(j, 2)
        r_o[h, :, 128 * e : 128 * e + 128] = (grown_q - read[:, 128:]).astype(BF)
        outs[h] = read[:, :128] if e == 0 else outs[h] + read[:, :128]
    m_o[:, 128:144] = rows[...]
    o_o[:, 0:128] = outs[0]
    o_o[:, 128:256] = outs[1]


def context_state(pos, rows, rate, write, decay, bias, extra):
    row = lax.broadcasted_iota(jnp.int32, (256, 256), 0)
    col = lax.broadcasted_iota(jnp.int32, (256, 256), 1)
    eye = row == col
    lane = pos[1] * 4 + pos[0]
    inside = (row - col) * (1 - 2 * (pos[0] % 2)) >= 0
    kh = rows[:, 0:128].astype(BF)
    kf = rows[:, 0:128]
    logs = -column(decay, lane) * softplus(rate)
    strength = sigmoid(write + column(bias, lane) + column(extra, lane))
    b = jnp.sum(jnp.where(eye, strength, 0.0), axis=1, keepdims=True)
    total = jnp.sum(jnp.where(inside, logs, 0.0), axis=1, keepdims=True)
    total_row = jnp.sum(jnp.where(eye, total, 0.0), axis=0, keepdims=True)
    last = jnp.sum(logs, axis=1, keepdims=True)
    unit = lax.rsqrt(jnp.sum(kf * kf, axis=1, keepdims=True) + EPS)
    unit_row = jnp.sum(jnp.where(eye, unit, 0.0), axis=0, keepdims=True)
    fade = jnp.where(inside, jnp.exp(jnp.where(inside, total - total_row, 0.0)), 0.0)
    lower = jnp.where(
        eye, 0.0, (b * unit) * (mm(kh, kh, ((1,), (1,))) * unit_row) * fade
    )
    solved = inverse_of([lower], row, col)[0]
    fresh = mm(solved, b * rows[:, 128:256])
    faded = kf * (unit * jnp.exp(last - total))
    return mm(faded, fresh, ((0,), (0,)))


def apply_to(linear, state):
    high = state.astype(BF)
    low = (state - high.astype(F32)).astype(BF)
    both = mm(linear, jnp.concatenate([high, low], axis=1))
    n = state.shape[1]
    return both[:, :n] + both[:, n:]


def compose_kernel(pos, maps, o, *, count):
    back = pos[0] % 2
    at = back * 3
    step = 1 - 2 * back
    total = maps[at][0:128].astype(F32)
    for _ in range(3):
        at = at + step
        total = total + maps[at][0:128].astype(F32) + apply_to(maps[at][0:128, 0:128], total)
    wide = [maps[i][128:].astype(F32) for i in range(4)]
    rows = [w[0:count] for w in wide]
    gates = sum(w[count : count + 2] for w in wide)
    out = jnp.concatenate([total, *rows, gates, jnp.zeros((14, 256), F32)], axis=0).astype(BF)
    for i in range(4):
        o[i] = out


def scan_kernel(pos, high, low, own, decay, bias, extra, o):
    back = pos[0] % 2
    step = 1 - 2 * back
    wide = [high[i][128:].astype(F32) for i in range(4)]
    rows = jnp.concatenate([w[0:64] for w in wide], axis=0)
    gates = sum(w[64:66] for w in wide)
    state = context_state(
        pos, rows, gates[0:1], gates[1:2], decay[...], bias[...], extra[...]
    )
    for maps, mine in ((high, pos[2]), (low, pos[3])):
        at = back * 3
        for _ in range(3):
            m = maps[at][0:128]
            moved = state + m[:, 128:256].astype(F32) + apply_to(m[:, 0:128], state)
            state = jnp.where((mine - at) * step > 0, moved, state)
            at = at + step
    at = back * 3
    for i in range(4):
        o[at] = state.astype(BF)
        if i < 3:
            m = own[at][0:128]
            state = state + m[:, 128:256].astype(F32) + apply_to(m[:, 0:128], state)
        at = at + step


def read_kernel(pos, states, reads, base, gain, weight, o):
    heads = []
    for h in range(2):
        first = states[(2 * h + pos[4]) % 4]
        second = states[(2 * h + 1 + pos[4]) % 4]
        total = base[:, 128 * h : 128 * h + 128] + (
            mm(reads[h][:, 0:128], first) + mm(reads[h][:, 128:256], second)
        )
        mean = jnp.mean(total * total, axis=1, keepdims=True)
        heads.append((total * lax.rsqrt(mean + EPS) * gain[...]).astype(BF))
    branch = mm(jnp.concatenate(heads, axis=1), weight[...]).astype(BF)
    for t in range(8):
        o[t] = branch[32 * t : 32 * t + 32]


def output_kernel(rows, fac, lat, o):
    branch = rows[0].astype(F32)
    for i in range(1, 8):
        branch = branch + rows[i].astype(F32)
    gates = []
    for t in range(8):
        f = (fac[t] + fac[8 + t]) + (fac[16 + t] + fac[24 + t])
        gates.append(f[2:3])
    gate = jnp.concatenate(gates, axis=1)
    o[...] = (lat[...].astype(F32) + gate * branch).astype(BF)


def call(kernel, outs, specs, scratch=(), flops=1):
    def shape(s):
        return jax.ShapeDtypeStruct(*s)

    many = isinstance(outs, list)
    return pl.pallas_call(
        kernel,
        out_shape=[shape(s) for s in outs] if many else shape(outs),
        in_specs=specs,
        out_specs=[VM] * len(outs) if many else VM,
        scratch_shapes=scratch,
        compiler_params=pltpu.CompilerParams(vmem_limit_bytes=24 * 2**20),
        cost_estimate=pl.CostEstimate(flops=flops, bytes_accessed=1, transcendentals=0),
    )


def to_all(value, axes, count):
    return lax.all_to_all(
        jnp.broadcast_to(value[None], (count, *value.shape)), axes, 0, 0, tiled=True
    )


def per_device(
    latent,
    condition,
    context,
    context_condition_vector,
    modulation_matrix,
    query_matrix,
    key_matrix,
    value_matrix,
    decay_input_weight,
    write_strength_weight,
    head_decay_rate,
    write_strength_bias,
    context_write_offset_bias,
    log_spike_added,
    head_norm_gain,
    output_matrix,
):
    zh, zl, y = (lax.axis_index("zh"), lax.axis_index("zl"), lax.axis_index("y"))
    x, c = (lax.axis_index("x"), lax.axis_index("c"))
    sp_index = lax.axis_index(SP)
    pos = jnp.stack([(y + c) % 4, x * 2 + c, zh, zl, (4 - c) % 4, sp_index * 4, c, x])
    pos = pos.astype(jnp.int32)
    parts = [latent]
    for d in range(1, 4):
        parts.append(lax.ppermute(latent, "x", [(i, (i + d) % 4) for i in range(4)]))
    mine = jnp.stack(parts)
    other = lax.ppermute(mine, "c", [(0, 1), (1, 0)])
    signals = jnp.stack([condition, context_condition_vector])
    signals = lax.dynamic_slice_in_dim(jax.nn.silu(signals), sp_index * 32, 32, 1)
    mod = modulation_matrix.astype(F32)
    part = jnp.concatenate(
        [
            jnp.sum(mod * signals[0][None, :, None], axis=1),
            jnp.sum(mod[:2] * signals[1][None, :, None], axis=1),
        ]
    )
    part = to_all(part, Z, 16)
    part = jnp.sum(part, axis=0)
    fac = to_all(part, ("y", "x", "c"), 32)

    queries, keys, values, rate, write, rows = call(
        project_kernel,
        [
            ((256, 256), BF),
            ((256, 256), BF),
            ((256, 256), BF),
            ((32, 256), F32),
            ((32, 256), F32),
            ((4, 16, 256), BF),
        ],
        [SM] + [VM] * 9,
        [pltpu.VMEM((272, D), BF)],
        flops=10**9,
    )(
        pos,
        mine,
        other,
        context,
        fac,
        query_matrix,
        key_matrix,
        value_matrix,
        decay_input_weight.T,
        write_strength_weight.T,
    )
    maps, reads, base = call(
        chunk_kernel,
        [((4, 144, 256), BF), ((2, 256, 256), BF), ((256, 256), F32)],
        [SM] + [VM] * 9,
        flops=4 * 10**9,
    )(
        pos,
        queries,
        keys,
        values,
        rate,
        write,
        rows,
        log_spike_added.T,
        head_decay_rate.reshape(32, 1),
        write_strength_bias.reshape(32, 1),
    )
    of_y = lax.all_to_all(maps, "y", 0, 0, tiled=True)
    low = call(partial(compose_kernel, count=4), ((4, 160, 256), BF), [SM, VM])(pos, of_y)
    of_low = lax.all_to_all(low, "zl", 0, 0, tiled=True)
    high = call(partial(compose_kernel, count=16), ((4, 208, 256), BF), [SM, VM])(pos, of_low)
    of_high = lax.all_to_all(high, "zh", 0, 0, tiled=True)
    states = call(scan_kernel, ((4, 128, 128), BF), [SM] + [VM] * 6, flops=10**8)(
        pos,
        of_high,
        of_low,
        of_y,
        head_decay_rate.reshape(1, 32),
        write_strength_bias.reshape(1, 32),
        context_write_offset_bias.reshape(1, 32),
    )
    states = lax.all_to_all(states, "y", 0, 0, tiled=True)
    branch = call(read_kernel, ((8, 32, D), BF), [SM] + [VM] * 5, flops=10**8)(
        pos, states, reads, base, head_norm_gain.reshape(1, 128), output_matrix
    )
    branch = lax.all_to_all(branch, TP, 0, 0, tiled=True)
    return call(output_kernel, ((32, D), BF), [VM] * 3, flops=10**8)(branch, fac, latent)


def solution(mesh):
    split = Mesh(mesh.devices.reshape(4, 4, 4, 4, 2), ALL)
    return jax.shard_map(
        per_device,
        mesh=split,
        in_specs=(
            P(ALL, None),
            P(),
            P(SP, None),
            P(),
            P(None, SP, TP),
            P(None, TP),
            P(None, TP),
            P(None, TP),
            P(),
            P(),
            P(),
            P(),
            P(),
            P(SP, None),
            P(),
            P(TP, None),
        ),
        out_specs=P(ALL, None),
        check_vma=False,
    )
```

time: 202 us -> 170 us (0.84)
  blocking collectives: 65.5 us -> 105 us
  waiting for transfers between devices: 40.8 us -> 7.3 us
  starting transfers between devices: 48.4 us -> 28.7 us
  Pallas kernels: 34.5 us -> 18.8 us
    all_to_all x1 -> x4, blocking collectives: 9.06 us -> 71.6 us  [the longest x1 27.8 us: per_device(): of_high = lax.all_to_all(high, 'zh', 0, 0, tiled=True)]
    all_to_all x2 -> x1, blocking collectives: 46.7 us -> 24.2 us  [to_all(): lax.all_to_all(jnp.broadcast_to(value[None], (count, *value.shape)), axes...]
    all_to_all x3 -> x1, waiting for transfers between devices: 25.4 us -> 6.07 us  [to_all(): lax.all_to_all(jnp.broadcast_to(value[None], (count, *value.shape)), axes...]
    all_to_all x3 -> x0, starting transfers between devices: 14.7 us -> none  [the longest x1 6.76 us: per_device(): of_high = lax.all_to_all(group(pos, of_low), 'zh', 0, 0, tiled=True)]
    pallas_call x7 -> x6, Pallas kernels: 29.1 us -> 15.7 us  [the longest x1 6.19 us: per_device(): call(chunk_kernel, [((4, 144, 256), BF), ((2, 256, 256), BF), ((256, 256)...]
    ppermute x7 -> x4, waiting for transfers between devices: 10.7 us -> 1.23 us  [the longest x3 1.23 us: per_device(): lax.ppermute(latent, 'x', [(i, (i + d) % 4) for i in range(4)])]
    all_to_all x3 -> x0, waiting for transfers between devices: 4.7 us -> none  [the longest x1 4.69 us: per_device(): heads = lax.all_to_all(normed.reshape(8, 32, 256), TP, 0, 0, tiled=True)]
    all_to_all x3 -> x1, starting transfers between devices: 13.9 us -> 9.58 us  [to_all(): lax.all_to_all(jnp.broadcast_to(value[None], (count, *value.shape)), axes...]
  transfers between devices with their start and end apart: 13 -> 5, of which waited for: 5 -> 2; matrix products, arithmetic and copies ran while one was open for 3% -> 2% of each run, Pallas kernels for 7% -> 0%
where the time goes in v1:
time: 170 us; the launch traced here: 169 us
  blocking collectives  105 us (62%)
  starting transfers between devices  28.7 us (17%)
  Pallas kernels  18.8 us (11%)
  local copies, waits for them, and re-layouts  7.93 us (5%)
  waiting for transfers between devices  7.3 us (4%)
    all_to_all x1, blocking collectives, per_device(): of_high = lax.all_to_all(high, 'zh', 0, 0, tiled=True)  27.8 us
    all_to_all x1, blocking collectives, to_all(): lax.all_to_all(jnp.broadcast_to(value[None], (count, *value.shape)), axes...  24.2 us
    all_to_all x1, blocking collectives, per_device(): branch = lax.all_to_all(branch, TP, 0, 0, tiled=True)  23.8 us
    all_to_all x1, blocking collectives, per_device(): of_low = lax.all_to_all(low, 'zl', 0, 0, tiled=True)  12.8 us
    ppermute x3, starting transfers between devices, per_device(): lax.ppermute(latent, 'x', [(i, (i + d) % 4) for i in range(4)])  12.1 us
    all_to_all x1, starting transfers between devices, to_all(): lax.all_to_all(jnp.broadcast_to(value[None], (count, *value.shape)), axes...  9.58 us
    all_to_all x1, blocking collectives, per_device(): of_y = lax.all_to_all(maps, 'y', 0, 0, tiled=True)  9.04 us
    all_to_all x1, blocking collectives, per_device(): states = lax.all_to_all(states, 'y', 0, 0, tiled=True)  7.21 us
  transfers between devices with their start and end apart: 5, of which 2 were waited for; matrix products, arithmetic and copies ran while one was open for 2% of the time, Pallas kernels for 0%

profile of v1, /device:TPU:1, one launch (start us, length us, event | category | flops | bytes accessed | tf_op | source)
XLA Modules:
  0.0 168.9 jit_solution(3725683089212398505)
XLA Ops:
  0.0 5.6 %collective-permute-start.1 = (bf16[32,2048]{1,0:T(8,128)(2,1)}, bf16[32,2048]{1,0:T(8,128)(2,1)S(1)}, u32[]{:S(2)}, u32[]{:S(2)}) collective-permute-start(bf16[32,2048]{1,0:T(8,128)(2,1)} %lat.1), channel_id=1, source_target_pairs={{0,4},{2,6},{4,0},{6,2},{1,5},{3,7},{5,1},{7,3},{8,12},{10,14},{12... | collective-permute-start | bytes 393224 | tf_op jit(solution)/shard_map/ppermute | solution.py:334
  5.6 2.2 %collective-permute-start = (bf16[32,2048]{1,0:T(8,128)(2,1)}, bf16[32,2048]{1,0:T(8,128)(2,1)S(1)}, u32[]{:S(2)}, u32[]{:S(2)}) collective-permute-start(bf16[32,2048]{1,0:T(8,128)(2,1)} %lat.1), channel_id=1, source_target_pairs={{0,2},{2,4},{4,6},{6,0},{1,3},{3,5},{5,7},{7,1},{8,10},{10,12},{12... | collective-permute-start | bytes 393224 | tf_op jit(solution)/shard_map/ppermute | solution.py:334
  7.8 4.3 %collective-permute-start.2 = (bf16[32,2048]{1,0:T(8,128)(2,1)}, bf16[32,2048]{1,0:T(8,128)(2,1)S(1)}, u32[]{:S(2)}, u32[]{:S(2)}) collective-permute-start(bf16[32,2048]{1,0:T(8,128)(2,1)} %lat.1), channel_id=1, source_target_pairs={{0,6},{2,0},{4,2},{6,4},{1,7},{3,1},{5,3},{7,5},{8,14},{10,8},{12,... | collective-permute-start | bytes 393224 | tf_op jit(solution)/shard_map/ppermute | solution.py:334
  12.1 0.8 divide_multiply_fusion
  12.9 0.0 copy-done.15
  12.9 0.0 copy-start.4
  12.9 0.1 fusion
  13.0 0.1 multiply_reduce_fusion
  13.1 0.0 collective-permute-done.1
  13.1 0.0 collective-permute-done
  13.1 1.2 collective-permute-done.2
  14.4 0.0 copy-done.4
  14.4 0.1 pad_maximum_fusion.one
  14.4 7.0 %collective-permute-start.3 = (bf16[4,32,2048]{2,1,0:T(8,128)(2,1)S(1)}, bf16[4,32,2048]{2,1,0:T(8,128)(2,1)S(1)}, u32[]{:S(2)}, u32[]{:S(2)}) collective-permute-start(bf16[4,32,2048]{2,1,0:T(8,128)(2,1)S(1)} %pad_maximum_fusion.one), channel_id=1, source_target_pairs={{0,1},{1,0},{2,3},{3,2},{4,5},{5,4},{6,7},{7,6},{8,9},{9,8},{10,11... | collective-permute-start | bytes 1572872 | tf_op jit(solution)/shard_map/ppermute | solution.py:336
  21.5 24.2 %all_to_all.35 = f32[16,5,256]{2,1,0:T(8,128)S(1)} all-to-all(f32[16,5,256]{2,1,0:T(8,128)S(1)} %broadcast_in_dim.4), channel_id=1, replica_groups=mesh['zh'=4,'zl'=4,'y'=4,'x'=4,'c'=2] {'zh','zl'}, dimensions={0} | all-to-all | bytes 163840 | tf_op jit(solution)/shard_map/all_to_all | solution.py:304
  45.7 0.7 broadcast_in_dim.5
  46.5 9.6 %all-to-all-start.1 = ((f32[32,5,256]{2,1,0:T(8,128)}), f32[32,5,256]{2,1,0:T(8,128)S(1)}, u32[]{:S(2)}, u32[]{:S(2)}) async-start(f32[32,5,256]{2,1,0:T(8,128)} %broadcast_in_dim.5), calls=%async_computation.1 | async-start | bytes 524288 | tf_op jit(solution)/shard_map/all_to_all | solution.py:304
  56.1 0.0 copy-start.11
  56.1 0.6 copy-done.11
  56.7 0.7 copy.23.bias
  57.4 0.7 copy-done.10
  58.1 0.7 copy.22.decay
  58.8 0.1 stack.59.pos
  58.8 6.1 %all-to-all-done.1.fac = f32[32,5,256]{2,1,0:T(8,128)S(1)} async-done(((f32[32,5,256]{2,1,0:T(8,128)}), f32[32,5,256]{2,1,0:T(8,128)S(1)}, u32[]{:S(2)}, u32[]{:S(2)}) %all-to-all-start.1) | async-done | bytes 163872 | tf_op jit(solution)/shard_map/all_to_all | solution.py:304
  64.9 0.0 collective-permute-done.3.two
  64.9 0.0 copy-done
  64.9 0.0 copy-done.1
  64.9 0.0 copy-start.2
  64.9 1.2 copy-done.2
  66.2 0.9 copy-done.5
  67.1 0.9 copy-done.6
  68.0 0.7 copy-done.7
  68.7 3.0 %shard_map.154 = (bf16[256,256]{1,0:T(8,128)(2,1)S(1)}, bf16[256,256]{1,0:T(8,128)(2,1)S(1)}, bf16[256,256]{1,0:T(8,128)(2,1)S(1)}, f32[32,256]{1,0:T(8,128)S(1)...) custom-call(s32[8]{0:T(128)S(1)} %stack.59.pos, bf16[4,32,2048]{2,1,0:T(8,128)(2,1)S(1)} %pad_maximum_fusion.one, ...), custom_call_target="tpu_custom_call" | custom-call | flops 1000000000 | bytes 1 | tf_op jit(solution)/shard_map/pallas_call | solution.py:350
  71.7 0.0 copy-done.8
  71.7 0.0 copy-done.9
  71.8 6.2 %shard_map.155 = (bf16[4,144,256]{2,1,0:T(8,128)(2,1)S(1)}, bf16[2,256,256]{2,1,0:T(8,128)(2,1)S(1)}, f32[256,256]{1,0:T(8,128)S(1)}) custom-call(s32[8]{0:T(128)S(1)} %stack.59.pos, bf16[256,256]{1,0:T(8,128)(2,1)S(1)} %get-tuple-element.14.q, bf16[256,256]{1,0:T(8,128)(2,1)S(1)} %get-tuple-element.15.k, bf16[256,256]{1,0:T(8,128)(2,1)S(1)} %get-tuple-element.16.v, ...), custom_call_target="tpu_custom_call" | custom-call | flops 4000000000 | bytes 1 | tf_op jit(solution)/shard_map/pallas_call | solution.py:375
  78.0 9.0 %all_to_all.36.maps.own = bf16[4,144,256]{2,1,0:T(8,128)(2,1)S(1)} all-to-all(bf16[4,144,256]{2,1,0:T(8,128)(2,1)S(1)} %get-tuple-element.20), channel_id=1, replica_groups=mesh['zh'=4,'zl'=4,'y'=4,'x'=4,'c'=2] {'y'}, dimensions={0} | all-to-all | bytes 589824 | tf_op jit(solution)/shard_map/all_to_all | solution.py:392
  87.0 1.1 shard_map.156
  88.1 12.8 %all_to_all.37.maps.low = bf16[4,160,256]{2,1,0:T(8,128)(2,1)S(1)} all-to-all(bf16[4,160,256]{2,1,0:T(8,128)(2,1)S(1)} %shard_map.156), channel_id=1, replica_groups=mesh['zh'=4,'zl'=4,'y'=4,'x'=4,'c'=2] {'zl'}, dimensions={0} | all-to-all | bytes 655360 | tf_op jit(solution)/shard_map/all_to_all | solution.py:394
  100.9 1.1 shard_map.157
  102.0 0.0 copy-start.3
  102.1 27.8 %all_to_all.38.high = bf16[4,208,256]{2,1,0:T(8,128)(2,1)S(1)} all-to-all(bf16[4,208,256]{2,1,0:T(8,128)(2,1)S(1)} %shard_map.157), channel_id=1, replica_groups=mesh['zh'=4,'zl'=4,'y'=4,'x'=4,'c'=2] {'zh'}, dimensions={0} | all-to-all | bytes 851968 | tf_op jit(solution)/shard_map/all_to_all | solution.py:396
  129.8 5.3 %shard_map.158 = bf16[4,128,128]{2,1,0:T(8,128)(2,1)S(1)} custom-call(s32[8]{0:T(128)S(1)} %stack.59.pos, bf16[4,208,256]{2,1,0:T(8,128)(2,1)S(1)} %all_to_all.38.high, bf16[4,160,256]{2,1,0:T(8,128)(2,1)S(1)} %all_to_all.37.maps.low, bf16[4,144,256]{2,1,0:T(8,128)(2,1)S(1)} %all_to_all.36.maps.own, f32[1,32]{1,0:T(1,128)S(1)} %bitcast.31, ...), custom_call_target="tpu_custom_call" | custom-call | flops 100000000 | bytes 1 | tf_op jit(solution)/shard_map/pallas_call | solution.py:397
  135.1 7.2 %all_to_all.39.states = bf16[4,128,128]{2,1,0:T(8,128)(2,1)S(1)} all-to-all(bf16[4,128,128]{2,1,0:T(8,128)(2,1)S(1)} %shard_map.158), channel_id=1, replica_groups=mesh['zh'=4,'zl'=4,'y'=4,'x'=4,'c'=2] {'y'}, dimensions={0} | all-to-all | bytes 262144 | tf_op jit(solution)/shard_map/all_to_all | solution.py:406
  142.3 0.7 copy-done.13
  143.0 1.2 shard_map.159
  144.2 23.8 %all_to_all.40.rows = bf16[8,32,2048]{2,1,0:T(8,128)(2,1)S(1)} all-to-all(bf16[8,32,2048]{2,1,0:T(8,128)(2,1)S(1)} %shard_map.159), channel_id=1, replica_groups=mesh['zh'=4,'zl'=4,'y'=4,'x'=4,'c'=2] {'x','c'}, dimensions={0} | all-to-all | bytes 2097152 | tf_op jit(solution)/shard_map/all_to_all | solution.py:410
  168.0 0.8 shard_map.160
  (20 shorter events, 0.1 us)
Async XLA Ops:
  0.0 12.9 %copy-start.15 = (bf16[3,32,256]{2,1,0:T(8,128)(2,1)S(1)}, bf16[3,32,256]{2,1,0:T(8,128)(2,1)}, u32[]{:S(2)}) copy-start(bf16[3,32,256]{2,1,0:T(8,128)(2,1)} %param.20) | copy-start | bytes 147460
  0.0 13.1 %collective-permute-start.1 = (bf16[32,2048]{1,0:T(8,128)(2,1)}, bf16[32,2048]{1,0:T(8,128)(2,1)S(1)}, u32[]{:S(2)}, u32[]{:S(2)}) collective-permute-start(bf16[32,2048]{1,0:T(8,128)(2,1)} %lat.1), channel_id=1, source_target_pairs={{0,4},{2,6},{4,0},{6,2},{1,5},{3,7},{5,1},{7,3},{8,12},{10,14},{12... | collective-permute-start | bytes 393224 | tf_op jit(solution)/shard_map/ppermute | solution.py:334
  5.6 7.5 %collective-permute-start = (bf16[32,2048]{1,0:T(8,128)(2,1)}, bf16[32,2048]{1,0:T(8,128)(2,1)S(1)}, u32[]{:S(2)}, u32[]{:S(2)}) collective-permute-start(bf16[32,2048]{1,0:T(8,128)(2,1)} %lat.1), channel_id=1, source_target_pairs={{0,2},{2,4},{4,6},{6,0},{1,3},{3,5},{5,7},{7,1},{8,10},{10,12},{12... | collective-permute-start | bytes 393224 | tf_op jit(solution)/shard_map/ppermute | solution.py:334
  7.8 6.5 %collective-permute-start.2 = (bf16[32,2048]{1,0:T(8,128)(2,1)}, bf16[32,2048]{1,0:T(8,128)(2,1)S(1)}, u32[]{:S(2)}, u32[]{:S(2)}) collective-permute-start(bf16[32,2048]{1,0:T(8,128)(2,1)} %lat.1), channel_id=1, source_target_pairs={{0,6},{2,0},{4,2},{6,4},{1,7},{3,1},{5,3},{7,5},{8,14},{10,8},{12,... | collective-permute-start | bytes 393224 | tf_op jit(solution)/shard_map/ppermute | solution.py:334
  12.9 1.5 copy-start.4
  14.4 50.6 %copy-start = (bf16[2048,256]{1,0:T(8,128)(2,1)S(1)}, bf16[2048,256]{1,0:T(8,128)(2,1)}, u32[]{:S(2)}) copy-start(bf16[2048,256]{1,0:T(8,128)(2,1)} %wq.1) | copy-start | bytes 3145732
  14.4 50.6 %copy-start.1 = (bf16[2048,256]{1,0:T(8,128)(2,1)S(1)}, bf16[2048,256]{1,0:T(8,128)(2,1)}, u32[]{:S(2)}) copy-start(bf16[2048,256]{1,0:T(8,128)(2,1)} %wk.1) | copy-start | bytes 3145732
  14.4 50.5 %collective-permute-start.3 = (bf16[4,32,2048]{2,1,0:T(8,128)(2,1)S(1)}, bf16[4,32,2048]{2,1,0:T(8,128)(2,1)S(1)}, u32[]{:S(2)}, u32[]{:S(2)}) collective-permute-start(bf16[4,32,2048]{2,1,0:T(8,128)(2,1)S(1)} %pad_maximum_fusion.one), channel_id=1, source_target_pairs={{0,1},{1,0},{2,3},{3,2},{4,5},{5,4},{6,7},{7,6},{8,9},{9,8},{10,11... | collective-permute-start | bytes 1572872 | tf_op jit(solution)/shard_map/ppermute | solution.py:336
  46.5 18.5 %all-to-all-start.1 = ((f32[32,5,256]{2,1,0:T(8,128)}), f32[32,5,256]{2,1,0:T(8,128)S(1)}, u32[]{:S(2)}, u32[]{:S(2)}) async-start(f32[32,5,256]{2,1,0:T(8,128)} %broadcast_in_dim.5), calls=%async_computation.1 | async-start | bytes 524288 | tf_op jit(solution)/shard_map/all_to_all | solution.py:304
  56.1 0.7 copy-start.11
  57.4 0.7 copy-start.10
  64.9 1.2 copy-start.2
  66.2 0.9 copy-start.5
  67.1 0.9 copy-start.6
  68.0 0.7 copy-start.7
  68.7 3.1 %copy-start.8 = (f32[32,1]{1,0:T(8,128)S(1)}, f32[32,1]{1,0:T(8,128)}, u32[]{:S(2)}) copy-start(f32[32,1]{1,0:T(8,128)} %copy.23.bias) | copy-start | bytes 388
  68.7 3.1 %copy-start.9 = (f32[32,1]{1,0:T(8,128)S(1)}, f32[32,1]{1,0:T(8,128)}, u32[]{:S(2)}) copy-start(f32[32,1]{1,0:T(8,128)} %copy.22.decay) | copy-start | bytes 388
  68.7 3.1 %copy-start.14 = (f32[256,32]{0,1:T(8,128)S(1)}, f32[256,32]{0,1:T(8,128)}, u32[]{:S(2)}) copy-start(f32[256,32]{0,1:T(8,128)} %param.29) | copy-start | bytes 98308
  100.9 28.9 %copy-start.12 = (f32[32]{0:T(128)S(1)}, f32[32]{0:T(128)}, u32[]{:S(2)}) copy-start(f32[32]{0:T(128)} %param.28) | copy-start | bytes 388
  102.0 40.3 %copy-start.3 = (bf16[256,2048]{1,0:T(8,128)(2,1)S(1)}, bf16[256,2048]{1,0:T(8,128)(2,1)}, u32[]{:S(2)}) copy-start(bf16[256,2048]{1,0:T(8,128)(2,1)} %weight.1) | copy-start | bytes 3145732
  142.3 0.7 copy-start.13

commit v2 on v1

--- a/solution.py
+++ b/solution.py
@@ -1,5 +1,3 @@
-from functools import partial
-
 import jax
 import jax.numpy as jnp
 from jax import lax
@@ -20,6 +18,7 @@
 ALL = ("zh", "zl", "y", "x", "c")
 VM = pl.BlockSpec(memory_space=pltpu.VMEM)
 SM = pl.BlockSpec(memory_space=pltpu.SMEM)
+HB = pl.BlockSpec(memory_space=pltpu.HBM)
 
 
 def mm(a, b, dims=((1,), (0,))):
@@ -75,24 +74,38 @@
     return out
 
 
-def project_kernel(pos, one, two, ctx, fac, wq, wk, wv, wd, ww, q_o, k_o, v_o, r_o, w_o, c_o, hid):
+def project_kernel(
+    pos, p0, p1, p2, p3, fac, wq, wk, wv_h, wd_h, ww_h, ctx_h,
+    q_o, k_o, v_o, r_o, w_o, c_o,
+    hid, wv, wd, ww, ctx, sems,
+):
+    copies = [
+        pltpu.make_async_copy(source, target, sems.at[i])
+        for i, (source, target) in enumerate(((ctx_h, ctx), (wv_h, wv), (wd_h, wd), (ww_h, ww)))
+    ]
+    for copy in copies:
+        copy.start()
     factors = [[], [], [], []]
     for t in range(8):
         f = (fac[t] + fac[8 + t]) + (fac[16 + t] + fac[24 + t])
         for slot, r in enumerate((0, 1, 3, 4)):
             factors[slot].append(f[r : r + 1])
     shift, scale, c_shift, c_scale = (jnp.concatenate(f, axis=1) for f in factors)
-    for d in range(4):
-        for lat, core in ((one, pos[6]), (two, 1 - pos[6])):
+    for d, pair in enumerate((p0, p1, p2, p3)):
+        for i in range(2):
+            core = pos[6] if i == 0 else 1 - pos[6]
             spot = (2 * ((pos[7] + 4 - d) % 4) + core) * 32
-            hid[pl.ds(pl.multiple_of(spot, 32), 32)] = norm_rows(lat[d], scale, shift)
+            hid[pl.ds(pl.multiple_of(spot, 32), 32)] = norm_rows(pair[i], scale, shift)
+    copies[0].wait()
     hid[256:260] = norm_rows(ctx[...], c_scale, c_shift)
     hid[260:272] = jnp.zeros((12, D), BF)
     rows = hid[...]
     q_o[...] = mm(hid[0:256], wq[...]).astype(BF)
     keys = mm(rows, wk[...]).astype(BF)
+    k_o[...] = keys[:256]
+    for copy in copies[1:]:
+        copy.wait()
     values = mm(rows, wv[...]).astype(BF)
-    k_o[...] = keys[:256]
     v_o[...] = values[:256]
     last_two = ((1,), (1,))
     r_o[...] = mm(wd[...], hid[0:256], last_two).astype(BF).astype(F32)
@@ -100,22 +113,23 @@
     rate = mm(hid[256:264], wd[...], last_two).astype(BF).astype(F32)
     write = mm(hid[256:264], ww[...], last_two).astype(BF).astype(F32)
     lanes = lax.broadcasted_iota(jnp.int32, (8, 256), 1)
-    spots = lanes == lax.broadcasted_iota(jnp.int32, (8, 256), 0) + pos[5]
-    wide = [rows_of[256:264].astype(F32) for rows_of in (keys, values)]
+    rank = lax.broadcasted_iota(jnp.int32, (8, 256), 0)
+    spots = (lanes == rank + pos[5]) & (rank < 4)
+    wide = [rows_of[256:264].astype(F32)[0:4] for rows_of in (keys, values)]
+    pieces = [jnp.concatenate(wide, axis=1)]
     for j in range(4):
-        h = j // 2
-        to = (j + pos[4]) % 4
         lane = pos[1] * 4 + j
-        pieces = [
-            jnp.concatenate([w[0:4, 128 * h : 128 * h + 128] for w in wide], axis=1),
-            jnp.sum(jnp.where(spots, column(rate, lane), 0.0), axis=0, keepdims=True),
-            jnp.sum(jnp.where(spots, column(write, lane), 0.0), axis=0, keepdims=True),
-            jnp.zeros((10, 256), F32),
+        gates = [
+            jnp.sum(jnp.where(spots, column(g, lane), 0.0), axis=0, keepdims=True)
+            for g in (rate, write)
         ]
-        c_o[to] = jnp.concatenate(pieces, axis=0).astype(BF)
-
-
-def chunk_kernel(pos, q, k, v, rate, write, rows, spike, decay, bias, m_o, r_o, o_o):
+        pieces.append(jnp.concatenate(gates, axis=1))
+    out = jnp.concatenate(pieces, axis=0).astype(BF)
+    for i in range(4):
+        c_o[i] = out
+
+
+def chunk_kernel(pos, q, k, v, rate, write, spike, decay, bias, m_o, r_o, o_o):
     row = lax.broadcasted_iota(jnp.int32, (256, 256), 0)
     col = lax.broadcasted_iota(jnp.int32, (256, 256), 1)
     eye = row == col
@@ -177,7 +191,7 @@
         h, e = divmod(j, 2)
         r_o[h, :, 128 * e : 128 * e + 128] = (grown_q - read[:, 128:]).astype(BF)
         outs[h] = read[:, :128] if e == 0 else outs[h] + read[:, :128]
-    m_o[:, 128:144] = rows[...]
+    m_o[:, 128:160] = jnp.zeros((4, 32, 256), BF)
     o_o[:, 0:128] = outs[0]
     o_o[:, 128:256] = outs[1]
 
@@ -216,7 +230,21 @@
     return both[:, :n] + both[:, n:]
 
 
-def compose_kernel(pos, maps, o, *, count):
+def pack_kernel(pos, maps, rows, o):
+    wide = [rows[i].astype(F32) for i in range(4)]
+    for j in range(4):
+        h = j // 2
+        to = (j + pos[4]) % 4
+        parts = []
+        for w in wide:
+            sides = [w[0:4, at + 128 * h : at + 128 * h + 128] for at in (0, 256)]
+            parts.append(jnp.concatenate(sides, axis=1))
+        gates = sum(w[4 + j : 5 + j] for w in wide)
+        parts += [gates[:, 0:256], gates[:, 256:512], jnp.zeros((14, 256), F32)]
+        o[to, 128:160] = jnp.concatenate(parts, axis=0).astype(BF)
+
+
+def composed(pos, maps):
     back = pos[0] % 2
     at = back * 3
     step = 1 - 2 * back
@@ -224,36 +252,51 @@
     for _ in range(3):
         at = at + step
         total = total + maps[at][0:128].astype(F32) + apply_to(maps[at][0:128, 0:128], total)
+    return total
+
+
+def low_kernel(pos, maps, o):
+    total = composed(pos, maps)
     wide = [maps[i][128:].astype(F32) for i in range(4)]
-    rows = [w[0:count] for w in wide]
-    gates = sum(w[count : count + 2] for w in wide)
-    out = jnp.concatenate([total, *rows, gates, jnp.zeros((14, 256), F32)], axis=0).astype(BF)
+    parts = [w[4 * i : 4 * i + 4] for i in range(4) for w in wide]
+    parts += [sum(w[16:18] for w in wide), jnp.zeros((14, 256), F32)]
+    out = jnp.concatenate([total, *parts], axis=0).astype(BF)
     for i in range(4):
         o[i] = out
 
 
-def scan_kernel(pos, high, low, own, decay, bias, extra, o):
+def high_kernel(pos, maps, o):
+    o[...] = composed(pos, maps).astype(BF)
+
+
+def context_kernel(pos, low, decay, bias, extra, o):
+    wide = [low[i][128:].astype(F32) for i in range(4)]
+    rows = jnp.concatenate([w[16 * i : 16 * i + 16] for i in range(4) for w in wide], axis=0)
+    gates = sum(w[64:66] for w in wide)
+    o[...] = context_state(
+        pos, rows, gates[0:1], gates[1:2], decay[...], bias[...], extra[...]
+    )
+
+
+def moved(maps, state):
+    return state + maps[:, 128:256].astype(F32) + apply_to(maps[:, 0:128], state)
+
+
+def scan_kernel(pos, start, far, middle, near, low, own, o):
     back = pos[0] % 2
     step = 1 - 2 * back
-    wide = [high[i][128:].astype(F32) for i in range(4)]
-    rows = jnp.concatenate([w[0:64] for w in wide], axis=0)
-    gates = sum(w[64:66] for w in wide)
-    state = context_state(
-        pos, rows, gates[0:1], gates[1:2], decay[...], bias[...], extra[...]
-    )
-    for maps, mine in ((high, pos[2]), (low, pos[3])):
-        at = back * 3
-        for _ in range(3):
-            m = maps[at][0:128]
-            moved = state + m[:, 128:256].astype(F32) + apply_to(m[:, 0:128], state)
-            state = jnp.where((mine - at) * step > 0, moved, state)
-            at = at + step
+    state = start[...]
+    for maps in (far, middle, near):
+        state = moved(maps[...], state)
+    at = back * 3
+    for _ in range(3):
+        state = jnp.where((pos[3] - at) * step > 0, moved(low[at][0:128], state), state)
+        at = at + step
     at = back * 3
     for i in range(4):
         o[at] = state.astype(BF)
         if i < 3:
-            m = own[at][0:128]
-            state = state + m[:, 128:256].astype(F32) + apply_to(m[:, 0:128], state)
+            state = moved(own[at][0:128], state)
         at = at + step
 
 
@@ -284,7 +327,7 @@
     o[...] = (lat[...].astype(F32) + gate * branch).astype(BF)
 
 
-def call(kernel, outs, specs, scratch=(), flops=1):
+def call(kernel, outs, specs, scratch=(), flops=1, aliases=None):
     def shape(s):
         return jax.ShapeDtypeStruct(*s)
 
@@ -295,6 +338,7 @@
         in_specs=specs,
         out_specs=[VM] * len(outs) if many else VM,
         scratch_shapes=scratch,
+        input_output_aliases=aliases or {},
         compiler_params=pltpu.CompilerParams(vmem_limit_bytes=24 * 2**20),
         cost_estimate=pl.CostEstimate(flops=flops, bytes_accessed=1, transcendentals=0),
     )
@@ -304,6 +348,17 @@
     return lax.all_to_all(
         jnp.broadcast_to(value[None], (count, *value.shape)), axes, 0, 0, tiled=True
     )
+
+
+def onward(d):
+    pairs = []
+    for zh in range(4):
+        for y in range(4):
+            for c in range(2):
+                to = zh + d if (y + c) % 2 == 0 else zh - d
+                if 0 <= to < 4:
+                    pairs.append((zh * 8 + y * 2 + c, to * 8 + y * 2 + c))
+    return pairs
 
 
 def per_device(
@@ -329,11 +384,10 @@
     sp_index = lax.axis_index(SP)
     pos = jnp.stack([(y + c) % 4, x * 2 + c, zh, zl, (4 - c) % 4, sp_index * 4, c, x])
     pos = pos.astype(jnp.int32)
-    parts = [latent]
+    other = lax.ppermute(latent, "c", [(0, 1), (1, 0)])
+    pairs = [jnp.stack([latent, other])]
     for d in range(1, 4):
-        parts.append(lax.ppermute(latent, "x", [(i, (i + d) % 4) for i in range(4)]))
-    mine = jnp.stack(parts)
-    other = lax.ppermute(mine, "c", [(0, 1), (1, 0)])
+        pairs.append(lax.ppermute(pairs[0], "x", [(i, (i + d) % 4) for i in range(4)]))
     signals = jnp.stack([condition, context_condition_vector])
     signals = lax.dynamic_slice_in_dim(jax.nn.silu(signals), sp_index * 32, 32, 1)
     mod = modulation_matrix.astype(F32)
@@ -355,27 +409,34 @@
             ((256, 256), BF),
             ((32, 256), F32),
             ((32, 256), F32),
-            ((4, 16, 256), BF),
+            ((4, 8, 512), BF),
         ],
-        [SM] + [VM] * 9,
-        [pltpu.VMEM((272, D), BF)],
+        [SM] + [VM] * 7 + [HB] * 4,
+        [
+            pltpu.VMEM((272, D), BF),
+            pltpu.VMEM((D, 256), BF),
+            pltpu.VMEM((32, D), BF),
+            pltpu.VMEM((32, D), BF),
+            pltpu.VMEM((4, D), BF),
+            pltpu.SemaphoreType.DMA((4,)),
+        ],
         flops=10**9,
     )(
         pos,
-        mine,
-        other,
-        context,
+        *pairs,
         fac,
         query_matrix,
         key_matrix,
         value_matrix,
         decay_input_weight.T,
         write_strength_weight.T,
-    )
+        context,
+    )
+    rows = lax.all_to_all(rows, "zh", 0, 0, tiled=True)
     maps, reads, base = call(
         chunk_kernel,
-        [((4, 144, 256), BF), ((2, 256, 256), BF), ((256, 256), F32)],
-        [SM] + [VM] * 9,
+        [((4, 160, 256), BF), ((2, 256, 256), BF), ((256, 256), F32)],
+        [SM] + [VM] * 8,
         flops=4 * 10**9,
     )(
         pos,
@@ -384,24 +445,29 @@
         values,
         rate,
         write,
-        rows,
         log_spike_added.T,
         head_decay_rate.reshape(32, 1),
         write_strength_bias.reshape(32, 1),
     )
+    maps = call(pack_kernel, ((4, 160, 256), BF), [SM, VM, VM], aliases={1: 0})(
+        pos, maps, rows
+    )
     of_y = lax.all_to_all(maps, "y", 0, 0, tiled=True)
-    low = call(partial(compose_kernel, count=4), ((4, 160, 256), BF), [SM, VM])(pos, of_y)
+    low = call(low_kernel, ((4, 208, 256), BF), [SM, VM])(pos, of_y)
     of_low = lax.all_to_all(low, "zl", 0, 0, tiled=True)
-    high = call(partial(compose_kernel, count=16), ((4, 208, 256), BF), [SM, VM])(pos, of_low)
-    of_high = lax.all_to_all(high, "zh", 0, 0, tiled=True)
-    states = call(scan_kernel, ((4, 128, 128), BF), [SM] + [VM] * 6, flops=10**8)(
+    high = call(high_kernel, ((128, 256), BF), [SM, VM])(pos, of_low)
+    of_high = []
+    for d in (3, 2, 1):
+        of_high.append(lax.ppermute(high, ("zh", "y", "c"), onward(d)))
+    start = call(context_kernel, ((128, 128), F32), [SM] + [VM] * 4, flops=10**9)(
         pos,
-        of_high,
         of_low,
-        of_y,
         head_decay_rate.reshape(1, 32),
         write_strength_bias.reshape(1, 32),
         context_write_offset_bias.reshape(1, 32),
+    )
+    states = call(scan_kernel, ((4, 128, 128), BF), [SM] + [VM] * 6, flops=10**8)(
+        pos, start, *of_high, of_low, of_y
     )
     states = lax.all_to_all(states, "y", 0, 0, tiled=True)
     branch = call(read_kernel, ((8, 32, D), BF), [SM] + [VM] * 5, flops=10**8)(

time: 170 us -> 160 us (0.941)
  blocking collectives: 105 us -> 51.9 us
  starting transfers between devices: 28.7 us -> 48.2 us
  waiting for transfers between devices: 7.3 us -> 21.4 us
  local copies, waits for them, and re-layouts: 7.93 us -> 15.9 us
  Pallas kernels: 18.8 us -> 20.7 us
    all_to_all x2 -> x0, blocking collectives: 52 us -> none  [the longest x1 27.8 us: per_device(): of_high = lax.all_to_all(high, 'zh', 0, 0, tiled=True)]
    all_to_all x1 -> x2, starting transfers between devices: 9.58 us -> 18.6 us  [to_all(): lax.all_to_all(jnp.broadcast_to(value[None], (count, *value.shape)), axes...]
    ppermute x4 -> x7, waiting for transfers between devices: 1.23 us -> 9.82 us  [the longest x3 9.81 us: per_device(): of_high.append(lax.ppermute(high, ('zh', 'y', 'c'), onward(d)))]
    unnamed x32 -> x54, local copies, waits for them, and re-layouts: 5.74 us -> 13.1 us
    all_to_all x0 -> x1, starting transfers between devices: none -> 7.28 us  [per_device(): rows = lax.all_to_all(rows, 'zh', 0, 0, tiled=True)]
    pallas_call x3 -> x5, Pallas kernels: 8.38 us -> 12.8 us  [the longest x1 6.2 us: per_device(): call(chunk_kernel, [((4, 160, 256), BF), ((2, 256, 256), BF), ((256, 256)...]
    all_to_all x1 -> x2, waiting for transfers between devices: 6.07 us -> 10.3 us  [to_all(): lax.all_to_all(jnp.broadcast_to(value[None], (count, *value.shape)), axes...]
    pallas_call x1, Pallas kernels: 5.26 us -> 1.93 us  [per_device(): call(scan_kernel, ((4, 128, 128), BF), [SM] + [VM] * 6, flops=10 ** 8)]
  transfers between devices with their start and end apart: 5 -> 10, of which waited for: 2 -> 6; matrix products, arithmetic and copies ran while one was open for 2% -> 2% of each run, Pallas kernels for 0% -> 6%
where the time goes in v2:
time: 160 us; the launch traced here: 159 us
  blocking collectives  51.9 us (32%)
  starting transfers between devices  48.2 us (30%)
  waiting for transfers between devices  21.4 us (13%)
  Pallas kernels  20.7 us (13%)
  local copies, waits for them, and re-layouts  15.9 us (10%)
    all_to_all x1, blocking collectives, per_device(): branch = lax.all_to_all(branch, TP, 0, 0, tiled=True)  21.6 us
    all_to_all x2, starting transfers between devices, to_all(): lax.all_to_all(jnp.broadcast_to(value[None], (count, *value.shape)), axes...  18.6 us
    all_to_all x1, blocking collectives, per_device(): of_low = lax.all_to_all(low, 'zl', 0, 0, tiled=True)  13.2 us
    unnamed x54, local copies, waits for them, and re-layouts  13.1 us
    all_to_all x2, waiting for transfers between devices, to_all(): lax.all_to_all(jnp.broadcast_to(value[None], (count, *value.shape)), axes...  10.3 us
    ppermute x3, waiting for transfers between devices, per_device(): of_high.append(lax.ppermute(high, ('zh', 'y', 'c'), onward(d)))  9.81 us
    ppermute x3, starting transfers between devices, per_device(): lax.ppermute(pairs[0], 'x', [(i, (i + d) % 4) for i in range(4)])  9.33 us
    ppermute x1, starting transfers between devices, per_device(): other = lax.ppermute(latent, 'c', [(0, 1), (1, 0)])  8.87 us
  transfers between devices with their start and end apart: 10, of which 6 were waited for; matrix products, arithmetic and copies ran while one was open for 2% of the time, Pallas kernels for 6%

profile of v2, /device:TPU:1, one launch (start us, length us, event | category | flops | bytes accessed | tf_op | source)
XLA Modules:
  0.0 159.4 jit_solution(14877157973746002387)
XLA Ops:
  0.0 8.9 %collective-permute-start = (bf16[32,2048]{1,0:T(8,128)(2,1)}, bf16[32,2048]{1,0:T(8,128)(2,1)S(1)}, u32[]{:S(2)}, u32[]{:S(2)}) collective-permute-start(bf16[32,2048]{1,0:T(8,128)(2,1)} %lat.1), channel_id=1, source_target_pairs={{0,1},{1,0},{2,3},{3,2},{4,5},{5,4},{6,7},{7,6},{8,9},{9,8},{10,11... | collective-permute-start | bytes 393224 | tf_op jit(solution)/shard_map/ppermute | solution.py:387
  8.9 0.8 divide_multiply_fusion
  9.9 0.7 broadcast_in_dim.4
  10.6 9.6 %all-to-all-start = ((f32[16,5,256]{2,1,0:T(8,128)}), f32[16,5,256]{2,1,0:T(8,128)S(1)}, u32[]{:S(2)}, u32[]{:S(2)}) async-start(f32[16,5,256]{2,1,0:T(8,128)} %broadcast_in_dim.4), calls=%async_computation | async-start | bytes 262144 | tf_op jit(solution)/shard_map/all_to_all | solution.py:348
  20.2 4.4 %collective-permute-start.3 = (bf16[2,32,2048]{2,1,0:T(8,128)(2,1)S(1)}, bf16[2,32,2048]{2,1,0:T(8,128)(2,1)S(1)}, u32[]{:S(2)}, u32[]{:S(2)}) collective-permute-start(bf16[2,32,2048]{2,1,0:T(8,128)(2,1)S(1)} %pad_maximum_fusion.p0), channel_id=1, source_target_pairs={{0,6},{2,0},{4,2},{6,4},{1,7},{3,1},{5,3},{7,5},{8,14},{10,8},{12,... | collective-permute-start | bytes 786440 | tf_op jit(solution)/shard_map/ppermute | solution.py:390
  24.6 2.4 %collective-permute-start.2 = (bf16[2,32,2048]{2,1,0:T(8,128)(2,1)S(1)}, bf16[2,32,2048]{2,1,0:T(8,128)(2,1)S(1)}, u32[]{:S(2)}, u32[]{:S(2)}) collective-permute-start(bf16[2,32,2048]{2,1,0:T(8,128)(2,1)S(1)} %pad_maximum_fusion.p0), channel_id=1, source_target_pairs={{0,4},{2,6},{4,0},{6,2},{1,5},{3,7},{5,1},{7,3},{8,12},{10,14},{12... | collective-permute-start | bytes 786440 | tf_op jit(solution)/shard_map/ppermute | solution.py:390
  27.1 2.5 %collective-permute-start.1 = (bf16[2,32,2048]{2,1,0:T(8,128)(2,1)S(1)}, bf16[2,32,2048]{2,1,0:T(8,128)(2,1)S(1)}, u32[]{:S(2)}, u32[]{:S(2)}) collective-permute-start(bf16[2,32,2048]{2,1,0:T(8,128)(2,1)S(1)} %pad_maximum_fusion.p0), channel_id=1, source_target_pairs={{0,2},{2,4},{4,6},{6,0},{1,3},{3,5},{5,7},{7,1},{8,10},{10,12},{12... | collective-permute-start | bytes 786440 | tf_op jit(solution)/shard_map/ppermute | solution.py:390
  29.6 3.0 %all-to-all-done = f32[16,5,256]{2,1,0:T(8,128)S(1)} async-done(((f32[16,5,256]{2,1,0:T(8,128)}), f32[16,5,256]{2,1,0:T(8,128)S(1)}, u32[]{:S(2)}, u32[]{:S(2)}) %all-to-all-start) | async-done | bytes 81952 | tf_op jit(solution)/shard_map/all_to_all | solution.py:348
  32.6 0.7 broadcast_in_dim.5
  33.3 9.1 %all-to-all-start.1 = ((f32[32,5,256]{2,1,0:T(8,128)}), f32[32,5,256]{2,1,0:T(8,128)S(1)}, u32[]{:S(2)}, u32[]{:S(2)}) async-start(f32[32,5,256]{2,1,0:T(8,128)} %broadcast_in_dim.5), calls=%async_computation.1 | async-start | bytes 524288 | tf_op jit(solution)/shard_map/all_to_all | solution.py:348
  42.4 0.7 copy.24.bias
  43.1 0.7 copy.23.decay
  43.9 7.4 %all-to-all-done.1.fac = f32[32,5,256]{2,1,0:T(8,128)S(1)} async-done(((f32[32,5,256]{2,1,0:T(8,128)}), f32[32,5,256]{2,1,0:T(8,128)S(1)}, u32[]{:S(2)}, u32[]{:S(2)}) %all-to-all-start.1) | async-done | bytes 163872 | tf_op jit(solution)/shard_map/all_to_all | solution.py:348
  51.3 1.2 copy-done.2
  52.5 0.9 copy-done.5
  53.4 0.9 copy-done.6
  54.3 0.7 copy-done.8
  55.0 3.9 %shard_map.154 = (bf16[256,256]{1,0:T(8,128)(2,1)S(1)}, bf16[256,256]{1,0:T(8,128)(2,1)S(1)}, bf16[256,256]{1,0:T(8,128)(2,1)S(1)}, f32[32,256]{1,0:T(8,128)S(1)...) custom-call(s32[8]{0:T(128)S(1)} %stack.53.pos, bf16[2,32,2048]{2,1,0:T(8,128)(2,1)S(1)} %pad_maximum_fusion.p0, ...), custom_call_target="tpu_custom_call" | custom-call | flops 1000000000 | bytes 1 | tf_op jit(solution)/shard_map/pallas_call | solution.py:404
  59.5 0.7 copy-done.14
  60.2 0.6 copy-done.16
  60.8 0.6 copy-done.18
  61.5 0.6 copy-done.21
  62.7 7.3 %all-to-all-start.2 = ((bf16[4,8,512]{2,1,0:T(8,128)(2,1)}), bf16[4,8,512]{2,1,0:T(8,128)(2,1)S(1)}, u32[]{:S(2)}, u32[]{:S(2)}) async-start(bf16[4,8,512]{2,1,0:T(8,128)(2,1)} %copy-done.7), calls=%async_computation.2 | async-start | bytes 65536 | tf_op jit(solution)/shard_map/all_to_all | solution.py:435
  70.0 0.9 copy-done.15
  70.9 0.9 copy-done.17
  71.8 0.9 copy-done.19
  72.7 0.8 copy-done.22
  73.5 0.8 copy-done.24
  74.2 6.2 %shard_map.155 = (bf16[4,160,256]{2,1,0:T(8,128)(2,1)S(1)}, bf16[2,256,256]{2,1,0:T(8,128)(2,1)S(1)}, f32[256,256]{1,0:T(8,128)S(1)}) custom-call(s32[8]{0:T(128)S(1)} %stack.53.pos, bf16[256,256]{1,0:T(8,128)(2,1)S(1)} %copy-done.15, bf16[256,256]{1,0:T(8,128)(2,1)S(1)} %copy-done.17, bf16[256,256]{1,0:T(8,128)(2,1)S(1)} %copy-done.19, ...), custom_call_target="tpu_custom_call" | custom-call | flops 4000000000 | bytes 1 | tf_op jit(solution)/shard_map/pallas_call | solution.py:436
  80.4 1.2 all-to-all-done.2.rows
  82.2 8.3 %all_to_all.35.maps.own = bf16[4,160,256]{2,1,0:T(8,128)(2,1)S(1)} all-to-all(bf16[4,160,256]{2,1,0:T(8,128)(2,1)S(1)} %shard_map.156), channel_id=1, replica_groups=mesh['zh'=4,'zl'=4,'y'=4,'x'=4,'c'=2] {'y'}, dimensions={0} | all-to-all | bytes 655360 | tf_op jit(solution)/shard_map/all_to_all | solution.py:455
  90.5 1.1 shard_map.157
  91.6 13.2 %all_to_all.36.low.maps = bf16[4,208,256]{2,1,0:T(8,128)(2,1)S(1)} all-to-all(bf16[4,208,256]{2,1,0:T(8,128)(2,1)S(1)} %shard_map.157), channel_id=1, replica_groups=mesh['zh'=4,'zl'=4,'y'=4,'x'=4,'c'=2] {'zl'}, dimensions={0} | all-to-all | bytes 851968 | tf_op jit(solution)/shard_map/all_to_all | solution.py:457
  104.7 1.1 shard_map.159
  105.8 1.3 collective-permute-start.6
  107.1 1.3 collective-permute-start.5
  108.4 1.5 collective-permute-start.4
  109.9 0.6 copy-done.25
  110.6 3.9 %shard_map.158.start = f32[128,128]{1,0:T(8,128)S(1)} custom-call(s32[8]{0:T(128)S(1)} %stack.53.pos, bf16[4,208,256]{2,1,0:T(8,128)(2,1)S(1)} %all_to_all.36.low.maps, f32[1,32]{1,0:T(1,128)S(1)} %bitcast.30, f32[1,32]{1,0:T(1,128)S(1)} %bitcast.32, f32[1,32]{1,0:T(1,128)S(1)} %bitcast.34), custom_call_target="tpu_custom_call" | custom-call | flops 1000000000 | bytes 1 | tf_op jit(solution)/shard_map/pallas_call | solution.py:462
  114.5 2.5 %collective-permute-done.6.near = bf16[128,256]{1,0:T(8,128)(2,1)S(1)} collective-permute-done((bf16[128,256]{1,0:T(8,128)(2,1)S(1)}, bf16[128,256]{1,0:T(8,128)(2,1)S(1)}, u32[]{:S(2)}, u32[]{:S(2)}) %collective-permute-start.6) | collective-permute-done | bytes 65568 | tf_op jit(solution)/shard_map/ppermute | solution.py:461
  117.0 4.6 %collective-permute-done.5.middle = bf16[128,256]{1,0:T(8,128)(2,1)S(1)} collective-permute-done((bf16[128,256]{1,0:T(8,128)(2,1)S(1)}, bf16[128,256]{1,0:T(8,128)(2,1)S(1)}, u32[]{:S(2)}, u32[]{:S(2)}) %collective-permute-start.5) | collective-permute-done | bytes 65568 | tf_op jit(solution)/shard_map/ppermute | solution.py:461
  121.6 2.7 %collective-permute-done.4.far = bf16[128,256]{1,0:T(8,128)(2,1)S(1)} collective-permute-done((bf16[128,256]{1,0:T(8,128)(2,1)S(1)}, bf16[128,256]{1,0:T(8,128)(2,1)S(1)}, u32[]{:S(2)}, u32[]{:S(2)}) %collective-permute-start.4) | collective-permute-done | bytes 65568 | tf_op jit(solution)/shard_map/ppermute | solution.py:461
  124.3 1.9 %shard_map.160 = bf16[4,128,128]{2,1,0:T(8,128)(2,1)S(1)} custom-call(s32[8]{0:T(128)S(1)} %stack.53.pos, f32[128,128]{1,0:T(8,128)S(1)} %shard_map.158.start, bf16[128,256]{1,0:T(8,128)(2,1)S(1)} %collective-permute-done.4.far, bf16[128,256]{1,0:T(8,128)(2,1)S(1)} %collective-permute-done.5.middle, bf16[128,256]{1,0:T(8,128)(2,1)S(1)} %collective-permute-done.6.near, ...), custom_call_target="tpu_custom_call" | custom-call | flops 100000000 | bytes 1 | tf_op jit(solution)/shard_map/pallas_call | solution.py:469
  126.2 8.8 %all_to_all.37.states = bf16[4,128,128]{2,1,0:T(8,128)(2,1)S(1)} all-to-all(bf16[4,128,128]{2,1,0:T(8,128)(2,1)S(1)} %shard_map.160), channel_id=1, replica_groups=mesh['zh'=4,'zl'=4,'y'=4,'x'=4,'c'=2] {'y'}, dimensions={0} | all-to-all | bytes 262144 | tf_op jit(solution)/shard_map/all_to_all | solution.py:472
  135.0 0.7 copy-done.11
  135.7 1.3 shard_map.161
  136.9 21.6 %all_to_all.38.rows = bf16[8,32,2048]{2,1,0:T(8,128)(2,1)S(1)} all-to-all(bf16[8,32,2048]{2,1,0:T(8,128)(2,1)S(1)} %shard_map.161), channel_id=1, replica_groups=mesh['zh'=4,'zl'=4,'y'=4,'x'=4,'c'=2] {'x','c'}, dimensions={0} | all-to-all | bytes 2097152 | tf_op jit(solution)/shard_map/all_to_all | solution.py:476
  158.6 0.8 shard_map.162
  (52 shorter events, 2.2 us)
Async XLA Ops:
  0.0 9.7 %copy-start.26 = (bf16[3,32,256]{2,1,0:T(8,128)(2,1)S(1)}, bf16[3,32,256]{2,1,0:T(8,128)(2,1)}, u32[]{:S(2)}) copy-start(bf16[3,32,256]{2,1,0:T(8,128)(2,1)} %param.20) | copy-start | bytes 147460
  0.0 20.2 %collective-permute-start = (bf16[32,2048]{1,0:T(8,128)(2,1)}, bf16[32,2048]{1,0:T(8,128)(2,1)S(1)}, u32[]{:S(2)}, u32[]{:S(2)}) collective-permute-start(bf16[32,2048]{1,0:T(8,128)(2,1)} %lat.1), channel_id=1, source_target_pairs={{0,1},{1,0},{2,3},{3,2},{4,5},{5,4},{6,7},{7,6},{8,9},{9,8},{10,11... | collective-permute-start | bytes 393224 | tf_op jit(solution)/shard_map/ppermute | solution.py:387
  9.7 10.5 %copy-start.4 = (bf16[32,2048]{1,0:T(8,128)(2,1)S(1)}, bf16[32,2048]{1,0:T(8,128)(2,1)}, u32[]{:S(2)}) copy-start(bf16[32,2048]{1,0:T(8,128)(2,1)} %lat.1) | copy-start | bytes 393220
  9.7 32.7 %copy-start.13 = (f32[32]{0:T(128)S(1)}, f32[32]{0:T(128)}, u32[]{:S(2)}) copy-start(f32[32]{0:T(128)} %param.27) | copy-start | bytes 388
  9.7 33.4 %copy-start.12 = (f32[32]{0:T(128)S(1)}, f32[32]{0:T(128)}, u32[]{:S(2)}) copy-start(f32[32]{0:T(128)} %param.26) | copy-start | bytes 388
  9.7 41.5 %copy-start.1 = (bf16[2048,256]{1,0:T(8,128)(2,1)S(1)}, bf16[2048,256]{1,0:T(8,128)(2,1)}, u32[]{:S(2)}) copy-start(bf16[2048,256]{1,0:T(8,128)(2,1)} %wk.1) | copy-start | bytes 3145732
  9.8 41.4 %copy-start = (bf16[2048,256]{1,0:T(8,128)(2,1)S(1)}, bf16[2048,256]{1,0:T(8,128)(2,1)}, u32[]{:S(2)}) copy-start(bf16[2048,256]{1,0:T(8,128)(2,1)} %wq.1) | copy-start | bytes 3145732
  10.6 22.0 %all-to-all-start = ((f32[16,5,256]{2,1,0:T(8,128)}), f32[16,5,256]{2,1,0:T(8,128)S(1)}, u32[]{:S(2)}, u32[]{:S(2)}) async-start(f32[16,5,256]{2,1,0:T(8,128)} %broadcast_in_dim.4), calls=%async_computation | async-start | bytes 262144 | tf_op jit(solution)/shard_map/all_to_all | solution.py:348
  20.2 23.6 %collective-permute-start.3 = (bf16[2,32,2048]{2,1,0:T(8,128)(2,1)S(1)}, bf16[2,32,2048]{2,1,0:T(8,128)(2,1)S(1)}, u32[]{:S(2)}, u32[]{:S(2)}) collective-permute-start(bf16[2,32,2048]{2,1,0:T(8,128)(2,1)S(1)} %pad_maximum_fusion.p0), channel_id=1, source_target_pairs={{0,6},{2,0},{4,2},{6,4},{1,7},{3,1},{5,3},{7,5},{8,14},{10,8},{12,... | collective-permute-start | bytes 786440 | tf_op jit(solution)/shard_map/ppermute | solution.py:390
  24.6 19.2 %collective-permute-start.2 = (bf16[2,32,2048]{2,1,0:T(8,128)(2,1)S(1)}, bf16[2,32,2048]{2,1,0:T(8,128)(2,1)S(1)}, u32[]{:S(2)}, u32[]{:S(2)}) collective-permute-start(bf16[2,32,2048]{2,1,0:T(8,128)(2,1)S(1)} %pad_maximum_fusion.p0), channel_id=1, source_target_pairs={{0,4},{2,6},{4,0},{6,2},{1,5},{3,7},{5,1},{7,3},{8,12},{10,14},{12... | collective-permute-start | bytes 786440 | tf_op jit(solution)/shard_map/ppermute | solution.py:390
  27.1 16.8 %collective-permute-start.1 = (bf16[2,32,2048]{2,1,0:T(8,128)(2,1)S(1)}, bf16[2,32,2048]{2,1,0:T(8,128)(2,1)S(1)}, u32[]{:S(2)}, u32[]{:S(2)}) collective-permute-start(bf16[2,32,2048]{2,1,0:T(8,128)(2,1)S(1)} %pad_maximum_fusion.p0), channel_id=1, source_target_pairs={{0,2},{2,4},{4,6},{6,0},{1,3},{3,5},{5,7},{7,1},{8,10},{10,12},{12... | collective-permute-start | bytes 786440 | tf_op jit(solution)/shard_map/ppermute | solution.py:390
  33.3 17.9 %all-to-all-start.1 = ((f32[32,5,256]{2,1,0:T(8,128)}), f32[32,5,256]{2,1,0:T(8,128)S(1)}, u32[]{:S(2)}, u32[]{:S(2)}) async-start(f32[32,5,256]{2,1,0:T(8,128)} %broadcast_in_dim.5), calls=%async_computation.1 | async-start | bytes 524288 | tf_op jit(solution)/shard_map/all_to_all | solution.py:348
  51.3 1.2 copy-start.2
  52.5 0.9 copy-start.5
  53.4 0.9 copy-start.6
  54.3 0.7 copy-start.8
  58.9 0.6 copy-start.7
  59.5 0.7 copy-start.14
  60.2 0.6 copy-start.16
  60.8 0.6 copy-start.18
  61.5 0.6 copy-start.21
  62.1 0.6 copy-start.23
  62.7 7.3 %copy-start.9 = (f32[32,1]{1,0:T(8,128)S(1)}, f32[32,1]{1,0:T(8,128)}, u32[]{:S(2)}) copy-start(f32[32,1]{1,0:T(8,128)} %copy.24.bias) | copy-start | bytes 388
  62.7 7.3 %copy-start.10 = (f32[32,1]{1,0:T(8,128)S(1)}, f32[32,1]{1,0:T(8,128)}, u32[]{:S(2)}) copy-start(f32[32,1]{1,0:T(8,128)} %copy.23.decay) | copy-start | bytes 388
  62.7 7.3 %copy-start.20 = (f32[256,32]{0,1:T(8,128)S(1)}, f32[256,32]{0,1:T(8,128)}, u32[]{:S(2)}) copy-start(f32[256,32]{0,1:T(8,128)} %param.29) | copy-start | bytes 98308
  62.7 18.9 %all-to-all-start.2 = ((bf16[4,8,512]{2,1,0:T(8,128)(2,1)}), bf16[4,8,512]{2,1,0:T(8,128)(2,1)S(1)}, u32[]{:S(2)}, u32[]{:S(2)}) async-start(bf16[4,8,512]{2,1,0:T(8,128)(2,1)} %copy-done.7), calls=%async_computation.2 | async-start | bytes 65536 | tf_op jit(solution)/shard_map/all_to_all | solution.py:435
  70.0 0.9 copy-start.15
  70.9 0.9 copy-start.17
  71.8 0.9 copy-start.19
  72.7 0.8 copy-start.22
  73.5 0.8 copy-start.24
  105.8 11.1 %collective-permute-start.6 = (bf16[128,256]{1,0:T(8,128)(2,1)S(1)}, bf16[128,256]{1,0:T(8,128)(2,1)S(1)}, u32[]{:S(2)}, u32[]{:S(2)}) collective-permute-start(bf16[128,256]{1,0:T(8,128)(2,1)S(1)} %shard_map.159), channel_id=1, source_target_pairs={{0,128},{9,137},{16,144},{25,153},{128,256},{129,1},{136,8},{137,2... | collective-permute-start | bytes 196616 | tf_op jit(solution)/shard_map/ppermute | solution.py:461
  107.1 14.4 %collective-permute-start.5 = (bf16[128,256]{1,0:T(8,128)(2,1)S(1)}, bf16[128,256]{1,0:T(8,128)(2,1)S(1)}, u32[]{:S(2)}, u32[]{:S(2)}) collective-permute-start(bf16[128,256]{1,0:T(8,128)(2,1)S(1)} %shard_map.159), channel_id=1, source_target_pairs={{0,256},{9,265},{16,272},{25,281},{128,384},{137,393},{144,400},{1... | collective-permute-start | bytes 196616 | tf_op jit(solution)/shard_map/ppermute | solution.py:461
  108.4 15.8 %collective-permute-start.4 = (bf16[128,256]{1,0:T(8,128)(2,1)S(1)}, bf16[128,256]{1,0:T(8,128)(2,1)S(1)}, u32[]{:S(2)}, u32[]{:S(2)}) collective-permute-start(bf16[128,256]{1,0:T(8,128)(2,1)S(1)} %shard_map.159), channel_id=1, source_target_pairs={{0,384},{9,393},{16,400},{25,409},{385,1},{392,8},{401,17},{408,24... | collective-permute-start | bytes 196616 | tf_op jit(solution)/shard_map/ppermute | solution.py:461
  109.9 0.7 copy-start.25
  114.4 20.6 %copy-start.3 = (bf16[256,2048]{1,0:T(8,128)(2,1)S(1)}, bf16[256,2048]{1,0:T(8,128)(2,1)}, u32[]{:S(2)}) copy-start(bf16[256,2048]{1,0:T(8,128)(2,1)} %weight.1) | copy-start | bytes 3145732
  135.0 0.7 copy-start.11

commit v3 on v2

--- a/solution.py
+++ b/solution.py
@@ -75,8 +75,8 @@
 
 
 def project_kernel(
-    pos, p0, p1, p2, p3, fac, wq, wk, wv_h, wd_h, ww_h, ctx_h,
-    q_o, k_o, v_o, r_o, w_o, c_o,
+    pos, one, two, fac, wq, wk, wv_h, wd_h, ww_h, ctx_h,
+    p_o, c_o,
     hid, wv, wd, ww, ctx, sems,
 ):
     copies = [
@@ -91,25 +91,25 @@
         for slot, r in enumerate((0, 1, 3, 4)):
             factors[slot].append(f[r : r + 1])
     shift, scale, c_shift, c_scale = (jnp.concatenate(f, axis=1) for f in factors)
-    for d, pair in enumerate((p0, p1, p2, p3)):
-        for i in range(2):
+    for x in range(4):
+        for i, lat in enumerate((one, two)):
             core = pos[6] if i == 0 else 1 - pos[6]
-            spot = (2 * ((pos[7] + 4 - d) % 4) + core) * 32
-            hid[pl.ds(pl.multiple_of(spot, 32), 32)] = norm_rows(pair[i], scale, shift)
+            spot = (2 * x + core) * 32
+            hid[pl.ds(pl.multiple_of(spot, 32), 32)] = norm_rows(lat[x], scale, shift)
     copies[0].wait()
     hid[256:260] = norm_rows(ctx[...], c_scale, c_shift)
     hid[260:272] = jnp.zeros((12, D), BF)
     rows = hid[...]
-    q_o[...] = mm(hid[0:256], wq[...]).astype(BF)
+    p_o[0:256] = mm(hid[0:256], wq[...]).astype(BF)
     keys = mm(rows, wk[...]).astype(BF)
-    k_o[...] = keys[:256]
+    p_o[256:512] = keys[:256]
     for copy in copies[1:]:
         copy.wait()
     values = mm(rows, wv[...]).astype(BF)
-    v_o[...] = values[:256]
+    p_o[512:768] = values[:256]
     last_two = ((1,), (1,))
-    r_o[...] = mm(wd[...], hid[0:256], last_two).astype(BF).astype(F32)
-    w_o[...] = mm(ww[...], hid[0:256], last_two).astype(BF).astype(F32)
+    p_o[768:800] = mm(wd[...], hid[0:256], last_two).astype(BF)
+    p_o[800:832] = mm(ww[...], hid[0:256], last_two).astype(BF)
     rate = mm(hid[256:264], wd[...], last_two).astype(BF).astype(F32)
     write = mm(hid[256:264], ww[...], last_two).astype(BF).astype(F32)
     lanes = lax.broadcasted_iota(jnp.int32, (8, 256), 1)
@@ -129,12 +129,17 @@
         c_o[i] = out
 
 
-def chunk_kernel(pos, q, k, v, rate, write, spike, decay, bias, m_o, r_o, o_o):
+def chunk_kernel(pos, packed, spike, small, m_o, r_o, o_o):
     row = lax.broadcasted_iota(jnp.int32, (256, 256), 0)
     col = lax.broadcasted_iota(jnp.int32, (256, 256), 1)
     eye = row == col
-    logs = -decay[...] * softplus(rate[...]) + spike[...]
-    strength = sigmoid(write[...] + bias[...])
+    entry = lax.broadcasted_iota(jnp.int32, (32, 128), 0)
+    entry = entry == lax.broadcasted_iota(jnp.int32, (32, 128), 1)
+    decay, bias = (
+        jnp.sum(jnp.where(entry, small[i : i + 1], 0.0), axis=1, keepdims=True) for i in range(2)
+    )
+    logs = -decay * softplus(packed[768:800].astype(F32)) + spike[...]
+    strength = sigmoid(packed[800:832].astype(F32) + bias)
     entry = lax.broadcasted_iota(jnp.int32, (32, 256), 0) - pos[1] * 4
     below = (row >= col).astype(F32)
     above = (row <= col).astype(F32)
@@ -148,8 +153,7 @@
 
     lowers, parts = ([], [])
     for h in range(2):
-        kh = k[:, 128 * h : 128 * h + 128]
-        qh = q[:, 128 * h : 128 * h + 128]
+        qh, kh, vh = (packed[256 * i : 256 * i + 256, 128 * h : 128 * h + 128] for i in range(3))
         kf = kh.astype(F32)
         unit = lax.rsqrt(jnp.sum(kf * kf, axis=1, keepdims=True) + EPS)
         unit_row = jnp.sum(jnp.where(eye, unit, 0.0), axis=0, keepdims=True)
@@ -167,7 +171,7 @@
             grown = jnp.exp(total)
             right = jnp.concatenate(
                 [
-                    b * v[:, 128 * h : 128 * h + 128].astype(F32),
+                    b * vh.astype(F32),
                     (b * unit * grown) * kf,
                 ],
                 axis=1,
@@ -269,12 +273,12 @@
     o[...] = composed(pos, maps).astype(BF)
 
 
-def context_kernel(pos, low, decay, bias, extra, o):
+def context_kernel(pos, low, small, o):
     wide = [low[i][128:].astype(F32) for i in range(4)]
     rows = jnp.concatenate([w[16 * i : 16 * i + 16] for i in range(4) for w in wide], axis=0)
     gates = sum(w[64:66] for w in wide)
     o[...] = context_state(
-        pos, rows, gates[0:1], gates[1:2], decay[...], bias[...], extra[...]
+        pos, rows, gates[0:1], gates[1:2], small[0:1], small[1:2], small[2:3]
     )
 
 
@@ -309,7 +313,7 @@
             mm(reads[h][:, 0:128], first) + mm(reads[h][:, 128:256], second)
         )
         mean = jnp.mean(total * total, axis=1, keepdims=True)
-        heads.append((total * lax.rsqrt(mean + EPS) * gain[...]).astype(BF))
+        heads.append((total * lax.rsqrt(mean + EPS) * gain[3:4]).astype(BF))
     branch = mm(jnp.concatenate(heads, axis=1), weight[...]).astype(BF)
     for t in range(8):
         o[t] = branch[32 * t : 32 * t + 32]
@@ -384,10 +388,8 @@
     sp_index = lax.axis_index(SP)
     pos = jnp.stack([(y + c) % 4, x * 2 + c, zh, zl, (4 - c) % 4, sp_index * 4, c, x])
     pos = pos.astype(jnp.int32)
-    other = lax.ppermute(latent, "c", [(0, 1), (1, 0)])
-    pairs = [jnp.stack([latent, other])]
-    for d in range(1, 4):
-        pairs.append(lax.ppermute(pairs[0], "x", [(i, (i + d) % 4) for i in range(4)]))
+    mine = to_all(latent, "x", 4)
+    other = lax.ppermute(mine, "c", [(0, 1), (1, 0)])
     signals = jnp.stack([condition, context_condition_vector])
     signals = lax.dynamic_slice_in_dim(jax.nn.silu(signals), sp_index * 32, 32, 1)
     mod = modulation_matrix.astype(F32)
@@ -401,17 +403,18 @@
     part = jnp.sum(part, axis=0)
     fac = to_all(part, ("y", "x", "c"), 32)
 
-    queries, keys, values, rate, write, rows = call(
+    small = jnp.stack(
+        [
+            jnp.pad(head_decay_rate, (0, 96)),
+            jnp.pad(write_strength_bias, (0, 96)),
+            jnp.pad(context_write_offset_bias, (0, 96)),
+            head_norm_gain,
+        ]
+    )
+    packed, rows = call(
         project_kernel,
-        [
-            ((256, 256), BF),
-            ((256, 256), BF),
-            ((256, 256), BF),
-            ((32, 256), F32),
-            ((32, 256), F32),
-            ((4, 8, 512), BF),
-        ],
-        [SM] + [VM] * 7 + [HB] * 4,
+        [((832, 256), BF), ((4, 8, 512), BF)],
+        [SM] + [VM] * 5 + [HB] * 4,
         [
             pltpu.VMEM((272, D), BF),
             pltpu.VMEM((D, 256), BF),
@@ -423,31 +426,33 @@
         flops=10**9,
     )(
         pos,
-        *pairs,
+        mine,
+        other,
         fac,
         query_matrix,
         key_matrix,
-        value_matrix,
-        decay_input_weight.T,
-        write_strength_weight.T,
-        context,
-    )
+        *(
+            pltpu.with_memory_space_constraint(a, pltpu.HBM)
+            for a in (
+                value_matrix,
+                decay_input_weight.T,
+                write_strength_weight.T,
+                context,
+            )
+        ),
+    )
+    packed = pltpu.with_memory_space_constraint(packed, pltpu.HBM)
     rows = lax.all_to_all(rows, "zh", 0, 0, tiled=True)
     maps, reads, base = call(
         chunk_kernel,
         [((4, 160, 256), BF), ((2, 256, 256), BF), ((256, 256), F32)],
-        [SM] + [VM] * 8,
+        [SM] + [VM] * 3,
         flops=4 * 10**9,
     )(
         pos,
-        queries,
-        keys,
-        values,
-        rate,
-        write,
+        packed,
         log_spike_added.T,
-        head_decay_rate.reshape(32, 1),
-        write_strength_bias.reshape(32, 1),
+        small,
     )
     maps = call(pack_kernel, ((4, 160, 256), BF), [SM, VM, VM], aliases={1: 0})(
         pos, maps, rows
@@ -459,19 +464,15 @@
     of_high = []
     for d in (3, 2, 1):
         of_high.append(lax.ppermute(high, ("zh", "y", "c"), onward(d)))
-    start = call(context_kernel, ((128, 128), F32), [SM] + [VM] * 4, flops=10**9)(
-        pos,
-        of_low,
-        head_decay_rate.reshape(1, 32),
-        write_strength_bias.reshape(1, 32),
-        context_write_offset_bias.reshape(1, 32),
+    start = call(context_kernel, ((128, 128), F32), [SM] + [VM] * 2, flops=10**9)(
+        pos, of_low, small
     )
     states = call(scan_kernel, ((4, 128, 128), BF), [SM] + [VM] * 6, flops=10**8)(
         pos, start, *of_high, of_low, of_y
     )
     states = lax.all_to_all(states, "y", 0, 0, tiled=True)
     branch = call(read_kernel, ((8, 32, D), BF), [SM] + [VM] * 5, flops=10**8)(
-        pos, states, reads, base, head_norm_gain.reshape(1, 128), output_matrix
+        pos, states, reads, base, small, output_matrix
     )
     branch = lax.all_to_all(branch, TP, 0, 0, tiled=True)
     return call(output_kernel, ((32, D), BF), [VM] * 3, flops=10**8)(branch, fac, latent)

time: 160 us -> 160 us (level)
  waiting for transfers between devices: 21.4 us -> 36.9 us
  local copies, waits for them, and re-layouts: 15.9 us -> 4.72 us
  starting transfers between devices: 48.2 us -> 42.3 us
    ppermute x4 -> x1, starting transfers between devices: 18.2 us -> 4.29 us  [per_device(): other = lax.ppermute(mine, 'c', [(0, 1), (1, 0)])]
    all_to_all x2 -> x3, waiting for transfers between devices: 10.3 us -> 22.3 us  [to_all(): lax.all_to_all(jnp.broadcast_to(value[None], (count, *value.shape)), axes...]
    all_to_all x2 -> x3, starting transfers between devices: 18.6 us -> 30.5 us  [to_all(): lax.all_to_all(jnp.broadcast_to(value[None], (count, *value.shape)), axes...]
    unnamed x54 -> x26, local copies, waits for them, and re-layouts: 13.1 us -> 1.46 us
    all_to_all x1, waiting for transfers between devices: 1.21 us -> 5.11 us  [per_device(): rows = lax.all_to_all(rows, 'zh', 0, 0, tiled=True)]
    all_to_all x1, starting transfers between devices: 7.28 us -> 3.48 us  [per_device(): rows = lax.all_to_all(rows, 'zh', 0, 0, tiled=True)]
    broadcast_in_dim x2 -> x3, local copies, waits for them, and re-layouts: 1.38 us -> 3.16 us  [to_all(): jnp.broadcast_to(value[None], (count, *value.shape))]
  transfers between devices with their start and end apart: 10 -> 8, of which waited for: 6 -> 7; matrix products, arithmetic and copies ran while one was open for 2% -> 1% of each run, Pallas kernels for 6% -> 7%
where the time goes in v3:
time: 160 us; the launch traced here: 159 us
  blocking collectives  52.6 us (33%)
  starting transfers between devices  42.3 us (26%)
  waiting for transfers between devices  36.9 us (23%)
  Pallas kernels  21.8 us (14%)
  local copies, waits for them, and re-layouts  4.72 us (3%)
    all_to_all x3, starting transfers between devices, to_all(): lax.all_to_all(jnp.broadcast_to(value[None], (count, *value.shape)), axes...  30.5 us
    all_to_all x1, blocking collectives, per_device(): branch = lax.all_to_all(branch, TP, 0, 0, tiled=True)  22.8 us
    all_to_all x3, waiting for transfers between devices, to_all(): lax.all_to_all(jnp.broadcast_to(value[None], (count, *value.shape)), axes...  22.3 us
    all_to_all x1, blocking collectives, per_device(): of_low = lax.all_to_all(low, 'zl', 0, 0, tiled=True)  14.4 us
    ppermute x3, waiting for transfers between devices, per_device(): of_high.append(lax.ppermute(high, ('zh', 'y', 'c'), onward(d)))  9.42 us
    all_to_all x1, blocking collectives, per_device(): of_y = lax.all_to_all(maps, 'y', 0, 0, tiled=True)  8.25 us
    all_to_all x1, blocking collectives, per_device(): states = lax.all_to_all(states, 'y', 0, 0, tiled=True)  7.21 us
    pallas_call x1, Pallas kernels, per_device(): call(chunk_kernel, [((4, 160, 256), BF), ((2, 256, 256), BF), ((256, 256)...  6.67 us
  transfers between devices with their start and end apart: 8, of which 7 were waited for; matrix products, arithmetic and copies ran while one was open for 1% of the time, Pallas kernels for 7%

profile of v3, /device:TPU:1, one launch (start us, length us, event | category | flops | bytes accessed | tf_op | source)
XLA Modules:
  0.0 158.9 jit_solution(9051109336311815547)
XLA Ops:
  0.0 1.8 %broadcast_in_dim.6 = bf16[4,32,2048]{2,1,0:T(8,128)(2,1)} broadcast(bf16[32,2048]{1,0:T(8,128)(2,1)} %lat.1), dimensions={1,2} | broadcast | bytes 655360 | tf_op jit(solution)/shard_map/broadcast_in_dim | solution.py:353
  1.8 5.0 %all-to-all-start = ((bf16[4,32,2048]{2,1,0:T(8,128)(2,1)}), bf16[4,32,2048]{2,1,0:T(8,128)(2,1)S(1)}, u32[]{:S(2)}, u32[]{:S(2)}) async-start(bf16[4,32,2048]{2,1,0:T(8,128)(2,1)} %broadcast_in_dim.6), calls=%async_computation | async-start | bytes 1048576 | tf_op jit(solution)/shard_map/all_to_all | solution.py:352
  6.8 0.0 copy-done.7
  6.8 0.0 copy-done.8
  6.8 0.1 divide_multiply_fusion
  6.9 0.1 fusion
  7.0 0.1 multiply_reduce_fusion
  7.1 6.6 %all-to-all-done.one = bf16[4,32,2048]{2,1,0:T(8,128)(2,1)S(1)} async-done(((bf16[4,32,2048]{2,1,0:T(8,128)(2,1)}), bf16[4,32,2048]{2,1,0:T(8,128)(2,1)S(1)}, u32[]{:S(2)}, u32[]{:S(2)}) %all-to-all-start) | async-done | bytes 524320 | tf_op jit(solution)/shard_map/all_to_all | solution.py:352
  13.7 0.7 broadcast_in_dim.7
  14.4 16.3 %all-to-all-start.1 = ((f32[16,5,256]{2,1,0:T(8,128)}), f32[16,5,256]{2,1,0:T(8,128)S(1)}, u32[]{:S(2)}, u32[]{:S(2)}) async-start(f32[16,5,256]{2,1,0:T(8,128)} %broadcast_in_dim.7), calls=%async_computation.1 | async-start | bytes 262144 | tf_op jit(solution)/shard_map/all_to_all | solution.py:352
  30.7 4.3 %collective-permute-start = (bf16[4,32,2048]{2,1,0:T(8,128)(2,1)S(1)}, bf16[4,32,2048]{2,1,0:T(8,128)(2,1)S(1)}, u32[]{:S(2)}, u32[]{:S(2)}) collective-permute-start(bf16[4,32,2048]{2,1,0:T(8,128)(2,1)S(1)} %all-to-all-done.one), channel_id=1, source_target_pairs={{0,1},{1,0},{2,3},{3,2},{4,5},{5,4},{6,7},{7,6},{8,9},{9,8},{10,11... | collective-permute-start | bytes 1572872 | tf_op jit(solution)/shard_map/ppermute | solution.py:392
  35.0 0.0 copy-done.9
  35.0 0.0 copy-done.10
  35.0 7.6 %all-to-all-done.1 = f32[16,5,256]{2,1,0:T(8,128)S(1)} async-done(((f32[16,5,256]{2,1,0:T(8,128)}), f32[16,5,256]{2,1,0:T(8,128)S(1)}, u32[]{:S(2)}, u32[]{:S(2)}) %all-to-all-start.1) | async-done | bytes 81952 | tf_op jit(solution)/shard_map/all_to_all | solution.py:352
  42.7 0.7 broadcast_in_dim.8
  43.4 9.2 %all-to-all-start.2 = ((f32[32,5,256]{2,1,0:T(8,128)}), f32[32,5,256]{2,1,0:T(8,128)S(1)}, u32[]{:S(2)}, u32[]{:S(2)}) async-start(f32[32,5,256]{2,1,0:T(8,128)} %broadcast_in_dim.8), calls=%async_computation.2 | async-start | bytes 524288 | tf_op jit(solution)/shard_map/all_to_all | solution.py:352
  52.6 0.1 stack.59.pos
  52.7 0.7 copy-done.11
  53.4 8.1 %all-to-all-done.2.fac = f32[32,5,256]{2,1,0:T(8,128)S(1)} async-done(((f32[32,5,256]{2,1,0:T(8,128)}), f32[32,5,256]{2,1,0:T(8,128)S(1)}, u32[]{:S(2)}, u32[]{:S(2)}) %all-to-all-start.2) | async-done | bytes 163872 | tf_op jit(solution)/shard_map/all_to_all | solution.py:352
  61.5 0.0 collective-permute-done.two
  61.5 0.0 copy-done
  61.5 4.5 %shard_map.154 = (bf16[832,256]{1,0:T(8,128)(2,1)S(1)}, bf16[4,8,512]{2,1,0:T(8,128)(2,1)}) custom-call(s32[8]{0:T(128)S(1)} %stack.59.pos, bf16[4,32,2048]{2,1,0:T(8,128)(2,1)S(1)} %all-to-all-done.one, bf16[4,32,2048]{2,1,0:T(8,128)(2,1)S(1)} %collective-permute-done.two, f32[32,5,256]{2,1,0:T(8,128)S(1)} %all-to-all-done.2.fac, ...), custom_call_target="tpu_custom_call" | custom-call | flops 1000000000 | bytes 1 | tf_op jit(solution)/shard_map/pallas_call | solution.py:414
  66.0 0.0 copy-start.4
  66.0 0.8 copy-done.4
  66.8 3.5 %all-to-all-start.3 = ((bf16[4,8,512]{2,1,0:T(8,128)(2,1)}), bf16[4,8,512]{2,1,0:T(8,128)(2,1)S(1)}, u32[]{:S(2)}, u32[]{:S(2)}) async-start(bf16[4,8,512]{2,1,0:T(8,128)(2,1)} %get-tuple-element.12), calls=%async_computation.3 | async-start | bytes 65536 | tf_op jit(solution)/shard_map/all_to_all | solution.py:445
  70.3 6.7 %shard_map.155 = (bf16[4,160,256]{2,1,0:T(8,128)(2,1)S(1)}, bf16[2,256,256]{2,1,0:T(8,128)(2,1)S(1)}, f32[256,256]{1,0:T(8,128)S(1)}) custom-call(s32[8]{0:T(128)S(1)} %stack.59.pos, bf16[832,256]{1,0:T(8,128)(2,1)} %copy-done.4, f32[32,256]{1,0:T(8,128)S(1)} %bitcast.24, f32[4,128]{1,0:T(4,128)S(1)} %pad_maximum_fusion.1.small.gain), custom_call_target="tpu_custom_call" | custom-call | flops 4000000000 | bytes 1 | tf_op jit(solution)/shard_map/pallas_call | solution.py:446
  76.9 5.1 %all-to-all-done.3.rows = bf16[4,8,512]{2,1,0:T(8,128)(2,1)S(1)} async-done(((bf16[4,8,512]{2,1,0:T(8,128)(2,1)}), bf16[4,8,512]{2,1,0:T(8,128)(2,1)S(1)}, u32[]{:S(2)}, u32[]{:S(2)}) %all-to-all-start.3) | async-done | bytes 32800 | tf_op jit(solution)/shard_map/all_to_all | solution.py:445
  82.0 0.6 shard_map.156
  82.6 8.3 %all_to_all.40.maps.own = bf16[4,160,256]{2,1,0:T(8,128)(2,1)S(1)} all-to-all(bf16[4,160,256]{2,1,0:T(8,128)(2,1)S(1)} %shard_map.156), channel_id=1, replica_groups=mesh['zh'=4,'zl'=4,'y'=4,'x'=4,'c'=2] {'y'}, dimensions={0} | all-to-all | bytes 655360 | tf_op jit(solution)/shard_map/all_to_all | solution.py:460
  90.9 1.1 shard_map.157
  92.0 14.4 %all_to_all.41.low.maps = bf16[4,208,256]{2,1,0:T(8,128)(2,1)S(1)} all-to-all(bf16[4,208,256]{2,1,0:T(8,128)(2,1)S(1)} %shard_map.157), channel_id=1, replica_groups=mesh['zh'=4,'zl'=4,'y'=4,'x'=4,'c'=2] {'zl'}, dimensions={0} | all-to-all | bytes 851968 | tf_op jit(solution)/shard_map/all_to_all | solution.py:462
  106.4 1.1 shard_map.159
  107.5 1.3 collective-permute-start.3
  108.8 1.3 collective-permute-start.2
  110.1 1.5 collective-permute-start.1
  111.6 3.9 %shard_map.158.start = f32[128,128]{1,0:T(8,128)S(1)} custom-call(s32[8]{0:T(128)S(1)} %stack.59.pos, bf16[4,208,256]{2,1,0:T(8,128)(2,1)S(1)} %all_to_all.41.low.maps, f32[4,128]{1,0:T(4,128)S(1)} %pad_maximum_fusion.1.small.gain), custom_call_target="tpu_custom_call" | custom-call | flops 1000000000 | bytes 1 | tf_op jit(solution)/shard_map/pallas_call | solution.py:467
  115.4 0.0 copy-start.2
  115.5 1.0 collective-permute-done.3.near
  116.4 6.2 %collective-permute-done.2.middle = bf16[128,256]{1,0:T(8,128)(2,1)S(1)} collective-permute-done((bf16[128,256]{1,0:T(8,128)(2,1)S(1)}, bf16[128,256]{1,0:T(8,128)(2,1)S(1)}, u32[]{:S(2)}, u32[]{:S(2)}) %collective-permute-start.2) | collective-permute-done | bytes 65568 | tf_op jit(solution)/shard_map/ppermute | solution.py:466
  122.6 2.2 %collective-permute-done.1.far = bf16[128,256]{1,0:T(8,128)(2,1)S(1)} collective-permute-done((bf16[128,256]{1,0:T(8,128)(2,1)S(1)}, bf16[128,256]{1,0:T(8,128)(2,1)S(1)}, u32[]{:S(2)}, u32[]{:S(2)}) %collective-permute-start.1) | collective-permute-done | bytes 65568 | tf_op jit(solution)/shard_map/ppermute | solution.py:466
  124.9 1.9 %shard_map.160 = bf16[4,128,128]{2,1,0:T(8,128)(2,1)S(1)} custom-call(s32[8]{0:T(128)S(1)} %stack.59.pos, f32[128,128]{1,0:T(8,128)S(1)} %shard_map.158.start, bf16[128,256]{1,0:T(8,128)(2,1)S(1)} %collective-permute-done.1.far, bf16[128,256]{1,0:T(8,128)(2,1)S(1)} %collective-permute-done.2.middle, bf16[128,256]{1,0:T(8,128)(2,1)S(1)} %collective-permute-done.3.near, ...), custom_call_target="tpu_custom_call" | custom-call | flops 100000000 | bytes 1 | tf_op jit(solution)/shard_map/pallas_call | solution.py:470
  126.8 7.2 %all_to_all.42.states = bf16[4,128,128]{2,1,0:T(8,128)(2,1)S(1)} all-to-all(bf16[4,128,128]{2,1,0:T(8,128)(2,1)S(1)} %shard_map.160), channel_id=1, replica_groups=mesh['zh'=4,'zl'=4,'y'=4,'x'=4,'c'=2] {'y'}, dimensions={0} | all-to-all | bytes 262144 | tf_op jit(solution)/shard_map/all_to_all | solution.py:473
  134.0 0.0 copy-done.2
  134.0 1.2 shard_map.161
  135.3 0.0 copy-start.3
  135.3 22.8 %all_to_all.43.rows = bf16[8,32,2048]{2,1,0:T(8,128)(2,1)S(1)} all-to-all(bf16[8,32,2048]{2,1,0:T(8,128)(2,1)S(1)} %shard_map.161), channel_id=1, replica_groups=mesh['zh'=4,'zl'=4,'y'=4,'x'=4,'c'=2] {'x','c'}, dimensions={0} | all-to-all | bytes 2097152 | tf_op jit(solution)/shard_map/all_to_all | solution.py:477
  158.1 0.0 copy-done.3
  158.1 0.8 shard_map.162
  (21 shorter events, 0.1 us)
Async XLA Ops:
  0.0 6.8 %copy-start.7 = (f32[2048]{0:T(1024)S(1)}, f32[2048]{0:T(1024)}, u32[]{:S(2)}) copy-start(f32[2048]{0:T(1024)} %param.19) | copy-start | bytes 24580
  0.0 6.8 %copy-start.8 = (f32[2048]{0:T(1024)S(1)}, f32[2048]{0:T(1024)}, u32[]{:S(2)}) copy-start(f32[2048]{0:T(1024)} %param.17) | copy-start | bytes 24580
  1.8 5.1 %copy-start.6 = (bf16[3,32,256]{2,1,0:T(8,128)(2,1)S(1)}, bf16[3,32,256]{2,1,0:T(8,128)(2,1)}, u32[]{:S(2)}) copy-start(bf16[3,32,256]{2,1,0:T(8,128)(2,1)} %param.20) | copy-start | bytes 147460
  1.8 33.2 %copy-start.9 = (f32[32]{0:T(128)S(1)}, f32[32]{0:T(128)}, u32[]{:S(2)}) copy-start(f32[32]{0:T(128)} %param.28) | copy-start | bytes 388
  1.8 33.2 %copy-start.10 = (f32[32]{0:T(128)S(1)}, f32[32]{0:T(128)}, u32[]{:S(2)}) copy-start(f32[32]{0:T(128)} %param.27) | copy-start | bytes 388
  1.8 59.7 %copy-start.1 = (bf16[2048,256]{1,0:T(8,128)(2,1)S(1)}, bf16[2048,256]{1,0:T(8,128)(2,1)}, u32[]{:S(2)}) copy-start(bf16[2048,256]{1,0:T(8,128)(2,1)} %wk.1) | copy-start | bytes 3145732
  1.8 11.9 %all-to-all-start = ((bf16[4,32,2048]{2,1,0:T(8,128)(2,1)}), bf16[4,32,2048]{2,1,0:T(8,128)(2,1)S(1)}, u32[]{:S(2)}, u32[]{:S(2)}) async-start(bf16[4,32,2048]{2,1,0:T(8,128)(2,1)} %broadcast_in_dim.6), calls=%async_computation | async-start | bytes 1048576 | tf_op jit(solution)/shard_map/all_to_all | solution.py:352
  6.8 54.7 %copy-start = (bf16[2048,256]{1,0:T(8,128)(2,1)S(1)}, bf16[2048,256]{1,0:T(8,128)(2,1)}, u32[]{:S(2)}) copy-start(bf16[2048,256]{1,0:T(8,128)(2,1)} %wq.1) | copy-start | bytes 3145732
  14.4 28.3 %all-to-all-start.1 = ((f32[16,5,256]{2,1,0:T(8,128)}), f32[16,5,256]{2,1,0:T(8,128)S(1)}, u32[]{:S(2)}, u32[]{:S(2)}) async-start(f32[16,5,256]{2,1,0:T(8,128)} %broadcast_in_dim.7), calls=%async_computation.1 | async-start | bytes 262144 | tf_op jit(solution)/shard_map/all_to_all | solution.py:352
  30.7 30.8 %collective-permute-start = (bf16[4,32,2048]{2,1,0:T(8,128)(2,1)S(1)}, bf16[4,32,2048]{2,1,0:T(8,128)(2,1)S(1)}, u32[]{:S(2)}, u32[]{:S(2)}) collective-permute-start(bf16[4,32,2048]{2,1,0:T(8,128)(2,1)S(1)} %all-to-all-done.one), channel_id=1, source_target_pairs={{0,1},{1,0},{2,3},{3,2},{4,5},{5,4},{6,7},{7,6},{8,9},{9,8},{10,11... | collective-permute-start | bytes 1572872 | tf_op jit(solution)/shard_map/ppermute | solution.py:392
  43.4 9.2 %copy-start.12 = (f32[32]{0:T(128)S(1)}, f32[32]{0:T(128)}, u32[]{:S(2)}) copy-start(f32[32]{0:T(128)} %param.26) | copy-start | bytes 388
  43.4 18.1 %all-to-all-start.2 = ((f32[32,5,256]{2,1,0:T(8,128)}), f32[32,5,256]{2,1,0:T(8,128)S(1)}, u32[]{:S(2)}, u32[]{:S(2)}) async-start(f32[32,5,256]{2,1,0:T(8,128)} %broadcast_in_dim.8), calls=%async_computation.2 | async-start | bytes 524288 | tf_op jit(solution)/shard_map/all_to_all | solution.py:352
  52.7 0.7 copy-start.11
  66.0 0.8 copy-start.4
  66.8 3.5 %copy-start.5 = (f32[256,32]{0,1:T(8,128)S(1)}, f32[256,32]{0,1:T(8,128)}, u32[]{:S(2)}) copy-start(f32[256,32]{0,1:T(8,128)} %param.29) | copy-start | bytes 98308
  66.8 15.3 %all-to-all-start.3 = ((bf16[4,8,512]{2,1,0:T(8,128)(2,1)}), bf16[4,8,512]{2,1,0:T(8,128)(2,1)S(1)}, u32[]{:S(2)}, u32[]{:S(2)}) async-start(bf16[4,8,512]{2,1,0:T(8,128)(2,1)} %get-tuple-element.12), calls=%async_computation.3 | async-start | bytes 65536 | tf_op jit(solution)/shard_map/all_to_all | solution.py:445
  107.5 8.9 %collective-permute-start.3 = (bf16[128,256]{1,0:T(8,128)(2,1)S(1)}, bf16[128,256]{1,0:T(8,128)(2,1)S(1)}, u32[]{:S(2)}, u32[]{:S(2)}) collective-permute-start(bf16[128,256]{1,0:T(8,128)(2,1)S(1)} %shard_map.159), channel_id=1, source_target_pairs={{0,128},{9,137},{16,144},{25,153},{128,256},{129,1},{136,8},{137,2... | collective-permute-start | bytes 196616 | tf_op jit(solution)/shard_map/ppermute | solution.py:466
  108.8 13.9 %collective-permute-start.2 = (bf16[128,256]{1,0:T(8,128)(2,1)S(1)}, bf16[128,256]{1,0:T(8,128)(2,1)S(1)}, u32[]{:S(2)}, u32[]{:S(2)}) collective-permute-start(bf16[128,256]{1,0:T(8,128)(2,1)S(1)} %shard_map.159), channel_id=1, source_target_pairs={{0,256},{9,265},{16,272},{25,281},{128,384},{137,393},{144,400},{1... | collective-permute-start | bytes 196616 | tf_op jit(solution)/shard_map/ppermute | solution.py:466
  110.1 14.8 %collective-permute-start.1 = (bf16[128,256]{1,0:T(8,128)(2,1)S(1)}, bf16[128,256]{1,0:T(8,128)(2,1)S(1)}, u32[]{:S(2)}, u32[]{:S(2)}) collective-permute-start(bf16[128,256]{1,0:T(8,128)(2,1)S(1)} %shard_map.159), channel_id=1, source_target_pairs={{0,384},{9,393},{16,400},{25,409},{385,1},{392,8},{401,17},{408,24... | collective-permute-start | bytes 196616 | tf_op jit(solution)/shard_map/ppermute | solution.py:466
  115.4 18.6 %copy-start.2 = (bf16[256,2048]{1,0:T(8,128)(2,1)S(1)}, bf16[256,2048]{1,0:T(8,128)(2,1)}, u32[]{:S(2)}) copy-start(bf16[256,2048]{1,0:T(8,128)(2,1)} %weight.1) | copy-start | bytes 3145732
  135.3 22.8 %copy-start.3 = (bf16[32,2048]{1,0:T(8,128)(2,1)S(1)}, bf16[32,2048]{1,0:T(8,128)(2,1)}, u32[]{:S(2)}) copy-start(bf16[32,2048]{1,0:T(8,128)(2,1)} %lat.1) | copy-start | bytes 393220

commit v4 on v3

--- a/solution.py
+++ b/solution.py
@@ -74,14 +74,14 @@
     return out
 
 
-def project_kernel(
-    pos, one, two, fac, wq, wk, wv_h, wd_h, ww_h, ctx_h,
-    p_o, c_o,
-    hid, wv, wd, ww, ctx, sems,
+def front_kernel(
+    pos, one, two, ctx, fac, wq, wk, spike, small, wv_h, wd_h, ww_h,
+    m_o, r_o, o_o,
+    hid, packed, wv, wd, ww, sems,
 ):
     copies = [
         pltpu.make_async_copy(source, target, sems.at[i])
-        for i, (source, target) in enumerate(((ctx_h, ctx), (wv_h, wv), (wd_h, wd), (ww_h, ww)))
+        for i, (source, target) in enumerate(((wv_h, wv), (wd_h, wd), (ww_h, ww)))
     ]
     for copy in copies:
         copy.start()
@@ -91,45 +91,45 @@
         for slot, r in enumerate((0, 1, 3, 4)):
             factors[slot].append(f[r : r + 1])
     shift, scale, c_shift, c_scale = (jnp.concatenate(f, axis=1) for f in factors)
-    for x in range(4):
+    for d in range(4):
         for i, lat in enumerate((one, two)):
             core = pos[6] if i == 0 else 1 - pos[6]
-            spot = (2 * x + core) * 32
-            hid[pl.ds(pl.multiple_of(spot, 32), 32)] = norm_rows(lat[x], scale, shift)
-    copies[0].wait()
-    hid[256:260] = norm_rows(ctx[...], c_scale, c_shift)
-    hid[260:272] = jnp.zeros((12, D), BF)
+            spot = (2 * ((pos[7] + 4 - d) % 4) + core) * 32
+            hid[pl.ds(pl.multiple_of(spot, 32), 32)] = norm_rows(lat[d], scale, shift)
+    context_rows = jnp.concatenate([ctx[i].astype(F32) for i in range(4)], axis=0)
+    hid[256:272] = norm_rows(context_rows, c_scale, c_shift)
     rows = hid[...]
-    p_o[0:256] = mm(hid[0:256], wq[...]).astype(BF)
+    packed[0:256] = mm(hid[0:256], wq[...]).astype(BF)
     keys = mm(rows, wk[...]).astype(BF)
-    p_o[256:512] = keys[:256]
-    for copy in copies[1:]:
+    packed[256:512] = keys[:256]
+    for copy in copies:
         copy.wait()
     values = mm(rows, wv[...]).astype(BF)
-    p_o[512:768] = values[:256]
+    packed[512:768] = values[:256]
     last_two = ((1,), (1,))
-    p_o[768:800] = mm(wd[...], hid[0:256], last_two).astype(BF)
-    p_o[800:832] = mm(ww[...], hid[0:256], last_two).astype(BF)
-    rate = mm(hid[256:264], wd[...], last_two).astype(BF).astype(F32)
-    write = mm(hid[256:264], ww[...], last_two).astype(BF).astype(F32)
-    lanes = lax.broadcasted_iota(jnp.int32, (8, 256), 1)
-    rank = lax.broadcasted_iota(jnp.int32, (8, 256), 0)
-    spots = (lanes == rank + pos[5]) & (rank < 4)
-    wide = [rows_of[256:264].astype(F32)[0:4] for rows_of in (keys, values)]
-    pieces = [jnp.concatenate(wide, axis=1)]
+    packed[768:800] = mm(wd[...], hid[0:256], last_two).astype(BF)
+    packed[800:832] = mm(ww[...], hid[0:256], last_two).astype(BF)
+    rate = mm(hid[256:272], wd[...], last_two).astype(BF).astype(F32)
+    write = mm(hid[256:272], ww[...], last_two).astype(BF).astype(F32)
+    lanes = lax.broadcasted_iota(jnp.int32, (16, 256), 1)
+    rank = lax.broadcasted_iota(jnp.int32, (16, 256), 0)
+    spots = lanes == (rank // 4) * 64 + rank % 4 + pos[5]
     for j in range(4):
+        h = j // 2
+        to = (j + pos[4]) % 4
         lane = pos[1] * 4 + j
+        m_o[to, 128:144, 0:128] = keys[256:272, 128 * h : 128 * h + 128]
+        m_o[to, 128:144, 128:256] = values[256:272, 128 * h : 128 * h + 128]
         gates = [
             jnp.sum(jnp.where(spots, column(g, lane), 0.0), axis=0, keepdims=True)
             for g in (rate, write)
         ]
-        pieces.append(jnp.concatenate(gates, axis=1))
-    out = jnp.concatenate(pieces, axis=0).astype(BF)
-    for i in range(4):
-        c_o[i] = out
-
-
-def chunk_kernel(pos, packed, spike, small, m_o, r_o, o_o):
+        gates.append(jnp.zeros((14, 256), F32))
+        m_o[to, 144:160] = jnp.concatenate(gates, axis=0).astype(BF)
+    chunk(pos, packed, spike, small, m_o, r_o, o_o)
+
+
+def chunk(pos, packed, spike, small, m_o, r_o, o_o):
     row = lax.broadcasted_iota(jnp.int32, (256, 256), 0)
     col = lax.broadcasted_iota(jnp.int32, (256, 256), 1)
     eye = row == col
@@ -195,7 +195,6 @@
         h, e = divmod(j, 2)
         r_o[h, :, 128 * e : 128 * e + 128] = (grown_q - read[:, 128:]).astype(BF)
         outs[h] = read[:, :128] if e == 0 else outs[h] + read[:, :128]
-    m_o[:, 128:160] = jnp.zeros((4, 32, 256), BF)
     o_o[:, 0:128] = outs[0]
     o_o[:, 128:256] = outs[1]
 
@@ -232,20 +231,6 @@
     both = mm(linear, jnp.concatenate([high, low], axis=1))
     n = state.shape[1]
     return both[:, :n] + both[:, n:]
-
-
-def pack_kernel(pos, maps, rows, o):
-    wide = [rows[i].astype(F32) for i in range(4)]
-    for j in range(4):
-        h = j // 2
-        to = (j + pos[4]) % 4
-        parts = []
-        for w in wide:
-            sides = [w[0:4, at + 128 * h : at + 128 * h + 128] for at in (0, 256)]
-            parts.append(jnp.concatenate(sides, axis=1))
-        gates = sum(w[4 + j : 5 + j] for w in wide)
-        parts += [gates[:, 0:256], gates[:, 256:512], jnp.zeros((14, 256), F32)]
-        o[to, 128:160] = jnp.concatenate(parts, axis=0).astype(BF)
 
 
 def composed(pos, maps):
@@ -386,9 +371,13 @@
     zh, zl, y = (lax.axis_index("zh"), lax.axis_index("zl"), lax.axis_index("y"))
     x, c = (lax.axis_index("x"), lax.axis_index("c"))
     sp_index = lax.axis_index(SP)
-    pos = jnp.stack([(y + c) % 4, x * 2 + c, zh, zl, (4 - c) % 4, sp_index * 4, c, x])
+    pos = jnp.stack([(y + c) % 4, x * 2 + c, zh, zl, (4 - c) % 4, zl * 16 + y * 4, c, x])
     pos = pos.astype(jnp.int32)
-    mine = to_all(latent, "x", 4)
+    ctx = to_all(context, "zh", 4)
+    parts = [latent]
+    for d in range(1, 4):
+        parts.append(lax.ppermute(latent, "x", [(i, (i + d) % 4) for i in range(4)]))
+    mine = jnp.stack(parts)
     other = lax.ppermute(mine, "c", [(0, 1), (1, 0)])
     signals = jnp.stack([condition, context_condition_vector])
     signals = lax.dynamic_slice_in_dim(jax.nn.silu(signals), sp_index * 32, 32, 1)
@@ -411,51 +400,33 @@
             head_norm_gain,
         ]
     )
-    packed, rows = call(
-        project_kernel,
-        [((832, 256), BF), ((4, 8, 512), BF)],
-        [SM] + [VM] * 5 + [HB] * 4,
+    maps, reads, base = call(
+        front_kernel,
+        [((4, 160, 256), BF), ((2, 256, 256), BF), ((256, 256), F32)],
+        [SM] + [VM] * 8 + [HB] * 3,
         [
             pltpu.VMEM((272, D), BF),
+            pltpu.VMEM((832, 256), BF),
             pltpu.VMEM((D, 256), BF),
             pltpu.VMEM((32, D), BF),
             pltpu.VMEM((32, D), BF),
-            pltpu.VMEM((4, D), BF),
-            pltpu.SemaphoreType.DMA((4,)),
+            pltpu.SemaphoreType.DMA((3,)),
         ],
-        flops=10**9,
+        flops=5 * 10**9,
     )(
         pos,
         mine,
         other,
+        ctx,
         fac,
         query_matrix,
         key_matrix,
+        log_spike_added.T,
+        small,
         *(
             pltpu.with_memory_space_constraint(a, pltpu.HBM)
-            for a in (
-                value_matrix,
-                decay_input_weight.T,
-                write_strength_weight.T,
-                context,
-            )
+            for a in (value_matrix, decay_input_weight.T, write_strength_weight.T)
         ),
-    )
-    packed = pltpu.with_memory_space_constraint(packed, pltpu.HBM)
-    rows = lax.all_to_all(rows, "zh", 0, 0, tiled=True)
-    maps, reads, base = call(
-        chunk_kernel,
-        [((4, 160, 256), BF), ((2, 256, 256), BF), ((256, 256), F32)],
-        [SM] + [VM] * 3,
-        flops=4 * 10**9,
-    )(
-        pos,
-        packed,
-        log_spike_added.T,
-        small,
-    )
-    maps = call(pack_kernel, ((4, 160, 256), BF), [SM, VM, VM], aliases={1: 0})(
-        pos, maps, rows
     )
     of_y = lax.all_to_all(maps, "y", 0, 0, tiled=True)
     low = call(low_kernel, ((4, 208, 256), BF), [SM, VM])(pos, of_y)

time: 160 us -> 165 us (1.031)
  starting transfers between devices: 42.3 us -> 49.3 us
  local copies, waits for them, and re-layouts: 4.72 us -> 2.84 us
    ppermute x0 -> x3, starting transfers between devices: none -> 12.1 us  [per_device(): lax.ppermute(latent, 'x', [(i, (i + d) % 4) for i in range(4)])]
    all_to_all x3, waiting for transfers between devices: 22.3 us -> 27.8 us  [to_all(): lax.all_to_all(jnp.broadcast_to(value[None], (count, *value.shape)), axes...]
    all_to_all x1 -> x0, waiting for transfers between devices: 5.11 us -> none  [per_device(): rows = lax.all_to_all(rows, 'zh', 0, 0, tiled=True)]
    all_to_all x1 -> x0, starting transfers between devices: 3.48 us -> none  [per_device(): rows = lax.all_to_all(rows, 'zh', 0, 0, tiled=True)]
    pallas_call x3 -> x1, Pallas kernels: 11.8 us -> 10.4 us  [per_device(): call(front_kernel, [((4, 160, 256), BF), ((2, 256, 256), BF), ((256, 256)...]
  transfers between devices with their start and end apart: 8 -> 10, of which waited for: 7 -> 6; matrix products, arithmetic and copies ran while one was open for 1% -> 2% of each run, Pallas kernels for 7% -> 2%
where the time goes in v4:
time: 165 us; the launch traced here: 164 us
  blocking collectives  52.9 us (32%)
  starting transfers between devices  49.3 us (30%)
  waiting for transfers between devices  37.4 us (23%)
  Pallas kernels  20.4 us (12%)
  local copies, waits for them, and re-layouts  2.84 us (2%)
    all_to_all x3, starting transfers between devices, to_all(): lax.all_to_all(jnp.broadcast_to(value[None], (count, *value.shape)), axes...  29.3 us
    all_to_all x3, waiting for transfers between devices, to_all(): lax.all_to_all(jnp.broadcast_to(value[None], (count, *value.shape)), axes...  27.8 us
    all_to_all x1, blocking collectives, per_device(): branch = lax.all_to_all(branch, TP, 0, 0, tiled=True)  21.6 us
    all_to_all x1, blocking collectives, per_device(): of_low = lax.all_to_all(low, 'zl', 0, 0, tiled=True)  14.3 us
    ppermute x3, starting transfers between devices, per_device(): lax.ppermute(latent, 'x', [(i, (i + d) % 4) for i in range(4)])  12.1 us
    pallas_call x1, Pallas kernels, per_device(): call(front_kernel, [((4, 160, 256), BF), ((2, 256, 256), BF), ((256, 256)...  10.4 us
    all_to_all x1, blocking collectives, per_device(): of_y = lax.all_to_all(maps, 'y', 0, 0, tiled=True)  9.7 us
    ppermute x3, waiting for transfers between devices, per_device(): of_high.append(lax.ppermute(high, ('zh', 'y', 'c'), onward(d)))  9.56 us
  transfers between devices with their start and end apart: 10, of which 6 were waited for; matrix products, arithmetic and copies ran while one was open for 2% of the time, Pallas kernels for 2%

profile of v4, /device:TPU:1, one launch (start us, length us, event | category | flops | bytes accessed | tf_op | source)
XLA Modules:
  0.0 164.2 jit_solution(9603437473418057578)
XLA Ops:
  0.0 5.6 %collective-permute-start.1 = (bf16[32,2048]{1,0:T(8,128)(2,1)}, bf16[32,2048]{1,0:T(8,128)(2,1)S(1)}, u32[]{:S(2)}, u32[]{:S(2)}) collective-permute-start(bf16[32,2048]{1,0:T(8,128)(2,1)} %lat.1), channel_id=1, source_target_pairs={{0,4},{2,6},{4,0},{6,2},{1,5},{3,7},{5,1},{7,3},{8,12},{10,14},{12... | collective-permute-start | bytes 393224 | tf_op jit(solution)/shard_map/ppermute | solution.py:379
  5.6 2.2 %collective-permute-start = (bf16[32,2048]{1,0:T(8,128)(2,1)}, bf16[32,2048]{1,0:T(8,128)(2,1)S(1)}, u32[]{:S(2)}, u32[]{:S(2)}) collective-permute-start(bf16[32,2048]{1,0:T(8,128)(2,1)} %lat.1), channel_id=1, source_target_pairs={{0,2},{2,4},{4,6},{6,0},{1,3},{3,5},{5,7},{7,1},{8,10},{10,12},{12... | collective-permute-start | bytes 393224 | tf_op jit(solution)/shard_map/ppermute | solution.py:379
  7.8 4.3 %collective-permute-start.2 = (bf16[32,2048]{1,0:T(8,128)(2,1)}, bf16[32,2048]{1,0:T(8,128)(2,1)S(1)}, u32[]{:S(2)}, u32[]{:S(2)}) collective-permute-start(bf16[32,2048]{1,0:T(8,128)(2,1)} %lat.1), channel_id=1, source_target_pairs={{0,6},{2,0},{4,2},{6,4},{1,7},{3,1},{5,3},{7,5},{8,14},{10,8},{12,... | collective-permute-start | bytes 393224 | tf_op jit(solution)/shard_map/ppermute | solution.py:379
  12.1 0.8 divide_multiply_fusion
  12.9 0.1 multiply_reduce_fusion
  13.0 0.1 fusion
  13.1 0.7 broadcast_in_dim.7
  13.8 15.1 %all-to-all-start.1 = ((f32[16,5,256]{2,1,0:T(8,128)}), f32[16,5,256]{2,1,0:T(8,128)S(1)}, u32[]{:S(2)}, u32[]{:S(2)}) async-start(f32[16,5,256]{2,1,0:T(8,128)} %broadcast_in_dim.7), calls=%async_computation.1 | async-start | bytes 262144 | tf_op jit(solution)/shard_map/all_to_all | solution.py:337
  28.9 0.0 collective-permute-done.1
  28.9 0.0 collective-permute-done
  28.9 0.0 collective-permute-done.2
  28.9 0.0 copy-done.1
  28.9 0.0 copy-start.2
  28.9 0.0 copy-start.3
  28.9 0.1 pad_maximum_fusion.one
  29.0 3.8 %collective-permute-start.3 = (bf16[4,32,2048]{2,1,0:T(8,128)(2,1)S(1)}, bf16[4,32,2048]{2,1,0:T(8,128)(2,1)}, u32[]{:S(2)}, u32[]{:S(2)}) collective-permute-start(bf16[4,32,2048]{2,1,0:T(8,128)(2,1)S(1)} %pad_maximum_fusion.one), channel_id=1, source_target_pairs={{0,1},{1,0},{2,3},{3,2},{4,5},{5,4},{6,7},{7,6},{8,9},{9,8},{10,11... | collective-permute-start | bytes 1572872 | tf_op jit(solution)/shard_map/ppermute | solution.py:381
  32.8 8.0 %all-to-all-done.1 = f32[16,5,256]{2,1,0:T(8,128)S(1)} async-done(((f32[16,5,256]{2,1,0:T(8,128)}), f32[16,5,256]{2,1,0:T(8,128)S(1)}, u32[]{:S(2)}, u32[]{:S(2)}) %all-to-all-start.1) | async-done | bytes 81952 | tf_op jit(solution)/shard_map/all_to_all | solution.py:337
  40.8 0.6 broadcast_in_dim.6
  41.5 5.2 %all-to-all-start = ((bf16[4,4,2048]{2,1,0:T(4,128)(2,1)}), bf16[4,4,2048]{2,1,0:T(4,128)(2,1)S(1)}, u32[]{:S(2)}, u32[]{:S(2)}) async-start(bf16[4,4,2048]{2,1,0:T(4,128)(2,1)} %broadcast_in_dim.6), calls=%async_computation | async-start | bytes 131072 | tf_op jit(solution)/shard_map/all_to_all | solution.py:337
  46.6 0.0 copy-done.7
  46.7 11.7 %all-to-all-done.ctx = bf16[4,4,2048]{2,1,0:T(4,128)(2,1)S(1)} async-done(((bf16[4,4,2048]{2,1,0:T(4,128)(2,1)}), bf16[4,4,2048]{2,1,0:T(4,128)(2,1)S(1)}, u32[]{:S(2)}, u32[]{:S(2)}) %all-to-all-start) | async-done | bytes 65568 | tf_op jit(solution)/shard_map/all_to_all | solution.py:337
  58.4 0.7 broadcast_in_dim.8
  59.1 9.1 %all-to-all-start.2 = ((f32[32,5,256]{2,1,0:T(8,128)}), f32[32,5,256]{2,1,0:T(8,128)S(1)}, u32[]{:S(2)}, u32[]{:S(2)}) async-start(f32[32,5,256]{2,1,0:T(8,128)} %broadcast_in_dim.8), calls=%async_computation.2 | async-start | bytes 524288 | tf_op jit(solution)/shard_map/all_to_all | solution.py:337
  68.2 0.0 copy-start.4
  68.3 0.1 stack.74.pos
  68.4 0.7 copy-done.9
  69.0 8.1 %all-to-all-done.2.fac = f32[32,5,256]{2,1,0:T(8,128)S(1)} async-done(((f32[32,5,256]{2,1,0:T(8,128)}), f32[32,5,256]{2,1,0:T(8,128)S(1)}, u32[]{:S(2)}, u32[]{:S(2)}) %all-to-all-start.2) | async-done | bytes 163872 | tf_op jit(solution)/shard_map/all_to_all | solution.py:337
  77.1 0.0 collective-permute-done.3.two
  77.1 0.0 copy-done.4
  77.1 10.4 %shard_map.154 = (bf16[4,160,256]{2,1,0:T(8,128)(2,1)S(1)}, bf16[2,256,256]{2,1,0:T(8,128)(2,1)S(1)}, f32[256,256]{1,0:T(8,128)S(1)}) custom-call(s32[8]{0:T(128)S(1)} %stack.74.pos, bf16[4,32,2048]{2,1,0:T(8,128)(2,1)S(1)} %pad_maximum_fusion.one, bf16[4,32,2048]{2,1,0:T(8,128)(2,1)} %collective-permute-done.3.two, ...), custom_call_target="tpu_custom_call" | custom-call | flops 5000000000 | bytes 1 | tf_op jit(solution)/shard_map/pallas_call | solution.py:403
  87.5 9.7 %all_to_all.35.maps.own = bf16[4,160,256]{2,1,0:T(8,128)(2,1)S(1)} all-to-all(bf16[4,160,256]{2,1,0:T(8,128)(2,1)S(1)} %get-tuple-element.8), channel_id=1, replica_groups=mesh['zh'=4,'zl'=4,'y'=4,'x'=4,'c'=2] {'y'}, dimensions={0} | all-to-all | bytes 655360 | tf_op jit(solution)/shard_map/all_to_all | solution.py:431
  97.2 1.1 shard_map.155
  98.3 14.3 %all_to_all.36.low.maps = bf16[4,208,256]{2,1,0:T(8,128)(2,1)S(1)} all-to-all(bf16[4,208,256]{2,1,0:T(8,128)(2,1)S(1)} %shard_map.155), channel_id=1, replica_groups=mesh['zh'=4,'zl'=4,'y'=4,'x'=4,'c'=2] {'zl'}, dimensions={0} | all-to-all | bytes 851968 | tf_op jit(solution)/shard_map/all_to_all | solution.py:433
  112.6 1.1 shard_map.157
  113.7 1.3 collective-permute-start.6
  115.0 1.3 collective-permute-start.5
  116.3 1.5 collective-permute-start.4
  117.8 3.9 %shard_map.156.start = f32[128,128]{1,0:T(8,128)S(1)} custom-call(s32[8]{0:T(128)S(1)} %stack.74.pos, bf16[4,208,256]{2,1,0:T(8,128)(2,1)S(1)} %all_to_all.36.low.maps, f32[4,128]{1,0:T(4,128)S(1)} %pad_maximum_fusion.2.small.gain), custom_call_target="tpu_custom_call" | custom-call | flops 1000000000 | bytes 1 | tf_op jit(solution)/shard_map/pallas_call | solution.py:438
  121.7 0.0 copy-start
  121.7 1.7 %collective-permute-done.6.near = bf16[128,256]{1,0:T(8,128)(2,1)S(1)} collective-permute-done((bf16[128,256]{1,0:T(8,128)(2,1)S(1)}, bf16[128,256]{1,0:T(8,128)(2,1)S(1)}, u32[]{:S(2)}, u32[]{:S(2)}) %collective-permute-start.6) | collective-permute-done | bytes 65568 | tf_op jit(solution)/shard_map/ppermute | solution.py:437
  123.4 5.4 %collective-permute-done.5.middle = bf16[128,256]{1,0:T(8,128)(2,1)S(1)} collective-permute-done((bf16[128,256]{1,0:T(8,128)(2,1)S(1)}, bf16[128,256]{1,0:T(8,128)(2,1)S(1)}, u32[]{:S(2)}, u32[]{:S(2)}) %collective-permute-start.5) | collective-permute-done | bytes 65568 | tf_op jit(solution)/shard_map/ppermute | solution.py:437
  128.9 2.4 %collective-permute-done.4.far = bf16[128,256]{1,0:T(8,128)(2,1)S(1)} collective-permute-done((bf16[128,256]{1,0:T(8,128)(2,1)S(1)}, bf16[128,256]{1,0:T(8,128)(2,1)S(1)}, u32[]{:S(2)}, u32[]{:S(2)}) %collective-permute-start.4) | collective-permute-done | bytes 65568 | tf_op jit(solution)/shard_map/ppermute | solution.py:437
  131.3 1.9 %shard_map.158 = bf16[4,128,128]{2,1,0:T(8,128)(2,1)S(1)} custom-call(s32[8]{0:T(128)S(1)} %stack.74.pos, f32[128,128]{1,0:T(8,128)S(1)} %shard_map.156.start, bf16[128,256]{1,0:T(8,128)(2,1)S(1)} %collective-permute-done.4.far, bf16[128,256]{1,0:T(8,128)(2,1)S(1)} %collective-permute-done.5.middle, bf16[128,256]{1,0:T(8,128)(2,1)S(1)} %collective-permute-done.6.near, ...), custom_call_target="tpu_custom_call" | custom-call | flops 100000000 | bytes 1 | tf_op jit(solution)/shard_map/pallas_call | solution.py:441
  133.2 7.2 %all_to_all.37.states = bf16[4,128,128]{2,1,0:T(8,128)(2,1)S(1)} all-to-all(bf16[4,128,128]{2,1,0:T(8,128)(2,1)S(1)} %shard_map.158), channel_id=1, replica_groups=mesh['zh'=4,'zl'=4,'y'=4,'x'=4,'c'=2] {'y'}, dimensions={0} | all-to-all | bytes 262144 | tf_op jit(solution)/shard_map/all_to_all | solution.py:444
  140.4 0.0 copy-done
  140.4 1.3 shard_map.159
  141.7 21.6 %all_to_all.38.rows = bf16[8,32,2048]{2,1,0:T(8,128)(2,1)S(1)} all-to-all(bf16[8,32,2048]{2,1,0:T(8,128)(2,1)S(1)} %shard_map.159), channel_id=1, replica_groups=mesh['zh'=4,'zl'=4,'y'=4,'x'=4,'c'=2] {'x','c'}, dimensions={0} | all-to-all | bytes 2097152 | tf_op jit(solution)/shard_map/all_to_all | solution.py:448
  163.3 0.8 shard_map.160
  (20 shorter events, 0.1 us)
Async XLA Ops:
  0.0 12.9 %copy-start.5 = (bf16[3,32,256]{2,1,0:T(8,128)(2,1)S(1)}, bf16[3,32,256]{2,1,0:T(8,128)(2,1)}, u32[]{:S(2)}) copy-start(bf16[3,32,256]{2,1,0:T(8,128)(2,1)} %param.20) | copy-start | bytes 147460
  0.0 28.9 %collective-permute-start.1 = (bf16[32,2048]{1,0:T(8,128)(2,1)}, bf16[32,2048]{1,0:T(8,128)(2,1)S(1)}, u32[]{:S(2)}, u32[]{:S(2)}) collective-permute-start(bf16[32,2048]{1,0:T(8,128)(2,1)} %lat.1), channel_id=1, source_target_pairs={{0,4},{2,6},{4,0},{6,2},{1,5},{3,7},{5,1},{7,3},{8,12},{10,14},{12... | collective-permute-start | bytes 393224 | tf_op jit(solution)/shard_map/ppermute | solution.py:379
  5.6 23.3 %collective-permute-start = (bf16[32,2048]{1,0:T(8,128)(2,1)}, bf16[32,2048]{1,0:T(8,128)(2,1)S(1)}, u32[]{:S(2)}, u32[]{:S(2)}) collective-permute-start(bf16[32,2048]{1,0:T(8,128)(2,1)} %lat.1), channel_id=1, source_target_pairs={{0,2},{2,4},{4,6},{6,0},{1,3},{3,5},{5,7},{7,1},{8,10},{10,12},{12... | collective-permute-start | bytes 393224 | tf_op jit(solution)/shard_map/ppermute | solution.py:379
  7.8 21.0 %collective-permute-start.2 = (bf16[32,2048]{1,0:T(8,128)(2,1)}, bf16[32,2048]{1,0:T(8,128)(2,1)S(1)}, u32[]{:S(2)}, u32[]{:S(2)}) collective-permute-start(bf16[32,2048]{1,0:T(8,128)(2,1)} %lat.1), channel_id=1, source_target_pairs={{0,6},{2,0},{4,2},{6,4},{1,7},{3,1},{5,3},{7,5},{8,14},{10,8},{12,... | collective-permute-start | bytes 393224 | tf_op jit(solution)/shard_map/ppermute | solution.py:379
  13.8 15.1 %copy-start.1 = (bf16[32,2048]{1,0:T(8,128)(2,1)S(1)}, bf16[32,2048]{1,0:T(8,128)(2,1)}, u32[]{:S(2)}) copy-start(bf16[32,2048]{1,0:T(8,128)(2,1)} %lat.1) | copy-start | bytes 393220
  13.8 27.0 %copy-start.6 = (bf16[4,2048]{1,0:T(4,128)(2,1)S(1)}, bf16[4,2048]{1,0:T(4,128)(2,1)}, u32[]{:S(2)}) copy-start(bf16[4,2048]{1,0:T(4,128)(2,1)} %param.18) | copy-start | bytes 49156
  13.8 32.9 %copy-start.7 = (f32[32]{0:T(128)S(1)}, f32[32]{0:T(128)}, u32[]{:S(2)}) copy-start(f32[32]{0:T(128)} %param.28) | copy-start | bytes 388
  13.8 32.9 %copy-start.8 = (f32[32]{0:T(128)S(1)}, f32[32]{0:T(128)}, u32[]{:S(2)}) copy-start(f32[32]{0:T(128)} %param.27) | copy-start | bytes 388
  13.8 27.0 %all-to-all-start.1 = ((f32[16,5,256]{2,1,0:T(8,128)}), f32[16,5,256]{2,1,0:T(8,128)S(1)}, u32[]{:S(2)}, u32[]{:S(2)}) async-start(f32[16,5,256]{2,1,0:T(8,128)} %broadcast_in_dim.7), calls=%async_computation.1 | async-start | bytes 262144 | tf_op jit(solution)/shard_map/all_to_all | solution.py:337
  28.9 48.2 %copy-start.2 = (bf16[2048,256]{1,0:T(8,128)(2,1)S(1)}, bf16[2048,256]{1,0:T(8,128)(2,1)}, u32[]{:S(2)}) copy-start(bf16[2048,256]{1,0:T(8,128)(2,1)} %wq.1) | copy-start | bytes 3145732
  28.9 48.2 %copy-start.3 = (bf16[2048,256]{1,0:T(8,128)(2,1)S(1)}, bf16[2048,256]{1,0:T(8,128)(2,1)}, u32[]{:S(2)}) copy-start(bf16[2048,256]{1,0:T(8,128)(2,1)} %wk.1) | copy-start | bytes 3145732
  29.0 48.1 %collective-permute-start.3 = (bf16[4,32,2048]{2,1,0:T(8,128)(2,1)S(1)}, bf16[4,32,2048]{2,1,0:T(8,128)(2,1)}, u32[]{:S(2)}, u32[]{:S(2)}) collective-permute-start(bf16[4,32,2048]{2,1,0:T(8,128)(2,1)S(1)} %pad_maximum_fusion.one), channel_id=1, source_target_pairs={{0,1},{1,0},{2,3},{3,2},{4,5},{5,4},{6,7},{7,6},{8,9},{9,8},{10,11... | collective-permute-start | bytes 1572872 | tf_op jit(solution)/shard_map/ppermute | solution.py:381
  41.5 16.9 %all-to-all-start = ((bf16[4,4,2048]{2,1,0:T(4,128)(2,1)}), bf16[4,4,2048]{2,1,0:T(4,128)(2,1)S(1)}, u32[]{:S(2)}, u32[]{:S(2)}) async-start(bf16[4,4,2048]{2,1,0:T(4,128)(2,1)} %broadcast_in_dim.6), calls=%async_computation | async-start | bytes 131072 | tf_op jit(solution)/shard_map/all_to_all | solution.py:337
  59.1 9.1 %copy-start.10 = (f32[32]{0:T(128)S(1)}, f32[32]{0:T(128)}, u32[]{:S(2)}) copy-start(f32[32]{0:T(128)} %param.26) | copy-start | bytes 388
  59.1 17.9 %all-to-all-start.2 = ((f32[32,5,256]{2,1,0:T(8,128)}), f32[32,5,256]{2,1,0:T(8,128)S(1)}, u32[]{:S(2)}, u32[]{:S(2)}) async-start(f32[32,5,256]{2,1,0:T(8,128)} %broadcast_in_dim.8), calls=%async_computation.2 | async-start | bytes 524288 | tf_op jit(solution)/shard_map/all_to_all | solution.py:337
  68.2 8.8 %copy-start.4 = (f32[256,32]{0,1:T(8,128)S(1)}, f32[256,32]{0,1:T(8,128)}, u32[]{:S(2)}) copy-start(f32[256,32]{0,1:T(8,128)} %param.29) | copy-start | bytes 98308
  68.4 0.7 copy-start.9
  113.7 9.7 %collective-permute-start.6 = (bf16[128,256]{1,0:T(8,128)(2,1)S(1)}, bf16[128,256]{1,0:T(8,128)(2,1)S(1)}, u32[]{:S(2)}, u32[]{:S(2)}) collective-permute-start(bf16[128,256]{1,0:T(8,128)(2,1)S(1)} %shard_map.157), channel_id=1, source_target_pairs={{0,128},{9,137},{16,144},{25,153},{128,256},{129,1},{136,8},{137,2... | collective-permute-start | bytes 196616 | tf_op jit(solution)/shard_map/ppermute | solution.py:437
  115.0 13.8 %collective-permute-start.5 = (bf16[128,256]{1,0:T(8,128)(2,1)S(1)}, bf16[128,256]{1,0:T(8,128)(2,1)S(1)}, u32[]{:S(2)}, u32[]{:S(2)}) collective-permute-start(bf16[128,256]{1,0:T(8,128)(2,1)S(1)} %shard_map.157), channel_id=1, source_target_pairs={{0,256},{9,265},{16,272},{25,281},{128,384},{137,393},{144,400},{1... | collective-permute-start | bytes 196616 | tf_op jit(solution)/shard_map/ppermute | solution.py:437
  116.3 14.9 %collective-permute-start.4 = (bf16[128,256]{1,0:T(8,128)(2,1)S(1)}, bf16[128,256]{1,0:T(8,128)(2,1)S(1)}, u32[]{:S(2)}, u32[]{:S(2)}) collective-permute-start(bf16[128,256]{1,0:T(8,128)(2,1)S(1)} %shard_map.157), channel_id=1, source_target_pairs={{0,384},{9,393},{16,400},{25,409},{385,1},{392,8},{401,17},{408,24... | collective-permute-start | bytes 196616 | tf_op jit(solution)/shard_map/ppermute | solution.py:437
  121.7 18.7 %copy-start = (bf16[256,2048]{1,0:T(8,128)(2,1)S(1)}, bf16[256,2048]{1,0:T(8,128)(2,1)}, u32[]{:S(2)}) copy-start(bf16[256,2048]{1,0:T(8,128)(2,1)} %weight.1) | copy-start | bytes 3145732

commit v5 on v3

--- a/solution.py
+++ b/solution.py
@@ -74,48 +74,36 @@
     return out
 
 
-def project_kernel(
-    pos, one, two, fac, wq, wk, wv_h, wd_h, ww_h, ctx_h,
-    p_o, c_o,
-    hid, wv, wd, ww, ctx, sems,
-):
+def start_copies(sources, targets, sems):
     copies = [
         pltpu.make_async_copy(source, target, sems.at[i])
-        for i, (source, target) in enumerate(((ctx_h, ctx), (wv_h, wv), (wd_h, wd), (ww_h, ww)))
+        for i, (source, target) in enumerate(zip(sources, targets))
     ]
     for copy in copies:
         copy.start()
-    factors = [[], [], [], []]
-    for t in range(8):
-        f = (fac[t] + fac[8 + t]) + (fac[16 + t] + fac[24 + t])
-        for slot, r in enumerate((0, 1, 3, 4)):
-            factors[slot].append(f[r : r + 1])
-    shift, scale, c_shift, c_scale = (jnp.concatenate(f, axis=1) for f in factors)
-    for x in range(4):
-        for i, lat in enumerate((one, two)):
-            core = pos[6] if i == 0 else 1 - pos[6]
-            spot = (2 * x + core) * 32
-            hid[pl.ds(pl.multiple_of(spot, 32), 32)] = norm_rows(lat[x], scale, shift)
-    copies[0].wait()
-    hid[256:260] = norm_rows(ctx[...], c_scale, c_shift)
-    hid[260:272] = jnp.zeros((12, D), BF)
+    return copies
+
+
+def factor(fac, r):
+    parts = [(fac[t] + fac[8 + t]) + (fac[16 + t] + fac[24 + t]) for t in range(8)]
+    return jnp.concatenate([f[r : r + 1] for f in parts], axis=1)
+
+
+def rows_kernel(pos, ctx, fac, wk, wv_h, wd_h, ww_h, c_o, hid, wv, wd, ww, sems):
+    copies = start_copies((wv_h, wd_h, ww_h), (wv, wd, ww), sems)
+    hid[0:4] = norm_rows(ctx[...], factor(fac, 4), factor(fac, 3))
+    hid[4:16] = jnp.zeros((12, D), BF)
     rows = hid[...]
-    p_o[0:256] = mm(hid[0:256], wq[...]).astype(BF)
     keys = mm(rows, wk[...]).astype(BF)
-    p_o[256:512] = keys[:256]
-    for copy in copies[1:]:
+    for copy in copies:
         copy.wait()
     values = mm(rows, wv[...]).astype(BF)
-    p_o[512:768] = values[:256]
-    last_two = ((1,), (1,))
-    p_o[768:800] = mm(wd[...], hid[0:256], last_two).astype(BF)
-    p_o[800:832] = mm(ww[...], hid[0:256], last_two).astype(BF)
-    rate = mm(hid[256:264], wd[...], last_two).astype(BF).astype(F32)
-    write = mm(hid[256:264], ww[...], last_two).astype(BF).astype(F32)
-    lanes = lax.broadcasted_iota(jnp.int32, (8, 256), 1)
-    rank = lax.broadcasted_iota(jnp.int32, (8, 256), 0)
+    rate = mm(rows, wd[...], ((1,), (1,))).astype(BF).astype(F32)
+    write = mm(rows, ww[...], ((1,), (1,))).astype(BF).astype(F32)
+    lanes = lax.broadcasted_iota(jnp.int32, (16, 256), 1)
+    rank = lax.broadcasted_iota(jnp.int32, (16, 256), 0)
     spots = (lanes == rank + pos[5]) & (rank < 4)
-    wide = [rows_of[256:264].astype(F32)[0:4] for rows_of in (keys, values)]
+    wide = [side.astype(F32)[0:4] for side in (keys, values)]
     pieces = [jnp.concatenate(wide, axis=1)]
     for j in range(4):
         lane = pos[1] * 4 + j
@@ -129,7 +117,30 @@
         c_o[i] = out
 
 
-def chunk_kernel(pos, packed, spike, small, m_o, r_o, o_o):
+def front_kernel(
+    pos, one, two, fac, wq, wk, spike, small, wv_h, wd_h, ww_h,
+    m_o, r_o, o_o,
+    hid, packed, wv, wd, ww, sems,
+):
+    copies = start_copies((wv_h, wd_h, ww_h), (wv, wd, ww), sems)
+    shift, scale = (factor(fac, 0), factor(fac, 1))
+    for d in range(4):
+        for i, lat in enumerate((one, two)):
+            core = pos[6] if i == 0 else 1 - pos[6]
+            spot = (2 * ((pos[7] + 4 - d) % 4) + core) * 32
+            hid[pl.ds(pl.multiple_of(spot, 32), 32)] = norm_rows(lat[d], scale, shift)
+    rows = hid[...]
+    packed[0:256] = mm(rows, wq[...]).astype(BF)
+    packed[256:512] = mm(rows, wk[...]).astype(BF)
+    for copy in copies:
+        copy.wait()
+    packed[512:768] = mm(rows, wv[...]).astype(BF)
+    packed[768:800] = mm(wd[...], rows, ((1,), (1,))).astype(BF)
+    packed[800:832] = mm(ww[...], rows, ((1,), (1,))).astype(BF)
+    chunk(pos, packed, spike, small, m_o, r_o, o_o)
+
+
+def chunk(pos, packed, spike, small, m_o, r_o, o_o):
     row = lax.broadcasted_iota(jnp.int32, (256, 256), 0)
     col = lax.broadcasted_iota(jnp.int32, (256, 256), 1)
     eye = row == col
@@ -195,7 +206,6 @@
         h, e = divmod(j, 2)
         r_o[h, :, 128 * e : 128 * e + 128] = (grown_q - read[:, 128:]).astype(BF)
         outs[h] = read[:, :128] if e == 0 else outs[h] + read[:, :128]
-    m_o[:, 128:160] = jnp.zeros((4, 32, 256), BF)
     o_o[:, 0:128] = outs[0]
     o_o[:, 128:256] = outs[1]
 
@@ -304,7 +314,7 @@
         at = at + step
 
 
-def read_kernel(pos, states, reads, base, gain, weight, o):
+def read_kernel(pos, states, reads, base, gain, weight, keep, give):
     heads = []
     for h in range(2):
         first = states[(2 * h + pos[4]) % 4]
@@ -315,20 +325,30 @@
         mean = jnp.mean(total * total, axis=1, keepdims=True)
         heads.append((total * lax.rsqrt(mean + EPS) * gain[3:4]).astype(BF))
     branch = mm(jnp.concatenate(heads, axis=1), weight[...]).astype(BF)
-    for t in range(8):
-        o[t] = branch[32 * t : 32 * t + 32]
+
+    def split(even, odd):
+        for i in range(4):
+            even[i] = branch[64 * i : 64 * i + 32]
+            odd[i] = branch[64 * i + 32 : 64 * i + 64]
+
+    @pl.when(pos[6] == 0)
+    def _():
+        split(keep, give)
+
+    @pl.when(pos[6] != 0)
+    def _():
+        split(give, keep)
+
+
+def merge_kernel(keep, got, o):
+    o[...] = (keep[...].astype(F32) + got[...].astype(F32)).astype(BF)
 
 
 def output_kernel(rows, fac, lat, o):
-    branch = rows[0].astype(F32)
-    for i in range(1, 8):
-        branch = branch + rows[i].astype(F32)
-    gates = []
-    for t in range(8):
-        f = (fac[t] + fac[8 + t]) + (fac[16 + t] + fac[24 + t])
-        gates.append(f[2:3])
-    gate = jnp.concatenate(gates, axis=1)
-    o[...] = (lat[...].astype(F32) + gate * branch).astype(BF)
+    branch = (rows[0].astype(F32) + rows[1].astype(F32)) + (
+        rows[2].astype(F32) + rows[3].astype(F32)
+    )
+    o[...] = (lat[...].astype(F32) + factor(fac, 2) * branch).astype(BF)
 
 
 def call(kernel, outs, specs, scratch=(), flops=1, aliases=None):
@@ -388,7 +408,10 @@
     sp_index = lax.axis_index(SP)
     pos = jnp.stack([(y + c) % 4, x * 2 + c, zh, zl, (4 - c) % 4, sp_index * 4, c, x])
     pos = pos.astype(jnp.int32)
-    mine = to_all(latent, "x", 4)
+    parts = [latent]
+    for d in range(1, 4):
+        parts.append(lax.ppermute(latent, "x", [(i, (i + d) % 4) for i in range(4)]))
+    mine = jnp.stack(parts)
     other = lax.ppermute(mine, "c", [(0, 1), (1, 0)])
     signals = jnp.stack([condition, context_condition_vector])
     signals = lax.dynamic_slice_in_dim(jax.nn.silu(signals), sp_index * 32, 32, 1)
@@ -411,19 +434,30 @@
             head_norm_gain,
         ]
     )
-    packed, rows = call(
-        project_kernel,
-        [((832, 256), BF), ((4, 8, 512), BF)],
-        [SM] + [VM] * 5 + [HB] * 4,
-        [
-            pltpu.VMEM((272, D), BF),
-            pltpu.VMEM((D, 256), BF),
-            pltpu.VMEM((32, D), BF),
-            pltpu.VMEM((32, D), BF),
-            pltpu.VMEM((4, D), BF),
-            pltpu.SemaphoreType.DMA((4,)),
-        ],
-        flops=10**9,
+    slow = [
+        pltpu.with_memory_space_constraint(a, pltpu.HBM)
+        for a in (value_matrix, decay_input_weight.T, write_strength_weight.T)
+    ]
+    room = [
+        pltpu.VMEM((D, 256), BF),
+        pltpu.VMEM((32, D), BF),
+        pltpu.VMEM((32, D), BF),
+        pltpu.SemaphoreType.DMA((3,)),
+    ]
+    rows = call(
+        rows_kernel,
+        ((4, 8, 512), BF),
+        [SM] + [VM] * 3 + [HB] * 3,
+        [pltpu.VMEM((16, D), BF), *room],
+        flops=10**8,
+    )(pos, context, fac, key_matrix, *slow)
+    rows = lax.all_to_all(rows, "zh", 0, 0, tiled=True)
+    maps, reads, base = call(
+        front_kernel,
+        [((4, 160, 256), BF), ((2, 256, 256), BF), ((256, 256), F32)],
+        [SM] + [VM] * 7 + [HB] * 3,
+        [pltpu.VMEM((256, D), BF), pltpu.VMEM((832, 256), BF), *room],
+        flops=5 * 10**9,
     )(
         pos,
         mine,
@@ -431,28 +465,9 @@
         fac,
         query_matrix,
         key_matrix,
-        *(
-            pltpu.with_memory_space_constraint(a, pltpu.HBM)
-            for a in (
-                value_matrix,
-                decay_input_weight.T,
-                write_strength_weight.T,
-                context,
-            )
-        ),
-    )
-    packed = pltpu.with_memory_space_constraint(packed, pltpu.HBM)
-    rows = lax.all_to_all(rows, "zh", 0, 0, tiled=True)
-    maps, reads, base = call(
-        chunk_kernel,
-        [((4, 160, 256), BF), ((2, 256, 256), BF), ((256, 256), F32)],
-        [SM] + [VM] * 3,
-        flops=4 * 10**9,
-    )(
-        pos,
-        packed,
         log_spike_added.T,
         small,
+        *slow,
     )
     maps = call(pack_kernel, ((4, 160, 256), BF), [SM, VM, VM], aliases={1: 0})(
         pos, maps, rows
@@ -471,10 +486,12 @@
         pos, start, *of_high, of_low, of_y
     )
     states = lax.all_to_all(states, "y", 0, 0, tiled=True)
-    branch = call(read_kernel, ((8, 32, D), BF), [SM] + [VM] * 5, flops=10**8)(
-        pos, states, reads, base, small, output_matrix
-    )
-    branch = lax.all_to_all(branch, TP, 0, 0, tiled=True)
+    keep, give = call(
+        read_kernel, [((4, 32, D), BF)] * 2, [SM] + [VM] * 5, flops=10**8
+    )(pos, states, reads, base, small, output_matrix)
+    got = lax.ppermute(give, "c", [(0, 1), (1, 0)])
+    branch = call(merge_kernel, ((4, 32, D), BF), [VM] * 2)(keep, got)
+    branch = lax.all_to_all(branch, "x", 0, 0, tiled=True)
     return call(output_kernel, ((32, D), BF), [VM] * 3, flops=10**8)(branch, fac, latent)
 
 

time: 160 us -> 155 us (0.969)
  waiting for transfers between devices: 36.9 us -> 25.4 us
  starting transfers between devices: 42.3 us -> 53.5 us
  blocking collectives: 52.6 us -> 46.6 us
  Pallas kernels: 21.8 us -> 23.6 us
    ppermute x0 -> x4, starting transfers between devices: none -> 16.9 us  [the longest x3 10.9 us: per_device(): lax.ppermute(latent, 'x', [(i, (i + d) % 4) for i in range(4)])]
    all_to_all x1, blocking collectives: 22.8 us -> 11.5 us  [per_device(): branch = lax.all_to_all(branch, 'x', 0, 0, tiled=True)]
    all_to_all x3 -> x2, waiting for transfers between devices: 22.3 us -> 16 us  [to_all(): lax.all_to_all(jnp.broadcast_to(value[None], (count, *value.shape)), axes...]
    all_to_all x1, blocking collectives: 7.21 us -> 12.4 us  [per_device(): states = lax.all_to_all(states, 'y', 0, 0, tiled=True)]
    all_to_all x3 -> x2, starting transfers between devices: 30.5 us -> 25.5 us  [to_all(): lax.all_to_all(jnp.broadcast_to(value[None], (count, *value.shape)), axes...]
    all_to_all x1, waiting for transfers between devices: 5.11 us -> 0.83 us  [per_device(): rows = lax.all_to_all(rows, 'zh', 0, 0, tiled=True)]
    ppermute x3, waiting for transfers between devices: 9.42 us -> 7.07 us  [per_device(): of_high.append(lax.ppermute(high, ('zh', 'y', 'c'), onward(d)))]
    pallas_call x3 -> x4, Pallas kernels: 12.5 us -> 14.3 us  [the longest x1 9.73 us: per_device(): call(front_kernel, [((4, 160, 256), BF), ((2, 256, 256), BF), ((256, 256)...]
  transfers between devices with their start and end apart: 8 -> 11, of which waited for: 7 -> 6; matrix products, arithmetic and copies ran while one was open for 1% -> 2% of each run, Pallas kernels for 7% -> 11%
where the time goes in v5:
time: 155 us; the launch traced here: 154 us
  starting transfers between devices  53.5 us (35%)
  blocking collectives  46.6 us (30%)
  waiting for transfers between devices  25.4 us (16%)
  Pallas kernels  23.6 us (15%)
  local copies, waits for them, and re-layouts  3.42 us (2%)
    all_to_all x2, starting transfers between devices, to_all(): lax.all_to_all(jnp.broadcast_to(value[None], (count, *value.shape)), axes...  25.5 us
    all_to_all x2, waiting for transfers between devices, to_all(): lax.all_to_all(jnp.broadcast_to(value[None], (count, *value.shape)), axes...  16 us
    all_to_all x1, blocking collectives, per_device(): of_low = lax.all_to_all(low, 'zl', 0, 0, tiled=True)  14.4 us
    all_to_all x1, blocking collectives, per_device(): states = lax.all_to_all(states, 'y', 0, 0, tiled=True)  12.4 us
    all_to_all x1, blocking collectives, per_device(): branch = lax.all_to_all(branch, 'x', 0, 0, tiled=True)  11.5 us
    ppermute x3, starting transfers between devices, per_device(): lax.ppermute(latent, 'x', [(i, (i + d) % 4) for i in range(4)])  10.9 us
    pallas_call x1, Pallas kernels, per_device(): call(front_kernel, [((4, 160, 256), BF), ((2, 256, 256), BF), ((256, 256)...  9.73 us
    all_to_all x1, blocking collectives, per_device(): of_y = lax.all_to_all(maps, 'y', 0, 0, tiled=True)  8.25 us
  transfers between devices with their start and end apart: 11, of which 6 were waited for; matrix products, arithmetic and copies ran while one was open for 2% of the time, Pallas kernels for 11%

profile of v5, /device:TPU:1, one launch (start us, length us, event | category | flops | bytes accessed | tf_op | source)
XLA Modules:
  0.0 154.0 jit_solution(16216178196567358627)
XLA Ops:
  0.0 5.6 %collective-permute-start.1 = (bf16[32,2048]{1,0:T(8,128)(2,1)}, bf16[32,2048]{1,0:T(8,128)(2,1)S(1)}, u32[]{:S(2)}, u32[]{:S(2)}) collective-permute-start(bf16[32,2048]{1,0:T(8,128)(2,1)} %lat.1), channel_id=1, source_target_pairs={{0,4},{2,6},{4,0},{6,2},{1,5},{3,7},{5,1},{7,3},{8,12},{10,14},{12... | collective-permute-start | bytes 393224 | tf_op jit(solution)/shard_map/ppermute | solution.py:413
  5.6 2.8 %collective-permute-start.2 = (bf16[32,2048]{1,0:T(8,128)(2,1)}, bf16[32,2048]{1,0:T(8,128)(2,1)S(1)}, u32[]{:S(2)}, u32[]{:S(2)}) collective-permute-start(bf16[32,2048]{1,0:T(8,128)(2,1)} %lat.1), channel_id=1, source_target_pairs={{0,6},{2,0},{4,2},{6,4},{1,7},{3,1},{5,3},{7,5},{8,14},{10,8},{12,... | collective-permute-start | bytes 393224 | tf_op jit(solution)/shard_map/ppermute | solution.py:413
  8.4 2.5 %collective-permute-start = (bf16[32,2048]{1,0:T(8,128)(2,1)}, bf16[32,2048]{1,0:T(8,128)(2,1)S(1)}, u32[]{:S(2)}, u32[]{:S(2)}) collective-permute-start(bf16[32,2048]{1,0:T(8,128)(2,1)} %lat.1), channel_id=1, source_target_pairs={{0,2},{2,4},{4,6},{6,0},{1,3},{3,5},{5,7},{7,1},{8,10},{10,12},{12... | collective-permute-start | bytes 393224 | tf_op jit(solution)/shard_map/ppermute | solution.py:413
  10.9 0.8 divide_multiply_fusion
  11.7 0.1 multiply_reduce_fusion
  11.8 0.1 fusion
  11.9 0.7 broadcast_in_dim.4
  12.6 15.0 %all-to-all-start = ((f32[16,5,256]{2,1,0:T(8,128)}), f32[16,5,256]{2,1,0:T(8,128)S(1)}, u32[]{:S(2)}, u32[]{:S(2)}) async-start(f32[16,5,256]{2,1,0:T(8,128)} %broadcast_in_dim.4), calls=%async_computation | async-start | bytes 262144 | tf_op jit(solution)/shard_map/all_to_all | solution.py:372
  27.6 0.0 copy-start
  27.6 0.0 collective-permute-done.1
  27.7 0.0 copy-start.7
  27.7 0.0 copy-start.8
  27.7 0.1 pad_maximum_fusion.one
  27.8 3.8 %collective-permute-start.3 = (bf16[4,32,2048]{2,1,0:T(8,128)(2,1)S(1)}, bf16[4,32,2048]{2,1,0:T(8,128)(2,1)S(1)}, u32[]{:S(2)}, u32[]{:S(2)}) collective-permute-start(bf16[4,32,2048]{2,1,0:T(8,128)(2,1)S(1)} %pad_maximum_fusion.one), channel_id=1, source_target_pairs={{0,1},{1,0},{2,3},{3,2},{4,5},{5,4},{6,7},{7,6},{8,9},{9,8},{10,11... | collective-permute-start | bytes 1572872 | tf_op jit(solution)/shard_map/ppermute | solution.py:415
  31.7 7.9 %all-to-all-done = f32[16,5,256]{2,1,0:T(8,128)S(1)} async-done(((f32[16,5,256]{2,1,0:T(8,128)}), f32[16,5,256]{2,1,0:T(8,128)S(1)}, u32[]{:S(2)}, u32[]{:S(2)}) %all-to-all-start) | async-done | bytes 81952 | tf_op jit(solution)/shard_map/all_to_all | solution.py:372
  39.6 0.7 broadcast_in_dim.5
  40.3 10.4 %all-to-all-start.1 = ((f32[32,5,256]{2,1,0:T(8,128)}), f32[32,5,256]{2,1,0:T(8,128)S(1)}, u32[]{:S(2)}, u32[]{:S(2)}) async-start(f32[32,5,256]{2,1,0:T(8,128)} %broadcast_in_dim.5), calls=%async_computation.1 | async-start | bytes 524288 | tf_op jit(solution)/shard_map/all_to_all | solution.py:372
  50.8 0.0 copy-start.3
  50.8 0.1 stack.74.pos
  50.9 0.7 copy-done.9
  51.6 8.1 %all-to-all-done.1.fac = f32[32,5,256]{2,1,0:T(8,128)S(1)} async-done(((f32[32,5,256]{2,1,0:T(8,128)}), f32[32,5,256]{2,1,0:T(8,128)S(1)}, u32[]{:S(2)}, u32[]{:S(2)}) %all-to-all-start.1) | async-done | bytes 163872 | tf_op jit(solution)/shard_map/all_to_all | solution.py:372
  59.7 3.1 %shard_map.155 = bf16[4,8,512]{2,1,0:T(8,128)(2,1)} custom-call(s32[8]{0:T(128)S(1)} %stack.74.pos, bf16[4,2048]{1,0:T(4,128)(2,1)S(1)} %copy-done.3, f32[32,5,256]{2,1,0:T(8,128)S(1)} %all-to-all-done.1.fac, bf16[2048,256]{1,0:T(8,128)(2,1)S(1)} %copy-done, bf16[2048,256]{1,0:T(8,128)(2,1)} %wv_h.3, bf16[32,2048]{1,0:T(8,128)(2,1)} %bitcast.30, ...), custom_call_target="tpu_custom_call" | custom-call | flops 100000000 | bytes 1 | tf_op jit(solution)/shard_map/pallas_call | solution.py:447
  62.8 0.0 copy-start.5
  62.8 3.3 %all-to-all-start.2 = ((bf16[4,8,512]{2,1,0:T(8,128)(2,1)}), bf16[4,8,512]{2,1,0:T(8,128)(2,1)S(1)}, u32[]{:S(2)}, u32[]{:S(2)}) async-start(bf16[4,8,512]{2,1,0:T(8,128)(2,1)} %shard_map.155), calls=%async_computation.2 | async-start | bytes 65536 | tf_op jit(solution)/shard_map/all_to_all | solution.py:454
  66.1 0.0 copy-start.4
  66.1 1.2 copy-done.4
  67.3 9.7 %shard_map.154 = (bf16[4,160,256]{2,1,0:T(8,128)(2,1)S(1)}, bf16[2,256,256]{2,1,0:T(8,128)(2,1)S(1)}, f32[256,256]{1,0:T(8,128)S(1)}) custom-call(s32[8]{0:T(128)S(1)} %stack.74.pos, bf16[4,32,2048]{2,1,0:T(8,128)(2,1)S(1)} %pad_maximum_fusion.one, bf16[4,32,2048]{2,1,0:T(8,128)(2,1)S(1)} %collective-permute-done.3.two, ...), custom_call_target="tpu_custom_call" | custom-call | flops 5000000000 | bytes 1 | tf_op jit(solution)/shard_map/pallas_call | solution.py:455
  77.1 0.8 all-to-all-done.2.rows
  77.9 0.6 shard_map.156
  78.5 8.3 %all_to_all.35.maps.own = bf16[4,160,256]{2,1,0:T(8,128)(2,1)S(1)} all-to-all(bf16[4,160,256]{2,1,0:T(8,128)(2,1)S(1)} %shard_map.156), channel_id=1, replica_groups=mesh['zh'=4,'zl'=4,'y'=4,'x'=4,'c'=2] {'y'}, dimensions={0} | all-to-all | bytes 655360 | tf_op jit(solution)/shard_map/all_to_all | solution.py:475
  86.7 1.1 shard_map.157
  87.8 14.4 %all_to_all.36.low.maps = bf16[4,208,256]{2,1,0:T(8,128)(2,1)S(1)} all-to-all(bf16[4,208,256]{2,1,0:T(8,128)(2,1)S(1)} %shard_map.157), channel_id=1, replica_groups=mesh['zh'=4,'zl'=4,'y'=4,'x'=4,'c'=2] {'zl'}, dimensions={0} | all-to-all | bytes 851968 | tf_op jit(solution)/shard_map/all_to_all | solution.py:477
  102.2 1.1 shard_map.159
  103.3 1.3 collective-permute-start.4
  104.6 1.3 collective-permute-start.5
  105.9 1.5 collective-permute-start.6
  107.4 3.9 %shard_map.158.start = f32[128,128]{1,0:T(8,128)S(1)} custom-call(s32[8]{0:T(128)S(1)} %stack.74.pos, bf16[4,208,256]{2,1,0:T(8,128)(2,1)S(1)} %all_to_all.36.low.maps, f32[4,128]{1,0:T(4,128)S(1)} %pad_maximum_fusion.2.small.gain), custom_call_target="tpu_custom_call" | custom-call | flops 1000000000 | bytes 1 | tf_op jit(solution)/shard_map/pallas_call | solution.py:482
  111.2 0.0 copy-start.1
  111.2 1.4 collective-permute-done.4.far
  112.7 5.6 %collective-permute-done.5.middle = bf16[128,256]{1,0:T(8,128)(2,1)S(1)} collective-permute-done((bf16[128,256]{1,0:T(8,128)(2,1)S(1)}, bf16[128,256]{1,0:T(8,128)(2,1)S(1)}, u32[]{:S(2)}, u32[]{:S(2)}) %collective-permute-start.5) | collective-permute-done | bytes 65568 | tf_op jit(solution)/shard_map/ppermute | solution.py:481
  118.3 1.9 %shard_map.160 = bf16[4,128,128]{2,1,0:T(8,128)(2,1)S(1)} custom-call(s32[8]{0:T(128)S(1)} %stack.74.pos, f32[128,128]{1,0:T(8,128)S(1)} %shard_map.158.start, bf16[128,256]{1,0:T(8,128)(2,1)S(1)} %collective-permute-done.4.far, bf16[128,256]{1,0:T(8,128)(2,1)S(1)} %collective-permute-done.5.middle, bf16[128,256]{1,0:T(8,128)(2,1)S(1)} %collective-permute-done.6.near, ...), custom_call_target="tpu_custom_call" | custom-call | flops 100000000 | bytes 1 | tf_op jit(solution)/shard_map/pallas_call | solution.py:485
  120.3 12.4 %all_to_all.37.states = bf16[4,128,128]{2,1,0:T(8,128)(2,1)S(1)} all-to-all(bf16[4,128,128]{2,1,0:T(8,128)(2,1)S(1)} %shard_map.160), channel_id=1, replica_groups=mesh['zh'=4,'zl'=4,'y'=4,'x'=4,'c'=2] {'y'}, dimensions={0} | all-to-all | bytes 262144 | tf_op jit(solution)/shard_map/all_to_all | solution.py:488
  132.7 1.3 shard_map.161
  134.1 6.0 %collective-permute-start.7 = (bf16[4,32,2048]{2,1,0:T(8,128)(2,1)S(1)}, bf16[4,32,2048]{2,1,0:T(8,128)(2,1)S(1)}, u32[]{:S(2)}, u32[]{:S(2)}) collective-permute-start(bf16[4,32,2048]{2,1,0:T(8,128)(2,1)S(1)} %get-tuple-element.14), channel_id=1, source_target_pairs={{0,1},{1,0},{2,3},{3,2},{4,5},{5,4},{6,7},{7,6},{8,9},{9,8},{10,11... | collective-permute-start | bytes 1572872 | tf_op jit(solution)/shard_map/ppermute | solution.py:492
  140.1 1.5 collective-permute-done.7.got
  141.6 0.1 shard_map.162
  141.7 11.5 %all_to_all.38.rows = bf16[4,32,2048]{2,1,0:T(8,128)(2,1)S(1)} all-to-all(bf16[4,32,2048]{2,1,0:T(8,128)(2,1)S(1)} %shard_map.162), channel_id=1, replica_groups=mesh['zh'=4,'zl'=4,'y'=4,'x'=4,'c'=2] {'x'}, dimensions={0} | all-to-all | bytes 1048576 | tf_op jit(solution)/shard_map/all_to_all | solution.py:494
  153.2 0.8 shard_map.163
  (24 shorter events, 0.1 us)
Async XLA Ops:
  0.0 11.7 %copy-start.6 = (bf16[3,32,256]{2,1,0:T(8,128)(2,1)S(1)}, bf16[3,32,256]{2,1,0:T(8,128)(2,1)}, u32[]{:S(2)}) copy-start(bf16[3,32,256]{2,1,0:T(8,128)(2,1)} %param.20) | copy-start | bytes 147460
  0.0 27.6 %collective-permute-start.1 = (bf16[32,2048]{1,0:T(8,128)(2,1)}, bf16[32,2048]{1,0:T(8,128)(2,1)S(1)}, u32[]{:S(2)}, u32[]{:S(2)}) collective-permute-start(bf16[32,2048]{1,0:T(8,128)(2,1)} %lat.1), channel_id=1, source_target_pairs={{0,4},{2,6},{4,0},{6,2},{1,5},{3,7},{5,1},{7,3},{8,12},{10,14},{12... | collective-permute-start | bytes 393224 | tf_op jit(solution)/shard_map/ppermute | solution.py:413
  5.6 22.0 %collective-permute-start.2 = (bf16[32,2048]{1,0:T(8,128)(2,1)}, bf16[32,2048]{1,0:T(8,128)(2,1)S(1)}, u32[]{:S(2)}, u32[]{:S(2)}) collective-permute-start(bf16[32,2048]{1,0:T(8,128)(2,1)} %lat.1), channel_id=1, source_target_pairs={{0,6},{2,0},{4,2},{6,4},{1,7},{3,1},{5,3},{7,5},{8,14},{10,8},{12,... | collective-permute-start | bytes 393224 | tf_op jit(solution)/shard_map/ppermute | solution.py:413
  8.4 19.3 %collective-permute-start = (bf16[32,2048]{1,0:T(8,128)(2,1)}, bf16[32,2048]{1,0:T(8,128)(2,1)S(1)}, u32[]{:S(2)}, u32[]{:S(2)}) collective-permute-start(bf16[32,2048]{1,0:T(8,128)(2,1)} %lat.1), channel_id=1, source_target_pairs={{0,2},{2,4},{4,6},{6,0},{1,3},{3,5},{5,7},{7,1},{8,10},{10,12},{12... | collective-permute-start | bytes 393224 | tf_op jit(solution)/shard_map/ppermute | solution.py:413
  12.6 15.1 %copy-start.2 = (bf16[32,2048]{1,0:T(8,128)(2,1)S(1)}, bf16[32,2048]{1,0:T(8,128)(2,1)}, u32[]{:S(2)}) copy-start(bf16[32,2048]{1,0:T(8,128)(2,1)} %lat.1) | copy-start | bytes 393220
  12.6 27.0 %all-to-all-start = ((f32[16,5,256]{2,1,0:T(8,128)}), f32[16,5,256]{2,1,0:T(8,128)S(1)}, u32[]{:S(2)}, u32[]{:S(2)}) async-start(f32[16,5,256]{2,1,0:T(8,128)} %broadcast_in_dim.4), calls=%async_computation | async-start | bytes 262144 | tf_op jit(solution)/shard_map/all_to_all | solution.py:372
  27.6 32.0 %copy-start = (bf16[2048,256]{1,0:T(8,128)(2,1)S(1)}, bf16[2048,256]{1,0:T(8,128)(2,1)}, u32[]{:S(2)}) copy-start(bf16[2048,256]{1,0:T(8,128)(2,1)} %wk.3) | copy-start | bytes 3145732
  27.7 3.9 %copy-start.7 = (f32[32]{0:T(128)S(1)}, f32[32]{0:T(128)}, u32[]{:S(2)}) copy-start(f32[32]{0:T(128)} %param.28) | copy-start | bytes 388
  27.7 3.9 %copy-start.8 = (f32[32]{0:T(128)S(1)}, f32[32]{0:T(128)}, u32[]{:S(2)}) copy-start(f32[32]{0:T(128)} %param.27) | copy-start | bytes 388
  27.8 38.3 %collective-permute-start.3 = (bf16[4,32,2048]{2,1,0:T(8,128)(2,1)S(1)}, bf16[4,32,2048]{2,1,0:T(8,128)(2,1)S(1)}, u32[]{:S(2)}, u32[]{:S(2)}) collective-permute-start(bf16[4,32,2048]{2,1,0:T(8,128)(2,1)S(1)} %pad_maximum_fusion.one), channel_id=1, source_target_pairs={{0,1},{1,0},{2,3},{3,2},{4,5},{5,4},{6,7},{7,6},{8,9},{9,8},{10,11... | collective-permute-start | bytes 1572872 | tf_op jit(solution)/shard_map/ppermute | solution.py:415
  40.3 10.4 %copy-start.10 = (f32[32]{0:T(128)S(1)}, f32[32]{0:T(128)}, u32[]{:S(2)}) copy-start(f32[32]{0:T(128)} %param.26) | copy-start | bytes 388
  40.3 19.3 %all-to-all-start.1 = ((f32[32,5,256]{2,1,0:T(8,128)}), f32[32,5,256]{2,1,0:T(8,128)S(1)}, u32[]{:S(2)}, u32[]{:S(2)}) async-start(f32[32,5,256]{2,1,0:T(8,128)} %broadcast_in_dim.5), calls=%async_computation.1 | async-start | bytes 524288 | tf_op jit(solution)/shard_map/all_to_all | solution.py:372
  50.8 8.8 %copy-start.3 = (bf16[4,2048]{1,0:T(4,128)(2,1)S(1)}, bf16[4,2048]{1,0:T(4,128)(2,1)}, u32[]{:S(2)}) copy-start(bf16[4,2048]{1,0:T(4,128)(2,1)} %ctx.1) | copy-start | bytes 49156
  50.9 0.7 copy-start.9
  62.8 3.3 %copy-start.5 = (f32[256,32]{0,1:T(8,128)S(1)}, f32[256,32]{0,1:T(8,128)}, u32[]{:S(2)}) copy-start(f32[256,32]{0,1:T(8,128)} %param.29) | copy-start | bytes 98308
  62.8 15.1 %all-to-all-start.2 = ((bf16[4,8,512]{2,1,0:T(8,128)(2,1)}), bf16[4,8,512]{2,1,0:T(8,128)(2,1)S(1)}, u32[]{:S(2)}, u32[]{:S(2)}) async-start(bf16[4,8,512]{2,1,0:T(8,128)(2,1)} %shard_map.155), calls=%async_computation.2 | async-start | bytes 65536 | tf_op jit(solution)/shard_map/all_to_all | solution.py:454
  66.1 1.2 copy-start.4
  103.3 9.4 %collective-permute-start.4 = (bf16[128,256]{1,0:T(8,128)(2,1)S(1)}, bf16[128,256]{1,0:T(8,128)(2,1)S(1)}, u32[]{:S(2)}, u32[]{:S(2)}) collective-permute-start(bf16[128,256]{1,0:T(8,128)(2,1)S(1)} %shard_map.159), channel_id=1, source_target_pairs={{0,384},{9,393},{16,400},{25,409},{385,1},{392,8},{401,17},{408,24... | collective-permute-start | bytes 196616 | tf_op jit(solution)/shard_map/ppermute | solution.py:481
  104.6 13.7 %collective-permute-start.5 = (bf16[128,256]{1,0:T(8,128)(2,1)S(1)}, bf16[128,256]{1,0:T(8,128)(2,1)S(1)}, u32[]{:S(2)}, u32[]{:S(2)}) collective-permute-start(bf16[128,256]{1,0:T(8,128)(2,1)S(1)} %shard_map.159), channel_id=1, source_target_pairs={{0,256},{9,265},{16,272},{25,281},{128,384},{137,393},{144,400},{1... | collective-permute-start | bytes 196616 | tf_op jit(solution)/shard_map/ppermute | solution.py:481
  105.9 12.4 %collective-permute-start.6 = (bf16[128,256]{1,0:T(8,128)(2,1)S(1)}, bf16[128,256]{1,0:T(8,128)(2,1)S(1)}, u32[]{:S(2)}, u32[]{:S(2)}) collective-permute-start(bf16[128,256]{1,0:T(8,128)(2,1)S(1)} %shard_map.159), channel_id=1, source_target_pairs={{0,128},{9,137},{16,144},{25,153},{128,256},{129,1},{136,8},{137,2... | collective-permute-start | bytes 196616 | tf_op jit(solution)/shard_map/ppermute | solution.py:481
  111.2 21.5 %copy-start.1 = (bf16[256,2048]{1,0:T(8,128)(2,1)S(1)}, bf16[256,2048]{1,0:T(8,128)(2,1)}, u32[]{:S(2)}) copy-start(bf16[256,2048]{1,0:T(8,128)(2,1)} %weight.1) | copy-start | bytes 3145732
  134.1 7.5 %collective-permute-start.7 = (bf16[4,32,2048]{2,1,0:T(8,128)(2,1)S(1)}, bf16[4,32,2048]{2,1,0:T(8,128)(2,1)S(1)}, u32[]{:S(2)}, u32[]{:S(2)}) collective-permute-start(bf16[4,32,2048]{2,1,0:T(8,128)(2,1)S(1)} %get-tuple-element.14), channel_id=1, source_target_pairs={{0,1},{1,0},{2,3},{3,2},{4,5},{5,4},{6,7},{7,6},{8,9},{9,8},{10,11... | collective-permute-start | bytes 1572872 | tf_op jit(solution)/shard_map/ppermute | solution.py:492

commit v6 on v5

--- a/solution.py
+++ b/solution.py
@@ -89,54 +89,51 @@
     return jnp.concatenate([f[r : r + 1] for f in parts], axis=1)
 
 
-def rows_kernel(pos, ctx, fac, wk, wv_h, wd_h, ww_h, c_o, hid, wv, wd, ww, sems):
-    copies = start_copies((wv_h, wd_h, ww_h), (wv, wd, ww), sems)
-    hid[0:4] = norm_rows(ctx[...], factor(fac, 4), factor(fac, 3))
-    hid[4:16] = jnp.zeros((12, D), BF)
-    rows = hid[...]
-    keys = mm(rows, wk[...]).astype(BF)
-    for copy in copies:
-        copy.wait()
-    values = mm(rows, wv[...]).astype(BF)
-    rate = mm(rows, wd[...], ((1,), (1,))).astype(BF).astype(F32)
-    write = mm(rows, ww[...], ((1,), (1,))).astype(BF).astype(F32)
-    lanes = lax.broadcasted_iota(jnp.int32, (16, 256), 1)
-    rank = lax.broadcasted_iota(jnp.int32, (16, 256), 0)
-    spots = (lanes == rank + pos[5]) & (rank < 4)
-    wide = [side.astype(F32)[0:4] for side in (keys, values)]
-    pieces = [jnp.concatenate(wide, axis=1)]
-    for j in range(4):
-        lane = pos[1] * 4 + j
-        gates = [
-            jnp.sum(jnp.where(spots, column(g, lane), 0.0), axis=0, keepdims=True)
-            for g in (rate, write)
-        ]
-        pieces.append(jnp.concatenate(gates, axis=1))
-    out = jnp.concatenate(pieces, axis=0).astype(BF)
-    for i in range(4):
-        c_o[i] = out
-
-
 def front_kernel(
-    pos, one, two, fac, wq, wk, spike, small, wv_h, wd_h, ww_h,
+    pos, one, two, fac, small, ctx_h, wq_h, wk_h, wv_h, wd_h, ww_h, spike_h,
     m_o, r_o, o_o,
-    hid, packed, wv, wd, ww, sems,
+    hid, packed, ctx, wq, wk, wv, wd, ww, spike, sems,
 ):
-    copies = start_copies((wv_h, wd_h, ww_h), (wv, wd, ww), sems)
+    copies = start_copies(
+        (ctx_h, wq_h, wk_h, wv_h, wd_h, ww_h, spike_h), (ctx, wq, wk, wv, wd, ww, spike), sems
+    )
     shift, scale = (factor(fac, 0), factor(fac, 1))
     for d in range(4):
         for i, lat in enumerate((one, two)):
             core = pos[6] if i == 0 else 1 - pos[6]
             spot = (2 * ((pos[7] + 4 - d) % 4) + core) * 32
             hid[pl.ds(pl.multiple_of(spot, 32), 32)] = norm_rows(lat[d], scale, shift)
+    copies[0].wait()
+    hid[256:260] = norm_rows(ctx[...], factor(fac, 4), factor(fac, 3))
+    hid[260:272] = jnp.zeros((12, D), BF)
     rows = hid[...]
-    packed[0:256] = mm(rows, wq[...]).astype(BF)
-    packed[256:512] = mm(rows, wk[...]).astype(BF)
-    for copy in copies:
+    copies[1].wait()
+    packed[0:256] = mm(hid[0:256], wq[...]).astype(BF)
+    copies[2].wait()
+    keys = mm(rows, wk[...]).astype(BF)
+    packed[256:512] = keys[:256]
+    for copy in copies[3:]:
         copy.wait()
-    packed[512:768] = mm(rows, wv[...]).astype(BF)
-    packed[768:800] = mm(wd[...], rows, ((1,), (1,))).astype(BF)
-    packed[800:832] = mm(ww[...], rows, ((1,), (1,))).astype(BF)
+    values = mm(rows, wv[...]).astype(BF)
+    packed[512:768] = values[:256]
+    packed[768:800] = mm(wd[...], hid[0:256], ((1,), (1,))).astype(BF)
+    packed[800:832] = mm(ww[...], hid[0:256], ((1,), (1,))).astype(BF)
+    rate = mm(hid[256:272], wd[...], ((1,), (1,))).astype(BF).astype(F32)
+    write = mm(hid[256:272], ww[...], ((1,), (1,))).astype(BF).astype(F32)
+    lanes = lax.broadcasted_iota(jnp.int32, (16, 256), 1)
+    rank = lax.broadcasted_iota(jnp.int32, (16, 256), 0)
+    spots = (lanes == rank + pos[5]) & (rank < 4)
+    wide = [side[256:272].astype(F32)[0:4] for side in (keys, values)]
+    for j in range(4):
+        h = j // 2
+        lane = pos[1] * 4 + j
+        pieces = [jnp.concatenate([w[:, 128 * h : 128 * h + 128] for w in wide], axis=1)]
+        pieces += [
+            jnp.sum(jnp.where(spots, column(g, lane), 0.0), axis=0, keepdims=True)
+            for g in (rate, write)
+        ]
+        pieces.append(jnp.zeros((10, 256), F32))
+        m_o[(j + pos[4]) % 4, 128:144] = jnp.concatenate(pieces, axis=0).astype(BF)
     chunk(pos, packed, spike, small, m_o, r_o, o_o)
 
 
@@ -244,20 +241,6 @@
     return both[:, :n] + both[:, n:]
 
 
-def pack_kernel(pos, maps, rows, o):
-    wide = [rows[i].astype(F32) for i in range(4)]
-    for j in range(4):
-        h = j // 2
-        to = (j + pos[4]) % 4
-        parts = []
-        for w in wide:
-            sides = [w[0:4, at + 128 * h : at + 128 * h + 128] for at in (0, 256)]
-            parts.append(jnp.concatenate(sides, axis=1))
-        gates = sum(w[4 + j : 5 + j] for w in wide)
-        parts += [gates[:, 0:256], gates[:, 256:512], jnp.zeros((14, 256), F32)]
-        o[to, 128:160] = jnp.concatenate(parts, axis=0).astype(BF)
-
-
 def composed(pos, maps):
     back = pos[0] % 2
     at = back * 3
@@ -272,20 +255,26 @@
 def low_kernel(pos, maps, o):
     total = composed(pos, maps)
     wide = [maps[i][128:].astype(F32) for i in range(4)]
-    parts = [w[4 * i : 4 * i + 4] for i in range(4) for w in wide]
-    parts += [sum(w[16:18] for w in wide), jnp.zeros((14, 256), F32)]
+    parts = [w[0:4] for w in wide]
+    parts += [sum(w[4:6] for w in wide), jnp.zeros((14, 256), F32)]
     out = jnp.concatenate([total, *parts], axis=0).astype(BF)
     for i in range(4):
         o[i] = out
 
 
-def high_kernel(pos, maps, o):
+def high_kernel(pos, maps, o, rows):
+    wide = [maps[i][128:].astype(F32) for i in range(4)]
+    parts = [w[0:16] for w in wide]
+    parts += [sum(w[16:18] for w in wide), jnp.zeros((6, 256), F32)]
+    out = jnp.concatenate(parts, axis=0).astype(BF)
+    for i in range(4):
+        rows[i] = out
     o[...] = composed(pos, maps).astype(BF)
 
 
-def context_kernel(pos, low, small, o):
-    wide = [low[i][128:].astype(F32) for i in range(4)]
-    rows = jnp.concatenate([w[16 * i : 16 * i + 16] for i in range(4) for w in wide], axis=0)
+def context_kernel(pos, all_rows, small, o):
+    wide = [all_rows[i].astype(F32) for i in range(4)]
+    rows = jnp.concatenate([w[0:64] for w in wide], axis=0)
     gates = sum(w[64:66] for w in wide)
     o[...] = context_state(
         pos, rows, gates[0:1], gates[1:2], small[0:1], small[1:2], small[2:3]
@@ -436,52 +425,49 @@
     )
     slow = [
         pltpu.with_memory_space_constraint(a, pltpu.HBM)
-        for a in (value_matrix, decay_input_weight.T, write_strength_weight.T)
+        for a in (
+            context,
+            query_matrix,
+            key_matrix,
+            value_matrix,
+            decay_input_weight.T,
+            write_strength_weight.T,
+            log_spike_added.T,
+        )
     ]
     room = [
+        pltpu.VMEM((4, D), BF),
+        pltpu.VMEM((D, 256), BF),
+        pltpu.VMEM((D, 256), BF),
         pltpu.VMEM((D, 256), BF),
         pltpu.VMEM((32, D), BF),
         pltpu.VMEM((32, D), BF),
-        pltpu.SemaphoreType.DMA((3,)),
+        pltpu.VMEM((32, 256), F32),
+        pltpu.SemaphoreType.DMA((7,)),
     ]
-    rows = call(
-        rows_kernel,
-        ((4, 8, 512), BF),
-        [SM] + [VM] * 3 + [HB] * 3,
-        [pltpu.VMEM((16, D), BF), *room],
-        flops=10**8,
-    )(pos, context, fac, key_matrix, *slow)
-    rows = lax.all_to_all(rows, "zh", 0, 0, tiled=True)
     maps, reads, base = call(
         front_kernel,
-        [((4, 160, 256), BF), ((2, 256, 256), BF), ((256, 256), F32)],
-        [SM] + [VM] * 7 + [HB] * 3,
-        [pltpu.VMEM((256, D), BF), pltpu.VMEM((832, 256), BF), *room],
+        [((4, 144, 256), BF), ((2, 256, 256), BF), ((256, 256), F32)],
+        [SM] + [VM] * 4 + [HB] * 7,
+        [pltpu.VMEM((272, D), BF), pltpu.VMEM((832, 256), BF), *room],
         flops=5 * 10**9,
     )(
         pos,
         mine,
         other,
         fac,
-        query_matrix,
-        key_matrix,
-        log_spike_added.T,
         small,
         *slow,
     )
-    maps = call(pack_kernel, ((4, 160, 256), BF), [SM, VM, VM], aliases={1: 0})(
-        pos, maps, rows
-    )
     of_y = lax.all_to_all(maps, "y", 0, 0, tiled=True)
-    low = call(low_kernel, ((4, 208, 256), BF), [SM, VM])(pos, of_y)
+    low = call(low_kernel, ((4, 160, 256), BF), [SM, VM])(pos, of_y)
     of_low = lax.all_to_all(low, "zl", 0, 0, tiled=True)
-    high = call(high_kernel, ((128, 256), BF), [SM, VM])(pos, of_low)
+    high, rows = call(high_kernel, [((128, 256), BF), ((4, 72, 256), BF)], [SM, VM])(pos, of_low)
+    rows = lax.all_to_all(rows, "zh", 0, 0, tiled=True)
     of_high = []
     for d in (3, 2, 1):
         of_high.append(lax.ppermute(high, ("zh", "y", "c"), onward(d)))
-    start = call(context_kernel, ((128, 128), F32), [SM] + [VM] * 2, flops=10**9)(
-        pos, of_low, small
-    )
+    start = call(context_kernel, ((128, 128), F32), [SM] + [VM] * 2, flops=10**9)(pos, rows, small)
     states = call(scan_kernel, ((4, 128, 128), BF), [SM] + [VM] * 6, flops=10**8)(
         pos, start, *of_high, of_low, of_y
     )

time: 155 us -> 150 us (0.968)
  blocking collectives: 46.6 us -> 39.2 us
  waiting for transfers between devices: 25.4 us -> 30.6 us
  Pallas kernels: 23.6 us -> 21.2 us
    all_to_all x1, waiting for transfers between devices: 0.83 us -> 9.99 us  [per_device(): rows = lax.all_to_all(rows, 'zh', 0, 0, tiled=True)]
    all_to_all x1, blocking collectives: 12.4 us -> 7.21 us  [per_device(): states = lax.all_to_all(states, 'y', 0, 0, tiled=True)]
    ppermute x3, waiting for transfers between devices: 7.07 us -> 2.94 us  [per_device(): of_high.append(lax.ppermute(high, ('zh', 'y', 'c'), onward(d)))]
    all_to_all x1, blocking collectives: 14.4 us -> 11.4 us  [per_device(): of_low = lax.all_to_all(low, 'zl', 0, 0, tiled=True)]
    pallas_call x5 -> x3, Pallas kernels: 15.6 us -> 13.2 us  [the longest x1 10.4 us: per_device(): call(front_kernel, [((4, 144, 256), BF), ((2, 256, 256), BF), ((256, 256)...]
    all_to_all x2, starting transfers between devices: 25.5 us -> 23.7 us  [to_all(): lax.all_to_all(jnp.broadcast_to(value[None], (count, *value.shape)), axes...]
  transfers between devices with their start and end apart: 11 -> 11, of which waited for: 6 -> 5; matrix products, arithmetic and copies ran while one was open for 2% -> 2% of each run, Pallas kernels for 11% -> 3%
where the time goes in v6:
time: 150 us; the launch traced here: 149 us
  starting transfers between devices  54.4 us (36%)
  blocking collectives  39.2 us (26%)
  waiting for transfers between devices  30.6 us (20%)
  Pallas kernels  21.2 us (14%)
  local copies, waits for them, and re-layouts  2.17 us (1%)
    all_to_all x2, starting transfers between devices, to_all(): lax.all_to_all(jnp.broadcast_to(value[None], (count, *value.shape)), axes...  23.7 us
    all_to_all x2, waiting for transfers between devices, to_all(): lax.all_to_all(jnp.broadcast_to(value[None], (count, *value.shape)), axes...  16.1 us
    ppermute x3, starting transfers between devices, per_device(): lax.ppermute(latent, 'x', [(i, (i + d) % 4) for i in range(4)])  12.1 us
    all_to_all x1, blocking collectives, per_device(): branch = lax.all_to_all(branch, 'x', 0, 0, tiled=True)  11.5 us
    all_to_all x1, blocking collectives, per_device(): of_low = lax.all_to_all(low, 'zl', 0, 0, tiled=True)  11.4 us
    pallas_call x1, Pallas kernels, per_device(): call(front_kernel, [((4, 144, 256), BF), ((2, 256, 256), BF), ((256, 256)...  10.4 us
    all_to_all x1, waiting for transfers between devices, per_device(): rows = lax.all_to_all(rows, 'zh', 0, 0, tiled=True)  9.99 us
    all_to_all x1, blocking collectives, per_device(): of_y = lax.all_to_all(maps, 'y', 0, 0, tiled=True)  9.04 us
  transfers between devices with their start and end apart: 11, of which 5 were waited for; matrix products, arithmetic and copies ran while one was open for 2% of the time, Pallas kernels for 3%

profile of v6, /device:TPU:1, one launch (start us, length us, event | category | flops | bytes accessed | tf_op | source)
XLA Modules:
  0.0 148.9 jit_solution(1224305616912636673)
XLA Ops:
  0.0 5.6 %collective-permute-start.1 = (bf16[32,2048]{1,0:T(8,128)(2,1)}, bf16[32,2048]{1,0:T(8,128)(2,1)S(1)}, u32[]{:S(2)}, u32[]{:S(2)}) collective-permute-start(bf16[32,2048]{1,0:T(8,128)(2,1)} %lat.1), channel_id=1, source_target_pairs={{0,4},{2,6},{4,0},{6,2},{1,5},{3,7},{5,1},{7,3},{8,12},{10,14},{12... | collective-permute-start | bytes 393224 | tf_op jit(solution)/shard_map/ppermute | solution.py:402
  5.6 2.2 %collective-permute-start = (bf16[32,2048]{1,0:T(8,128)(2,1)}, bf16[32,2048]{1,0:T(8,128)(2,1)S(1)}, u32[]{:S(2)}, u32[]{:S(2)}) collective-permute-start(bf16[32,2048]{1,0:T(8,128)(2,1)} %lat.1), channel_id=1, source_target_pairs={{0,2},{2,4},{4,6},{6,0},{1,3},{3,5},{5,7},{7,1},{8,10},{10,12},{12... | collective-permute-start | bytes 393224 | tf_op jit(solution)/shard_map/ppermute | solution.py:402
  7.8 4.3 %collective-permute-start.2 = (bf16[32,2048]{1,0:T(8,128)(2,1)}, bf16[32,2048]{1,0:T(8,128)(2,1)S(1)}, u32[]{:S(2)}, u32[]{:S(2)}) collective-permute-start(bf16[32,2048]{1,0:T(8,128)(2,1)} %lat.1), channel_id=1, source_target_pairs={{0,6},{2,0},{4,2},{6,4},{1,7},{3,1},{5,3},{7,5},{8,14},{10,8},{12,... | collective-permute-start | bytes 393224 | tf_op jit(solution)/shard_map/ppermute | solution.py:402
  12.1 0.8 divide_multiply_fusion
  12.9 0.0 copy-done.2
  12.9 0.1 multiply_reduce_fusion
  13.0 0.1 fusion
  13.1 0.7 broadcast_in_dim.4
  13.8 15.0 %all-to-all-start = ((f32[16,5,256]{2,1,0:T(8,128)}), f32[16,5,256]{2,1,0:T(8,128)S(1)}, u32[]{:S(2)}, u32[]{:S(2)}) async-start(f32[16,5,256]{2,1,0:T(8,128)} %broadcast_in_dim.4), calls=%async_computation | async-start | bytes 262144 | tf_op jit(solution)/shard_map/all_to_all | solution.py:361
  28.8 0.0 collective-permute-done.1
  28.8 0.0 collective-permute-done
  28.9 0.0 collective-permute-done.2
  28.9 0.0 copy-done.1
  28.9 0.0 copy-start.3
  28.9 0.0 copy-start.4
  28.9 0.1 pad_maximum_fusion.one
  29.0 3.7 %collective-permute-start.3 = (bf16[4,32,2048]{2,1,0:T(8,128)(2,1)S(1)}, bf16[4,32,2048]{2,1,0:T(8,128)(2,1)S(1)}, u32[]{:S(2)}, u32[]{:S(2)}) collective-permute-start(bf16[4,32,2048]{2,1,0:T(8,128)(2,1)S(1)} %pad_maximum_fusion.one), channel_id=1, source_target_pairs={{0,1},{1,0},{2,3},{3,2},{4,5},{5,4},{6,7},{7,6},{8,9},{9,8},{10,11... | collective-permute-start | bytes 1572872 | tf_op jit(solution)/shard_map/ppermute | solution.py:404
  32.7 8.1 %all-to-all-done = f32[16,5,256]{2,1,0:T(8,128)S(1)} async-done(((f32[16,5,256]{2,1,0:T(8,128)}), f32[16,5,256]{2,1,0:T(8,128)S(1)}, u32[]{:S(2)}, u32[]{:S(2)}) %all-to-all-start) | async-done | bytes 81952 | tf_op jit(solution)/shard_map/all_to_all | solution.py:361
  40.8 0.7 broadcast_in_dim.5
  41.5 8.6 %all-to-all-start.1 = ((f32[32,5,256]{2,1,0:T(8,128)}), f32[32,5,256]{2,1,0:T(8,128)S(1)}, u32[]{:S(2)}, u32[]{:S(2)}) async-start(f32[32,5,256]{2,1,0:T(8,128)} %broadcast_in_dim.5), calls=%async_computation.1 | async-start | bytes 524288 | tf_op jit(solution)/shard_map/all_to_all | solution.py:361
  50.2 0.0 copy-done.6
  50.2 0.1 stack.74.pos
  50.3 0.7 copy-done.5
  51.0 8.1 %all-to-all-done.1.fac = f32[32,5,256]{2,1,0:T(8,128)S(1)} async-done(((f32[32,5,256]{2,1,0:T(8,128)}), f32[32,5,256]{2,1,0:T(8,128)S(1)}, u32[]{:S(2)}, u32[]{:S(2)}) %all-to-all-start.1) | async-done | bytes 163872 | tf_op jit(solution)/shard_map/all_to_all | solution.py:361
  59.1 0.0 collective-permute-done.3.two
  59.1 10.4 %shard_map.154 = (bf16[4,144,256]{2,1,0:T(8,128)(2,1)S(1)}, bf16[2,256,256]{2,1,0:T(8,128)(2,1)S(1)}, f32[256,256]{1,0:T(8,128)S(1)}) custom-call(s32[8]{0:T(128)S(1)} %stack.74.pos, bf16[4,32,2048]{2,1,0:T(8,128)(2,1)S(1)} %pad_maximum_fusion.one, bf16[4,32,2048]{2,1,0:T(8,128)(2,1)S(1)} %collective-permute-done.3.two, ...), custom_call_target="tpu_custom_call" | custom-call | flops 5000000000 | bytes 1 | tf_op jit(solution)/shard_map/pallas_call | solution.py:448
  69.5 9.0 %all_to_all.35.maps.own = bf16[4,144,256]{2,1,0:T(8,128)(2,1)S(1)} all-to-all(bf16[4,144,256]{2,1,0:T(8,128)(2,1)S(1)} %get-tuple-element.12), channel_id=1, replica_groups=mesh['zh'=4,'zl'=4,'y'=4,'x'=4,'c'=2] {'y'}, dimensions={0} | all-to-all | bytes 589824 | tf_op jit(solution)/shard_map/all_to_all | solution.py:462
  78.5 1.1 shard_map.155
  79.6 11.4 %all_to_all.36.maps.low = bf16[4,160,256]{2,1,0:T(8,128)(2,1)S(1)} all-to-all(bf16[4,160,256]{2,1,0:T(8,128)(2,1)S(1)} %shard_map.155), channel_id=1, replica_groups=mesh['zh'=4,'zl'=4,'y'=4,'x'=4,'c'=2] {'zl'}, dimensions={0} | all-to-all | bytes 655360 | tf_op jit(solution)/shard_map/all_to_all | solution.py:464
  91.0 1.7 %shard_map.156 = (bf16[128,256]{1,0:T(8,128)(2,1)S(1)}, bf16[4,72,256]{2,1,0:T(8,128)(2,1)}) custom-call(s32[8]{0:T(128)S(1)} %stack.74.pos, bf16[4,160,256]{2,1,0:T(8,128)(2,1)S(1)} %all_to_all.36.maps.low), custom_call_target="tpu_custom_call" | custom-call | flops 1 | bytes 1 | tf_op jit(solution)/shard_map/pallas_call | solution.py:465
  92.7 4.7 %all-to-all-start.4 = ((bf16[4,72,256]{2,1,0:T(8,128)(2,1)}), bf16[4,72,256]{2,1,0:T(8,128)(2,1)S(1)}, u32[]{:S(2)}, u32[]{:S(2)}) async-start(bf16[4,72,256]{2,1,0:T(8,128)(2,1)} %get-tuple-element.13), calls=%async_computation.4 | async-start | bytes 294912 | tf_op jit(solution)/shard_map/all_to_all | solution.py:466
  97.4 1.3 collective-permute-start.6
  98.6 1.3 collective-permute-start.5
  99.9 1.5 collective-permute-start.4
  101.4 10.0 %all-to-all-done.4.all_rows = bf16[4,72,256]{2,1,0:T(8,128)(2,1)S(1)} async-done(((bf16[4,72,256]{2,1,0:T(8,128)(2,1)}), bf16[4,72,256]{2,1,0:T(8,128)(2,1)S(1)}, u32[]{:S(2)}, u32[]{:S(2)}) %all-to-all-start.4) | async-done | bytes 147488 | tf_op jit(solution)/shard_map/all_to_all | solution.py:466
  111.4 3.9 %shard_map.157.start = f32[128,128]{1,0:T(8,128)S(1)} custom-call(s32[8]{0:T(128)S(1)} %stack.74.pos, bf16[4,72,256]{2,1,0:T(8,128)(2,1)S(1)} %all-to-all-done.4.all_rows, f32[4,128]{1,0:T(4,128)S(1)} %pad_maximum_fusion.2.small.gain), custom_call_target="tpu_custom_call" | custom-call | flops 1000000000 | bytes 1 | tf_op jit(solution)/shard_map/pallas_call | solution.py:470
  115.3 0.0 copy-start
  115.3 0.0 collective-permute-done.6.near
  115.3 0.0 collective-permute-done.5.middle
  115.3 2.9 %collective-permute-done.4.far = bf16[128,256]{1,0:T(8,128)(2,1)S(1)} collective-permute-done((bf16[128,256]{1,0:T(8,128)(2,1)S(1)}, bf16[128,256]{1,0:T(8,128)(2,1)S(1)}, u32[]{:S(2)}, u32[]{:S(2)}) %collective-permute-start.4) | collective-permute-done | bytes 65568 | tf_op jit(solution)/shard_map/ppermute | solution.py:469
  118.2 1.9 %shard_map.158 = bf16[4,128,128]{2,1,0:T(8,128)(2,1)S(1)} custom-call(s32[8]{0:T(128)S(1)} %stack.74.pos, f32[128,128]{1,0:T(8,128)S(1)} %shard_map.157.start, bf16[128,256]{1,0:T(8,128)(2,1)S(1)} %collective-permute-done.4.far, bf16[128,256]{1,0:T(8,128)(2,1)S(1)} %collective-permute-done.5.middle, bf16[128,256]{1,0:T(8,128)(2,1)S(1)} %collective-permute-done.6.near, ...), custom_call_target="tpu_custom_call" | custom-call | flops 100000000 | bytes 1 | tf_op jit(solution)/shard_map/pallas_call | solution.py:471
  120.2 7.2 %all_to_all.37.states = bf16[4,128,128]{2,1,0:T(8,128)(2,1)S(1)} all-to-all(bf16[4,128,128]{2,1,0:T(8,128)(2,1)S(1)} %shard_map.158), channel_id=1, replica_groups=mesh['zh'=4,'zl'=4,'y'=4,'x'=4,'c'=2] {'y'}, dimensions={0} | all-to-all | bytes 262144 | tf_op jit(solution)/shard_map/all_to_all | solution.py:474
  127.4 1.4 shard_map.159
  128.8 6.2 %collective-permute-start.7 = (bf16[4,32,2048]{2,1,0:T(8,128)(2,1)S(1)}, bf16[4,32,2048]{2,1,0:T(8,128)(2,1)S(1)}, u32[]{:S(2)}, u32[]{:S(2)}) collective-permute-start(bf16[4,32,2048]{2,1,0:T(8,128)(2,1)S(1)} %get-tuple-element.18), channel_id=1, source_target_pairs={{0,1},{1,0},{2,3},{3,2},{4,5},{5,4},{6,7},{7,6},{8,9},{9,8},{10,11... | collective-permute-start | bytes 1572872 | tf_op jit(solution)/shard_map/ppermute | solution.py:478
  135.0 1.5 %collective-permute-done.7.got = bf16[4,32,2048]{2,1,0:T(8,128)(2,1)S(1)} collective-permute-done((bf16[4,32,2048]{2,1,0:T(8,128)(2,1)S(1)}, bf16[4,32,2048]{2,1,0:T(8,128)(2,1)S(1)}, u32[]{:S(2)}, u32[]{:S(2)}) %collective-permute-start.7) | collective-permute-done | bytes 524320 | tf_op jit(solution)/shard_map/ppermute | solution.py:478
  136.5 0.1 shard_map.160
  136.6 11.5 %all_to_all.38.rows = bf16[4,32,2048]{2,1,0:T(8,128)(2,1)S(1)} all-to-all(bf16[4,32,2048]{2,1,0:T(8,128)(2,1)S(1)} %shard_map.160), channel_id=1, replica_groups=mesh['zh'=4,'zl'=4,'y'=4,'x'=4,'c'=2] {'x'}, dimensions={0} | all-to-all | bytes 1048576 | tf_op jit(solution)/shard_map/all_to_all | solution.py:480
  148.1 0.8 shard_map.161
  (14 shorter events, 0.1 us)
Async XLA Ops:
  0.0 12.9 %copy-start.2 = (bf16[3,32,256]{2,1,0:T(8,128)(2,1)S(1)}, bf16[3,32,256]{2,1,0:T(8,128)(2,1)}, u32[]{:S(2)}) copy-start(bf16[3,32,256]{2,1,0:T(8,128)(2,1)} %param.20) | copy-start | bytes 147460
  0.0 28.8 %collective-permute-start.1 = (bf16[32,2048]{1,0:T(8,128)(2,1)}, bf16[32,2048]{1,0:T(8,128)(2,1)S(1)}, u32[]{:S(2)}, u32[]{:S(2)}) collective-permute-start(bf16[32,2048]{1,0:T(8,128)(2,1)} %lat.1), channel_id=1, source_target_pairs={{0,4},{2,6},{4,0},{6,2},{1,5},{3,7},{5,1},{7,3},{8,12},{10,14},{12... | collective-permute-start | bytes 393224 | tf_op jit(solution)/shard_map/ppermute | solution.py:402
  5.6 23.2 %collective-permute-start = (bf16[32,2048]{1,0:T(8,128)(2,1)}, bf16[32,2048]{1,0:T(8,128)(2,1)S(1)}, u32[]{:S(2)}, u32[]{:S(2)}) collective-permute-start(bf16[32,2048]{1,0:T(8,128)(2,1)} %lat.1), channel_id=1, source_target_pairs={{0,2},{2,4},{4,6},{6,0},{1,3},{3,5},{5,7},{7,1},{8,10},{10,12},{12... | collective-permute-start | bytes 393224 | tf_op jit(solution)/shard_map/ppermute | solution.py:402
  7.8 21.0 %collective-permute-start.2 = (bf16[32,2048]{1,0:T(8,128)(2,1)}, bf16[32,2048]{1,0:T(8,128)(2,1)S(1)}, u32[]{:S(2)}, u32[]{:S(2)}) collective-permute-start(bf16[32,2048]{1,0:T(8,128)(2,1)} %lat.1), channel_id=1, source_target_pairs={{0,6},{2,0},{4,2},{6,4},{1,7},{3,1},{5,3},{7,5},{8,14},{10,8},{12,... | collective-permute-start | bytes 393224 | tf_op jit(solution)/shard_map/ppermute | solution.py:402
  13.8 15.1 %copy-start.1 = (bf16[32,2048]{1,0:T(8,128)(2,1)S(1)}, bf16[32,2048]{1,0:T(8,128)(2,1)}, u32[]{:S(2)}) copy-start(bf16[32,2048]{1,0:T(8,128)(2,1)} %lat.1) | copy-start | bytes 393220
  13.8 27.0 %all-to-all-start = ((f32[16,5,256]{2,1,0:T(8,128)}), f32[16,5,256]{2,1,0:T(8,128)S(1)}, u32[]{:S(2)}, u32[]{:S(2)}) async-start(f32[16,5,256]{2,1,0:T(8,128)} %broadcast_in_dim.4), calls=%async_computation | async-start | bytes 262144 | tf_op jit(solution)/shard_map/all_to_all | solution.py:361
  28.9 3.8 %copy-start.3 = (f32[32]{0:T(128)S(1)}, f32[32]{0:T(128)}, u32[]{:S(2)}) copy-start(f32[32]{0:T(128)} %param.28) | copy-start | bytes 388
  28.9 3.8 %copy-start.4 = (f32[32]{0:T(128)S(1)}, f32[32]{0:T(128)}, u32[]{:S(2)}) copy-start(f32[32]{0:T(128)} %param.27) | copy-start | bytes 388
  29.0 30.1 %collective-permute-start.3 = (bf16[4,32,2048]{2,1,0:T(8,128)(2,1)S(1)}, bf16[4,32,2048]{2,1,0:T(8,128)(2,1)S(1)}, u32[]{:S(2)}, u32[]{:S(2)}) collective-permute-start(bf16[4,32,2048]{2,1,0:T(8,128)(2,1)S(1)} %pad_maximum_fusion.one), channel_id=1, source_target_pairs={{0,1},{1,0},{2,3},{3,2},{4,5},{5,4},{6,7},{7,6},{8,9},{9,8},{10,11... | collective-permute-start | bytes 1572872 | tf_op jit(solution)/shard_map/ppermute | solution.py:404
  41.5 8.7 %copy-start.6 = (f32[32]{0:T(128)S(1)}, f32[32]{0:T(128)}, u32[]{:S(2)}) copy-start(f32[32]{0:T(128)} %param.26) | copy-start | bytes 388
  41.5 17.5 %all-to-all-start.1 = ((f32[32,5,256]{2,1,0:T(8,128)}), f32[32,5,256]{2,1,0:T(8,128)S(1)}, u32[]{:S(2)}, u32[]{:S(2)}) async-start(f32[32,5,256]{2,1,0:T(8,128)} %broadcast_in_dim.5), calls=%async_computation.1 | async-start | bytes 524288 | tf_op jit(solution)/shard_map/all_to_all | solution.py:361
  50.3 0.7 copy-start.5
  92.7 18.7 %all-to-all-start.4 = ((bf16[4,72,256]{2,1,0:T(8,128)(2,1)}), bf16[4,72,256]{2,1,0:T(8,128)(2,1)S(1)}, u32[]{:S(2)}, u32[]{:S(2)}) async-start(bf16[4,72,256]{2,1,0:T(8,128)(2,1)} %get-tuple-element.13), calls=%async_computation.4 | async-start | bytes 294912 | tf_op jit(solution)/shard_map/all_to_all | solution.py:466
  97.4 17.9 %collective-permute-start.6 = (bf16[128,256]{1,0:T(8,128)(2,1)S(1)}, bf16[128,256]{1,0:T(8,128)(2,1)S(1)}, u32[]{:S(2)}, u32[]{:S(2)}) collective-permute-start(bf16[128,256]{1,0:T(8,128)(2,1)S(1)} %get-tuple-element.14), channel_id=1, source_target_pairs={{0,128},{9,137},{16,144},{25,153},{128,256},{129,1},{136,8},{137,2... | collective-permute-start | bytes 196616 | tf_op jit(solution)/shard_map/ppermute | solution.py:469
  98.6 16.7 %collective-permute-start.5 = (bf16[128,256]{1,0:T(8,128)(2,1)S(1)}, bf16[128,256]{1,0:T(8,128)(2,1)S(1)}, u32[]{:S(2)}, u32[]{:S(2)}) collective-permute-start(bf16[128,256]{1,0:T(8,128)(2,1)S(1)} %get-tuple-element.14), channel_id=1, source_target_pairs={{0,256},{9,265},{16,272},{25,281},{128,384},{137,393},{144,400},{1... | collective-permute-start | bytes 196616 | tf_op jit(solution)/shard_map/ppermute | solution.py:469
  99.9 18.3 %collective-permute-start.4 = (bf16[128,256]{1,0:T(8,128)(2,1)S(1)}, bf16[128,256]{1,0:T(8,128)(2,1)S(1)}, u32[]{:S(2)}, u32[]{:S(2)}) collective-permute-start(bf16[128,256]{1,0:T(8,128)(2,1)S(1)} %get-tuple-element.14), channel_id=1, source_target_pairs={{0,384},{9,393},{16,400},{25,409},{385,1},{392,8},{401,17},{408,24... | collective-permute-start | bytes 196616 | tf_op jit(solution)/shard_map/ppermute | solution.py:469
  115.3 12.1 %copy-start = (bf16[256,2048]{1,0:T(8,128)(2,1)S(1)}, bf16[256,2048]{1,0:T(8,128)(2,1)}, u32[]{:S(2)}) copy-start(bf16[256,2048]{1,0:T(8,128)(2,1)} %weight.1) | copy-start | bytes 3145732
  128.8 7.7 %collective-permute-start.7 = (bf16[4,32,2048]{2,1,0:T(8,128)(2,1)S(1)}, bf16[4,32,2048]{2,1,0:T(8,128)(2,1)S(1)}, u32[]{:S(2)}, u32[]{:S(2)}) collective-permute-start(bf16[4,32,2048]{2,1,0:T(8,128)(2,1)S(1)} %get-tuple-element.18), channel_id=1, source_target_pairs={{0,1},{1,0},{2,3},{3,2},{4,5},{5,4},{6,7},{7,6},{8,9},{9,8},{10,11... | collective-permute-start | bytes 1572872 | tf_op jit(solution)/shard_map/ppermute | solution.py:478

commit v7 on v6

--- a/solution.py
+++ b/solution.py
@@ -252,29 +252,33 @@
     return total
 
 
-def low_kernel(pos, maps, o):
-    total = composed(pos, maps)
+def low_kernel(pos, maps, o, rows):
     wide = [maps[i][128:].astype(F32) for i in range(4)]
     parts = [w[0:4] for w in wide]
-    parts += [sum(w[4:6] for w in wide), jnp.zeros((14, 256), F32)]
-    out = jnp.concatenate([total, *parts], axis=0).astype(BF)
+    parts += [sum(w[4:6] for w in wide), jnp.zeros((6, 256), F32)]
+    rows[...] = jnp.concatenate(parts, axis=0).astype(BF)
+    out = composed(pos, maps).astype(BF)
     for i in range(4):
         o[i] = out
 
 
-def high_kernel(pos, maps, o, rows):
-    wide = [maps[i][128:].astype(F32) for i in range(4)]
-    parts = [w[0:16] for w in wide]
-    parts += [sum(w[16:18] for w in wide), jnp.zeros((6, 256), F32)]
-    out = jnp.concatenate(parts, axis=0).astype(BF)
+def high_kernel(pos, maps, r0, r1, r2, r3, o, rows):
+    gates = jnp.zeros((2, 256), F32)
+    for d, part in enumerate((r0, r1, r2, r3)):
+        wide = part[...].astype(F32)
+        gates = gates + wide[16:18]
+        spot = pl.multiple_of(((pos[2] + 4 - d) % 4) * 16, 16)
+        for i in range(4):
+            rows[i, pl.ds(spot, 16)] = part[0:16]
+    tail = jnp.concatenate([gates, jnp.zeros((14, 256), F32)], axis=0).astype(BF)
     for i in range(4):
-        rows[i] = out
+        rows[i, 64:80] = tail
     o[...] = composed(pos, maps).astype(BF)
 
 
 def context_kernel(pos, all_rows, small, o):
     wide = [all_rows[i].astype(F32) for i in range(4)]
-    rows = jnp.concatenate([w[0:64] for w in wide], axis=0)
+    rows = jnp.concatenate([w[16 * i : 16 * i + 16] for i in range(4) for w in wide], axis=0)
     gates = sum(w[64:66] for w in wide)
     o[...] = context_state(
         pos, rows, gates[0:1], gates[1:2], small[0:1], small[1:2], small[2:3]
@@ -460,10 +464,17 @@
         *slow,
     )
     of_y = lax.all_to_all(maps, "y", 0, 0, tiled=True)
-    low = call(low_kernel, ((4, 160, 256), BF), [SM, VM])(pos, of_y)
+    low, rows = call(
+        low_kernel, [((4, 128, 256), BF), ((24, 256), BF)], [SM, VM]
+    )(pos, of_y)
     of_low = lax.all_to_all(low, "zl", 0, 0, tiled=True)
-    high, rows = call(high_kernel, [((128, 256), BF), ((4, 72, 256), BF)], [SM, VM])(pos, of_low)
-    rows = lax.all_to_all(rows, "zh", 0, 0, tiled=True)
+    parts = [rows]
+    for d in range(1, 4):
+        parts.append(lax.ppermute(rows, "zh", [(i, (i + d) % 4) for i in range(4)]))
+    high, rows = call(
+        high_kernel, [((128, 256), BF), ((4, 80, 256), BF)], [SM] + [VM] * 5
+    )(pos, of_low, *parts)
+    rows = lax.all_to_all(rows, "zl", 0, 0, tiled=True)
     of_high = []
     for d in (3, 2, 1):
         of_high.append(lax.ppermute(high, ("zh", "y", "c"), onward(d)))

time: 150 us -> 161 us (1.073)
  starting transfers between devices: 54.4 us -> 72.7 us
  blocking collectives: 39.2 us -> 27.8 us
  waiting for transfers between devices: 30.6 us -> 34.7 us
    ppermute x0 -> x3, starting transfers between devices: none -> 13.5 us  [per_device(): parts.append(lax.ppermute(rows, 'zh', [(i, (i + d) % 4) for i in range(4)]))]
    all_to_all x1 -> x0, blocking collectives: 11.4 us -> none  [per_device(): of_low = lax.all_to_all(low, 'zl', 0, 0, tiled=True)]
    all_to_all x1 -> x2, waiting for transfers between devices: 9.99 us -> 0.79 us  [the longest x1 0.79 us: per_device(): rows = lax.all_to_all(rows, 'zl', 0, 0, tiled=True)]
    ppermute x3, waiting for transfers between devices: 2.94 us -> 10.6 us  [per_device(): of_high.append(lax.ppermute(high, ('zh', 'y', 'c'), onward(d)))]
    ppermute x0 -> x3, waiting for transfers between devices: none -> 5.63 us  [per_device(): parts.append(lax.ppermute(rows, 'zh', [(i, (i + d) % 4) for i in range(4)]))]
    all_to_all x1 -> x2, starting transfers between devices: 4.68 us -> 8.15 us  [the longest x1 4.74 us: per_device(): rows = lax.all_to_all(rows, 'zl', 0, 0, tiled=True)]
  transfers between devices with their start and end apart: 11 -> 15, of which waited for: 5 -> 9; matrix products, arithmetic and copies ran while one was open for 2% -> 2% of each run, Pallas kernels for 3% -> 2%
where the time goes in v7:
time: 161 us
  starting transfers between devices  72.7 us (45%)
  waiting for transfers between devices  34.7 us (22%)
  blocking collectives  27.8 us (17%)
  Pallas kernels  21.9 us (14%)
  local copies, waits for them, and re-layouts  2.17 us (1%)
    all_to_all x2, starting transfers between devices, to_all(): lax.all_to_all(jnp.broadcast_to(value[None], (count, *value.shape)), axes...  23.7 us
    all_to_all x2, waiting for transfers between devices, to_all(): lax.all_to_all(jnp.broadcast_to(value[None], (count, *value.shape)), axes...  16.1 us
    ppermute x3, starting transfers between devices, per_device(): parts.append(lax.ppermute(rows, 'zh', [(i, (i + d) % 4) for i in range(4)]))  13.5 us
    ppermute x3, starting transfers between devices, per_device(): lax.ppermute(latent, 'x', [(i, (i + d) % 4) for i in range(4)])  12.1 us
    all_to_all x1, blocking collectives, per_device(): branch = lax.all_to_all(branch, 'x', 0, 0, tiled=True)  11.5 us
    ppermute x3, waiting for transfers between devices, per_device(): of_high.append(lax.ppermute(high, ('zh', 'y', 'c'), onward(d)))  10.6 us
    pallas_call x1, Pallas kernels, per_device(): call(front_kernel, [((4, 144, 256), BF), ((2, 256, 256), BF), ((256, 256)...  10.4 us
    all_to_all x1, blocking collectives, per_device(): of_y = lax.all_to_all(maps, 'y', 0, 0, tiled=True)  9.04 us
  transfers between devices with their start and end apart: 15, of which 9 were waited for; matrix products, arithmetic and copies ran while one was open for 2% of the time, Pallas kernels for 2%

profile of v7, /device:TPU:1, one launch (start us, length us, event | category | flops | bytes accessed | tf_op | source)
XLA Modules:
  0.0 160.6 jit_solution(6514278620334918748)
XLA Ops:
  0.0 5.6 %collective-permute-start.1 = (bf16[32,2048]{1,0:T(8,128)(2,1)}, bf16[32,2048]{1,0:T(8,128)(2,1)S(1)}, u32[]{:S(2)}, u32[]{:S(2)}) collective-permute-start(bf16[32,2048]{1,0:T(8,128)(2,1)} %lat.1), channel_id=1, source_target_pairs={{0,4},{2,6},{4,0},{6,2},{1,5},{3,7},{5,1},{7,3},{8,12},{10,14},{12... | collective-permute-start | bytes 393224 | tf_op jit(solution)/shard_map/ppermute | solution.py:406
  5.6 2.2 %collective-permute-start = (bf16[32,2048]{1,0:T(8,128)(2,1)}, bf16[32,2048]{1,0:T(8,128)(2,1)S(1)}, u32[]{:S(2)}, u32[]{:S(2)}) collective-permute-start(bf16[32,2048]{1,0:T(8,128)(2,1)} %lat.1), channel_id=1, source_target_pairs={{0,2},{2,4},{4,6},{6,0},{1,3},{3,5},{5,7},{7,1},{8,10},{10,12},{12... | collective-permute-start | bytes 393224 | tf_op jit(solution)/shard_map/ppermute | solution.py:406
  7.8 4.3 %collective-permute-start.2 = (bf16[32,2048]{1,0:T(8,128)(2,1)}, bf16[32,2048]{1,0:T(8,128)(2,1)S(1)}, u32[]{:S(2)}, u32[]{:S(2)}) collective-permute-start(bf16[32,2048]{1,0:T(8,128)(2,1)} %lat.1), channel_id=1, source_target_pairs={{0,6},{2,0},{4,2},{6,4},{1,7},{3,1},{5,3},{7,5},{8,14},{10,8},{12,... | collective-permute-start | bytes 393224 | tf_op jit(solution)/shard_map/ppermute | solution.py:406
  12.1 0.8 divide_multiply_fusion
  12.9 0.1 multiply_reduce_fusion
  13.0 0.1 fusion
  13.1 0.7 broadcast_in_dim.4
  13.8 15.0 %all-to-all-start = ((f32[16,5,256]{2,1,0:T(8,128)}), f32[16,5,256]{2,1,0:T(8,128)S(1)}, u32[]{:S(2)}, u32[]{:S(2)}) async-start(f32[16,5,256]{2,1,0:T(8,128)} %broadcast_in_dim.4), calls=%async_computation | async-start | bytes 262144 | tf_op jit(solution)/shard_map/all_to_all | solution.py:365
  28.8 0.0 collective-permute-done
  28.9 0.0 collective-permute-done.2
  28.9 0.0 copy-start.3
  28.9 0.0 copy-start.4
  28.9 0.1 pad_maximum_fusion.one
  29.0 3.7 %collective-permute-start.3 = (bf16[4,32,2048]{2,1,0:T(8,128)(2,1)S(1)}, bf16[4,32,2048]{2,1,0:T(8,128)(2,1)S(1)}, u32[]{:S(2)}, u32[]{:S(2)}) collective-permute-start(bf16[4,32,2048]{2,1,0:T(8,128)(2,1)S(1)} %pad_maximum_fusion.one), channel_id=1, source_target_pairs={{0,1},{1,0},{2,3},{3,2},{4,5},{5,4},{6,7},{7,6},{8,9},{9,8},{10,11... | collective-permute-start | bytes 1572872 | tf_op jit(solution)/shard_map/ppermute | solution.py:408
  32.7 8.1 %all-to-all-done = f32[16,5,256]{2,1,0:T(8,128)S(1)} async-done(((f32[16,5,256]{2,1,0:T(8,128)}), f32[16,5,256]{2,1,0:T(8,128)S(1)}, u32[]{:S(2)}, u32[]{:S(2)}) %all-to-all-start) | async-done | bytes 81952 | tf_op jit(solution)/shard_map/all_to_all | solution.py:365
  40.8 0.7 broadcast_in_dim.5
  41.5 8.6 %all-to-all-start.1 = ((f32[32,5,256]{2,1,0:T(8,128)}), f32[32,5,256]{2,1,0:T(8,128)S(1)}, u32[]{:S(2)}, u32[]{:S(2)}) async-start(f32[32,5,256]{2,1,0:T(8,128)} %broadcast_in_dim.5), calls=%async_computation.1 | async-start | bytes 524288 | tf_op jit(solution)/shard_map/all_to_all | solution.py:365
  50.2 0.1 stack.74.pos
  50.3 0.7 copy-done.5
  51.0 8.1 %all-to-all-done.1.fac = f32[32,5,256]{2,1,0:T(8,128)S(1)} async-done(((f32[32,5,256]{2,1,0:T(8,128)}), f32[32,5,256]{2,1,0:T(8,128)S(1)}, u32[]{:S(2)}, u32[]{:S(2)}) %all-to-all-start.1) | async-done | bytes 163872 | tf_op jit(solution)/shard_map/all_to_all | solution.py:365
  59.1 10.4 %shard_map.154 = (bf16[4,144,256]{2,1,0:T(8,128)(2,1)S(1)}, bf16[2,256,256]{2,1,0:T(8,128)(2,1)S(1)}, f32[256,256]{1,0:T(8,128)S(1)}) custom-call(s32[8]{0:T(128)S(1)} %stack.74.pos, bf16[4,32,2048]{2,1,0:T(8,128)(2,1)S(1)} %pad_maximum_fusion.one, bf16[4,32,2048]{2,1,0:T(8,128)(2,1)S(1)} %collective-permute-done.3.two, ...), custom_call_target="tpu_custom_call" | custom-call | flops 5000000000 | bytes 1 | tf_op jit(solution)/shard_map/pallas_call | solution.py:452
  69.5 9.0 %all_to_all.35.maps.own = bf16[4,144,256]{2,1,0:T(8,128)(2,1)S(1)} all-to-all(bf16[4,144,256]{2,1,0:T(8,128)(2,1)S(1)} %get-tuple-element.14), channel_id=1, replica_groups=mesh['zh'=4,'zl'=4,'y'=4,'x'=4,'c'=2] {'y'}, dimensions={0} | all-to-all | bytes 589824 | tf_op jit(solution)/shard_map/all_to_all | solution.py:466
  78.5 1.8 %shard_map.155 = (bf16[4,128,256]{2,1,0:T(8,128)(2,1)}, bf16[24,256]{1,0:T(8,128)(2,1)S(1)}) custom-call(s32[8]{0:T(128)S(1)} %stack.74.pos, bf16[4,144,256]{2,1,0:T(8,128)(2,1)S(1)} %all_to_all.35.maps.own), custom_call_target="tpu_custom_call" | custom-call | flops 1 | bytes 1 | tf_op jit(solution)/shard_map/pallas_call | solution.py:467
  80.3 3.4 %all-to-all-start.3 = ((bf16[4,128,256]{2,1,0:T(8,128)(2,1)}), bf16[4,128,256]{2,1,0:T(8,128)(2,1)S(1)}, u32[]{:S(2)}, u32[]{:S(2)}) async-start(bf16[4,128,256]{2,1,0:T(8,128)(2,1)} %get-tuple-element.15), calls=%async_computation.3 | async-start | bytes 524288 | tf_op jit(solution)/shard_map/all_to_all | solution.py:470
  83.7 4.6 %collective-permute-start.6 = (bf16[24,256]{1,0:T(8,128)(2,1)S(1)}, bf16[24,256]{1,0:T(8,128)(2,1)S(1)}, u32[]{:S(2)}, u32[]{:S(2)}) collective-permute-start(bf16[24,256]{1,0:T(8,128)(2,1)S(1)} %get-tuple-element.16.r0), channel_id=1, source_target_pairs={{0,384},{128,0},{256,128},{384,256},{1,385},{129,1},{257,129},{385... | collective-permute-start | bytes 36872 | tf_op jit(solution)/shard_map/ppermute | solution.py:473
  88.3 5.9 %collective-permute-start.5 = (bf16[24,256]{1,0:T(8,128)(2,1)S(1)}, bf16[24,256]{1,0:T(8,128)(2,1)S(1)}, u32[]{:S(2)}, u32[]{:S(2)}) collective-permute-start(bf16[24,256]{1,0:T(8,128)(2,1)S(1)} %get-tuple-element.16.r0), channel_id=1, source_target_pairs={{0,256},{128,384},{256,0},{384,128},{1,257},{129,385},{257,1},{385... | collective-permute-start | bytes 36872 | tf_op jit(solution)/shard_map/ppermute | solution.py:473
  94.3 3.0 %collective-permute-start.4 = (bf16[24,256]{1,0:T(8,128)(2,1)S(1)}, bf16[24,256]{1,0:T(8,128)(2,1)S(1)}, u32[]{:S(2)}, u32[]{:S(2)}) collective-permute-start(bf16[24,256]{1,0:T(8,128)(2,1)S(1)} %get-tuple-element.16.r0), channel_id=1, source_target_pairs={{0,128},{128,256},{256,384},{384,0},{1,129},{129,257},{257,385},{3... | collective-permute-start | bytes 36872 | tf_op jit(solution)/shard_map/ppermute | solution.py:473
  97.3 4.2 %collective-permute-done.5.r2 = bf16[24,256]{1,0:T(8,128)(2,1)S(1)} collective-permute-done((bf16[24,256]{1,0:T(8,128)(2,1)S(1)}, bf16[24,256]{1,0:T(8,128)(2,1)S(1)}, u32[]{:S(2)}, u32[]{:S(2)}) %collective-permute-start.5) | collective-permute-done | bytes 12320 | tf_op jit(solution)/shard_map/ppermute | solution.py:473
  101.5 1.4 collective-permute-done.4.r1
  102.9 1.6 %shard_map.156 = (bf16[128,256]{1,0:T(8,128)(2,1)S(1)}, bf16[4,80,256]{2,1,0:T(8,128)(2,1)}) custom-call(s32[8]{0:T(128)S(1)} %stack.74.pos, bf16[4,128,256]{2,1,0:T(8,128)(2,1)S(1)} %all-to-all-done.3.maps.low, bf16[24,256]{1,0:T(8,128)(2,1)S(1)} %get-tuple-element.16.r0, bf16[24,256]{1,0:T(8,128)(2,1)S(1)} %collective-permute-done.4.r1, ...), custom_call_target="tpu_custom_call" | custom-call | flops 1 | bytes 1 | tf_op jit(solution)/shard_map/pallas_call | solution.py:474
  104.6 4.7 %all-to-all-start.4 = ((bf16[4,80,256]{2,1,0:T(8,128)(2,1)}), bf16[4,80,256]{2,1,0:T(8,128)(2,1)S(1)}, u32[]{:S(2)}, u32[]{:S(2)}) async-start(bf16[4,80,256]{2,1,0:T(8,128)(2,1)} %get-tuple-element.17), calls=%async_computation.4 | async-start | bytes 327680 | tf_op jit(solution)/shard_map/all_to_all | solution.py:477
  109.3 1.3 collective-permute-start.9
  110.6 1.3 collective-permute-start.8
  111.9 1.5 collective-permute-start.7
  113.4 0.8 all-to-all-done.4.all_rows
  114.2 3.8 %shard_map.157.start = f32[128,128]{1,0:T(8,128)S(1)} custom-call(s32[8]{0:T(128)S(1)} %stack.74.pos, bf16[4,80,256]{2,1,0:T(8,128)(2,1)S(1)} %all-to-all-done.4.all_rows, f32[4,128]{1,0:T(4,128)S(1)} %pad_maximum_fusion.2.small.gain), custom_call_target="tpu_custom_call" | custom-call | flops 1000000000 | bytes 1 | tf_op jit(solution)/shard_map/pallas_call | solution.py:481
  118.0 0.0 copy-start
  118.1 0.3 collective-permute-done.9.near
  118.3 6.1 %collective-permute-done.8.middle = bf16[128,256]{1,0:T(8,128)(2,1)S(1)} collective-permute-done((bf16[128,256]{1,0:T(8,128)(2,1)S(1)}, bf16[128,256]{1,0:T(8,128)(2,1)S(1)}, u32[]{:S(2)}, u32[]{:S(2)}) %collective-permute-start.8) | collective-permute-done | bytes 65568 | tf_op jit(solution)/shard_map/ppermute | solution.py:480
  124.4 4.3 %collective-permute-done.7.far = bf16[128,256]{1,0:T(8,128)(2,1)S(1)} collective-permute-done((bf16[128,256]{1,0:T(8,128)(2,1)S(1)}, bf16[128,256]{1,0:T(8,128)(2,1)S(1)}, u32[]{:S(2)}, u32[]{:S(2)}) %collective-permute-start.7) | collective-permute-done | bytes 65568 | tf_op jit(solution)/shard_map/ppermute | solution.py:480
  128.7 1.9 %shard_map.158 = bf16[4,128,128]{2,1,0:T(8,128)(2,1)S(1)} custom-call(s32[8]{0:T(128)S(1)} %stack.74.pos, f32[128,128]{1,0:T(8,128)S(1)} %shard_map.157.start, bf16[128,256]{1,0:T(8,128)(2,1)S(1)} %collective-permute-done.7.far, bf16[128,256]{1,0:T(8,128)(2,1)S(1)} %collective-permute-done.8.middle, bf16[128,256]{1,0:T(8,128)(2,1)S(1)} %collective-permute-done.9.near, ...), custom_call_target="tpu_custom_call" | custom-call | flops 100000000 | bytes 1 | tf_op jit(solution)/shard_map/pallas_call | solution.py:482
  130.6 7.2 %all_to_all.36.states = bf16[4,128,128]{2,1,0:T(8,128)(2,1)S(1)} all-to-all(bf16[4,128,128]{2,1,0:T(8,128)(2,1)S(1)} %shard_map.158), channel_id=1, replica_groups=mesh['zh'=4,'zl'=4,'y'=4,'x'=4,'c'=2] {'y'}, dimensions={0} | all-to-all | bytes 262144 | tf_op jit(solution)/shard_map/all_to_all | solution.py:485
  137.8 1.4 shard_map.159
  139.2 7.5 %collective-permute-start.10 = (bf16[4,32,2048]{2,1,0:T(8,128)(2,1)S(1)}, bf16[4,32,2048]{2,1,0:T(8,128)(2,1)S(1)}, u32[]{:S(2)}, u32[]{:S(2)}) collective-permute-start(bf16[4,32,2048]{2,1,0:T(8,128)(2,1)S(1)} %get-tuple-element.22), channel_id=1, source_target_pairs={{0,1},{1,0},{2,3},{3,2},{4,5},{5,4},{6,7},{7,6},{8,9},{9,8},{10,11... | collective-permute-start | bytes 1572872 | tf_op jit(solution)/shard_map/ppermute | solution.py:489
  146.7 1.5 collective-permute-done.10.got
  148.2 0.1 shard_map.160
  148.4 11.5 %all_to_all.37.rows = bf16[4,32,2048]{2,1,0:T(8,128)(2,1)S(1)} all-to-all(bf16[4,32,2048]{2,1,0:T(8,128)(2,1)S(1)} %shard_map.160), channel_id=1, replica_groups=mesh['zh'=4,'zl'=4,'y'=4,'x'=4,'c'=2] {'x'}, dimensions={0} | all-to-all | bytes 1048576 | tf_op jit(solution)/shard_map/all_to_all | solution.py:491
  159.9 0.8 shard_map.161
  (21 shorter events, 0.1 us)
Async XLA Ops:
  0.0 12.9 %copy-start.2 = (bf16[3,32,256]{2,1,0:T(8,128)(2,1)S(1)}, bf16[3,32,256]{2,1,0:T(8,128)(2,1)}, u32[]{:S(2)}) copy-start(bf16[3,32,256]{2,1,0:T(8,128)(2,1)} %param.20) | copy-start | bytes 147460
  0.0 28.8 %collective-permute-start.1 = (bf16[32,2048]{1,0:T(8,128)(2,1)}, bf16[32,2048]{1,0:T(8,128)(2,1)S(1)}, u32[]{:S(2)}, u32[]{:S(2)}) collective-permute-start(bf16[32,2048]{1,0:T(8,128)(2,1)} %lat.1), channel_id=1, source_target_pairs={{0,4},{2,6},{4,0},{6,2},{1,5},{3,7},{5,1},{7,3},{8,12},{10,14},{12... | collective-permute-start | bytes 393224 | tf_op jit(solution)/shard_map/ppermute | solution.py:406
  5.6 23.2 %collective-permute-start = (bf16[32,2048]{1,0:T(8,128)(2,1)}, bf16[32,2048]{1,0:T(8,128)(2,1)S(1)}, u32[]{:S(2)}, u32[]{:S(2)}) collective-permute-start(bf16[32,2048]{1,0:T(8,128)(2,1)} %lat.1), channel_id=1, source_target_pairs={{0,2},{2,4},{4,6},{6,0},{1,3},{3,5},{5,7},{7,1},{8,10},{10,12},{12... | collective-permute-start | bytes 393224 | tf_op jit(solution)/shard_map/ppermute | solution.py:406
  7.8 21.0 %collective-permute-start.2 = (bf16[32,2048]{1,0:T(8,128)(2,1)}, bf16[32,2048]{1,0:T(8,128)(2,1)S(1)}, u32[]{:S(2)}, u32[]{:S(2)}) collective-permute-start(bf16[32,2048]{1,0:T(8,128)(2,1)} %lat.1), channel_id=1, source_target_pairs={{0,6},{2,0},{4,2},{6,4},{1,7},{3,1},{5,3},{7,5},{8,14},{10,8},{12,... | collective-permute-start | bytes 393224 | tf_op jit(solution)/shard_map/ppermute | solution.py:406
  13.8 15.1 %copy-start.1 = (bf16[32,2048]{1,0:T(8,128)(2,1)S(1)}, bf16[32,2048]{1,0:T(8,128)(2,1)}, u32[]{:S(2)}) copy-start(bf16[32,2048]{1,0:T(8,128)(2,1)} %lat.1) | copy-start | bytes 393220
  13.8 27.0 %all-to-all-start = ((f32[16,5,256]{2,1,0:T(8,128)}), f32[16,5,256]{2,1,0:T(8,128)S(1)}, u32[]{:S(2)}, u32[]{:S(2)}) async-start(f32[16,5,256]{2,1,0:T(8,128)} %broadcast_in_dim.4), calls=%async_computation | async-start | bytes 262144 | tf_op jit(solution)/shard_map/all_to_all | solution.py:365
  28.9 3.8 %copy-start.3 = (f32[32]{0:T(128)S(1)}, f32[32]{0:T(128)}, u32[]{:S(2)}) copy-start(f32[32]{0:T(128)} %param.28) | copy-start | bytes 388
  28.9 3.8 %copy-start.4 = (f32[32]{0:T(128)S(1)}, f32[32]{0:T(128)}, u32[]{:S(2)}) copy-start(f32[32]{0:T(128)} %param.27) | copy-start | bytes 388
  29.0 30.1 %collective-permute-start.3 = (bf16[4,32,2048]{2,1,0:T(8,128)(2,1)S(1)}, bf16[4,32,2048]{2,1,0:T(8,128)(2,1)S(1)}, u32[]{:S(2)}, u32[]{:S(2)}) collective-permute-start(bf16[4,32,2048]{2,1,0:T(8,128)(2,1)S(1)} %pad_maximum_fusion.one), channel_id=1, source_target_pairs={{0,1},{1,0},{2,3},{3,2},{4,5},{5,4},{6,7},{7,6},{8,9},{9,8},{10,11... | collective-permute-start | bytes 1572872 | tf_op jit(solution)/shard_map/ppermute | solution.py:408
  41.5 8.7 %copy-start.6 = (f32[32]{0:T(128)S(1)}, f32[32]{0:T(128)}, u32[]{:S(2)}) copy-start(f32[32]{0:T(128)} %param.26) | copy-start | bytes 388
  41.5 17.5 %all-to-all-start.1 = ((f32[32,5,256]{2,1,0:T(8,128)}), f32[32,5,256]{2,1,0:T(8,128)S(1)}, u32[]{:S(2)}, u32[]{:S(2)}) async-start(f32[32,5,256]{2,1,0:T(8,128)} %broadcast_in_dim.5), calls=%async_computation.1 | async-start | bytes 524288 | tf_op jit(solution)/shard_map/all_to_all | solution.py:365
  50.3 0.7 copy-start.5
  80.3 22.6 %all-to-all-start.3 = ((bf16[4,128,256]{2,1,0:T(8,128)(2,1)}), bf16[4,128,256]{2,1,0:T(8,128)(2,1)S(1)}, u32[]{:S(2)}, u32[]{:S(2)}) async-start(bf16[4,128,256]{2,1,0:T(8,128)(2,1)} %get-tuple-element.15), calls=%async_computation.3 | async-start | bytes 524288 | tf_op jit(solution)/shard_map/all_to_all | solution.py:470
  83.7 13.6 %collective-permute-start.6 = (bf16[24,256]{1,0:T(8,128)(2,1)S(1)}, bf16[24,256]{1,0:T(8,128)(2,1)S(1)}, u32[]{:S(2)}, u32[]{:S(2)}) collective-permute-start(bf16[24,256]{1,0:T(8,128)(2,1)S(1)} %get-tuple-element.16.r0), channel_id=1, source_target_pairs={{0,384},{128,0},{256,128},{384,256},{1,385},{129,1},{257,129},{385... | collective-permute-start | bytes 36872 | tf_op jit(solution)/shard_map/ppermute | solution.py:473
  88.3 13.2 %collective-permute-start.5 = (bf16[24,256]{1,0:T(8,128)(2,1)S(1)}, bf16[24,256]{1,0:T(8,128)(2,1)S(1)}, u32[]{:S(2)}, u32[]{:S(2)}) collective-permute-start(bf16[24,256]{1,0:T(8,128)(2,1)S(1)} %get-tuple-element.16.r0), channel_id=1, source_target_pairs={{0,256},{128,384},{256,0},{384,128},{1,257},{129,385},{257,1},{385... | collective-permute-start | bytes 36872 | tf_op jit(solution)/shard_map/ppermute | solution.py:473
  94.3 8.6 %collective-permute-start.4 = (bf16[24,256]{1,0:T(8,128)(2,1)S(1)}, bf16[24,256]{1,0:T(8,128)(2,1)S(1)}, u32[]{:S(2)}, u32[]{:S(2)}) collective-permute-start(bf16[24,256]{1,0:T(8,128)(2,1)S(1)} %get-tuple-element.16.r0), channel_id=1, source_target_pairs={{0,128},{128,256},{256,384},{384,0},{1,129},{129,257},{257,385},{3... | collective-permute-start | bytes 36872 | tf_op jit(solution)/shard_map/ppermute | solution.py:473
  104.6 9.6 %all-to-all-start.4 = ((bf16[4,80,256]{2,1,0:T(8,128)(2,1)}), bf16[4,80,256]{2,1,0:T(8,128)(2,1)S(1)}, u32[]{:S(2)}, u32[]{:S(2)}) async-start(bf16[4,80,256]{2,1,0:T(8,128)(2,1)} %get-tuple-element.17), calls=%async_computation.4 | async-start | bytes 327680 | tf_op jit(solution)/shard_map/all_to_all | solution.py:477
  109.3 9.0 %collective-permute-start.9 = (bf16[128,256]{1,0:T(8,128)(2,1)S(1)}, bf16[128,256]{1,0:T(8,128)(2,1)S(1)}, u32[]{:S(2)}, u32[]{:S(2)}) collective-permute-start(bf16[128,256]{1,0:T(8,128)(2,1)S(1)} %get-tuple-element.18), channel_id=1, source_target_pairs={{0,128},{9,137},{16,144},{25,153},{128,256},{129,1},{136,8},{137,2... | collective-permute-start | bytes 196616 | tf_op jit(solution)/shard_map/ppermute | solution.py:480
  110.6 13.8 %collective-permute-start.8 = (bf16[128,256]{1,0:T(8,128)(2,1)S(1)}, bf16[128,256]{1,0:T(8,128)(2,1)S(1)}, u32[]{:S(2)}, u32[]{:S(2)}) collective-permute-start(bf16[128,256]{1,0:T(8,128)(2,1)S(1)} %get-tuple-element.18), channel_id=1, source_target_pairs={{0,256},{9,265},{16,272},{25,281},{128,384},{137,393},{144,400},{1... | collective-permute-start | bytes 196616 | tf_op jit(solution)/shard_map/ppermute | solution.py:480
  111.9 16.7 %collective-permute-start.7 = (bf16[128,256]{1,0:T(8,128)(2,1)S(1)}, bf16[128,256]{1,0:T(8,128)(2,1)S(1)}, u32[]{:S(2)}, u32[]{:S(2)}) collective-permute-start(bf16[128,256]{1,0:T(8,128)(2,1)S(1)} %get-tuple-element.18), channel_id=1, source_target_pairs={{0,384},{9,393},{16,400},{25,409},{385,1},{392,8},{401,17},{408,24... | collective-permute-start | bytes 196616 | tf_op jit(solution)/shard_map/ppermute | solution.py:480
  118.0 19.8 %copy-start = (bf16[256,2048]{1,0:T(8,128)(2,1)S(1)}, bf16[256,2048]{1,0:T(8,128)(2,1)}, u32[]{:S(2)}) copy-start(bf16[256,2048]{1,0:T(8,128)(2,1)} %weight.1) | copy-start | bytes 3145732
  139.2 9.0 %collective-permute-start.10 = (bf16[4,32,2048]{2,1,0:T(8,128)(2,1)S(1)}, bf16[4,32,2048]{2,1,0:T(8,128)(2,1)S(1)}, u32[]{:S(2)}, u32[]{:S(2)}) collective-permute-start(bf16[4,32,2048]{2,1,0:T(8,128)(2,1)S(1)} %get-tuple-element.22), channel_id=1, source_target_pairs={{0,1},{1,0},{2,3},{3,2},{4,5},{5,4},{6,7},{7,6},{8,9},{9,8},{10,11... | collective-permute-start | bytes 1572872 | tf_op jit(solution)/shard_map/ppermute | solution.py:489

commit v8 on v6

--- a/solution.py
+++ b/solution.py
@@ -90,12 +90,12 @@
 
 
 def front_kernel(
-    pos, one, two, fac, small, ctx_h, wq_h, wk_h, wv_h, wd_h, ww_h, spike_h,
+    pos, one, two, fac, small, ctx, wq_h, wk_h, wv_h, wd_h, ww_h, spike_h,
     m_o, r_o, o_o,
-    hid, packed, ctx, wq, wk, wv, wd, ww, spike, sems,
+    hid, packed, wq, wk, wv, wd, ww, spike, sems,
 ):
     copies = start_copies(
-        (ctx_h, wq_h, wk_h, wv_h, wd_h, ww_h, spike_h), (ctx, wq, wk, wv, wd, ww, spike), sems
+        (wq_h, wk_h, wv_h, wd_h, ww_h, spike_h), (wq, wk, wv, wd, ww, spike), sems
     )
     shift, scale = (factor(fac, 0), factor(fac, 1))
     for d in range(4):
@@ -103,37 +103,36 @@
             core = pos[6] if i == 0 else 1 - pos[6]
             spot = (2 * ((pos[7] + 4 - d) % 4) + core) * 32
             hid[pl.ds(pl.multiple_of(spot, 32), 32)] = norm_rows(lat[d], scale, shift)
+    hid[256:320] = norm_rows(ctx[...], factor(fac, 4), factor(fac, 3))
+    rows = hid[...]
     copies[0].wait()
-    hid[256:260] = norm_rows(ctx[...], factor(fac, 4), factor(fac, 3))
-    hid[260:272] = jnp.zeros((12, D), BF)
-    rows = hid[...]
+    packed[0:256] = mm(hid[0:256], wq[...]).astype(BF)
     copies[1].wait()
-    packed[0:256] = mm(hid[0:256], wq[...]).astype(BF)
-    copies[2].wait()
     keys = mm(rows, wk[...]).astype(BF)
     packed[256:512] = keys[:256]
-    for copy in copies[3:]:
+    for copy in copies[2:]:
         copy.wait()
     values = mm(rows, wv[...]).astype(BF)
     packed[512:768] = values[:256]
     packed[768:800] = mm(wd[...], hid[0:256], ((1,), (1,))).astype(BF)
     packed[800:832] = mm(ww[...], hid[0:256], ((1,), (1,))).astype(BF)
-    rate = mm(hid[256:272], wd[...], ((1,), (1,))).astype(BF).astype(F32)
-    write = mm(hid[256:272], ww[...], ((1,), (1,))).astype(BF).astype(F32)
-    lanes = lax.broadcasted_iota(jnp.int32, (16, 256), 1)
-    rank = lax.broadcasted_iota(jnp.int32, (16, 256), 0)
-    spots = (lanes == rank + pos[5]) & (rank < 4)
-    wide = [side[256:272].astype(F32)[0:4] for side in (keys, values)]
+    rate = mm(hid[256:320], wd[...], ((1,), (1,))).astype(BF).astype(F32)
+    write = mm(hid[256:320], ww[...], ((1,), (1,))).astype(BF).astype(F32)
+    lanes = lax.broadcasted_iota(jnp.int32, (64, 256), 1)
+    rank = lax.broadcasted_iota(jnp.int32, (64, 256), 0)
+    spots = lanes == (rank // 4) * 16 + rank % 4 + pos[5]
     for j in range(4):
         h = j // 2
         lane = pos[1] * 4 + j
-        pieces = [jnp.concatenate([w[:, 128 * h : 128 * h + 128] for w in wide], axis=1)]
-        pieces += [
+        to = (j + pos[4]) % 4
+        m_o[to, 128:192, 0:128] = keys[256:320, 128 * h : 128 * h + 128]
+        m_o[to, 128:192, 128:256] = values[256:320, 128 * h : 128 * h + 128]
+        pieces = [
             jnp.sum(jnp.where(spots, column(g, lane), 0.0), axis=0, keepdims=True)
             for g in (rate, write)
         ]
-        pieces.append(jnp.zeros((10, 256), F32))
-        m_o[(j + pos[4]) % 4, 128:144] = jnp.concatenate(pieces, axis=0).astype(BF)
+        pieces.append(jnp.zeros((14, 256), F32))
+        m_o[to, 192:208] = jnp.concatenate(pieces, axis=0).astype(BF)
     chunk(pos, packed, spike, small, m_o, r_o, o_o)
 
 
@@ -253,28 +252,18 @@
 
 
 def low_kernel(pos, maps, o):
-    total = composed(pos, maps)
-    wide = [maps[i][128:].astype(F32) for i in range(4)]
-    parts = [w[0:4] for w in wide]
-    parts += [sum(w[4:6] for w in wide), jnp.zeros((14, 256), F32)]
-    out = jnp.concatenate([total, *parts], axis=0).astype(BF)
+    out = composed(pos, maps).astype(BF)
     for i in range(4):
         o[i] = out
 
 
-def high_kernel(pos, maps, o, rows):
+def high_kernel(pos, maps, o):
+    o[...] = composed(pos, maps).astype(BF)
+
+
+def context_kernel(pos, maps, small, o):
     wide = [maps[i][128:].astype(F32) for i in range(4)]
-    parts = [w[0:16] for w in wide]
-    parts += [sum(w[16:18] for w in wide), jnp.zeros((6, 256), F32)]
-    out = jnp.concatenate(parts, axis=0).astype(BF)
-    for i in range(4):
-        rows[i] = out
-    o[...] = composed(pos, maps).astype(BF)
-
-
-def context_kernel(pos, all_rows, small, o):
-    wide = [all_rows[i].astype(F32) for i in range(4)]
-    rows = jnp.concatenate([w[0:64] for w in wide], axis=0)
+    rows = jnp.concatenate([w[4 * i : 4 * i + 4] for i in range(16) for w in wide], axis=0)
     gates = sum(w[64:66] for w in wide)
     o[...] = context_state(
         pos, rows, gates[0:1], gates[1:2], small[0:1], small[1:2], small[2:3]
@@ -395,7 +384,7 @@
     zh, zl, y = (lax.axis_index("zh"), lax.axis_index("zl"), lax.axis_index("y"))
     x, c = (lax.axis_index("x"), lax.axis_index("c"))
     sp_index = lax.axis_index(SP)
-    pos = jnp.stack([(y + c) % 4, x * 2 + c, zh, zl, (4 - c) % 4, sp_index * 4, c, x])
+    pos = jnp.stack([(y + c) % 4, x * 2 + c, zh, zl, (4 - c) % 4, y * 4, c, x])
     pos = pos.astype(jnp.int32)
     parts = [latent]
     for d in range(1, 4):
@@ -411,8 +400,18 @@
             jnp.sum(mod[:2] * signals[1][None, :, None], axis=1),
         ]
     )
-    part = to_all(part, Z, 16)
-    part = jnp.sum(part, axis=0)
+    high = lax.reduce_precision(part, 8, 7)
+    sent = jnp.concatenate(
+        [
+            high.astype(BF),
+            (part - high).astype(BF),
+            jnp.zeros((6, 256), BF),
+            context.reshape(32, 256),
+        ]
+    )
+    sent = to_all(sent, Z, 16)
+    part = jnp.sum(sent[:, 0:5].astype(F32) + sent[:, 5:10].astype(F32), axis=0)
+    ctx = sent[:, 16:48].reshape(64, D)
     fac = to_all(part, ("y", "x", "c"), 32)
 
     small = jnp.stack(
@@ -426,7 +425,6 @@
     slow = [
         pltpu.with_memory_space_constraint(a, pltpu.HBM)
         for a in (
-            context,
             query_matrix,
             key_matrix,
             value_matrix,
@@ -436,20 +434,19 @@
         )
     ]
     room = [
-        pltpu.VMEM((4, D), BF),
         pltpu.VMEM((D, 256), BF),
         pltpu.VMEM((D, 256), BF),
         pltpu.VMEM((D, 256), BF),
         pltpu.VMEM((32, D), BF),
         pltpu.VMEM((32, D), BF),
         pltpu.VMEM((32, 256), F32),
-        pltpu.SemaphoreType.DMA((7,)),
+        pltpu.SemaphoreType.DMA((6,)),
     ]
     maps, reads, base = call(
         front_kernel,
-        [((4, 144, 256), BF), ((2, 256, 256), BF), ((256, 256), F32)],
-        [SM] + [VM] * 4 + [HB] * 7,
-        [pltpu.VMEM((272, D), BF), pltpu.VMEM((832, 256), BF), *room],
+        [((4, 208, 256), BF), ((2, 256, 256), BF), ((256, 256), F32)],
+        [SM] + [VM] * 5 + [HB] * 6,
+        [pltpu.VMEM((320, D), BF), pltpu.VMEM((832, 256), BF), *room],
         flops=5 * 10**9,
     )(
         pos,
@@ -457,17 +454,17 @@
         other,
         fac,
         small,
+        ctx,
         *slow,
     )
     of_y = lax.all_to_all(maps, "y", 0, 0, tiled=True)
-    low = call(low_kernel, ((4, 160, 256), BF), [SM, VM])(pos, of_y)
+    low = call(low_kernel, ((4, 128, 256), BF), [SM, VM])(pos, of_y)
     of_low = lax.all_to_all(low, "zl", 0, 0, tiled=True)
-    high, rows = call(high_kernel, [((128, 256), BF), ((4, 72, 256), BF)], [SM, VM])(pos, of_low)
-    rows = lax.all_to_all(rows, "zh", 0, 0, tiled=True)
+    high = call(high_kernel, ((128, 256), BF), [SM, VM])(pos, of_low)
     of_high = []
     for d in (3, 2, 1):
         of_high.append(lax.ppermute(high, ("zh", "y", "c"), onward(d)))
-    start = call(context_kernel, ((128, 128), F32), [SM] + [VM] * 2, flops=10**9)(pos, rows, small)
+    start = call(context_kernel, ((128, 128), F32), [SM] + [VM] * 2, flops=10**9)(pos, of_y, small)
     states = call(scan_kernel, ((4, 128, 128), BF), [SM] + [VM] * 6, flops=10**8)(
         pos, start, *of_high, of_low, of_y
     )

time: 150 us -> 145 us (0.967)
  waiting for transfers between devices: 30.6 us -> 23.2 us
  starting transfers between devices: 54.4 us -> 56.1 us
    all_to_all x1 -> x0, waiting for transfers between devices: 9.99 us -> none  [per_device(): rows = lax.all_to_all(rows, 'zh', 0, 0, tiled=True)]
    ppermute x3, waiting for transfers between devices: 2.94 us -> 11.3 us  [per_device(): of_high.append(lax.ppermute(high, ('zh', 'y', 'c'), onward(d)))]
    all_to_all x2, waiting for transfers between devices: 16.1 us -> 8.51 us  [to_all(): lax.all_to_all(jnp.broadcast_to(value[None], (count, *value.shape)), axes...]
    all_to_all x2, starting transfers between devices: 23.7 us -> 29.7 us  [to_all(): lax.all_to_all(jnp.broadcast_to(value[None], (count, *value.shape)), axes...]
    all_to_all x1 -> x0, starting transfers between devices: 4.68 us -> none  [per_device(): rows = lax.all_to_all(rows, 'zh', 0, 0, tiled=True)]
    ppermute x3, waiting for transfers between devices: 0.01 us -> 1.92 us  [per_device(): lax.ppermute(latent, 'x', [(i, (i + d) % 4) for i in range(4)])]
    all_to_all x1, blocking collectives: 11.4 us -> 9.63 us  [per_device(): of_low = lax.all_to_all(low, 'zl', 0, 0, tiled=True)]
  transfers between devices with their start and end apart: 11 -> 10, of which waited for: 5 -> 8; matrix products, arithmetic and copies ran while one was open for 2% -> 1% of each run, Pallas kernels for 3% -> 3%
where the time goes in v8:
time: 145 us; the launch traced here: 144 us
  starting transfers between devices  56.1 us (39%)
  blocking collectives  38.8 us (27%)
  waiting for transfers between devices  23.2 us (16%)
  Pallas kernels  21.2 us (15%)
  local copies, waits for them, and re-layouts  3.2 us (2%)
    all_to_all x2, starting transfers between devices, to_all(): lax.all_to_all(jnp.broadcast_to(value[None], (count, *value.shape)), axes...  29.7 us
    all_to_all x1, blocking collectives, per_device(): branch = lax.all_to_all(branch, 'x', 0, 0, tiled=True)  11.5 us
    ppermute x3, waiting for transfers between devices, per_device(): of_high.append(lax.ppermute(high, ('zh', 'y', 'c'), onward(d)))  11.3 us
    ppermute x3, starting transfers between devices, per_device(): lax.ppermute(latent, 'x', [(i, (i + d) % 4) for i in range(4)])  11.1 us
    pallas_call x1, Pallas kernels, per_device(): call(front_kernel, [((4, 208, 256), BF), ((2, 256, 256), BF), ((256, 256)...  10.9 us
    all_to_all x1, blocking collectives, per_device(): of_y = lax.all_to_all(maps, 'y', 0, 0, tiled=True)  10.4 us
    all_to_all x1, blocking collectives, per_device(): of_low = lax.all_to_all(low, 'zl', 0, 0, tiled=True)  9.63 us
    all_to_all x2, waiting for transfers between devices, to_all(): lax.all_to_all(jnp.broadcast_to(value[None], (count, *value.shape)), axes...  8.51 us
  transfers between devices with their start and end apart: 10, of which 8 were waited for; matrix products, arithmetic and copies ran while one was open for 1% of the time, Pallas kernels for 3%

profile of v8, /device:TPU:1, one launch (start us, length us, event | category | flops | bytes accessed | tf_op | source)
XLA Modules:
  0.0 143.9 jit_solution(755053268320110792)
XLA Ops:
  0.0 0.8 divide_multiply_fusion
  0.8 0.1 copy-done.2
  0.8 0.0 copy-start.3
  0.9 0.1 multiply_reduce_fusion
  0.9 0.6 copy-done.3
  1.6 0.1 pad.19.clone
  1.7 0.1 fusion
  1.8 0.1 pad_maximum_fusion.1
  1.9 0.8 broadcast_in_dim.7
  2.6 15.9 %all-to-all-start = ((bf16[16,48,256]{2,1,0:T(8,128)(2,1)}), bf16[16,48,256]{2,1,0:T(8,128)(2,1)S(1)}, u32[]{:S(2)}, u32[]{:S(2)}) async-start(bf16[16,48,256]{2,1,0:T(8,128)(2,1)} %broadcast_in_dim.7), calls=%async_computation | async-start | bytes 786432 | tf_op jit(solution)/shard_map/all_to_all | solution.py:350
  18.5 0.0 copy-done.1
  18.5 4.7 %collective-permute-start.1 = (bf16[32,2048]{1,0:T(8,128)(2,1)S(1)}, bf16[32,2048]{1,0:T(8,128)(2,1)S(1)}, u32[]{:S(2)}, u32[]{:S(2)}) collective-permute-start(bf16[32,2048]{1,0:T(8,128)(2,1)S(1)} %copy-done.1), channel_id=1, source_target_pairs={{0,4},{2,6},{4,0},{6,2},{1,5},{3,7},{5,1},{7,3},{8,12},{10,14},{12... | collective-permute-start | bytes 393224 | tf_op jit(solution)/shard_map/ppermute | solution.py:391
  23.2 2.2 %collective-permute-start = (bf16[32,2048]{1,0:T(8,128)(2,1)S(1)}, bf16[32,2048]{1,0:T(8,128)(2,1)S(1)}, u32[]{:S(2)}, u32[]{:S(2)}) collective-permute-start(bf16[32,2048]{1,0:T(8,128)(2,1)S(1)} %copy-done.1), channel_id=1, source_target_pairs={{0,2},{2,4},{4,6},{6,0},{1,3},{3,5},{5,7},{7,1},{8,10},{10,12},{12... | collective-permute-start | bytes 393224 | tf_op jit(solution)/shard_map/ppermute | solution.py:391
  25.4 4.3 %collective-permute-start.2 = (bf16[32,2048]{1,0:T(8,128)(2,1)S(1)}, bf16[32,2048]{1,0:T(8,128)(2,1)S(1)}, u32[]{:S(2)}, u32[]{:S(2)}) collective-permute-start(bf16[32,2048]{1,0:T(8,128)(2,1)S(1)} %copy-done.1), channel_id=1, source_target_pairs={{0,6},{2,0},{4,2},{6,4},{1,7},{3,1},{5,3},{7,5},{8,14},{10,8},{12,... | collective-permute-start | bytes 393224 | tf_op jit(solution)/shard_map/ppermute | solution.py:391
  29.7 0.0 collective-permute-done.1
  29.7 0.4 collective-permute-done
  30.1 1.5 %collective-permute-done.2 = bf16[32,2048]{1,0:T(8,128)(2,1)S(1)} collective-permute-done((bf16[32,2048]{1,0:T(8,128)(2,1)S(1)}, bf16[32,2048]{1,0:T(8,128)(2,1)S(1)}, u32[]{:S(2)}, u32[]{:S(2)}) %collective-permute-start.2) | collective-permute-done | bytes 131104 | tf_op jit(solution)/shard_map/ppermute | solution.py:391
  31.6 0.1 pad_maximum_fusion.one
  31.7 4.3 %collective-permute-start.3 = (bf16[4,32,2048]{2,1,0:T(8,128)(2,1)S(1)}, bf16[4,32,2048]{2,1,0:T(8,128)(2,1)S(1)}, u32[]{:S(2)}, u32[]{:S(2)}) collective-permute-start(bf16[4,32,2048]{2,1,0:T(8,128)(2,1)S(1)} %pad_maximum_fusion.one), channel_id=1, source_target_pairs={{0,1},{1,0},{2,3},{3,2},{4,5},{5,4},{6,7},{7,6},{8,9},{9,8},{10,11... | collective-permute-start | bytes 1572872 | tf_op jit(solution)/shard_map/ppermute | solution.py:393
  36.0 0.6 all-to-all-done
  36.7 0.7 broadcast_in_dim.8
  37.4 13.9 %all-to-all-start.1 = ((f32[32,5,256]{2,1,0:T(8,128)}), f32[32,5,256]{2,1,0:T(8,128)S(1)}, u32[]{:S(2)}, u32[]{:S(2)}) async-start(f32[32,5,256]{2,1,0:T(8,128)} %broadcast_in_dim.8), calls=%async_computation.1 | async-start | bytes 524288 | tf_op jit(solution)/shard_map/all_to_all | solution.py:350
  51.3 0.1 stack.74.pos
  51.4 0.7 copy-done.6
  52.1 0.1 reshape.11.ctx
  52.2 0.0 collective-permute-done.3.two
  52.2 7.9 %all-to-all-done.1.fac = f32[32,5,256]{2,1,0:T(8,128)S(1)} async-done(((f32[32,5,256]{2,1,0:T(8,128)}), f32[32,5,256]{2,1,0:T(8,128)S(1)}, u32[]{:S(2)}, u32[]{:S(2)}) %all-to-all-start.1) | async-done | bytes 163872 | tf_op jit(solution)/shard_map/all_to_all | solution.py:350
  60.1 10.9 %shard_map.154 = (bf16[4,208,256]{2,1,0:T(8,128)(2,1)S(1)}, bf16[2,256,256]{2,1,0:T(8,128)(2,1)S(1)}, f32[256,256]{1,0:T(8,128)S(1)}) custom-call(s32[8]{0:T(128)S(1)} %stack.74.pos, bf16[4,32,2048]{2,1,0:T(8,128)(2,1)S(1)} %pad_maximum_fusion.one, bf16[4,32,2048]{2,1,0:T(8,128)(2,1)S(1)} %collective-permute-done.3.two, ...), custom_call_target="tpu_custom_call" | custom-call | flops 5000000000 | bytes 1 | tf_op jit(solution)/shard_map/pallas_call | solution.py:445
  71.1 10.4 %all_to_all.30.maps.own = bf16[4,208,256]{2,1,0:T(8,128)(2,1)S(1)} all-to-all(bf16[4,208,256]{2,1,0:T(8,128)(2,1)S(1)} %get-tuple-element.10), channel_id=1, replica_groups=mesh['zh'=4,'zl'=4,'y'=4,'x'=4,'c'=2] {'y'}, dimensions={0} | all-to-all | bytes 851968 | tf_op jit(solution)/shard_map/all_to_all | solution.py:460
  81.5 1.1 shard_map.156
  82.6 9.6 %all_to_all.31.maps.low = bf16[4,128,256]{2,1,0:T(8,128)(2,1)S(1)} all-to-all(bf16[4,128,256]{2,1,0:T(8,128)(2,1)S(1)} %shard_map.156), channel_id=1, replica_groups=mesh['zh'=4,'zl'=4,'y'=4,'x'=4,'c'=2] {'zl'}, dimensions={0} | all-to-all | bytes 524288 | tf_op jit(solution)/shard_map/all_to_all | solution.py:462
  92.2 1.1 shard_map.157
  93.3 1.3 collective-permute-start.6
  94.6 1.3 collective-permute-start.5
  95.9 1.5 %collective-permute-start.4 = (bf16[128,256]{1,0:T(8,128)(2,1)S(1)}, bf16[128,256]{1,0:T(8,128)(2,1)S(1)}, u32[]{:S(2)}, u32[]{:S(2)}) collective-permute-start(bf16[128,256]{1,0:T(8,128)(2,1)S(1)} %shard_map.157), channel_id=1, source_target_pairs={{0,384},{9,393},{16,400},{25,409},{385,1},{392,8},{401,17},{408,24... | collective-permute-start | bytes 196616 | tf_op jit(solution)/shard_map/ppermute | solution.py:466
  97.4 3.9 %shard_map.155.start = f32[128,128]{1,0:T(8,128)S(1)} custom-call(s32[8]{0:T(128)S(1)} %stack.74.pos, bf16[4,208,256]{2,1,0:T(8,128)(2,1)S(1)} %all_to_all.30.maps.own, f32[4,128]{1,0:T(4,128)S(1)} %pad_maximum_fusion.3.small.gain), custom_call_target="tpu_custom_call" | custom-call | flops 1000000000 | bytes 1 | tf_op jit(solution)/shard_map/pallas_call | solution.py:467
  101.3 0.0 copy-start
  101.3 1.0 collective-permute-done.6.near
  102.3 8.9 %collective-permute-done.5.middle = bf16[128,256]{1,0:T(8,128)(2,1)S(1)} collective-permute-done((bf16[128,256]{1,0:T(8,128)(2,1)S(1)}, bf16[128,256]{1,0:T(8,128)(2,1)S(1)}, u32[]{:S(2)}, u32[]{:S(2)}) %collective-permute-start.5) | collective-permute-done | bytes 65568 | tf_op jit(solution)/shard_map/ppermute | solution.py:466
  111.1 1.4 %collective-permute-done.4.far = bf16[128,256]{1,0:T(8,128)(2,1)S(1)} collective-permute-done((bf16[128,256]{1,0:T(8,128)(2,1)S(1)}, bf16[128,256]{1,0:T(8,128)(2,1)S(1)}, u32[]{:S(2)}, u32[]{:S(2)}) %collective-permute-start.4) | collective-permute-done | bytes 65568 | tf_op jit(solution)/shard_map/ppermute | solution.py:466
  112.6 1.9 %shard_map.158 = bf16[4,128,128]{2,1,0:T(8,128)(2,1)S(1)} custom-call(s32[8]{0:T(128)S(1)} %stack.74.pos, f32[128,128]{1,0:T(8,128)S(1)} %shard_map.155.start, bf16[128,256]{1,0:T(8,128)(2,1)S(1)} %collective-permute-done.4.far, bf16[128,256]{1,0:T(8,128)(2,1)S(1)} %collective-permute-done.5.middle, bf16[128,256]{1,0:T(8,128)(2,1)S(1)} %collective-permute-done.6.near, ...), custom_call_target="tpu_custom_call" | custom-call | flops 100000000 | bytes 1 | tf_op jit(solution)/shard_map/pallas_call | solution.py:468
  114.5 7.2 %all_to_all.32.states = bf16[4,128,128]{2,1,0:T(8,128)(2,1)S(1)} all-to-all(bf16[4,128,128]{2,1,0:T(8,128)(2,1)S(1)} %shard_map.158), channel_id=1, replica_groups=mesh['zh'=4,'zl'=4,'y'=4,'x'=4,'c'=2] {'y'}, dimensions={0} | all-to-all | bytes 262144 | tf_op jit(solution)/shard_map/all_to_all | solution.py:471
  121.7 1.3 shard_map.159
  123.1 6.9 %collective-permute-start.7 = (bf16[4,32,2048]{2,1,0:T(8,128)(2,1)S(1)}, bf16[4,32,2048]{2,1,0:T(8,128)(2,1)S(1)}, u32[]{:S(2)}, u32[]{:S(2)}) collective-permute-start(bf16[4,32,2048]{2,1,0:T(8,128)(2,1)S(1)} %get-tuple-element.14), channel_id=1, source_target_pairs={{0,1},{1,0},{2,3},{3,2},{4,5},{5,4},{6,7},{7,6},{8,9},{9,8},{10,11... | collective-permute-start | bytes 1572872 | tf_op jit(solution)/shard_map/ppermute | solution.py:475
  130.0 1.5 %collective-permute-done.7.got = bf16[4,32,2048]{2,1,0:T(8,128)(2,1)S(1)} collective-permute-done((bf16[4,32,2048]{2,1,0:T(8,128)(2,1)S(1)}, bf16[4,32,2048]{2,1,0:T(8,128)(2,1)S(1)}, u32[]{:S(2)}, u32[]{:S(2)}) %collective-permute-start.7) | collective-permute-done | bytes 524320 | tf_op jit(solution)/shard_map/ppermute | solution.py:475
  131.5 0.1 shard_map.160
  131.6 11.5 %all_to_all.33.rows = bf16[4,32,2048]{2,1,0:T(8,128)(2,1)S(1)} all-to-all(bf16[4,32,2048]{2,1,0:T(8,128)(2,1)S(1)} %shard_map.160), channel_id=1, replica_groups=mesh['zh'=4,'zl'=4,'y'=4,'x'=4,'c'=2] {'x'}, dimensions={0} | all-to-all | bytes 1048576 | tf_op jit(solution)/shard_map/all_to_all | solution.py:477
  143.2 0.8 shard_map.161
  (20 shorter events, 0.1 us)
Async XLA Ops:
  0.0 0.8 copy-start.2
  0.8 0.7 copy-start.3
  2.6 15.9 %copy-start.1 = (bf16[32,2048]{1,0:T(8,128)(2,1)S(1)}, bf16[32,2048]{1,0:T(8,128)(2,1)}, u32[]{:S(2)}) copy-start(bf16[32,2048]{1,0:T(8,128)(2,1)} %lat.1) | copy-start | bytes 393220
  2.6 34.0 %all-to-all-start = ((bf16[16,48,256]{2,1,0:T(8,128)(2,1)}), bf16[16,48,256]{2,1,0:T(8,128)(2,1)S(1)}, u32[]{:S(2)}, u32[]{:S(2)}) async-start(bf16[16,48,256]{2,1,0:T(8,128)(2,1)} %broadcast_in_dim.7), calls=%async_computation | async-start | bytes 786432 | tf_op jit(solution)/shard_map/all_to_all | solution.py:350
  18.5 11.2 %collective-permute-start.1 = (bf16[32,2048]{1,0:T(8,128)(2,1)S(1)}, bf16[32,2048]{1,0:T(8,128)(2,1)S(1)}, u32[]{:S(2)}, u32[]{:S(2)}) collective-permute-start(bf16[32,2048]{1,0:T(8,128)(2,1)S(1)} %copy-done.1), channel_id=1, source_target_pairs={{0,4},{2,6},{4,0},{6,2},{1,5},{3,7},{5,1},{7,3},{8,12},{10,14},{12... | collective-permute-start | bytes 393224 | tf_op jit(solution)/shard_map/ppermute | solution.py:391
  23.2 6.9 %collective-permute-start = (bf16[32,2048]{1,0:T(8,128)(2,1)S(1)}, bf16[32,2048]{1,0:T(8,128)(2,1)S(1)}, u32[]{:S(2)}, u32[]{:S(2)}) collective-permute-start(bf16[32,2048]{1,0:T(8,128)(2,1)S(1)} %copy-done.1), channel_id=1, source_target_pairs={{0,2},{2,4},{4,6},{6,0},{1,3},{3,5},{5,7},{7,1},{8,10},{10,12},{12... | collective-permute-start | bytes 393224 | tf_op jit(solution)/shard_map/ppermute | solution.py:391
  25.4 6.2 %collective-permute-start.2 = (bf16[32,2048]{1,0:T(8,128)(2,1)S(1)}, bf16[32,2048]{1,0:T(8,128)(2,1)S(1)}, u32[]{:S(2)}, u32[]{:S(2)}) collective-permute-start(bf16[32,2048]{1,0:T(8,128)(2,1)S(1)} %copy-done.1), channel_id=1, source_target_pairs={{0,6},{2,0},{4,2},{6,4},{1,7},{3,1},{5,3},{7,5},{8,14},{10,8},{12,... | collective-permute-start | bytes 393224 | tf_op jit(solution)/shard_map/ppermute | solution.py:391
  31.6 4.4 %copy-start.4 = (f32[32]{0:T(128)S(1)}, f32[32]{0:T(128)}, u32[]{:S(2)}) copy-start(f32[32]{0:T(128)} %param.28) | copy-start | bytes 388
  31.6 4.4 %copy-start.5 = (f32[32]{0:T(128)S(1)}, f32[32]{0:T(128)}, u32[]{:S(2)}) copy-start(f32[32]{0:T(128)} %param.27) | copy-start | bytes 388
  31.7 20.5 %collective-permute-start.3 = (bf16[4,32,2048]{2,1,0:T(8,128)(2,1)S(1)}, bf16[4,32,2048]{2,1,0:T(8,128)(2,1)S(1)}, u32[]{:S(2)}, u32[]{:S(2)}) collective-permute-start(bf16[4,32,2048]{2,1,0:T(8,128)(2,1)S(1)} %pad_maximum_fusion.one), channel_id=1, source_target_pairs={{0,1},{1,0},{2,3},{3,2},{4,5},{5,4},{6,7},{7,6},{8,9},{9,8},{10,11... | collective-permute-start | bytes 1572872 | tf_op jit(solution)/shard_map/ppermute | solution.py:393
  37.4 13.9 %copy-start.7 = (f32[32]{0:T(128)S(1)}, f32[32]{0:T(128)}, u32[]{:S(2)}) copy-start(f32[32]{0:T(128)} %param.26) | copy-start | bytes 388
  37.4 22.7 %all-to-all-start.1 = ((f32[32,5,256]{2,1,0:T(8,128)}), f32[32,5,256]{2,1,0:T(8,128)S(1)}, u32[]{:S(2)}, u32[]{:S(2)}) async-start(f32[32,5,256]{2,1,0:T(8,128)} %broadcast_in_dim.8), calls=%async_computation.1 | async-start | bytes 524288 | tf_op jit(solution)/shard_map/all_to_all | solution.py:350
  51.4 0.7 copy-start.6
  93.3 8.9 %collective-permute-start.6 = (bf16[128,256]{1,0:T(8,128)(2,1)S(1)}, bf16[128,256]{1,0:T(8,128)(2,1)S(1)}, u32[]{:S(2)}, u32[]{:S(2)}) collective-permute-start(bf16[128,256]{1,0:T(8,128)(2,1)S(1)} %shard_map.157), channel_id=1, source_target_pairs={{0,128},{9,137},{16,144},{25,153},{128,256},{129,1},{136,8},{137,2... | collective-permute-start | bytes 196616 | tf_op jit(solution)/shard_map/ppermute | solution.py:466
  94.6 16.5 %collective-permute-start.5 = (bf16[128,256]{1,0:T(8,128)(2,1)S(1)}, bf16[128,256]{1,0:T(8,128)(2,1)S(1)}, u32[]{:S(2)}, u32[]{:S(2)}) collective-permute-start(bf16[128,256]{1,0:T(8,128)(2,1)S(1)} %shard_map.157), channel_id=1, source_target_pairs={{0,256},{9,265},{16,272},{25,281},{128,384},{137,393},{144,400},{1... | collective-permute-start | bytes 196616 | tf_op jit(solution)/shard_map/ppermute | solution.py:466
  95.9 16.6 %collective-permute-start.4 = (bf16[128,256]{1,0:T(8,128)(2,1)S(1)}, bf16[128,256]{1,0:T(8,128)(2,1)S(1)}, u32[]{:S(2)}, u32[]{:S(2)}) collective-permute-start(bf16[128,256]{1,0:T(8,128)(2,1)S(1)} %shard_map.157), channel_id=1, source_target_pairs={{0,384},{9,393},{16,400},{25,409},{385,1},{392,8},{401,17},{408,24... | collective-permute-start | bytes 196616 | tf_op jit(solution)/shard_map/ppermute | solution.py:466
  101.3 20.4 %copy-start = (bf16[256,2048]{1,0:T(8,128)(2,1)S(1)}, bf16[256,2048]{1,0:T(8,128)(2,1)}, u32[]{:S(2)}) copy-start(bf16[256,2048]{1,0:T(8,128)(2,1)} %weight.1) | copy-start | bytes 3145732
  123.1 8.4 %collective-permute-start.7 = (bf16[4,32,2048]{2,1,0:T(8,128)(2,1)S(1)}, bf16[4,32,2048]{2,1,0:T(8,128)(2,1)S(1)}, u32[]{:S(2)}, u32[]{:S(2)}) collective-permute-start(bf16[4,32,2048]{2,1,0:T(8,128)(2,1)S(1)} %get-tuple-element.14), channel_id=1, source_target_pairs={{0,1},{1,0},{2,3},{3,2},{4,5},{5,4},{6,7},{7,6},{8,9},{9,8},{10,11... | collective-permute-start | bytes 1572872 | tf_op jit(solution)/shard_map/ppermute | solution.py:475

commit v9 on v8

--- a/solution.py
+++ b/solution.py
@@ -90,7 +90,7 @@
 
 
 def front_kernel(
-    pos, one, two, fac, small, ctx, wq_h, wk_h, wv_h, wd_h, ww_h, spike_h,
+    pos, one, two, fac, small, half, rest, wq_h, wk_h, wv_h, wd_h, ww_h, spike_h,
     m_o, r_o, o_o,
     hid, packed, wq, wk, wv, wd, ww, spike, sems,
 ):
@@ -103,7 +103,11 @@
             core = pos[6] if i == 0 else 1 - pos[6]
             spot = (2 * ((pos[7] + 4 - d) % 4) + core) * 32
             hid[pl.ds(pl.multiple_of(spot, 32), 32)] = norm_rows(lat[d], scale, shift)
-    hid[256:320] = norm_rows(ctx[...], factor(fac, 4), factor(fac, 3))
+    first = pos[6] == 0
+    sides = (half[...].astype(F32), rest[...].astype(F32))
+    left, right = (jnp.where(first, *pair) for pair in (sides, sides[::-1]))
+    context_rows = jnp.concatenate([left, right], axis=1)
+    hid[256:320] = norm_rows(context_rows, factor(fac, 4), factor(fac, 3))
     rows = hid[...]
     copies[0].wait()
     packed[0:256] = mm(hid[0:256], wq[...]).astype(BF)
@@ -406,12 +410,13 @@
             high.astype(BF),
             (part - high).astype(BF),
             jnp.zeros((6, 256), BF),
-            context.reshape(32, 256),
+            lax.dynamic_slice_in_dim(context, c * (D // 2), D // 2, 1).reshape(16, 256),
         ]
     )
     sent = to_all(sent, Z, 16)
     part = jnp.sum(sent[:, 0:5].astype(F32) + sent[:, 5:10].astype(F32), axis=0)
-    ctx = sent[:, 16:48].reshape(64, D)
+    ctx = sent[:, 16:32].reshape(64, D // 2)
+    rest = lax.ppermute(ctx, "c", [(0, 1), (1, 0)])
     fac = to_all(part, ("y", "x", "c"), 32)
 
     small = jnp.stack(
@@ -445,7 +450,7 @@
     maps, reads, base = call(
         front_kernel,
         [((4, 208, 256), BF), ((2, 256, 256), BF), ((256, 256), F32)],
-        [SM] + [VM] * 5 + [HB] * 6,
+        [SM] + [VM] * 6 + [HB] * 6,
         [pltpu.VMEM((320, D), BF), pltpu.VMEM((832, 256), BF), *room],
         flops=5 * 10**9,
     )(
@@ -455,6 +460,7 @@
         fac,
         small,
         ctx,
+        rest,
         *slow,
     )
     of_y = lax.all_to_all(maps, "y", 0, 0, tiled=True)

time: 145 us -> 140 us (0.966)
  starting transfers between devices: 56.1 us -> 53.3 us
    all_to_all x2, starting transfers between devices: 29.7 us -> 23.2 us  [to_all(): lax.all_to_all(jnp.broadcast_to(value[None], (count, *value.shape)), axes...]
    ppermute x0 -> x1, starting transfers between devices: none -> 3.73 us  [per_device(): rest = lax.ppermute(ctx, 'c', [(0, 1), (1, 0)])]
  transfers between devices with their start and end apart: 10 -> 11, of which waited for: 8 -> 7; matrix products, arithmetic and copies ran while one was open for 1% -> 1% of each run, Pallas kernels for 3% -> 3%
where the time goes in v9:
time: 140 us
  starting transfers between devices  53.3 us (38%)
  blocking collectives  39.3 us (28%)
  waiting for transfers between devices  22 us (16%)
  Pallas kernels  21.2 us (15%)
  local copies, waits for them, and re-layouts  2.48 us (2%)
    all_to_all x2, starting transfers between devices, to_all(): lax.all_to_all(jnp.broadcast_to(value[None], (count, *value.shape)), axes...  23.2 us
    all_to_all x1, blocking collectives, per_device(): branch = lax.all_to_all(branch, 'x', 0, 0, tiled=True)  11.5 us
    ppermute x3, starting transfers between devices, per_device(): lax.ppermute(latent, 'x', [(i, (i + d) % 4) for i in range(4)])  11.1 us
    pallas_call x1, Pallas kernels, per_device(): call(front_kernel, [((4, 208, 256), BF), ((2, 256, 256), BF), ((256, 256)...  10.9 us
    ppermute x3, waiting for transfers between devices, per_device(): of_high.append(lax.ppermute(high, ('zh', 'y', 'c'), onward(d)))  10.6 us
    all_to_all x1, blocking collectives, per_device(): of_y = lax.all_to_all(maps, 'y', 0, 0, tiled=True)  10.4 us
    all_to_all x1, blocking collectives, per_device(): of_low = lax.all_to_all(low, 'zl', 0, 0, tiled=True)  10.1 us
    all_to_all x2, waiting for transfers between devices, to_all(): lax.all_to_all(jnp.broadcast_to(value[None], (count, *value.shape)), axes...  8.05 us
  transfers between devices with their start and end apart: 11, of which 7 were waited for; matrix products, arithmetic and copies ran while one was open for 1% of the time, Pallas kernels for 3%

profile of v9, /device:TPU:1, one launch (start us, length us, event | category | flops | bytes accessed | tf_op | source)
XLA Modules:
  0.0 139.7 jit_solution(12980984094278356257)
XLA Ops:
  0.0 0.8 divide_multiply_fusion
  0.8 0.1 copy-done.3
  0.9 0.1 multiply_reduce_fusion
  1.0 0.1 pad.19.clone
  1.1 0.1 fusion
  1.2 0.1 pad_maximum_fusion.1
  1.3 0.7 broadcast_in_dim.7
  2.0 15.9 %all-to-all-start = ((bf16[16,32,256]{2,1,0:T(8,128)(2,1)}), bf16[16,32,256]{2,1,0:T(8,128)(2,1)S(1)}, u32[]{:S(2)}, u32[]{:S(2)}) async-start(bf16[16,32,256]{2,1,0:T(8,128)(2,1)} %broadcast_in_dim.7), calls=%async_computation | async-start | bytes 524288 | tf_op jit(solution)/shard_map/all_to_all | solution.py:354
  17.9 4.7 %collective-permute-start.1 = (bf16[32,2048]{1,0:T(8,128)(2,1)S(1)}, bf16[32,2048]{1,0:T(8,128)(2,1)S(1)}, u32[]{:S(2)}, u32[]{:S(2)}) collective-permute-start(bf16[32,2048]{1,0:T(8,128)(2,1)S(1)} %copy-done.2), channel_id=1, source_target_pairs={{0,4},{2,6},{4,0},{6,2},{1,5},{3,7},{5,1},{7,3},{8,12},{10,14},{12... | collective-permute-start | bytes 393224 | tf_op jit(solution)/shard_map/ppermute | solution.py:395
  22.5 2.2 %collective-permute-start = (bf16[32,2048]{1,0:T(8,128)(2,1)S(1)}, bf16[32,2048]{1,0:T(8,128)(2,1)S(1)}, u32[]{:S(2)}, u32[]{:S(2)}) collective-permute-start(bf16[32,2048]{1,0:T(8,128)(2,1)S(1)} %copy-done.2), channel_id=1, source_target_pairs={{0,2},{2,4},{4,6},{6,0},{1,3},{3,5},{5,7},{7,1},{8,10},{10,12},{12... | collective-permute-start | bytes 393224 | tf_op jit(solution)/shard_map/ppermute | solution.py:395
  24.8 4.3 %collective-permute-start.2 = (bf16[32,2048]{1,0:T(8,128)(2,1)S(1)}, bf16[32,2048]{1,0:T(8,128)(2,1)S(1)}, u32[]{:S(2)}, u32[]{:S(2)}) collective-permute-start(bf16[32,2048]{1,0:T(8,128)(2,1)S(1)} %copy-done.2), channel_id=1, source_target_pairs={{0,6},{2,0},{4,2},{6,4},{1,7},{3,1},{5,3},{7,5},{8,14},{10,8},{12,... | collective-permute-start | bytes 393224 | tf_op jit(solution)/shard_map/ppermute | solution.py:395
  29.0 0.0 collective-permute-done.1
  29.1 0.7 collective-permute-done
  29.8 1.2 collective-permute-done.2
  31.0 0.1 pad_maximum_fusion.one
  31.0 4.3 %collective-permute-start.3 = (bf16[4,32,2048]{2,1,0:T(8,128)(2,1)S(1)}, bf16[4,32,2048]{2,1,0:T(8,128)(2,1)S(1)}, u32[]{:S(2)}, u32[]{:S(2)}) collective-permute-start(bf16[4,32,2048]{2,1,0:T(8,128)(2,1)S(1)} %pad_maximum_fusion.one), channel_id=1, source_target_pairs={{0,1},{1,0},{2,3},{3,2},{4,5},{5,4},{6,7},{7,6},{8,9},{9,8},{10,11... | collective-permute-start | bytes 1572872 | tf_op jit(solution)/shard_map/ppermute | solution.py:397
  35.3 0.0 copy-done.4
  35.4 0.0 all-to-all-done
  35.4 0.1 reshape.11.half
  35.5 3.7 %collective-permute-start.4 = (bf16[64,1024]{1,0:T(8,128)(2,1)S(1)}, bf16[64,1024]{1,0:T(8,128)(2,1)S(1)}, u32[]{:S(2)}, u32[]{:S(2)}) collective-permute-start(bf16[64,1024]{1,0:T(8,128)(2,1)S(1)} %reshape.11.half), channel_id=1, source_target_pairs={{0,1},{1,0},{2,3},{3,2},{4,5},{5,4},{6,7},{7,6},{8,9},{9,8},{10,11... | collective-permute-start | bytes 393224 | tf_op jit(solution)/shard_map/ppermute | solution.py:419
  39.3 0.7 broadcast_in_dim.8
  40.0 7.3 %all-to-all-start.1 = ((f32[32,5,256]{2,1,0:T(8,128)}), f32[32,5,256]{2,1,0:T(8,128)S(1)}, u32[]{:S(2)}, u32[]{:S(2)}) async-start(f32[32,5,256]{2,1,0:T(8,128)} %broadcast_in_dim.8), calls=%async_computation.1 | async-start | bytes 524288 | tf_op jit(solution)/shard_map/all_to_all | solution.py:354
  47.4 0.1 stack.74.pos
  47.5 0.7 copy-done.6
  48.1 0.0 collective-permute-done.3.two
  48.1 0.0 collective-permute-done.4.rest
  48.1 8.0 %all-to-all-done.1.fac = f32[32,5,256]{2,1,0:T(8,128)S(1)} async-done(((f32[32,5,256]{2,1,0:T(8,128)}), f32[32,5,256]{2,1,0:T(8,128)S(1)}, u32[]{:S(2)}, u32[]{:S(2)}) %all-to-all-start.1) | async-done | bytes 163872 | tf_op jit(solution)/shard_map/all_to_all | solution.py:354
  56.2 10.9 %shard_map.154 = (bf16[4,208,256]{2,1,0:T(8,128)(2,1)S(1)}, bf16[2,256,256]{2,1,0:T(8,128)(2,1)S(1)}, f32[256,256]{1,0:T(8,128)S(1)}) custom-call(s32[8]{0:T(128)S(1)} %stack.74.pos, bf16[4,32,2048]{2,1,0:T(8,128)(2,1)S(1)} %pad_maximum_fusion.one, bf16[4,32,2048]{2,1,0:T(8,128)(2,1)S(1)} %collective-permute-done.3.two, ...), custom_call_target="tpu_custom_call" | custom-call | flops 5000000000 | bytes 1 | tf_op jit(solution)/shard_map/pallas_call | solution.py:450
  67.1 10.4 %all_to_all.30.maps.own = bf16[4,208,256]{2,1,0:T(8,128)(2,1)S(1)} all-to-all(bf16[4,208,256]{2,1,0:T(8,128)(2,1)S(1)} %get-tuple-element.10), channel_id=1, replica_groups=mesh['zh'=4,'zl'=4,'y'=4,'x'=4,'c'=2] {'y'}, dimensions={0} | all-to-all | bytes 851968 | tf_op jit(solution)/shard_map/all_to_all | solution.py:466
  77.6 1.1 shard_map.156
  78.7 10.1 %all_to_all.31.maps.low = bf16[4,128,256]{2,1,0:T(8,128)(2,1)S(1)} all-to-all(bf16[4,128,256]{2,1,0:T(8,128)(2,1)S(1)} %shard_map.156), channel_id=1, replica_groups=mesh['zh'=4,'zl'=4,'y'=4,'x'=4,'c'=2] {'zl'}, dimensions={0} | all-to-all | bytes 524288 | tf_op jit(solution)/shard_map/all_to_all | solution.py:468
  88.8 1.1 shard_map.157
  89.9 1.3 collective-permute-start.7
  91.2 1.3 collective-permute-start.6
  92.5 1.5 %collective-permute-start.5 = (bf16[128,256]{1,0:T(8,128)(2,1)S(1)}, bf16[128,256]{1,0:T(8,128)(2,1)S(1)}, u32[]{:S(2)}, u32[]{:S(2)}) collective-permute-start(bf16[128,256]{1,0:T(8,128)(2,1)S(1)} %shard_map.157), channel_id=1, source_target_pairs={{0,384},{9,393},{16,400},{25,409},{385,1},{392,8},{401,17},{408,24... | collective-permute-start | bytes 196616 | tf_op jit(solution)/shard_map/ppermute | solution.py:472
  94.0 3.9 %shard_map.155.start = f32[128,128]{1,0:T(8,128)S(1)} custom-call(s32[8]{0:T(128)S(1)} %stack.74.pos, bf16[4,208,256]{2,1,0:T(8,128)(2,1)S(1)} %all_to_all.30.maps.own, f32[4,128]{1,0:T(4,128)S(1)} %pad_maximum_fusion.3.small.gain), custom_call_target="tpu_custom_call" | custom-call | flops 1000000000 | bytes 1 | tf_op jit(solution)/shard_map/pallas_call | solution.py:473
  97.8 0.0 copy-start.1
  97.8 1.0 collective-permute-done.7.near
  98.8 6.3 %collective-permute-done.6.middle = bf16[128,256]{1,0:T(8,128)(2,1)S(1)} collective-permute-done((bf16[128,256]{1,0:T(8,128)(2,1)S(1)}, bf16[128,256]{1,0:T(8,128)(2,1)S(1)}, u32[]{:S(2)}, u32[]{:S(2)}) %collective-permute-start.6) | collective-permute-done | bytes 65568 | tf_op jit(solution)/shard_map/ppermute | solution.py:472
  105.1 3.3 %collective-permute-done.5.far = bf16[128,256]{1,0:T(8,128)(2,1)S(1)} collective-permute-done((bf16[128,256]{1,0:T(8,128)(2,1)S(1)}, bf16[128,256]{1,0:T(8,128)(2,1)S(1)}, u32[]{:S(2)}, u32[]{:S(2)}) %collective-permute-start.5) | collective-permute-done | bytes 65568 | tf_op jit(solution)/shard_map/ppermute | solution.py:472
  108.4 1.9 %shard_map.158 = bf16[4,128,128]{2,1,0:T(8,128)(2,1)S(1)} custom-call(s32[8]{0:T(128)S(1)} %stack.74.pos, f32[128,128]{1,0:T(8,128)S(1)} %shard_map.155.start, bf16[128,256]{1,0:T(8,128)(2,1)S(1)} %collective-permute-done.5.far, bf16[128,256]{1,0:T(8,128)(2,1)S(1)} %collective-permute-done.6.middle, bf16[128,256]{1,0:T(8,128)(2,1)S(1)} %collective-permute-done.7.near, ...), custom_call_target="tpu_custom_call" | custom-call | flops 100000000 | bytes 1 | tf_op jit(solution)/shard_map/pallas_call | solution.py:474
  110.4 7.2 %all_to_all.32.states = bf16[4,128,128]{2,1,0:T(8,128)(2,1)S(1)} all-to-all(bf16[4,128,128]{2,1,0:T(8,128)(2,1)S(1)} %shard_map.158), channel_id=1, replica_groups=mesh['zh'=4,'zl'=4,'y'=4,'x'=4,'c'=2] {'y'}, dimensions={0} | all-to-all | bytes 262144 | tf_op jit(solution)/shard_map/all_to_all | solution.py:477
  117.6 1.3 shard_map.159
  118.9 6.9 %collective-permute-start.8 = (bf16[4,32,2048]{2,1,0:T(8,128)(2,1)S(1)}, bf16[4,32,2048]{2,1,0:T(8,128)(2,1)S(1)}, u32[]{:S(2)}, u32[]{:S(2)}) collective-permute-start(bf16[4,32,2048]{2,1,0:T(8,128)(2,1)S(1)} %get-tuple-element.14), channel_id=1, source_target_pairs={{0,1},{1,0},{2,3},{3,2},{4,5},{5,4},{6,7},{7,6},{8,9},{9,8},{10,11... | collective-permute-start | bytes 1572872 | tf_op jit(solution)/shard_map/ppermute | solution.py:481
  125.8 1.5 %collective-permute-done.8.got = bf16[4,32,2048]{2,1,0:T(8,128)(2,1)S(1)} collective-permute-done((bf16[4,32,2048]{2,1,0:T(8,128)(2,1)S(1)}, bf16[4,32,2048]{2,1,0:T(8,128)(2,1)S(1)}, u32[]{:S(2)}, u32[]{:S(2)}) %collective-permute-start.8) | collective-permute-done | bytes 524320 | tf_op jit(solution)/shard_map/ppermute | solution.py:481
  127.3 0.1 shard_map.160
  127.4 11.5 %all_to_all.33.rows = bf16[4,32,2048]{2,1,0:T(8,128)(2,1)S(1)} all-to-all(bf16[4,32,2048]{2,1,0:T(8,128)(2,1)S(1)} %shard_map.160), channel_id=1, replica_groups=mesh['zh'=4,'zl'=4,'y'=4,'x'=4,'c'=2] {'x'}, dimensions={0} | all-to-all | bytes 1048576 | tf_op jit(solution)/shard_map/all_to_all | solution.py:483
  139.0 0.8 shard_map.161
  (23 shorter events, 0.1 us)
Async XLA Ops:
  0.0 1.0 copy-start
  0.0 0.8 copy-start.3
  2.0 15.9 %copy-start.2 = (bf16[32,2048]{1,0:T(8,128)(2,1)S(1)}, bf16[32,2048]{1,0:T(8,128)(2,1)}, u32[]{:S(2)}) copy-start(bf16[32,2048]{1,0:T(8,128)(2,1)} %lat.1) | copy-start | bytes 393220
  2.0 33.4 %all-to-all-start = ((bf16[16,32,256]{2,1,0:T(8,128)(2,1)}), bf16[16,32,256]{2,1,0:T(8,128)(2,1)S(1)}, u32[]{:S(2)}, u32[]{:S(2)}) async-start(bf16[16,32,256]{2,1,0:T(8,128)(2,1)} %broadcast_in_dim.7), calls=%async_computation | async-start | bytes 524288 | tf_op jit(solution)/shard_map/all_to_all | solution.py:354
  17.9 11.2 %collective-permute-start.1 = (bf16[32,2048]{1,0:T(8,128)(2,1)S(1)}, bf16[32,2048]{1,0:T(8,128)(2,1)S(1)}, u32[]{:S(2)}, u32[]{:S(2)}) collective-permute-start(bf16[32,2048]{1,0:T(8,128)(2,1)S(1)} %copy-done.2), channel_id=1, source_target_pairs={{0,4},{2,6},{4,0},{6,2},{1,5},{3,7},{5,1},{7,3},{8,12},{10,14},{12... | collective-permute-start | bytes 393224 | tf_op jit(solution)/shard_map/ppermute | solution.py:395
  22.5 7.2 %collective-permute-start = (bf16[32,2048]{1,0:T(8,128)(2,1)S(1)}, bf16[32,2048]{1,0:T(8,128)(2,1)S(1)}, u32[]{:S(2)}, u32[]{:S(2)}) collective-permute-start(bf16[32,2048]{1,0:T(8,128)(2,1)S(1)} %copy-done.2), channel_id=1, source_target_pairs={{0,2},{2,4},{4,6},{6,0},{1,3},{3,5},{5,7},{7,1},{8,10},{10,12},{12... | collective-permute-start | bytes 393224 | tf_op jit(solution)/shard_map/ppermute | solution.py:395
  24.8 6.2 %collective-permute-start.2 = (bf16[32,2048]{1,0:T(8,128)(2,1)S(1)}, bf16[32,2048]{1,0:T(8,128)(2,1)S(1)}, u32[]{:S(2)}, u32[]{:S(2)}) collective-permute-start(bf16[32,2048]{1,0:T(8,128)(2,1)S(1)} %copy-done.2), channel_id=1, source_target_pairs={{0,6},{2,0},{4,2},{6,4},{1,7},{3,1},{5,3},{7,5},{8,14},{10,8},{12,... | collective-permute-start | bytes 393224 | tf_op jit(solution)/shard_map/ppermute | solution.py:395
  31.0 4.4 %copy-start.4 = (f32[32]{0:T(128)S(1)}, f32[32]{0:T(128)}, u32[]{:S(2)}) copy-start(f32[32]{0:T(128)} %param.28) | copy-start | bytes 388
  31.0 4.4 %copy-start.5 = (f32[32]{0:T(128)S(1)}, f32[32]{0:T(128)}, u32[]{:S(2)}) copy-start(f32[32]{0:T(128)} %param.27) | copy-start | bytes 388
  31.0 17.1 %collective-permute-start.3 = (bf16[4,32,2048]{2,1,0:T(8,128)(2,1)S(1)}, bf16[4,32,2048]{2,1,0:T(8,128)(2,1)S(1)}, u32[]{:S(2)}, u32[]{:S(2)}) collective-permute-start(bf16[4,32,2048]{2,1,0:T(8,128)(2,1)S(1)} %pad_maximum_fusion.one), channel_id=1, source_target_pairs={{0,1},{1,0},{2,3},{3,2},{4,5},{5,4},{6,7},{7,6},{8,9},{9,8},{10,11... | collective-permute-start | bytes 1572872 | tf_op jit(solution)/shard_map/ppermute | solution.py:397
  35.5 12.7 %collective-permute-start.4 = (bf16[64,1024]{1,0:T(8,128)(2,1)S(1)}, bf16[64,1024]{1,0:T(8,128)(2,1)S(1)}, u32[]{:S(2)}, u32[]{:S(2)}) collective-permute-start(bf16[64,1024]{1,0:T(8,128)(2,1)S(1)} %reshape.11.half), channel_id=1, source_target_pairs={{0,1},{1,0},{2,3},{3,2},{4,5},{5,4},{6,7},{7,6},{8,9},{9,8},{10,11... | collective-permute-start | bytes 393224 | tf_op jit(solution)/shard_map/ppermute | solution.py:419
  40.0 7.3 %copy-start.7 = (f32[32]{0:T(128)S(1)}, f32[32]{0:T(128)}, u32[]{:S(2)}) copy-start(f32[32]{0:T(128)} %param.26) | copy-start | bytes 388
  40.0 16.2 %all-to-all-start.1 = ((f32[32,5,256]{2,1,0:T(8,128)}), f32[32,5,256]{2,1,0:T(8,128)S(1)}, u32[]{:S(2)}, u32[]{:S(2)}) async-start(f32[32,5,256]{2,1,0:T(8,128)} %broadcast_in_dim.8), calls=%async_computation.1 | async-start | bytes 524288 | tf_op jit(solution)/shard_map/all_to_all | solution.py:354
  47.5 0.7 copy-start.6
  89.9 8.9 %collective-permute-start.7 = (bf16[128,256]{1,0:T(8,128)(2,1)S(1)}, bf16[128,256]{1,0:T(8,128)(2,1)S(1)}, u32[]{:S(2)}, u32[]{:S(2)}) collective-permute-start(bf16[128,256]{1,0:T(8,128)(2,1)S(1)} %shard_map.157), channel_id=1, source_target_pairs={{0,128},{9,137},{16,144},{25,153},{128,256},{129,1},{136,8},{137,2... | collective-permute-start | bytes 196616 | tf_op jit(solution)/shard_map/ppermute | solution.py:472
  91.2 13.9 %collective-permute-start.6 = (bf16[128,256]{1,0:T(8,128)(2,1)S(1)}, bf16[128,256]{1,0:T(8,128)(2,1)S(1)}, u32[]{:S(2)}, u32[]{:S(2)}) collective-permute-start(bf16[128,256]{1,0:T(8,128)(2,1)S(1)} %shard_map.157), channel_id=1, source_target_pairs={{0,256},{9,265},{16,272},{25,281},{128,384},{137,393},{144,400},{1... | collective-permute-start | bytes 196616 | tf_op jit(solution)/shard_map/ppermute | solution.py:472
  92.5 15.9 %collective-permute-start.5 = (bf16[128,256]{1,0:T(8,128)(2,1)S(1)}, bf16[128,256]{1,0:T(8,128)(2,1)S(1)}, u32[]{:S(2)}, u32[]{:S(2)}) collective-permute-start(bf16[128,256]{1,0:T(8,128)(2,1)S(1)} %shard_map.157), channel_id=1, source_target_pairs={{0,384},{9,393},{16,400},{25,409},{385,1},{392,8},{401,17},{408,24... | collective-permute-start | bytes 196616 | tf_op jit(solution)/shard_map/ppermute | solution.py:472
  97.8 19.7 %copy-start.1 = (bf16[256,2048]{1,0:T(8,128)(2,1)S(1)}, bf16[256,2048]{1,0:T(8,128)(2,1)}, u32[]{:S(2)}) copy-start(bf16[256,2048]{1,0:T(8,128)(2,1)} %weight.1) | copy-start | bytes 3145732
  118.9 8.4 %collective-permute-start.8 = (bf16[4,32,2048]{2,1,0:T(8,128)(2,1)S(1)}, bf16[4,32,2048]{2,1,0:T(8,128)(2,1)S(1)}, u32[]{:S(2)}, u32[]{:S(2)}) collective-permute-start(bf16[4,32,2048]{2,1,0:T(8,128)(2,1)S(1)} %get-tuple-element.14), channel_id=1, source_target_pairs={{0,1},{1,0},{2,3},{3,2},{4,5},{5,4},{6,7},{7,6},{8,9},{9,8},{10,11... | collective-permute-start | bytes 1572872 | tf_op jit(solution)/shard_map/ppermute | solution.py:481

commit v10 on v9

--- a/solution.py
+++ b/solution.py
@@ -404,18 +404,16 @@
             jnp.sum(mod[:2] * signals[1][None, :, None], axis=1),
         ]
     )
-    high = lax.reduce_precision(part, 8, 7)
     sent = jnp.concatenate(
         [
-            high.astype(BF),
-            (part - high).astype(BF),
-            jnp.zeros((6, 256), BF),
+            part.astype(BF),
+            jnp.zeros((3, 256), BF),
             lax.dynamic_slice_in_dim(context, c * (D // 2), D // 2, 1).reshape(16, 256),
         ]
     )
     sent = to_all(sent, Z, 16)
-    part = jnp.sum(sent[:, 0:5].astype(F32) + sent[:, 5:10].astype(F32), axis=0)
-    ctx = sent[:, 16:32].reshape(64, D // 2)
+    part = jnp.sum(sent[:, 0:5].astype(F32), axis=0)
+    ctx = sent[:, 8:24].reshape(64, D // 2)
     rest = lax.ppermute(ctx, "c", [(0, 1), (1, 0)])
     fac = to_all(part, ("y", "x", "c"), 32)
 

time: 140 us -> 140 us (level)
    ppermute x1, starting transfers between devices: 3.73 us -> 1.92 us  [per_device(): rest = lax.ppermute(ctx, 'c', [(0, 1), (1, 0)])]
where the time goes in v10:
time: 140 us; the launch traced here: 139 us
  starting transfers between devices  52.6 us (38%)
  blocking collectives  39.8 us (28%)
  waiting for transfers between devices  22 us (16%)
  Pallas kernels  21.1 us (15%)
  local copies, waits for them, and re-layouts  2.46 us (2%)
    all_to_all x2, starting transfers between devices, to_all(): lax.all_to_all(jnp.broadcast_to(value[None], (count, *value.shape)), axes...  24.2 us
    all_to_all x1, blocking collectives, per_device(): branch = lax.all_to_all(branch, 'x', 0, 0, tiled=True)  11.5 us
    ppermute x3, starting transfers between devices, per_device(): lax.ppermute(latent, 'x', [(i, (i + d) % 4) for i in range(4)])  11.1 us
    pallas_call x1, Pallas kernels, per_device(): call(front_kernel, [((4, 208, 256), BF), ((2, 256, 256), BF), ((256, 256)...  10.9 us
    all_to_all x1, blocking collectives, per_device(): of_low = lax.all_to_all(low, 'zl', 0, 0, tiled=True)  10.6 us
    ppermute x3, waiting for transfers between devices, per_device(): of_high.append(lax.ppermute(high, ('zh', 'y', 'c'), onward(d)))  10.5 us
    all_to_all x1, blocking collectives, per_device(): of_y = lax.all_to_all(maps, 'y', 0, 0, tiled=True)  10.4 us
    all_to_all x2, waiting for transfers between devices, to_all(): lax.all_to_all(jnp.broadcast_to(value[None], (count, *value.shape)), axes...  8.05 us
  transfers between devices with their start and end apart: 11, of which 7 were waited for; matrix products, arithmetic and copies ran while one was open for 1% of the time, Pallas kernels for 3%

profile of v10, /device:TPU:1, one launch (start us, length us, event | category | flops | bytes accessed | tf_op | source)
XLA Modules:
  0.0 139.5 jit_solution(12435783412650041287)
XLA Ops:
  0.0 0.8 divide_multiply_fusion
  0.8 0.1 copy-done.3
  0.9 0.1 multiply_reduce_fusion
  1.0 0.1 pad.19.clone
  1.1 0.1 fusion
  1.2 0.1 pad_maximum_fusion.1
  1.3 0.7 broadcast_in_dim.7
  2.0 15.9 %all-to-all-start = ((bf16[16,24,256]{2,1,0:T(8,128)(2,1)}), bf16[16,24,256]{2,1,0:T(8,128)(2,1)S(1)}, u32[]{:S(2)}, u32[]{:S(2)}) async-start(bf16[16,24,256]{2,1,0:T(8,128)(2,1)} %broadcast_in_dim.7), calls=%async_computation | async-start | bytes 393216 | tf_op jit(solution)/shard_map/all_to_all | solution.py:354
  17.8 4.7 %collective-permute-start.1 = (bf16[32,2048]{1,0:T(8,128)(2,1)S(1)}, bf16[32,2048]{1,0:T(8,128)(2,1)S(1)}, u32[]{:S(2)}, u32[]{:S(2)}) collective-permute-start(bf16[32,2048]{1,0:T(8,128)(2,1)S(1)} %copy-done.2), channel_id=1, source_target_pairs={{0,4},{2,6},{4,0},{6,2},{1,5},{3,7},{5,1},{7,3},{8,12},{10,14},{12... | collective-permute-start | bytes 393224 | tf_op jit(solution)/shard_map/ppermute | solution.py:395
  22.5 2.2 %collective-permute-start = (bf16[32,2048]{1,0:T(8,128)(2,1)S(1)}, bf16[32,2048]{1,0:T(8,128)(2,1)S(1)}, u32[]{:S(2)}, u32[]{:S(2)}) collective-permute-start(bf16[32,2048]{1,0:T(8,128)(2,1)S(1)} %copy-done.2), channel_id=1, source_target_pairs={{0,2},{2,4},{4,6},{6,0},{1,3},{3,5},{5,7},{7,1},{8,10},{10,12},{12... | collective-permute-start | bytes 393224 | tf_op jit(solution)/shard_map/ppermute | solution.py:395
  24.7 4.3 %collective-permute-start.2 = (bf16[32,2048]{1,0:T(8,128)(2,1)S(1)}, bf16[32,2048]{1,0:T(8,128)(2,1)S(1)}, u32[]{:S(2)}, u32[]{:S(2)}) collective-permute-start(bf16[32,2048]{1,0:T(8,128)(2,1)S(1)} %copy-done.2), channel_id=1, source_target_pairs={{0,6},{2,0},{4,2},{6,4},{1,7},{3,1},{5,3},{7,5},{8,14},{10,8},{12,... | collective-permute-start | bytes 393224 | tf_op jit(solution)/shard_map/ppermute | solution.py:395
  29.0 0.0 collective-permute-done.1
  29.0 0.7 collective-permute-done
  29.7 1.2 collective-permute-done.2
  30.9 0.1 pad_maximum_fusion.one
  31.0 4.3 %collective-permute-start.3 = (bf16[4,32,2048]{2,1,0:T(8,128)(2,1)S(1)}, bf16[4,32,2048]{2,1,0:T(8,128)(2,1)S(1)}, u32[]{:S(2)}, u32[]{:S(2)}) collective-permute-start(bf16[4,32,2048]{2,1,0:T(8,128)(2,1)S(1)} %pad_maximum_fusion.one), channel_id=1, source_target_pairs={{0,1},{1,0},{2,3},{3,2},{4,5},{5,4},{6,7},{7,6},{8,9},{9,8},{10,11... | collective-permute-start | bytes 1572872 | tf_op jit(solution)/shard_map/ppermute | solution.py:397
  35.3 0.0 copy-done.4
  35.3 0.0 all-to-all-done
  35.4 0.1 reshape.11.half
  35.4 1.9 %collective-permute-start.4 = (bf16[64,1024]{1,0:T(8,128)(2,1)S(1)}, bf16[64,1024]{1,0:T(8,128)(2,1)S(1)}, u32[]{:S(2)}, u32[]{:S(2)}) collective-permute-start(bf16[64,1024]{1,0:T(8,128)(2,1)S(1)} %reshape.11.half), channel_id=1, source_target_pairs={{0,1},{1,0},{2,3},{3,2},{4,5},{5,4},{6,7},{7,6},{8,9},{9,8},{10,11... | collective-permute-start | bytes 393224 | tf_op jit(solution)/shard_map/ppermute | solution.py:417
  37.4 0.7 broadcast_in_dim.8
  38.1 8.3 %all-to-all-start.1 = ((f32[32,5,256]{2,1,0:T(8,128)}), f32[32,5,256]{2,1,0:T(8,128)S(1)}, u32[]{:S(2)}, u32[]{:S(2)}) async-start(f32[32,5,256]{2,1,0:T(8,128)} %broadcast_in_dim.8), calls=%async_computation.1 | async-start | bytes 524288 | tf_op jit(solution)/shard_map/all_to_all | solution.py:354
  46.5 0.1 stack.74.pos
  46.6 0.7 copy-done.6
  47.3 0.0 collective-permute-done.3.two
  47.3 0.0 collective-permute-done.4.rest
  47.3 8.0 %all-to-all-done.1.fac = f32[32,5,256]{2,1,0:T(8,128)S(1)} async-done(((f32[32,5,256]{2,1,0:T(8,128)}), f32[32,5,256]{2,1,0:T(8,128)S(1)}, u32[]{:S(2)}, u32[]{:S(2)}) %all-to-all-start.1) | async-done | bytes 163872 | tf_op jit(solution)/shard_map/all_to_all | solution.py:354
  55.4 10.9 %shard_map.154 = (bf16[4,208,256]{2,1,0:T(8,128)(2,1)S(1)}, bf16[2,256,256]{2,1,0:T(8,128)(2,1)S(1)}, f32[256,256]{1,0:T(8,128)S(1)}) custom-call(s32[8]{0:T(128)S(1)} %stack.74.pos, bf16[4,32,2048]{2,1,0:T(8,128)(2,1)S(1)} %pad_maximum_fusion.one, bf16[4,32,2048]{2,1,0:T(8,128)(2,1)S(1)} %collective-permute-done.3.two, ...), custom_call_target="tpu_custom_call" | custom-call | flops 5000000000 | bytes 1 | tf_op jit(solution)/shard_map/pallas_call | solution.py:448
  66.3 10.4 %all_to_all.30.maps.own = bf16[4,208,256]{2,1,0:T(8,128)(2,1)S(1)} all-to-all(bf16[4,208,256]{2,1,0:T(8,128)(2,1)S(1)} %get-tuple-element.10), channel_id=1, replica_groups=mesh['zh'=4,'zl'=4,'y'=4,'x'=4,'c'=2] {'y'}, dimensions={0} | all-to-all | bytes 851968 | tf_op jit(solution)/shard_map/all_to_all | solution.py:464
  76.7 1.1 shard_map.156
  77.8 10.6 %all_to_all.31.maps.low = bf16[4,128,256]{2,1,0:T(8,128)(2,1)S(1)} all-to-all(bf16[4,128,256]{2,1,0:T(8,128)(2,1)S(1)} %shard_map.156), channel_id=1, replica_groups=mesh['zh'=4,'zl'=4,'y'=4,'x'=4,'c'=2] {'zl'}, dimensions={0} | all-to-all | bytes 524288 | tf_op jit(solution)/shard_map/all_to_all | solution.py:466
  88.5 1.1 shard_map.157
  89.6 1.3 collective-permute-start.7
  90.9 1.3 collective-permute-start.6
  92.2 1.5 %collective-permute-start.5 = (bf16[128,256]{1,0:T(8,128)(2,1)S(1)}, bf16[128,256]{1,0:T(8,128)(2,1)S(1)}, u32[]{:S(2)}, u32[]{:S(2)}) collective-permute-start(bf16[128,256]{1,0:T(8,128)(2,1)S(1)} %shard_map.157), channel_id=1, source_target_pairs={{0,384},{9,393},{16,400},{25,409},{385,1},{392,8},{401,17},{408,24... | collective-permute-start | bytes 196616 | tf_op jit(solution)/shard_map/ppermute | solution.py:470
  93.7 3.9 %shard_map.155.start = f32[128,128]{1,0:T(8,128)S(1)} custom-call(s32[8]{0:T(128)S(1)} %stack.74.pos, bf16[4,208,256]{2,1,0:T(8,128)(2,1)S(1)} %all_to_all.30.maps.own, f32[4,128]{1,0:T(4,128)S(1)} %pad_maximum_fusion.2.small.gain), custom_call_target="tpu_custom_call" | custom-call | flops 1000000000 | bytes 1 | tf_op jit(solution)/shard_map/pallas_call | solution.py:471
  97.5 0.0 copy-start.1
  97.5 1.0 collective-permute-done.7.near
  98.5 6.3 %collective-permute-done.6.middle = bf16[128,256]{1,0:T(8,128)(2,1)S(1)} collective-permute-done((bf16[128,256]{1,0:T(8,128)(2,1)S(1)}, bf16[128,256]{1,0:T(8,128)(2,1)S(1)}, u32[]{:S(2)}, u32[]{:S(2)}) %collective-permute-start.6) | collective-permute-done | bytes 65568 | tf_op jit(solution)/shard_map/ppermute | solution.py:470
  104.8 3.2 %collective-permute-done.5.far = bf16[128,256]{1,0:T(8,128)(2,1)S(1)} collective-permute-done((bf16[128,256]{1,0:T(8,128)(2,1)S(1)}, bf16[128,256]{1,0:T(8,128)(2,1)S(1)}, u32[]{:S(2)}, u32[]{:S(2)}) %collective-permute-start.5) | collective-permute-done | bytes 65568 | tf_op jit(solution)/shard_map/ppermute | solution.py:470
  108.1 1.9 %shard_map.158 = bf16[4,128,128]{2,1,0:T(8,128)(2,1)S(1)} custom-call(s32[8]{0:T(128)S(1)} %stack.74.pos, f32[128,128]{1,0:T(8,128)S(1)} %shard_map.155.start, bf16[128,256]{1,0:T(8,128)(2,1)S(1)} %collective-permute-done.5.far, bf16[128,256]{1,0:T(8,128)(2,1)S(1)} %collective-permute-done.6.middle, bf16[128,256]{1,0:T(8,128)(2,1)S(1)} %collective-permute-done.7.near, ...), custom_call_target="tpu_custom_call" | custom-call | flops 100000000 | bytes 1 | tf_op jit(solution)/shard_map/pallas_call | solution.py:472
  110.0 7.2 %all_to_all.32.states = bf16[4,128,128]{2,1,0:T(8,128)(2,1)S(1)} all-to-all(bf16[4,128,128]{2,1,0:T(8,128)(2,1)S(1)} %shard_map.158), channel_id=1, replica_groups=mesh['zh'=4,'zl'=4,'y'=4,'x'=4,'c'=2] {'y'}, dimensions={0} | all-to-all | bytes 262144 | tf_op jit(solution)/shard_map/all_to_all | solution.py:475
  117.2 1.3 shard_map.159
  118.6 7.0 %collective-permute-start.8 = (bf16[4,32,2048]{2,1,0:T(8,128)(2,1)S(1)}, bf16[4,32,2048]{2,1,0:T(8,128)(2,1)S(1)}, u32[]{:S(2)}, u32[]{:S(2)}) collective-permute-start(bf16[4,32,2048]{2,1,0:T(8,128)(2,1)S(1)} %get-tuple-element.14), channel_id=1, source_target_pairs={{0,1},{1,0},{2,3},{3,2},{4,5},{5,4},{6,7},{7,6},{8,9},{9,8},{10,11... | collective-permute-start | bytes 1572872 | tf_op jit(solution)/shard_map/ppermute | solution.py:479
  125.6 1.5 %collective-permute-done.8.got = bf16[4,32,2048]{2,1,0:T(8,128)(2,1)S(1)} collective-permute-done((bf16[4,32,2048]{2,1,0:T(8,128)(2,1)S(1)}, bf16[4,32,2048]{2,1,0:T(8,128)(2,1)S(1)}, u32[]{:S(2)}, u32[]{:S(2)}) %collective-permute-start.8) | collective-permute-done | bytes 524320 | tf_op jit(solution)/shard_map/ppermute | solution.py:479
  127.1 0.1 shard_map.160
  127.2 11.5 %all_to_all.33.rows = bf16[4,32,2048]{2,1,0:T(8,128)(2,1)S(1)} all-to-all(bf16[4,32,2048]{2,1,0:T(8,128)(2,1)S(1)} %shard_map.160), channel_id=1, replica_groups=mesh['zh'=4,'zl'=4,'y'=4,'x'=4,'c'=2] {'x'}, dimensions={0} | all-to-all | bytes 1048576 | tf_op jit(solution)/shard_map/all_to_all | solution.py:481
  138.7 0.8 shard_map.161
  (22 shorter events, 0.1 us)
Async XLA Ops:
  0.0 1.0 copy-start
  0.0 0.8 copy-start.3
  2.0 15.9 %copy-start.2 = (bf16[32,2048]{1,0:T(8,128)(2,1)S(1)}, bf16[32,2048]{1,0:T(8,128)(2,1)}, u32[]{:S(2)}) copy-start(bf16[32,2048]{1,0:T(8,128)(2,1)} %lat.1) | copy-start | bytes 393220
  2.0 33.4 %all-to-all-start = ((bf16[16,24,256]{2,1,0:T(8,128)(2,1)}), bf16[16,24,256]{2,1,0:T(8,128)(2,1)S(1)}, u32[]{:S(2)}, u32[]{:S(2)}) async-start(bf16[16,24,256]{2,1,0:T(8,128)(2,1)} %broadcast_in_dim.7), calls=%async_computation | async-start | bytes 393216 | tf_op jit(solution)/shard_map/all_to_all | solution.py:354
  17.8 11.2 %collective-permute-start.1 = (bf16[32,2048]{1,0:T(8,128)(2,1)S(1)}, bf16[32,2048]{1,0:T(8,128)(2,1)S(1)}, u32[]{:S(2)}, u32[]{:S(2)}) collective-permute-start(bf16[32,2048]{1,0:T(8,128)(2,1)S(1)} %copy-done.2), channel_id=1, source_target_pairs={{0,4},{2,6},{4,0},{6,2},{1,5},{3,7},{5,1},{7,3},{8,12},{10,14},{12... | collective-permute-start | bytes 393224 | tf_op jit(solution)/shard_map/ppermute | solution.py:395
  22.5 7.2 %collective-permute-start = (bf16[32,2048]{1,0:T(8,128)(2,1)S(1)}, bf16[32,2048]{1,0:T(8,128)(2,1)S(1)}, u32[]{:S(2)}, u32[]{:S(2)}) collective-permute-start(bf16[32,2048]{1,0:T(8,128)(2,1)S(1)} %copy-done.2), channel_id=1, source_target_pairs={{0,2},{2,4},{4,6},{6,0},{1,3},{3,5},{5,7},{7,1},{8,10},{10,12},{12... | collective-permute-start | bytes 393224 | tf_op jit(solution)/shard_map/ppermute | solution.py:395
  24.7 6.2 %collective-permute-start.2 = (bf16[32,2048]{1,0:T(8,128)(2,1)S(1)}, bf16[32,2048]{1,0:T(8,128)(2,1)S(1)}, u32[]{:S(2)}, u32[]{:S(2)}) collective-permute-start(bf16[32,2048]{1,0:T(8,128)(2,1)S(1)} %copy-done.2), channel_id=1, source_target_pairs={{0,6},{2,0},{4,2},{6,4},{1,7},{3,1},{5,3},{7,5},{8,14},{10,8},{12,... | collective-permute-start | bytes 393224 | tf_op jit(solution)/shard_map/ppermute | solution.py:395
  30.9 4.4 %copy-start.4 = (f32[32]{0:T(128)S(1)}, f32[32]{0:T(128)}, u32[]{:S(2)}) copy-start(f32[32]{0:T(128)} %param.28) | copy-start | bytes 388
  30.9 4.4 %copy-start.5 = (f32[32]{0:T(128)S(1)}, f32[32]{0:T(128)}, u32[]{:S(2)}) copy-start(f32[32]{0:T(128)} %param.27) | copy-start | bytes 388
  31.0 16.3 %collective-permute-start.3 = (bf16[4,32,2048]{2,1,0:T(8,128)(2,1)S(1)}, bf16[4,32,2048]{2,1,0:T(8,128)(2,1)S(1)}, u32[]{:S(2)}, u32[]{:S(2)}) collective-permute-start(bf16[4,32,2048]{2,1,0:T(8,128)(2,1)S(1)} %pad_maximum_fusion.one), channel_id=1, source_target_pairs={{0,1},{1,0},{2,3},{3,2},{4,5},{5,4},{6,7},{7,6},{8,9},{9,8},{10,11... | collective-permute-start | bytes 1572872 | tf_op jit(solution)/shard_map/ppermute | solution.py:397
  35.4 11.8 %collective-permute-start.4 = (bf16[64,1024]{1,0:T(8,128)(2,1)S(1)}, bf16[64,1024]{1,0:T(8,128)(2,1)S(1)}, u32[]{:S(2)}, u32[]{:S(2)}) collective-permute-start(bf16[64,1024]{1,0:T(8,128)(2,1)S(1)} %reshape.11.half), channel_id=1, source_target_pairs={{0,1},{1,0},{2,3},{3,2},{4,5},{5,4},{6,7},{7,6},{8,9},{9,8},{10,11... | collective-permute-start | bytes 393224 | tf_op jit(solution)/shard_map/ppermute | solution.py:417
  38.1 8.4 %copy-start.7 = (f32[32]{0:T(128)S(1)}, f32[32]{0:T(128)}, u32[]{:S(2)}) copy-start(f32[32]{0:T(128)} %param.26) | copy-start | bytes 388
  38.1 17.2 %all-to-all-start.1 = ((f32[32,5,256]{2,1,0:T(8,128)}), f32[32,5,256]{2,1,0:T(8,128)S(1)}, u32[]{:S(2)}, u32[]{:S(2)}) async-start(f32[32,5,256]{2,1,0:T(8,128)} %broadcast_in_dim.8), calls=%async_computation.1 | async-start | bytes 524288 | tf_op jit(solution)/shard_map/all_to_all | solution.py:354
  46.6 0.7 copy-start.6
  89.6 8.9 %collective-permute-start.7 = (bf16[128,256]{1,0:T(8,128)(2,1)S(1)}, bf16[128,256]{1,0:T(8,128)(2,1)S(1)}, u32[]{:S(2)}, u32[]{:S(2)}) collective-permute-start(bf16[128,256]{1,0:T(8,128)(2,1)S(1)} %shard_map.157), channel_id=1, source_target_pairs={{0,128},{9,137},{16,144},{25,153},{128,256},{129,1},{136,8},{137,2... | collective-permute-start | bytes 196616 | tf_op jit(solution)/shard_map/ppermute | solution.py:470
  90.9 13.9 %collective-permute-start.6 = (bf16[128,256]{1,0:T(8,128)(2,1)S(1)}, bf16[128,256]{1,0:T(8,128)(2,1)S(1)}, u32[]{:S(2)}, u32[]{:S(2)}) collective-permute-start(bf16[128,256]{1,0:T(8,128)(2,1)S(1)} %shard_map.157), channel_id=1, source_target_pairs={{0,256},{9,265},{16,272},{25,281},{128,384},{137,393},{144,400},{1... | collective-permute-start | bytes 196616 | tf_op jit(solution)/shard_map/ppermute | solution.py:470
  92.2 15.9 %collective-permute-start.5 = (bf16[128,256]{1,0:T(8,128)(2,1)S(1)}, bf16[128,256]{1,0:T(8,128)(2,1)S(1)}, u32[]{:S(2)}, u32[]{:S(2)}) collective-permute-start(bf16[128,256]{1,0:T(8,128)(2,1)S(1)} %shard_map.157), channel_id=1, source_target_pairs={{0,384},{9,393},{16,400},{25,409},{385,1},{392,8},{401,17},{408,24... | collective-permute-start | bytes 196616 | tf_op jit(solution)/shard_map/ppermute | solution.py:470
  97.5 19.7 %copy-start.1 = (bf16[256,2048]{1,0:T(8,128)(2,1)S(1)}, bf16[256,2048]{1,0:T(8,128)(2,1)}, u32[]{:S(2)}) copy-start(bf16[256,2048]{1,0:T(8,128)(2,1)} %weight.1) | copy-start | bytes 3145732
  118.6 8.5 %collective-permute-start.8 = (bf16[4,32,2048]{2,1,0:T(8,128)(2,1)S(1)}, bf16[4,32,2048]{2,1,0:T(8,128)(2,1)S(1)}, u32[]{:S(2)}, u32[]{:S(2)}) collective-permute-start(bf16[4,32,2048]{2,1,0:T(8,128)(2,1)S(1)} %get-tuple-element.14), channel_id=1, source_target_pairs={{0,1},{1,0},{2,3},{3,2},{4,5},{5,4},{6,7},{7,6},{8,9},{9,8},{10,11... | collective-permute-start | bytes 1572872 | tf_op jit(solution)/shard_map/ppermute | solution.py:479

commit v11 on v10

--- a/solution.py
+++ b/solution.py
@@ -85,7 +85,8 @@
 
 
 def factor(fac, r):
-    parts = [(fac[t] + fac[8 + t]) + (fac[16 + t] + fac[24 + t]) for t in range(8)]
+    wide = [fac[i].astype(F32) for i in range(32)]
+    parts = [(wide[t] + wide[8 + t]) + (wide[16 + t] + wide[24 + t]) for t in range(8)]
     return jnp.concatenate([f[r : r + 1] for f in parts], axis=1)
 
 
@@ -415,7 +416,7 @@
     part = jnp.sum(sent[:, 0:5].astype(F32), axis=0)
     ctx = sent[:, 8:24].reshape(64, D // 2)
     rest = lax.ppermute(ctx, "c", [(0, 1), (1, 0)])
-    fac = to_all(part, ("y", "x", "c"), 32)
+    fac = to_all(part.astype(BF), ("y", "x", "c"), 32)
 
     small = jnp.stack(
         [

time: 140 us -> 140 us (level)
  no operation moved by 1% of the time
where the time goes in v11:
time: 140 us; the launch traced here: 139 us
  starting transfers between devices  52.5 us (38%)
  blocking collectives  39.9 us (28%)
  Pallas kernels  21.2 us (15%)
  waiting for transfers between devices  20.9 us (15%)
  local copies, waits for them, and re-layouts  3.62 us (3%)
    all_to_all x2, starting transfers between devices, to_all(): lax.all_to_all(jnp.broadcast_to(value[None], (count, *value.shape)), axes...  24.1 us
    all_to_all x1, blocking collectives, per_device(): branch = lax.all_to_all(branch, 'x', 0, 0, tiled=True)  11.6 us
    ppermute x3, starting transfers between devices, per_device(): lax.ppermute(latent, 'x', [(i, (i + d) % 4) for i in range(4)])  11.1 us
    pallas_call x1, Pallas kernels, per_device(): call(front_kernel, [((4, 208, 256), BF), ((2, 256, 256), BF), ((256, 256)...  10.9 us
    all_to_all x1, blocking collectives, per_device(): of_low = lax.all_to_all(low, 'zl', 0, 0, tiled=True)  10.7 us
    ppermute x3, waiting for transfers between devices, per_device(): of_high.append(lax.ppermute(high, ('zh', 'y', 'c'), onward(d)))  10.5 us
    all_to_all x1, blocking collectives, per_device(): of_y = lax.all_to_all(maps, 'y', 0, 0, tiled=True)  10.5 us
    all_to_all x1, blocking collectives, per_device(): states = lax.all_to_all(states, 'y', 0, 0, tiled=True)  7.21 us
  transfers between devices with their start and end apart: 11, of which 7 were waited for; matrix products, arithmetic and copies ran while one was open for 1% of the time, Pallas kernels for 3%

profile of v11, /device:TPU:1, one launch (start us, length us, event | category | flops | bytes accessed | tf_op | source)
XLA Modules:
  0.0 139.5 jit_solution(13657435958338686780)
XLA Ops:
  0.0 0.8 divide_multiply_fusion
  0.8 0.1 copy-done.3
  0.9 0.1 multiply_reduce_fusion
  1.0 0.1 pad.19.clone
  1.1 0.1 fusion
  1.2 0.1 pad_maximum_fusion.1
  1.3 0.7 broadcast_in_dim.7
  2.0 15.9 %all-to-all-start = ((bf16[16,24,256]{2,1,0:T(8,128)(2,1)}), bf16[16,24,256]{2,1,0:T(8,128)(2,1)S(1)}, u32[]{:S(2)}, u32[]{:S(2)}) async-start(bf16[16,24,256]{2,1,0:T(8,128)(2,1)} %broadcast_in_dim.7), calls=%async_computation | async-start | bytes 393216 | tf_op jit(solution)/shard_map/all_to_all | solution.py:355
  17.8 4.7 %collective-permute-start.1 = (bf16[32,2048]{1,0:T(8,128)(2,1)S(1)}, bf16[32,2048]{1,0:T(8,128)(2,1)S(1)}, u32[]{:S(2)}, u32[]{:S(2)}) collective-permute-start(bf16[32,2048]{1,0:T(8,128)(2,1)S(1)} %copy-done.2), channel_id=1, source_target_pairs={{0,4},{2,6},{4,0},{6,2},{1,5},{3,7},{5,1},{7,3},{8,12},{10,14},{12... | collective-permute-start | bytes 393224 | tf_op jit(solution)/shard_map/ppermute | solution.py:396
  22.5 2.2 %collective-permute-start = (bf16[32,2048]{1,0:T(8,128)(2,1)S(1)}, bf16[32,2048]{1,0:T(8,128)(2,1)S(1)}, u32[]{:S(2)}, u32[]{:S(2)}) collective-permute-start(bf16[32,2048]{1,0:T(8,128)(2,1)S(1)} %copy-done.2), channel_id=1, source_target_pairs={{0,2},{2,4},{4,6},{6,0},{1,3},{3,5},{5,7},{7,1},{8,10},{10,12},{12... | collective-permute-start | bytes 393224 | tf_op jit(solution)/shard_map/ppermute | solution.py:396
  24.7 4.3 %collective-permute-start.2 = (bf16[32,2048]{1,0:T(8,128)(2,1)S(1)}, bf16[32,2048]{1,0:T(8,128)(2,1)S(1)}, u32[]{:S(2)}, u32[]{:S(2)}) collective-permute-start(bf16[32,2048]{1,0:T(8,128)(2,1)S(1)} %copy-done.2), channel_id=1, source_target_pairs={{0,6},{2,0},{4,2},{6,4},{1,7},{3,1},{5,3},{7,5},{8,14},{10,8},{12,... | collective-permute-start | bytes 393224 | tf_op jit(solution)/shard_map/ppermute | solution.py:396
  29.0 0.7 collective-permute-done
  29.7 1.2 collective-permute-done.2
  30.9 0.1 pad_maximum_fusion.one
  31.0 4.3 %collective-permute-start.3 = (bf16[4,32,2048]{2,1,0:T(8,128)(2,1)S(1)}, bf16[4,32,2048]{2,1,0:T(8,128)(2,1)S(1)}, u32[]{:S(2)}, u32[]{:S(2)}) collective-permute-start(bf16[4,32,2048]{2,1,0:T(8,128)(2,1)S(1)} %pad_maximum_fusion.one), channel_id=1, source_target_pairs={{0,1},{1,0},{2,3},{3,2},{4,5},{5,4},{6,7},{7,6},{8,9},{9,8},{10,11... | collective-permute-start | bytes 1572872 | tf_op jit(solution)/shard_map/ppermute | solution.py:398
  35.3 0.0 copy-start.7
  35.3 0.1 stack.74.pos
  35.4 0.6 copy-done.7
  36.0 0.6 copy-done.4
  36.6 0.0 copy-done.5
  36.7 0.1 reshape.11.half
  36.8 1.9 %collective-permute-start.4 = (bf16[64,1024]{1,0:T(8,128)(2,1)S(1)}, bf16[64,1024]{1,0:T(8,128)(2,1)S(1)}, u32[]{:S(2)}, u32[]{:S(2)}) collective-permute-start(bf16[64,1024]{1,0:T(8,128)(2,1)S(1)} %reshape.11.half), channel_id=1, source_target_pairs={{0,1},{1,0},{2,3},{3,2},{4,5},{5,4},{6,7},{7,6},{8,9},{9,8},{10,11... | collective-permute-start | bytes 393224 | tf_op jit(solution)/shard_map/ppermute | solution.py:418
  38.7 0.7 broadcast_in_dim.8
  39.4 8.2 %all-to-all-start.1 = ((bf16[32,5,256]{2,1,0:T(8,128)(2,1)}), bf16[32,5,256]{2,1,0:T(8,128)(2,1)S(1)}, u32[]{:S(2)}, u32[]{:S(2)}) async-start(bf16[32,5,256]{2,1,0:T(8,128)(2,1)} %broadcast_in_dim.8), calls=%async_computation.1 | async-start | bytes 262144 | tf_op jit(solution)/shard_map/all_to_all | solution.py:355
  47.6 0.0 copy-start.6
  47.6 0.6 copy-done.6
  48.3 6.9 %all-to-all-done.1.fac = bf16[32,5,256]{2,1,0:T(8,128)(2,1)S(1)} async-done(((bf16[32,5,256]{2,1,0:T(8,128)(2,1)}), bf16[32,5,256]{2,1,0:T(8,128)(2,1)S(1)}, u32[]{:S(2)}, u32[]{:S(2)}) %all-to-all-start.1) | async-done | bytes 81952 | tf_op jit(solution)/shard_map/all_to_all | solution.py:355
  55.2 10.9 %shard_map.154 = (bf16[4,208,256]{2,1,0:T(8,128)(2,1)S(1)}, bf16[2,256,256]{2,1,0:T(8,128)(2,1)S(1)}, f32[256,256]{1,0:T(8,128)S(1)}) custom-call(s32[8]{0:T(128)S(1)} %stack.74.pos, bf16[4,32,2048]{2,1,0:T(8,128)(2,1)S(1)} %pad_maximum_fusion.one, bf16[4,32,2048]{2,1,0:T(8,128)(2,1)S(1)} %collective-permute-done.3.two, ...), custom_call_target="tpu_custom_call" | custom-call | flops 5000000000 | bytes 1 | tf_op jit(solution)/shard_map/pallas_call | solution.py:449
  66.2 10.5 %all_to_all.30.maps.own = bf16[4,208,256]{2,1,0:T(8,128)(2,1)S(1)} all-to-all(bf16[4,208,256]{2,1,0:T(8,128)(2,1)S(1)} %get-tuple-element.10), channel_id=1, replica_groups=mesh['zh'=4,'zl'=4,'y'=4,'x'=4,'c'=2] {'y'}, dimensions={0} | all-to-all | bytes 851968 | tf_op jit(solution)/shard_map/all_to_all | solution.py:465
  76.6 1.1 shard_map.156
  77.7 10.7 %all_to_all.31.maps.low = bf16[4,128,256]{2,1,0:T(8,128)(2,1)S(1)} all-to-all(bf16[4,128,256]{2,1,0:T(8,128)(2,1)S(1)} %shard_map.156), channel_id=1, replica_groups=mesh['zh'=4,'zl'=4,'y'=4,'x'=4,'c'=2] {'zl'}, dimensions={0} | all-to-all | bytes 524288 | tf_op jit(solution)/shard_map/all_to_all | solution.py:467
  88.4 1.1 shard_map.157
  89.5 1.3 collective-permute-start.7
  90.8 1.3 collective-permute-start.6
  92.1 1.5 %collective-permute-start.5 = (bf16[128,256]{1,0:T(8,128)(2,1)S(1)}, bf16[128,256]{1,0:T(8,128)(2,1)S(1)}, u32[]{:S(2)}, u32[]{:S(2)}) collective-permute-start(bf16[128,256]{1,0:T(8,128)(2,1)S(1)} %shard_map.157), channel_id=1, source_target_pairs={{0,384},{9,393},{16,400},{25,409},{385,1},{392,8},{401,17},{408,24... | collective-permute-start | bytes 196616 | tf_op jit(solution)/shard_map/ppermute | solution.py:471
  93.6 3.9 %shard_map.155.start = f32[128,128]{1,0:T(8,128)S(1)} custom-call(s32[8]{0:T(128)S(1)} %stack.74.pos, bf16[4,208,256]{2,1,0:T(8,128)(2,1)S(1)} %all_to_all.30.maps.own, f32[4,128]{1,0:T(4,128)S(1)} %pad_maximum_fusion.2.small.gain), custom_call_target="tpu_custom_call" | custom-call | flops 1000000000 | bytes 1 | tf_op jit(solution)/shard_map/pallas_call | solution.py:472
  97.4 0.0 copy-start.1
  97.4 1.0 collective-permute-done.7.near
  98.4 6.3 %collective-permute-done.6.middle = bf16[128,256]{1,0:T(8,128)(2,1)S(1)} collective-permute-done((bf16[128,256]{1,0:T(8,128)(2,1)S(1)}, bf16[128,256]{1,0:T(8,128)(2,1)S(1)}, u32[]{:S(2)}, u32[]{:S(2)}) %collective-permute-start.6) | collective-permute-done | bytes 65568 | tf_op jit(solution)/shard_map/ppermute | solution.py:471
  104.7 3.3 %collective-permute-done.5.far = bf16[128,256]{1,0:T(8,128)(2,1)S(1)} collective-permute-done((bf16[128,256]{1,0:T(8,128)(2,1)S(1)}, bf16[128,256]{1,0:T(8,128)(2,1)S(1)}, u32[]{:S(2)}, u32[]{:S(2)}) %collective-permute-start.5) | collective-permute-done | bytes 65568 | tf_op jit(solution)/shard_map/ppermute | solution.py:471
  108.0 1.9 %shard_map.158 = bf16[4,128,128]{2,1,0:T(8,128)(2,1)S(1)} custom-call(s32[8]{0:T(128)S(1)} %stack.74.pos, f32[128,128]{1,0:T(8,128)S(1)} %shard_map.155.start, bf16[128,256]{1,0:T(8,128)(2,1)S(1)} %collective-permute-done.5.far, bf16[128,256]{1,0:T(8,128)(2,1)S(1)} %collective-permute-done.6.middle, bf16[128,256]{1,0:T(8,128)(2,1)S(1)} %collective-permute-done.7.near, ...), custom_call_target="tpu_custom_call" | custom-call | flops 100000000 | bytes 1 | tf_op jit(solution)/shard_map/pallas_call | solution.py:473
  109.9 7.2 %all_to_all.32.states = bf16[4,128,128]{2,1,0:T(8,128)(2,1)S(1)} all-to-all(bf16[4,128,128]{2,1,0:T(8,128)(2,1)S(1)} %shard_map.158), channel_id=1, replica_groups=mesh['zh'=4,'zl'=4,'y'=4,'x'=4,'c'=2] {'y'}, dimensions={0} | all-to-all | bytes 262144 | tf_op jit(solution)/shard_map/all_to_all | solution.py:476
  117.1 1.3 shard_map.159
  118.5 7.0 %collective-permute-start.8 = (bf16[4,32,2048]{2,1,0:T(8,128)(2,1)S(1)}, bf16[4,32,2048]{2,1,0:T(8,128)(2,1)S(1)}, u32[]{:S(2)}, u32[]{:S(2)}) collective-permute-start(bf16[4,32,2048]{2,1,0:T(8,128)(2,1)S(1)} %get-tuple-element.14), channel_id=1, source_target_pairs={{0,1},{1,0},{2,3},{3,2},{4,5},{5,4},{6,7},{7,6},{8,9},{9,8},{10,11... | collective-permute-start | bytes 1572872 | tf_op jit(solution)/shard_map/ppermute | solution.py:480
  125.5 1.5 %collective-permute-done.8.got = bf16[4,32,2048]{2,1,0:T(8,128)(2,1)S(1)} collective-permute-done((bf16[4,32,2048]{2,1,0:T(8,128)(2,1)S(1)}, bf16[4,32,2048]{2,1,0:T(8,128)(2,1)S(1)}, u32[]{:S(2)}, u32[]{:S(2)}) %collective-permute-start.8) | collective-permute-done | bytes 524320 | tf_op jit(solution)/shard_map/ppermute | solution.py:480
  127.0 0.1 shard_map.160
  127.1 11.6 %all_to_all.33.rows = bf16[4,32,2048]{2,1,0:T(8,128)(2,1)S(1)} all-to-all(bf16[4,32,2048]{2,1,0:T(8,128)(2,1)S(1)} %shard_map.160), channel_id=1, replica_groups=mesh['zh'=4,'zl'=4,'y'=4,'x'=4,'c'=2] {'x'}, dimensions={0} | all-to-all | bytes 1048576 | tf_op jit(solution)/shard_map/all_to_all | solution.py:482
  138.7 0.8 shard_map.161
  (22 shorter events, 0.1 us)
Async XLA Ops:
  0.0 1.0 copy-start
  0.0 0.8 copy-start.3
  2.0 15.9 %copy-start.2 = (bf16[32,2048]{1,0:T(8,128)(2,1)S(1)}, bf16[32,2048]{1,0:T(8,128)(2,1)}, u32[]{:S(2)}) copy-start(bf16[32,2048]{1,0:T(8,128)(2,1)} %lat.1) | copy-start | bytes 393220
  2.0 34.7 %all-to-all-start = ((bf16[16,24,256]{2,1,0:T(8,128)(2,1)}), bf16[16,24,256]{2,1,0:T(8,128)(2,1)S(1)}, u32[]{:S(2)}, u32[]{:S(2)}) async-start(bf16[16,24,256]{2,1,0:T(8,128)(2,1)} %broadcast_in_dim.7), calls=%async_computation | async-start | bytes 393216 | tf_op jit(solution)/shard_map/all_to_all | solution.py:355
  17.8 11.2 %collective-permute-start.1 = (bf16[32,2048]{1,0:T(8,128)(2,1)S(1)}, bf16[32,2048]{1,0:T(8,128)(2,1)S(1)}, u32[]{:S(2)}, u32[]{:S(2)}) collective-permute-start(bf16[32,2048]{1,0:T(8,128)(2,1)S(1)} %copy-done.2), channel_id=1, source_target_pairs={{0,4},{2,6},{4,0},{6,2},{1,5},{3,7},{5,1},{7,3},{8,12},{10,14},{12... | collective-permute-start | bytes 393224 | tf_op jit(solution)/shard_map/ppermute | solution.py:396
  22.5 7.2 %collective-permute-start = (bf16[32,2048]{1,0:T(8,128)(2,1)S(1)}, bf16[32,2048]{1,0:T(8,128)(2,1)S(1)}, u32[]{:S(2)}, u32[]{:S(2)}) collective-permute-start(bf16[32,2048]{1,0:T(8,128)(2,1)S(1)} %copy-done.2), channel_id=1, source_target_pairs={{0,2},{2,4},{4,6},{6,0},{1,3},{3,5},{5,7},{7,1},{8,10},{10,12},{12... | collective-permute-start | bytes 393224 | tf_op jit(solution)/shard_map/ppermute | solution.py:396
  24.7 6.2 %collective-permute-start.2 = (bf16[32,2048]{1,0:T(8,128)(2,1)S(1)}, bf16[32,2048]{1,0:T(8,128)(2,1)S(1)}, u32[]{:S(2)}, u32[]{:S(2)}) collective-permute-start(bf16[32,2048]{1,0:T(8,128)(2,1)S(1)} %copy-done.2), channel_id=1, source_target_pairs={{0,6},{2,0},{4,2},{6,4},{1,7},{3,1},{5,3},{7,5},{8,14},{10,8},{12,... | collective-permute-start | bytes 393224 | tf_op jit(solution)/shard_map/ppermute | solution.py:396
  31.0 17.3 %collective-permute-start.3 = (bf16[4,32,2048]{2,1,0:T(8,128)(2,1)S(1)}, bf16[4,32,2048]{2,1,0:T(8,128)(2,1)S(1)}, u32[]{:S(2)}, u32[]{:S(2)}) collective-permute-start(bf16[4,32,2048]{2,1,0:T(8,128)(2,1)S(1)} %pad_maximum_fusion.one), channel_id=1, source_target_pairs={{0,1},{1,0},{2,3},{3,2},{4,5},{5,4},{6,7},{7,6},{8,9},{9,8},{10,11... | collective-permute-start | bytes 1572872 | tf_op jit(solution)/shard_map/ppermute | solution.py:398
  35.3 0.7 copy-start.7
  36.0 0.7 copy-start.4
  36.0 0.7 copy-start.5
  36.8 18.4 %collective-permute-start.4 = (bf16[64,1024]{1,0:T(8,128)(2,1)S(1)}, bf16[64,1024]{1,0:T(8,128)(2,1)S(1)}, u32[]{:S(2)}, u32[]{:S(2)}) collective-permute-start(bf16[64,1024]{1,0:T(8,128)(2,1)S(1)} %reshape.11.half), channel_id=1, source_target_pairs={{0,1},{1,0},{2,3},{3,2},{4,5},{5,4},{6,7},{7,6},{8,9},{9,8},{10,11... | collective-permute-start | bytes 393224 | tf_op jit(solution)/shard_map/ppermute | solution.py:418
  39.4 15.8 %all-to-all-start.1 = ((bf16[32,5,256]{2,1,0:T(8,128)(2,1)}), bf16[32,5,256]{2,1,0:T(8,128)(2,1)S(1)}, u32[]{:S(2)}, u32[]{:S(2)}) async-start(bf16[32,5,256]{2,1,0:T(8,128)(2,1)} %broadcast_in_dim.8), calls=%async_computation.1 | async-start | bytes 262144 | tf_op jit(solution)/shard_map/all_to_all | solution.py:355
  47.6 0.7 copy-start.6
  89.5 8.9 %collective-permute-start.7 = (bf16[128,256]{1,0:T(8,128)(2,1)S(1)}, bf16[128,256]{1,0:T(8,128)(2,1)S(1)}, u32[]{:S(2)}, u32[]{:S(2)}) collective-permute-start(bf16[128,256]{1,0:T(8,128)(2,1)S(1)} %shard_map.157), channel_id=1, source_target_pairs={{0,128},{9,137},{16,144},{25,153},{128,256},{129,1},{136,8},{137,2... | collective-permute-start | bytes 196616 | tf_op jit(solution)/shard_map/ppermute | solution.py:471
  90.8 13.9 %collective-permute-start.6 = (bf16[128,256]{1,0:T(8,128)(2,1)S(1)}, bf16[128,256]{1,0:T(8,128)(2,1)S(1)}, u32[]{:S(2)}, u32[]{:S(2)}) collective-permute-start(bf16[128,256]{1,0:T(8,128)(2,1)S(1)} %shard_map.157), channel_id=1, source_target_pairs={{0,256},{9,265},{16,272},{25,281},{128,384},{137,393},{144,400},{1... | collective-permute-start | bytes 196616 | tf_op jit(solution)/shard_map/ppermute | solution.py:471
  92.1 15.9 %collective-permute-start.5 = (bf16[128,256]{1,0:T(8,128)(2,1)S(1)}, bf16[128,256]{1,0:T(8,128)(2,1)S(1)}, u32[]{:S(2)}, u32[]{:S(2)}) collective-permute-start(bf16[128,256]{1,0:T(8,128)(2,1)S(1)} %shard_map.157), channel_id=1, source_target_pairs={{0,384},{9,393},{16,400},{25,409},{385,1},{392,8},{401,17},{408,24... | collective-permute-start | bytes 196616 | tf_op jit(solution)/shard_map/ppermute | solution.py:471
  97.4 19.7 %copy-start.1 = (bf16[256,2048]{1,0:T(8,128)(2,1)S(1)}, bf16[256,2048]{1,0:T(8,128)(2,1)}, u32[]{:S(2)}) copy-start(bf16[256,2048]{1,0:T(8,128)(2,1)} %weight.1) | copy-start | bytes 3145732
  118.5 8.5 %collective-permute-start.8 = (bf16[4,32,2048]{2,1,0:T(8,128)(2,1)S(1)}, bf16[4,32,2048]{2,1,0:T(8,128)(2,1)S(1)}, u32[]{:S(2)}, u32[]{:S(2)}) collective-permute-start(bf16[4,32,2048]{2,1,0:T(8,128)(2,1)S(1)} %get-tuple-element.14), channel_id=1, source_target_pairs={{0,1},{1,0},{2,3},{3,2},{4,5},{5,4},{6,7},{7,6},{8,9},{9,8},{10,11... | collective-permute-start | bytes 1572872 | tf_op jit(solution)/shard_map/ppermute | solution.py:480
